TPU v7x, 32 devices: a whole 2x2x4 slice. The times are simulated.
32 devices in a mesh: grp: 2 (over y), sp: 4 (over z), tp: 4 (over x, core).
Axes of the slice: x: 2, y: 2, z: 4, core: 2. Of those that a mesh axis runs over, the one named last changes fastest.
Arguments:
- tokens: bfloat16 [1024, 2048], P(('grp', 'sp')), parts along dimension 0, may hold values from -6 to 6
- norm_gain: float32 [2048], replicated, may hold values from 0.1 to 1.9
- w_query: bfloat16 [2048, 512], P('sp', 'tp'), may hold values from -0.125 to 0.125
- w_key: bfloat16 [2048, 512], P('sp', 'tp'), may hold values from -0.125 to 0.125
- w_value: bfloat16 [2048, 512], P('sp', 'tp'), may hold values from -0.125 to 0.125
- w_glu_value: bfloat16 [2048, 1024], P('sp', 'tp'), may hold values from -0.125 to 0.125
- w_glu_gate: bfloat16 [2048, 1024], P('sp', 'tp'), may hold values from -0.125 to 0.125
- key_offset: bfloat16 [1024, 8], P(('grp', 'sp'), 'tp'), parts along dimension 0, may hold values from -13 to 0
- head_gain: float32 [8, 64], P('tp'), may hold values from 0.1 to 1.9
- conv_taps: float32 [31, 1024], P(None, 'tp'), may hold values from -2.873685 to 2.873685
- channel_gain: float32 [1024], P('tp'), may hold values from 0.1 to 1.9
- channel_bias: float32 [1024], P('tp'), may hold values from -3 to 3
- w_out_attn: bfloat16 [512, 2048], P('tp'), may hold values from -0.15625 to 0.15625
- w_out_conv: bfloat16 [1024, 2048], P('tp'), may hold values from -0.15625 to 0.15625
- out_gain: float32 [2048], replicated, may hold values from 0.1 to 1.9
Outputs:
- mixed: bfloat16 [1024, 2048], P(('grp', 'sp')), parts along dimension 0
- log_mass: float32 [8, 1024], P('tp', ('grp', 'sp')), parts along dimension 1
There are 2 independent parts, one for each index of `grp`. A program takes and returns all parts, laid end to end along the dimension named above; an argument that names none is the same for every part. Nothing has to cross between parts.
All inputs are finite; a program needn't handle non-finite values.
Results may differ from a plain program's by a relative error of at most 0.011.
Values may be sent and summed in bfloat16 or wider, within the bound.
No kernel may reach another device: no remote copies, remote signals or barrier semaphores. Data moves between devices by JAX's collectives and lax.ppermute only.
A program may use at most 64 MiB of HBM per device.

v0:
```python
import jax
import jax.numpy as jnp
from jax import lax
from jax.sharding import PartitionSpec as P

HD = 64
CW = 1024


norm_eps = 1e-06


def from_behind(value, axis, steps):
    count = lax.axis_size(axis)
    initial, last = (max(0, -steps), min(count, count - steps))
    return lax.ppermute(value, axis, [(source, source + steps) for source in range(initial, last)])


def row_norm(values_in, gain_vec):
    squares = jnp.mean(values_in * values_in, axis=-1, keepdims=True)
    return values_in * lax.rsqrt(squares + norm_eps) * gain_vec


def local(
    tokens,
    norm_gain,
    w_query,
    w_key,
    w_value,
    w_glu_value,
    w_glu_gate,
    key_offset,
    head_gain,
    conv_taps,
    channel_gain,
    channel_bias,
    w_out_attn,
    w_out_conv,
    out_gain,
):
    row_count = tokens.shape[0]
    normed = row_norm(tokens.astype(jnp.float32), norm_gain).astype(jnp.bfloat16)
    weights_in = (w_query, w_key, w_value, w_glu_value, w_glu_gate)
    pieces = (
        lax.all_gather(weights_in[0], "sp", axis=0, tiled=True),
        lax.all_gather(weights_in[1], "sp", axis=0, tiled=True),
        lax.all_gather(weights_in[2], "sp", axis=0, tiled=True),
        lax.all_gather(weights_in[3], "sp", axis=0, tiled=True),
        lax.all_gather(weights_in[4], "sp", axis=0, tiled=True),
    )
    projected = tuple(
        (jnp.dot(normed, shard_piece, preferred_element_type=jnp.float32) for shard_piece in pieces)
    )
    query, key_rows, value_rows, glu_value, glu_gate = [
        summed.astype(jnp.bfloat16) for summed in projected
    ]
    kv_local = key_rows.shape[1] // HD
    group_size = query.shape[1] // key_rows.shape[1]
    heads_local = kv_local * group_size
    all_keys, all_values, all_offsets = (
        lax.all_gather(key_rows, "sp", axis=0, tiled=True),
        lax.all_gather(value_rows, "sp", axis=0, tiled=True),
        lax.all_gather(key_offset, "sp", axis=0, tiled=True),
    )
    sequence_length_total = all_keys.shape[0]
    shard_count = lax.axis_size("sp")
    per_block = 1
    while (
        per_block * 2 <= shard_count
        and shard_count % (per_block * 2) == 0
        and (per_block * 2 * row_count <= 1024)
    ):
        per_block = per_block * 2
    span_len = per_block * row_count
    query_heads = query.reshape(row_count, kv_local, group_size, HD)
    key_heads = all_keys.reshape(sequence_length_total, kv_local, HD)
    value_heads = all_values.reshape(sequence_length_total, kv_local, HD)
    my_index = lax.axis_index("sp")
    query_pos = my_index * row_count + jnp.arange(row_count, dtype=jnp.int32)
    last_block = my_index // per_block
    zeros_mix = jnp.zeros((kv_local, group_size, row_count, HD), jnp.float32)
    zeros_row = jnp.zeros((kv_local, group_size, row_count), jnp.float32)

    def sweep(turn_index, carry):
        head_mix, mass_sum, carried = carry
        first_key = (last_block - turn_index) * span_len
        key_block = lax.dynamic_slice_in_dim(key_heads, first_key, span_len, 0)
        value_block = lax.dynamic_slice_in_dim(value_heads, first_key, span_len, 0)
        offset_block = lax.dynamic_slice_in_dim(all_offsets, first_key, span_len, 0).astype(
            jnp.float32
        )
        offset_block = offset_block.T.reshape(kv_local, group_size, 1, span_len)
        scores = (
            jnp.einsum("qhgd,khd->hgqk", query_heads, key_block, preferred_element_type=jnp.float32)
            * HD ** (-0.5)
            + offset_block
        )
        key_pos = first_key + jnp.arange(span_len, dtype=jnp.int32)
        allowed = key_pos[None, :] <= query_pos[:, None]
        log_not = jnp.where(allowed, jax.nn.log_sigmoid(-scores), 0.0)
        later = lax.cumsum(log_not, axis=3, reverse=True) - log_not + carried[..., None]
        weights = jnp.where(allowed, jnp.exp(jax.nn.log_sigmoid(scores) + later), 0.0)
        head_mix = head_mix + jnp.einsum(
            "hgqk,khd->hgqd",
            weights.astype(jnp.bfloat16),
            value_block,
            preferred_element_type=jnp.float32,
        )
        return (head_mix, mass_sum + jnp.sum(weights, axis=3), carried + jnp.sum(log_not, axis=3))

    head_mix, mass_sum, leftover = lax.fori_loop(
        0, last_block + 1, sweep, (zeros_mix, zeros_row, zeros_row)
    )
    log_mass = jnp.log(mass_sum).reshape(heads_local, row_count)
    head_rows = head_mix.transpose(2, 0, 1, 3).reshape(row_count, heads_local, HD)
    attended = (
        row_norm(head_rows, head_gain).astype(jnp.bfloat16).reshape(row_count, heads_local * HD)
    )
    gated = (glu_value.astype(jnp.float32) * jax.nn.sigmoid(glu_gate.astype(jnp.float32))).astype(
        jnp.bfloat16
    )
    reach_len = conv_taps.shape[0] - 1
    before = from_behind(gated[row_count - reach_len :], "sp", 1)
    padded = jnp.concatenate([before, gated], axis=0).astype(jnp.float32)
    conv_out = jnp.zeros(gated.shape, jnp.float32)
    for tap_index in range(conv_taps.shape[0]):
        conv_out = conv_out + conv_taps[tap_index] * padded[tap_index : tap_index + row_count]
    total_sum, total_squares = lax.psum(
        (jnp.sum(conv_out, axis=1), jnp.sum(conv_out * conv_out, axis=1)), "tp"
    )
    chan_mean = (total_sum / CW)[:, None]
    spread = (total_squares / CW)[:, None] - chan_mean * chan_mean
    centered = conv_out - chan_mean
    channel_out = jax.nn.silu(
        centered * lax.rsqrt(spread + norm_eps) * channel_gain + channel_bias
    ).astype(jnp.bfloat16)
    share = lax.psum_scatter(
        jnp.dot(attended, w_out_attn, preferred_element_type=jnp.float32)
        + jnp.dot(channel_out, w_out_conv, preferred_element_type=jnp.float32),
        "tp",
        scatter_dimension=0,
        tiled=True,
    )
    mixed = lax.all_gather(row_norm(share, out_gain).astype(jnp.bfloat16), "tp", axis=0, tiled=True)
    return (mixed, log_mass)


def solution(mesh):
    in_specs = (
        P(("grp", "sp"), None),
        P(),
        P("sp", "tp"),
        P("sp", "tp"),
        P("sp", "tp"),
        P("sp", "tp"),
        P("sp", "tp"),
        P(("grp", "sp"), "tp"),
        P("tp", None),
        P(None, "tp"),
        P("tp"),
        P("tp"),
        P("tp", None),
        P("tp", None),
        P(),
    )
    out_specs = (P(("grp", "sp"), None), P("tp", ("grp", "sp")))
    return jax.shard_map(local, mesh=mesh, in_specs=in_specs, out_specs=out_specs, check_vma=False)
```

profile of v0, /device:TPU:25, one launch (start us, length us, event | category | flops | bytes accessed | tf_op | source)
XLA Modules:
  0.0 166.8 jit_solution(18097645065637768242)
XLA Ops:
  7.2 0.7 all-gather.3.cloned.1.call-update
  8.0 0.7 all-gather.5.cloned.1.call-update
  9.0 0.7 copy-done.4
  9.7 15.8 %all_gather.28 = bf16[2048,128]{1,0:T(8,128)(2,1)S(1)} all-gather(bf16[512,128]{1,0:T(8,128)(2,1)S(1)} %copy-done.4), channel_id=1, replica_groups=mesh['grp'=2,'sp'=4,'tp'=4] {'sp'}, dimensions={0}, use_global_device_ids=true | all-gather | bytes 655360 | tf_op jit(solution)/shard_map/all_gather | solution.py:46
  25.8 12.2 %all_gather.29 = bf16[512,128]{1,0:T(8,128)(2,1)S(1)} all-gather(bf16[128,128]{1,0:T(8,128)(2,1)S(1)} %convolution_convert_fusion.3), channel_id=1, replica_groups=mesh['grp'=2,'sp'=4,'tp'=4] {'sp'}, dimensions={0}, use_global_device_ids=true | all-gather | bytes 163840 | tf_op jit(solution)/shard_map/all_gather | solution.py:61
  38.1 0.8 copy-done.5
  38.9 12.9 %all_gather.31 = bf16[2048,128]{1,0:T(8,128)(2,1)S(1)} all-gather(bf16[512,128]{1,0:T(8,128)(2,1)S(1)} %copy-done.5), channel_id=1, replica_groups=mesh['grp'=2,'sp'=4,'tp'=4] {'sp'}, dimensions={0}, use_global_device_ids=true | all-gather | bytes 655360 | tf_op jit(solution)/shard_map/all_gather | solution.py:47
  52.2 12.4 %all_gather.32 = bf16[512,128]{1,0:T(8,128)(2,1)S(1)} all-gather(bf16[128,128]{1,0:T(8,128)(2,1)S(1)} %convolution_convert_fusion.2), channel_id=1, replica_groups=mesh['grp'=2,'sp'=4,'tp'=4] {'sp'}, dimensions={0}, use_global_device_ids=true | all-gather | bytes 163840 | tf_op jit(solution)/shard_map/all_gather | solution.py:62
  64.7 0.8 copy-done.6
  65.5 16.1 %all_gather.27 = bf16[2048,128]{1,0:T(8,128)(2,1)S(1)} all-gather(bf16[512,128]{1,0:T(8,128)(2,1)S(1)} %copy-done.6), channel_id=1, replica_groups=mesh['grp'=2,'sp'=4,'tp'=4] {'sp'}, dimensions={0}, use_global_device_ids=true | all-gather | bytes 655360 | tf_op jit(solution)/shard_map/all_gather | solution.py:45
  81.6 0.4 convolution_convert_fusion.4
  82.1 0.6 copy-done.11
  82.7 5.6 %all_gather.30 = bf16[512,2]{0,1:T(2,128)(2,1)S(1)} all-gather(bf16[128,2]{0,1:T(2,128)(2,1)S(1)} %copy-done.11), channel_id=1, replica_groups=mesh['grp'=2,'sp'=4,'tp'=4] {'sp'}, dimensions={0}, use_global_device_ids=true | all-gather | bytes 2560 | tf_op jit(solution)/shard_map/all_gather | solution.py:63
  88.3 4.3 %while.15 = (s32[]{:T(128)}, f32[2,1,128,64]{2,3,0,1:T(8,128)S(1)}, f32[2,1,128]{2,1,0:T(1,128)S(1)}, f32[2,1,128]{2,0,1:T(2,128)S(1)}, s32[]{:T(128)}, /*index=...) while((s32[]{:T(128)}, f32[2,1,128,64]{2,3,0,1:T(8,128)S(1)}, ...), condition=%wide.region_6.7_spmd.clone, body=%wide.region_1.6_spmd.clone.sunk | while | flops 54744452 | bytes 5395625 | solution.py:111
  88.5 0.6 fusion.104
  89.0 2.4 %fusion.105 = f32[2,1,128,4,128]{2,3,4,1,0:T(4,128)S(1)} fusion(f32[2,1,128,4,128]{2,4,3,0,1:T(8,128)S(1)} %bitcast.128), kind=kOutput, calls=%fused_computation.18.clone.1 | output fusion | flops 16646144 | bytes 1048576 | tf_op jit(solution)/shard_map/reduce-window
  91.5 0.8 fusion.106
  92.6 0.7 copy-done.7
  93.4 1.6 fusion.27
  95.0 1.6 fusion.26
  96.6 1.3 collective-permute-start
  98.1 3.0 %collective-permute-done = bf16[30,256]{1,0:T(8,128)(2,1)S(1)} collective-permute-done((bf16[30,256]{1,0:T(8,128)(2,1)S(1)}, bf16[30,256]{1,0:T(8,128)(2,1)S(1)}, u32[]{:S(2)}, u32[]{:S(2)}) %collective-permute-start) | collective-permute-done | bytes 15392 | tf_op jit(solution)/shard_map/ppermute | solution.py:16
  101.1 0.6 fusion.76
  101.7 20.6 %all-reduce = (f32[128]{0:T(128)S(1)}, f32[128]{0:T(128)S(1)}) all-reduce(f32[128]{0:T(128)S(1)} %get-tuple-element.112, f32[128]{0:T(128)S(1)} %get-tuple-element.111), channel_id=1, replica_groups=mesh['grp'=2,'sp'=4,'tp'=4] {'tp'}, use_global_device_ids=true, to_apply=%region_11.12 | all-reduce | flops 256 | bytes 2048 | tf_op jit(solution)/shard_map/psum | solution.py:128
  122.3 0.7 copy-done.9
  123.3 0.7 copy-done.3
  124.0 1.3 convolution_add_fusion
  125.3 0.6 log_bitcast_fusion
  125.9 25.0 %reduce-scatter.2.cloned.1.call-done = f32[32,2048]{1,0:T(8,128)} async-done(((f32[128,2048]{1,0:T(8,128)}), f32[32,2048]{1,0:T(8,128)}) %reduce-scatter.2.cloned.1.call-update) | async-done | bytes 262160 | tf_op jit(solution)/shard_map/reduce_scatter | solution.py:137
  151.0 1.1 multiply_reduce_fusion
  152.2 7.3 %all_gather.35 = bf16[128,2048]{1,0:T(8,128)(2,1)S(1)} all-gather(bf16[32,2048]{1,0:T(8,128)(2,1)S(1)} %multiply_convert_fusion), channel_id=1, replica_groups=mesh['grp'=2,'sp'=4,'tp'=4] {'tp'}, dimensions={0}, use_global_device_ids=true | all-gather | bytes 655360 | tf_op jit(solution)/shard_map/all_gather | solution.py:144
  159.5 0.8 copy.53
  (59 shorter events, 2.5 us)
Async XLA Ops:
  7.2 115.1 %copy-start = (bf16[256,2048]{1,0:T(8,128)(2,1)S(1)}, bf16[256,2048]{1,0:T(8,128)(2,1)}, u32[]{:S(2)}) copy-start(bf16[256,2048]{1,0:T(8,128)(2,1)} %param.30) | copy-start | bytes 3145732
  7.2 1.6 copy-start.2
  7.2 86.2 %all-gather.3.cloned.1.call-start = ((), (), s32[]{:S(2)}) async-start(), calls=%async_computation.1 | async-start | bytes 1310720 | tf_op jit(solution)/shard_map/all_gather | solution.py:48
  7.9 87.1 %all-gather.5.cloned.1.call-start = ((), (), s32[]{:S(2)}) async-start(), calls=%async_computation.2 | async-start | bytes 1310720 | tf_op jit(solution)/shard_map/all_gather | solution.py:49
  8.7 142.3 %reduce-scatter.2.cloned.1.call-start = ((), (), s32[]{:S(2)}) async-start(), calls=%async_computation.3 | async-start | bytes 1310720 | tf_op jit(solution)/shard_map/reduce_scatter | solution.py:137
  8.7 0.9 copy-start.4
  9.7 15.8 %copy-start.12 = (f32[2048]{0:T(1024)S(1)}, f32[2048]{0:T(1024)}, u32[]{:S(2)}) copy-start(f32[2048]{0:T(1024)} %param.18) | copy-start | bytes 24580
  38.0 0.9 copy-start.5
  64.6 0.9 copy-start.6
  82.0 0.7 copy-start.11
  92.5 0.8 copy-start.7
  96.6 1.3 copy-start.13
  96.6 4.5 %collective-permute-start = (bf16[30,256]{1,0:T(8,128)(2,1)S(1)}, bf16[30,256]{1,0:T(8,128)(2,1)S(1)}, u32[]{:S(2)}, u32[]{:S(2)}) collective-permute-start(bf16[30,256]{1,0:T(8,128)(2,1)S(1)} %slice.262), channel_id=1, source_target_pairs={{0,4},{4,8},{8,12},{1,5},{5,9},{9,13},{2,6},{6,10},{10,14},{3,7},{... | collective-permute-start | bytes 46088 | tf_op jit(solution)/shard_map/ppermute | solution.py:16
  101.1 21.2 %copy-start.10 = (f32[256]{0:T(256)S(1)}, f32[256]{0:T(256)}, u32[]{:S(2)}) copy-start(f32[256]{0:T(256)} %param.27) | copy-start | bytes 3076
  122.3 0.7 copy-start.9
  123.0 1.0 copy-start.3
  125.3 26.8 %copy-start.8 = (f32[2048]{0:T(1024)S(1)}, f32[2048]{0:T(1024)}, u32[]{:S(2)}) copy-start(f32[2048]{0:T(1024)} %param.31) | copy-start | bytes 24580
  151.0 1.2 copy-start.1
Sparse Core Ops, SparseCore 0:
  9.6 32.7 all-gather.2
  44.0 34.6 all-gather.4
  125.5 25.4 reduce-scatter.1
where the time goes:
time: 169 us; the launch traced here: 167 us
  blocking collectives  103 us (61%)
  waiting for transfers between devices  29.5 us (17%)
  between operations  14 us (8%)
  local copies, waits for them, and re-layouts  6.76 us (4%)
  matrix products  6.76 us (4%)
  other arithmetic  5.54 us (3%)
    reduce_scatter x1, waiting for transfers between devices, local(): lax.psum_scatter(jnp.dot(attended, w_out_attn, preferred_element_type=jnp...  25 us
    psum x1, blocking collectives, local(): lax.psum((jnp.sum(conv_out, axis=1), jnp.sum(conv_out * conv_out, axis=1)...  20.6 us
    all_gather x1, blocking collectives, local(): lax.all_gather(weights_in[0], 'sp', axis=0, tiled=True)  16.1 us
    all_gather x1, blocking collectives, local(): lax.all_gather(weights_in[1], 'sp', axis=0, tiled=True)  15.8 us
    all_gather x1, blocking collectives, local(): lax.all_gather(weights_in[2], 'sp', axis=0, tiled=True)  12.9 us
    all_gather x1, blocking collectives, local(): lax.all_gather(value_rows, 'sp', axis=0, tiled=True)  12.4 us
    all_gather x1, blocking collectives, local(): lax.all_gather(key_rows, 'sp', axis=0, tiled=True)  12.2 us
    all_gather x1, blocking collectives, local(): lax.all_gather(row_norm(share, out_gain).astype(jnp.bfloat16), 'tp', axis...  7.28 us
  transfers between devices with their start and end apart: 4, of which 2 were waited for; matrix products, arithmetic and copies ran while one was open for 5% of the time, Pallas kernels for 0%

commit v1 on v0

--- a/solution.py
+++ b/solution.py
@@ -1,13 +1,20 @@
+import functools
+
 import jax
 import jax.numpy as jnp
 from jax import lax
+from jax.experimental import pallas as pl
+from jax.experimental.pallas import tpu as pltpu
 from jax.sharding import PartitionSpec as P
 
-HD = 64
-CW = 1024
-
-
 norm_eps = 1e-06
+BF16 = jnp.bfloat16
+F32 = jnp.float32
+
+
+def exchange(value, axis, bit):
+    count = lax.axis_size(axis)
+    return lax.ppermute(value, axis, [(s, s ^ bit) for s in range(count)])
 
 
 def from_behind(value, axis, steps):
@@ -21,7 +28,237 @@
     return values_in * lax.rsqrt(squares + norm_eps) * gain_vec
 
 
-def local(
+def dot_f32(a, b, dims=((1,), (0,))):
+    return lax.dot_general(a, b, (dims, ((), ())), preferred_element_type=F32)
+
+
+def attention_kernel(hd, q_ref, k_ref, v_ref, off_ref, gain_ref, out_ref, mass_ref, acc, mass, carry):
+    me = lax.axis_index("sp")
+    rows, width = q_ref.shape
+    heads = width // hd
+    lane = lax.broadcasted_iota(jnp.int32, (rows, width), 1) // hd
+    keys = rows
+    before = lax.broadcasted_iota(jnp.int32, (2 * keys, 2 * keys), 0) % keys
+    column = lax.broadcasted_iota(jnp.int32, (2 * keys, 2 * keys), 1)
+    suffix = jnp.where((column >= keys) | (before > column), 1.0, 0.0).astype(BF16)
+    q = q_ref[...]
+    scale = hd ** (-0.5)
+
+    def block(slot, first):
+        start = pl.multiple_of(slot * keys, keys)
+        k = k_ref[pl.ds(start, keys), :]
+        v = v_ref[pl.ds(start, keys), :]
+        off = off_ref[pl.ds(pl.multiple_of(slot * 8, 8), 8), :].astype(F32)
+        parts = []
+        for h in range(heads):
+            qh = jnp.where(lane == h, q, jnp.zeros_like(q))
+            s = dot_f32(qh, k, ((1,), (1,))) * scale + off[h : h + 1, :]
+            soft = jnp.maximum(s, 0.0) + jnp.log(1.0 + jnp.exp(-jnp.abs(s)))
+            if first:
+                allowed = lax.broadcasted_iota(jnp.int32, (rows, keys), 1) <= lax.broadcasted_iota(
+                    jnp.int32, (rows, keys), 0
+                )
+                log_not = jnp.where(allowed, -soft, 0.0)
+            else:
+                log_not = -soft
+            high = log_not.astype(BF16)
+            low = (log_not - high.astype(F32)).astype(BF16)
+            sums = dot_f32(jnp.concatenate([high, low], axis=1), suffix)
+            later, total = sums[:, :keys], sums[:, keys:]
+            if not first:
+                later = later + carry[h]
+            w = jnp.exp(s - soft + later)
+            if first:
+                w = jnp.where(allowed, w, 0.0)
+                mass[h] = w
+                carry[h] = total
+            else:
+                mass[h] = mass[h] + w
+                carry[h] = carry[h] + total
+            parts.append((w.astype(BF16), jnp.where(lane == h, v, jnp.zeros_like(v))))
+        mix = dot_f32(
+            jnp.concatenate([w for w, _ in parts], axis=1),
+            jnp.concatenate([v for _, v in parts], axis=0),
+        )
+        if first:
+            acc[...] = mix
+        else:
+            acc[...] = acc[...] + mix
+
+    block(0, True)
+
+    def earlier(t, _):
+        block(jnp.bitwise_xor(me - t, me), False)
+        return 0
+
+    lax.fori_loop(1, me + 1, earlier, 0)
+    mixed = acc[...]
+    squares = mixed * mixed
+    inverse = jnp.zeros_like(mixed)
+    for h in range(heads):
+        mean = jnp.sum(jnp.where(lane == h, squares, 0.0), axis=1, keepdims=True) / hd
+        inverse = jnp.where(lane == h, lax.rsqrt(mean + norm_eps), inverse)
+    out_ref[...] = (mixed * inverse * gain_ref[...]).astype(BF16)
+    for h in range(heads):
+        mass_ref[h : h + 1, :] = jnp.log(jnp.sum(jnp.transpose(mass[h]), axis=0, keepdims=True))
+
+
+def attention(q, k, v, off, head_gain):
+    rows, width = q.shape
+    heads, hd = head_gain.shape
+    out_shape = (jax.ShapeDtypeStruct((rows, width), BF16), jax.ShapeDtypeStruct((heads, rows), F32))
+    return pl.pallas_call(
+        functools.partial(attention_kernel, hd),
+        out_shape=out_shape,
+        in_specs=[pl.BlockSpec(memory_space=pltpu.VMEM)] * 5,
+        out_specs=[pl.BlockSpec(memory_space=pltpu.VMEM)] * 2,
+        scratch_shapes=[
+            pltpu.VMEM((rows, width), F32),
+            pltpu.VMEM((heads, rows, rows), F32),
+            pltpu.VMEM((heads, rows, rows), F32),
+        ],
+        cost_estimate=pl.CostEstimate(flops=400_000_000, bytes_accessed=1_000_000, transcendentals=400_000),
+        compiler_params=pltpu.CompilerParams(vmem_limit_bytes=16 * 1024 * 1024),
+        name="stick_attention",
+    )(q, k, v, off, head_gain.reshape(1, width))
+
+
+def final_kernel(aw, cw, mine, core, far, wa, wc, wcore, wx, wxc, gb0, gb1, gb2, gb3, gain_ref, out_ref):
+    acts = [mine[...], core[...], far[0], far[1]]
+    convs = [a[:, aw:].astype(F32) for a in acts]
+    count = len(convs) * cw
+    mean = sum(jnp.sum(v, axis=1, keepdims=True) for v in convs) / count
+    centered = [v - mean for v in convs]
+    spread = sum(jnp.sum(v * v, axis=1, keepdims=True) for v in centered) / count
+    inverse = lax.rsqrt(spread + norm_eps)
+    total = None
+    for slot, (v, gb) in enumerate(zip(centered, (gb0, gb1, gb2, gb3))):
+        y = v * inverse * gb[0:1, :] + gb[1:2, :]
+        y = (y * jax.nn.sigmoid(y)).astype(BF16)
+        att = acts[slot][:, :aw]
+        if slot == 0:
+            part = dot_f32(att, wa[...]) + dot_f32(y, wc[...])
+        else:
+            w = (wcore, wx, wxc)[slot - 1]
+            part = dot_f32(jnp.concatenate([att, y], axis=1), w[...])
+        total = part if total is None else total + part
+    squares = jnp.mean(total * total, axis=1, keepdims=True)
+    out_ref[...] = (total * lax.rsqrt(squares + norm_eps) * gain_ref[...]).astype(BF16)
+
+
+def finish(mine, core, far, wa, wc, wcore, wx, wxc, gbs, out_gain):
+    rows = mine.shape[0]
+    width = wa.shape[1]
+    return pl.pallas_call(
+        functools.partial(final_kernel, wa.shape[0], wc.shape[0]),
+        out_shape=jax.ShapeDtypeStruct((rows, width), BF16),
+        in_specs=[pl.BlockSpec(memory_space=pltpu.VMEM)] * 13,
+        out_specs=pl.BlockSpec(memory_space=pltpu.VMEM),
+        cost_estimate=pl.CostEstimate(flops=800_000_000, bytes_accessed=7_000_000, transcendentals=70_000),
+        compiler_params=pltpu.CompilerParams(vmem_limit_bytes=32 * 1024 * 1024),
+        name="finish_rows",
+    )(mine, core, far, wa, wc, wcore, wx, wxc, *gbs, out_gain.reshape(1, width))
+
+
+def depthwise(padded, conv_taps, rows):
+    out = jnp.zeros((rows, padded.shape[1]), F32)
+    for tap in range(conv_taps.shape[0]):
+        out = out + conv_taps[tap] * padded[tap : tap + rows]
+    return out
+
+
+def paired(
+    tokens,
+    norm_gain,
+    w_query,
+    w_key,
+    w_value,
+    w_glu_value,
+    w_glu_gate,
+    key_offset,
+    head_gain,
+    conv_taps,
+    channel_gain,
+    channel_bias,
+    w_out_attn,
+    w_out_conv,
+    out_gain,
+):
+    rows, features = tokens.shape
+    half_rows, block = rows // 2, w_query.shape[0]
+    half = 2 * block
+    heads, hd = head_gain.shape
+    aw, cw = heads * hd, conv_taps.shape[1]
+    me_sp, me_tp = lax.axis_index("sp"), lax.axis_index("tp")
+    side, low = me_sp // 2, me_sp % 2
+    core = me_tp % 2
+
+    normed = row_norm(tokens.astype(F32), norm_gain).astype(BF16)
+    x_send = lax.dynamic_slice(normed, (core * half_rows, (1 - side) * half), (half_rows, half))
+    x_got = exchange(x_send, "sp", 2)
+    w_attn = jnp.concatenate([w_query, w_key, w_value], axis=1)
+    w_attn_pair = exchange(w_attn, "sp", 1)
+    w_glu = jnp.concatenate([w_glu_value, w_glu_gate], axis=1)
+    w_glu_pair = exchange(w_glu, "sp", 1)
+    w_out = jnp.concatenate([w_out_attn, w_out_conv], axis=0)
+    w_out_x = exchange(w_out, "tp", 2)
+    w_out_core = exchange(w_out, "tp", 1)
+    gb = jnp.stack([channel_gain, channel_bias])
+    gb_core = exchange(gb, "tp", 1)
+    gb_x = exchange(jnp.concatenate([gb, gb_core]), "tp", 2)
+    x_other = exchange(x_got, "tp", 1)
+    w_out_xc = exchange(w_out_x, "tp", 1)
+
+    x_cross = jnp.where(
+        core == 0, jnp.concatenate([x_got, x_other]), jnp.concatenate([x_other, x_got])
+    )
+    x_mine = lax.dynamic_slice(normed, (0, side * half), (rows, half))
+    x_all = jnp.concatenate([x_mine, x_cross])
+    x_own = lax.dynamic_slice(x_all, (0, low * block), (2 * rows, block))
+    x_pair = lax.dynamic_slice(x_all, (0, (1 - low) * block), (2 * rows, block))
+
+    p = dot_f32(x_own, w_attn) + dot_f32(x_pair, w_attn_pair)
+    pq, pk, pv = (p[:, n * aw : (n + 1) * aw] for n in range(3))
+    off = jnp.pad(key_offset.T, ((0, 8 - heads), (0, 0)))
+    sent = jnp.concatenate([pq[rows:], pk[rows:], pv[rows:], pk[:rows], pv[:rows]]).astype(BF16)
+    got = exchange(jnp.concatenate([sent, off, off]), "sp", 2)
+    g = [got[n * rows : (n + 1) * rows].astype(F32) for n in range(5)]
+    q = (pq[:rows] + g[0]).astype(BF16)
+    k_two = jnp.concatenate([pk[:rows] + g[1], pk[rows:] + g[3]]).astype(BF16)
+    v_two = jnp.concatenate([pv[:rows] + g[2], pv[rows:] + g[4]]).astype(BF16)
+    off_two = jnp.concatenate([off, got[5 * rows : 5 * rows + 8]])
+    mine_two = jnp.concatenate([k_two, v_two, off_two])
+    pair_two = exchange(mine_two, "sp", 1)
+
+    def slots(first, size):
+        a, b = mine_two[first : first + 2 * size], pair_two[first : first + 2 * size]
+        return jnp.concatenate([a[:size], b[:size], a[size:], b[size:]])
+
+    k_all, v_all, off_all = slots(0, rows), slots(2 * rows, rows), slots(4 * rows, 8)
+
+    pg = dot_f32(x_own, w_glu) + dot_f32(x_pair, w_glu_pair)
+    glu = pg[:rows] + exchange(pg[rows:].astype(BF16), "sp", 2).astype(F32)
+    gated = (glu[:, :cw] * jax.nn.sigmoid(glu[:, cw:])).astype(BF16)
+    reach = conv_taps.shape[0] - 1
+    before = from_behind(gated[rows - reach :], "sp", 1)
+    padded = jnp.concatenate([before, gated]).astype(F32)
+    conv_out = depthwise(padded, conv_taps, rows).astype(BF16)
+
+    attended, log_mass = attention(q, k_all, v_all, off_all, head_gain)
+
+    act = jnp.concatenate([attended, conv_out], axis=1)
+    mine = lax.dynamic_slice(act, (core * half_rows, 0), (half_rows, aw + cw))
+    theirs = lax.dynamic_slice(act, ((1 - core) * half_rows, 0), (half_rows, aw + cw))
+    from_core = exchange(theirs, "tp", 1)
+    far = exchange(jnp.stack([mine, from_core]), "tp", 2)
+    gbs = (gb, gb_core, gb_x[:2], gb_x[2:])
+    done = finish(mine, from_core, far, w_out_attn, w_out_conv, w_out_core, w_out_x, w_out_xc, gbs, out_gain)
+    other = exchange(done, "tp", 1)
+    mixed = jnp.where(core == 0, jnp.concatenate([done, other]), jnp.concatenate([other, done]))
+    return (mixed, log_mass)
+
+
+def gathered(
     tokens,
     norm_gain,
     w_query,
@@ -39,6 +276,8 @@
     out_gain,
 ):
     row_count = tokens.shape[0]
+    hd = head_gain.shape[1]
+    channels = conv_taps.shape[1] * lax.axis_size("tp")
     normed = row_norm(tokens.astype(jnp.float32), norm_gain).astype(jnp.bfloat16)
     weights_in = (w_query, w_key, w_value, w_glu_value, w_glu_gate)
     pieces = (
@@ -54,7 +293,7 @@
     query, key_rows, value_rows, glu_value, glu_gate = [
         summed.astype(jnp.bfloat16) for summed in projected
     ]
-    kv_local = key_rows.shape[1] // HD
+    kv_local = key_rows.shape[1] // hd
     group_size = query.shape[1] // key_rows.shape[1]
     heads_local = kv_local * group_size
     all_keys, all_values, all_offsets = (
@@ -72,13 +311,13 @@
     ):
         per_block = per_block * 2
     span_len = per_block * row_count
-    query_heads = query.reshape(row_count, kv_local, group_size, HD)
-    key_heads = all_keys.reshape(sequence_length_total, kv_local, HD)
-    value_heads = all_values.reshape(sequence_length_total, kv_local, HD)
+    query_heads = query.reshape(row_count, kv_local, group_size, hd)
+    key_heads = all_keys.reshape(sequence_length_total, kv_local, hd)
+    value_heads = all_values.reshape(sequence_length_total, kv_local, hd)
     my_index = lax.axis_index("sp")
     query_pos = my_index * row_count + jnp.arange(row_count, dtype=jnp.int32)
     last_block = my_index // per_block
-    zeros_mix = jnp.zeros((kv_local, group_size, row_count, HD), jnp.float32)
+    zeros_mix = jnp.zeros((kv_local, group_size, row_count, hd), jnp.float32)
     zeros_row = jnp.zeros((kv_local, group_size, row_count), jnp.float32)
 
     def sweep(turn_index, carry):
@@ -92,7 +331,7 @@
         offset_block = offset_block.T.reshape(kv_local, group_size, 1, span_len)
         scores = (
             jnp.einsum("qhgd,khd->hgqk", query_heads, key_block, preferred_element_type=jnp.float32)
-            * HD ** (-0.5)
+            * hd ** (-0.5)
             + offset_block
         )
         key_pos = first_key + jnp.arange(span_len, dtype=jnp.int32)
@@ -112,9 +351,9 @@
         0, last_block + 1, sweep, (zeros_mix, zeros_row, zeros_row)
     )
     log_mass = jnp.log(mass_sum).reshape(heads_local, row_count)
-    head_rows = head_mix.transpose(2, 0, 1, 3).reshape(row_count, heads_local, HD)
+    head_rows = head_mix.transpose(2, 0, 1, 3).reshape(row_count, heads_local, hd)
     attended = (
-        row_norm(head_rows, head_gain).astype(jnp.bfloat16).reshape(row_count, heads_local * HD)
+        row_norm(head_rows, head_gain).astype(jnp.bfloat16).reshape(row_count, heads_local * hd)
     )
     gated = (glu_value.astype(jnp.float32) * jax.nn.sigmoid(glu_gate.astype(jnp.float32))).astype(
         jnp.bfloat16
@@ -128,8 +367,8 @@
     total_sum, total_squares = lax.psum(
         (jnp.sum(conv_out, axis=1), jnp.sum(conv_out * conv_out, axis=1)), "tp"
     )
-    chan_mean = (total_sum / CW)[:, None]
-    spread = (total_squares / CW)[:, None] - chan_mean * chan_mean
+    chan_mean = (total_sum / channels)[:, None]
+    spread = (total_squares / channels)[:, None] - chan_mean * chan_mean
     centered = conv_out - chan_mean
     channel_out = jax.nn.silu(
         centered * lax.rsqrt(spread + norm_eps) * channel_gain + channel_bias
@@ -164,4 +403,6 @@
         P(),
     )
     out_specs = (P(("grp", "sp"), None), P("tp", ("grp", "sp")))
+    small = mesh.shape["sp"] == 4 and mesh.shape["tp"] == 4
+    local = paired if small else gathered
     return jax.shard_map(local, mesh=mesh, in_specs=in_specs, out_specs=out_specs, check_vma=False)

time: 169 us -> 73.9 us (0.44)
  blocking collectives: 103 us -> 0 us
  between operations: 14 us -> 1.53 us
  starting transfers between devices: 1.41 us -> 13.5 us
  local copies, waits for them, and re-layouts: 6.76 us -> 13.6 us
  Pallas kernels: 0 us -> 5.68 us
  matrix products: 6.76 us -> 4.29 us
    all_gather x7 -> x0, blocking collectives: 82.3 us -> none  [the longest x1 16.1 us: local(): lax.all_gather(weights_in[0], 'sp', axis=0, tiled=True)]
    ppermute x0 -> x15, waiting for transfers between devices: none -> 28.3 us  [exchange(): return lax.ppermute(value, axis, [(s, s ^ bit) for s in range(count)])]
    reduce_scatter x1 -> x0, waiting for transfers between devices: 25 us -> none  [local(): lax.psum_scatter(jnp.dot(attended, w_out_attn, preferred_element_type=jnp...]
    psum x1 -> x0, blocking collectives: 20.6 us -> none  [local(): lax.psum((jnp.sum(conv_out, axis=1), jnp.sum(conv_out * conv_out, axis=1)...]
    ppermute x0 -> x15, starting transfers between devices: none -> 12.2 us  [exchange(): return lax.ppermute(value, axis, [(s, s ^ bit) for s in range(count)])]
    pallas_call x0 -> x2, Pallas kernels: none -> 5.68 us  [the longest x1 2.92 us: finish(): pl.pallas_call(functools.partial(final_kernel, wa.shape[0], wc.shape[0]),...]
    concatenate x0 -> x3, local copies, waits for them, and re-layouts: none -> 3.65 us  [the longest x1 1.67 us: paired(): w_glu = jnp.concatenate([w_glu_value, w_glu_gate], axis=1)]
    slice x3 -> x8, local copies, waits for them, and re-layouts: 0.04 us -> 3.32 us  [the longest x2 3.26 us: depthwise(): out = out + conv_taps[tap] * padded[tap:tap + rows]]
  transfers between devices with their start and end apart: 4 -> 16, of which waited for: 2 -> 9; matrix products, arithmetic and copies ran while one was open for 5% -> 24% of each run, Pallas kernels for 0% -> 4%
where the time goes in v1:
time: 73.9 us; the launch traced here: 73.3 us
  waiting for transfers between devices  30.8 us (42%)
  local copies, waits for them, and re-layouts  13.6 us (18%)
  starting transfers between devices  13.5 us (18%)
  Pallas kernels  5.68 us (8%)
  matrix products  4.29 us (6%)
  other arithmetic  3.88 us (5%)
  between operations  1.53 us (2%)
    ppermute x15, waiting for transfers between devices, exchange(): return lax.ppermute(value, axis, [(s, s ^ bit) for s in range(count)])  28.3 us
    ppermute x15, starting transfers between devices, exchange(): return lax.ppermute(value, axis, [(s, s ^ bit) for s in range(count)])  12.2 us
    unnamed x95, local copies, waits for them, and re-layouts  4.86 us
    dot_general x4, matrix products, dot_f32(): return lax.dot_general(a, b, (dims, ((), ())), preferred_element_type=F32)  4.29 us
    slice x2, local copies, waits for them, and re-layouts, depthwise(): out = out + conv_taps[tap] * padded[tap:tap + rows]  3.26 us
    pallas_call x1, Pallas kernels, finish(): pl.pallas_call(functools.partial(final_kernel, wa.shape[0], wc.shape[0]),...  2.92 us
    pallas_call x1, Pallas kernels, attention(): pl.pallas_call(functools.partial(attention_kernel, hd), out_shape=out_sha...  2.76 us
    ppermute x1, waiting for transfers between devices, from_behind(): lax.ppermute(value, axis, [(source, source + steps) for source in range(i...  2.59 us
  transfers between devices with their start and end apart: 16, of which 9 were waited for; matrix products, arithmetic and copies ran while one was open for 24% of the time, Pallas kernels for 4%

profile of v1, /device:TPU:25, one launch (start us, length us, event | category | flops | bytes accessed | tf_op | source)
XLA Modules:
  0.0 73.3 jit_solution(10792761212222776750)
XLA Ops:
  0.6 2.0 %constant_dynamic-update-slice_fusion.19 = bf16[384,2048]{1,0:T(8,128)(2,1)} fusion(bf16[128,2048]{1,0:T(8,128)(2,1)} %wa.1), kind=kLoop, calls=%fused_computation.125 | loop fusion | bytes 1048576
  2.7 1.0 %constant_dynamic-update-slice_fusion.18 = bf16[384,2048]{1,0:T(8,128)(2,1)} fusion(bf16[384,2048]{1,0:T(8,128)(2,1)} %constant_dynamic-update-slice_fusion.19, bf16[256,2048]{1,0:T(8,128)(2,1)S(1)} %copy-done), kind=kLoop, calls=%fused_computation.124 | loop fusion | bytes 2097152 | tf_op jit(solution)/shard_map/concatenate | solution.py:203
  4.4 1.2 %collective-permute-start.11 = (bf16[384,2048]{1,0:T(8,128)(2,1)}, bf16[384,2048]{1,0:T(8,128)(2,1)}, u32[]{:S(2)}, u32[]{:S(2)}) collective-permute-start(bf16[384,2048]{1,0:T(8,128)(2,1)} %constant_dynamic-update-slice_fusion.18), channel_id=1, source_target_pairs={{0,2},{1,3},{2,0},{3,1},{4,6},{5,7},{6,4},{7,5},{8,10},{9,11},{10,... | collective-permute-start | bytes 4718600 | tf_op jit(solution)/shard_map/ppermute | solution.py:17
  5.8 1.0 %fusion.2 = bf16[128,2048]{1,0:T(8,128)(2,1)} fusion(bf16[128,2048]{1,0:T(8,128)(2,1)S(1)} %copy-done.3, f32[2048]{0:T(1024)S(1)} %copy-done.6, f32[128]{0:T(128)S(1)} %add_rsqrt_fusion), kind=kLoop, calls=%fused_computation.6 | loop fusion | flops 1048576 | bytes 1057280 | tf_op jit(solution)/shard_map/convert_element_type | solution.py:196
  6.8 1.0 %dynamic_slice.19 = bf16[64,1024]{1,0:T(8,128)(2,1)S(1)} dynamic-slice(bf16[128,2048]{1,0:T(8,128)(2,1)} %fusion.2, s32[]{:T(128)S(6)} %select_n.55, s32[]{:T(128)S(6)} %select_n.56), dynamic_slice_sizes={64,1024} | dynamic-slice | bytes 262148 | tf_op jit(solution)/shard_map/dynamic_slice | solution.py:197
  8.7 1.7 %constant_dynamic-update-slice_fusion.16 = bf16[512,512]{1,0:T(8,128)(2,1)} fusion(bf16[512,512]{1,0:T(8,128)(2,1)} %constant_dynamic-update-slice_fusion.17, bf16[512,256]{1,0:T(8,128)(2,1)} %param.21), kind=kLoop, calls=%fused_computation.122 | loop fusion | bytes 524288 | tf_op jit(solution)/shard_map/concatenate | solution.py:201
  10.5 0.9 %constant_dynamic-update-slice_fusion.2 = bf16[512,384]{1,0:T(8,128)(2,1)S(1)} fusion(bf16[512,128]{1,0:T(8,128)(2,1)} %param.17), kind=kLoop, calls=%fused_computation.108 | loop fusion | bytes 262144
  11.4 0.9 %constant_dynamic-update-slice_fusion.1 = bf16[512,384]{1,0:T(8,128)(2,1)S(1)} fusion(bf16[512,384]{1,0:T(8,128)(2,1)S(1)} %constant_dynamic-update-slice_fusion.2, bf16[512,128]{1,0:T(8,128)(2,1)} %param.18), kind=kLoop, calls=%fused_computation.107 | loop fusion | bytes 262144
  12.4 0.9 %constant_dynamic-update-slice_fusion = bf16[512,384]{1,0:T(8,128)(2,1)S(1)} fusion(bf16[512,384]{1,0:T(8,128)(2,1)S(1)} %constant_dynamic-update-slice_fusion.1, bf16[512,128]{1,0:T(8,128)(2,1)} %param.19), kind=kLoop, calls=%fused_computation.106 | loop fusion | bytes 262144 | tf_op jit(solution)/shard_map/concatenate | solution.py:199
  13.3 1.4 %collective-permute-start.2 = (bf16[512,384]{1,0:T(8,128)(2,1)S(1)}, bf16[512,384]{1,0:T(8,128)(2,1)}, u32[]{:S(2)}, u32[]{:S(2)}) collective-permute-start(bf16[512,384]{1,0:T(8,128)(2,1)S(1)} %constant_dynamic-update-slice_fusion), channel_id=1, source_target_pairs={{0,4},{4,0},{8,12},{12,8},{1,5},{5,1},{9,13},{13,9},{2,6},{6,2},{1... | collective-permute-start | bytes 1179656 | tf_op jit(solution)/shard_map/ppermute | solution.py:17
  14.7 1.7 %fusion.53 = (f32[1,256]{1,0:T(1,128)S(1)}, f32[1,256]{1,0:T(1,128)}, f32[1,256]{1,0:T(1,128)}, f32[1,256]{1,0:T(1,128)}, f32[1,256]{1,0:T(1,128)}, /*index=5*/f...) fusion(f32[31,256]{1,0:T(8,128)} %param.24), kind=kLoop, calls=%fused_computation.136 | loop fusion | bytes 38912 | tf_op jit(solution)/shard_map/slice | solution.py:166
  16.4 1.6 %fusion.54 = (f32[1,256]{1,0:T(1,128)}, f32[1,256]{1,0:T(1,128)}, f32[1,256]{1,0:T(1,128)}, f32[1,256]{1,0:T(1,128)}, f32[1,256]{1,0:T(1,128)}, /*index=5*/f32[1...) fusion(f32[31,256]{1,0:T(8,128)} %param.24), kind=kLoop, calls=%fused_computation.137 | loop fusion | bytes 24576 | tf_op jit(solution)/shard_map/slice | solution.py:166
  18.0 1.2 %collective-permute-start.1 = (bf16[64,1024]{1,0:T(8,128)(2,1)}, bf16[64,1024]{1,0:T(8,128)(2,1)}, u32[]{:S(2)}, u32[]{:S(2)}) collective-permute-start(bf16[64,1024]{1,0:T(8,128)(2,1)} %collective-permute-done), channel_id=1, source_target_pairs={{0,1},{1,0},{2,3},{3,2},{4,5},{5,4},{6,7},{7,6},{8,9},{9,8},{10,11... | collective-permute-start | bytes 393224 | tf_op jit(solution)/shard_map/ppermute | solution.py:17
  19.2 0.8 %reshape.19.gain_ref = f32[1,128]{1,0:T(1,128)S(1)} reshape(f32[2,64]{1,0:T(2,128)} %param.23) | data formatting | bytes 1024 | tf_op jit(solution)/shard_map/reshape | solution.py:123
  20.8 1.2 %maximum_select_fusion.1 = bf16[128,1024]{1,0:T(8,128)(2,1)S(1)} fusion(bf16[64,1024]{1,0:T(8,128)(2,1)} %collective-permute-done.1, bf16[64,1024]{1,0:T(8,128)(2,1)} %collective-permute-done, pred[]{:T(512)S(6)} %eq.7), kind=kLoop, calls=%fused_computation.16 | loop fusion | flops 1179648 | bytes 524289 | tf_op jit(solution)/shard_map/jit(_where)/select_n | solution.py:212
  22.3 1.4 %fusion.44 = f32[256,512]{1,0:T(8,128)S(1)} fusion(bf16[512,512]{1,0:T(8,128)(2,1)} %constant_dynamic-update-slice_fusion.16, s32[]{:T(128)S(6)} %select_n.59, bf16[128,1024]{1,0:T(8,128)(2,1)S(1)} %constant_dynamic-slice_fusion, bf16[128,1024]{1,0:T(8,128)(2,1)S(1)} %maximum_select_fusion.1), kind=kOutput, calls=%fused_computation.131 | convolution fusion | flops 134742016 | bytes 1572868 | tf_op jit(solution)/shard_map/dot_general | solution.py:32
  23.7 11.0 %collective-permute-done.2 = bf16[512,384]{1,0:T(8,128)(2,1)} collective-permute-done((bf16[512,384]{1,0:T(8,128)(2,1)S(1)}, bf16[512,384]{1,0:T(8,128)(2,1)}, u32[]{:S(2)}, u32[]{:S(2)}) %collective-permute-start.2) | collective-permute-done | bytes 393248 | tf_op jit(solution)/shard_map/ppermute | solution.py:17
  34.7 1.3 %convolution_add_fusion.1 = f32[256,384]{1,0:T(8,128)S(1)} fusion(f32[256,384]{1,0:T(8,128)S(1)} %fusion.46, bf16[512,384]{1,0:T(8,128)(2,1)} %collective-permute-done.2, s32[]{:T(128)S(6)} %select_n.60, bf16[128,1024]{1,0:T(8,128)(2,1)S(1)} %constant_dynamic-slice_fusion, bf16[128,1024]{1,0:T(8,128)(2,1)S(1)} %maximum_select_fusion.1), kind=kOutput, calls=%fused_computation.3 | convolution fusion | flops 101285888 | bytes 1703940 | tf_op jit(solution)/shard_map/dot_general | solution.py:32
  36.2 1.4 %convolution_add_fusion = f32[256,512]{1,0:T(8,128)S(1)} fusion(f32[256,512]{1,0:T(8,128)S(1)} %fusion.44, bf16[512,512]{1,0:T(8,128)(2,1)} %collective-permute-done.5, s32[]{:T(128)S(6)} %select_n.60, bf16[128,1024]{1,0:T(8,128)(2,1)S(1)} %constant_dynamic-slice_fusion, bf16[128,1024]{1,0:T(8,128)(2,1)S(1)} %maximum_select_fusion.1), kind=kOutput, calls=%fused_computation.2 | convolution fusion | flops 134873088 | bytes 2097156 | tf_op jit(solution)/shard_map/dot_general | solution.py:32
  37.9 2.4 %collective-permute-start.6 = (bf16[128,512]{1,0:T(8,128)(2,1)S(1)}, bf16[128,512]{1,0:T(8,128)(2,1)S(1)}, u32[]{:S(2)}, u32[]{:S(2)}) collective-permute-start(bf16[128,512]{1,0:T(8,128)(2,1)S(1)} %slice.645), channel_id=1, source_target_pairs={{0,8},{4,12},{8,0},{12,4},{1,9},{5,13},{9,1},{13,5},{2,10},{6,14},... | collective-permute-start | bytes 393224 | tf_op jit(solution)/shard_map/ppermute | solution.py:17
  40.3 9.0 %collective-permute-done.3 = bf16[656,128]{1,0:T(8,128)(2,1)S(1)} collective-permute-done((bf16[656,128]{1,0:T(8,128)(2,1)S(1)}, bf16[656,128]{1,0:T(8,128)(2,1)S(1)}, u32[]{:S(2)}, u32[]{:S(2)}) %collective-permute-start.3) | collective-permute-done | bytes 167968 | tf_op jit(solution)/shard_map/ppermute | solution.py:17
  49.6 2.6 %collective-permute-done.6 = bf16[128,512]{1,0:T(8,128)(2,1)S(1)} collective-permute-done((bf16[128,512]{1,0:T(8,128)(2,1)S(1)}, bf16[128,512]{1,0:T(8,128)(2,1)S(1)}, u32[]{:S(2)}, u32[]{:S(2)}) %collective-permute-start.6) | collective-permute-done | bytes 131104 | tf_op jit(solution)/shard_map/ppermute | solution.py:17
  52.3 1.3 %collective-permute-start.7 = (bf16[30,256]{1,0:T(8,128)(2,1)S(1)}, bf16[30,256]{1,0:T(8,128)(2,1)S(1)}, u32[]{:S(2)}, u32[]{:S(2)}) collective-permute-start(bf16[30,256]{1,0:T(8,128)(2,1)S(1)} %slice.410), channel_id=1, source_target_pairs={{0,4},{4,8},{8,12},{1,5},{5,9},{9,13},{2,6},{6,10},{10,14},{3,7},{... | collective-permute-start | bytes 46088 | tf_op jit(solution)/shard_map/ppermute | solution.py:23
  54.2 2.6 %collective-permute-done.7 = bf16[30,256]{1,0:T(8,128)(2,1)S(1)} collective-permute-done((bf16[30,256]{1,0:T(8,128)(2,1)S(1)}, bf16[30,256]{1,0:T(8,128)(2,1)S(1)}, u32[]{:S(2)}, u32[]{:S(2)}) %collective-permute-start.7) | collective-permute-done | bytes 15392 | tf_op jit(solution)/shard_map/ppermute | solution.py:23
  57.6 2.8 %stick_attention.1 = (bf16[128,128]{1,0:T(8,128)(2,1)S(1)}, f32[2,128]{1,0:T(2,128)}) custom-call(bf16[128,128]{1,0:T(8,128)(2,1)S(1)} %fusion.41.q_ref, bf16[512,128]{1,0:T(8,128)(2,1)S(1)} %get-tuple-element.59.k_ref, bf16[512,128]{1,0:T(8,128)(2,1)S(1)} %get-tuple-element.60.v_ref, bf16[32,128]{1,0:T(8,128)(2,1)S(1)} %pad_maximum_fusion.3.off_ref, ...), custom_call_target="tpu_custom_call" | custom-call | flops 400000000 | bytes 1000000 | tf_op jit(solution)/shard_map/stick_attention/pallas_call | solution.py:110
  60.4 1.7 %collective-permute-start.8 = (bf16[64,384]{1,0:T(8,128)(2,1)S(1)}, bf16[64,384]{1,0:T(8,128)(2,1)S(1)}, u32[]{:S(2)}, u32[]{:S(2)}) collective-permute-start(bf16[64,384]{1,0:T(8,128)(2,1)S(1)} %get-tuple-element.22), channel_id=1, source_target_pairs={{0,1},{1,0},{2,3},{3,2},{4,5},{5,4},{6,7},{7,6},{8,9},{9,8},{10,11... | collective-permute-start | bytes 147464 | tf_op jit(solution)/shard_map/ppermute | solution.py:17
  63.7 0.9 %collective-permute-done.14 = f32[4,256]{1,0:T(4,128)S(1)} collective-permute-done((f32[4,256]{1,0:T(4,128)S(1)}, f32[4,256]{1,0:T(4,128)S(1)}, u32[]{:S(2)}, u32[]{:S(2)}) %collective-permute-start.14) | collective-permute-done | bytes 4128 | tf_op jit(solution)/shard_map/ppermute | solution.py:17
  64.6 2.4 %collective-permute-done.9.far = bf16[2,64,384]{2,1,0:T(8,128)(2,1)S(1)} collective-permute-done((bf16[2,64,384]{2,1,0:T(8,128)(2,1)S(1)}, bf16[2,64,384]{2,1,0:T(8,128)(2,1)S(1)}, u32[]{:S(2)}, u32[]{:S(2)}) %collective-permute-start.9) | collective-permute-done | bytes 98336 | tf_op jit(solution)/shard_map/ppermute | solution.py:17
  67.1 2.9 %finish_rows.1 = bf16[64,2048]{1,0:T(8,128)(2,1)S(1)} custom-call(bf16[64,384]{1,0:T(8,128)(2,1)S(1)} %get-tuple-element.23.mine, bf16[64,384]{1,0:T(8,128)(2,1)S(1)} %collective-permute-done.8.core, bf16[2,64,384]{2,1,0:T(8,128)(2,1)S(1)} %collective-permute-done.9.far, bf16[128,2048]{1,0:T(8,128)(2,1)S(1)} %copy-done.1, bf16[256,2048]{1,0:T(8,128)(2,1)S(1)} %copy-done, ...), custom_call_target="tpu_custom_call" | custom-call | flops 800000000 | bytes 7000000 | tf_op jit(solution)/shard_map/finish_rows/pallas_call | solution.py:152
  70.0 1.3 %collective-permute-start.15 = (bf16[64,2048]{1,0:T(8,128)(2,1)S(1)}, bf16[64,2048]{1,0:T(8,128)(2,1)S(1)}, u32[]{:S(2)}, u32[]{:S(2)}) collective-permute-start(bf16[64,2048]{1,0:T(8,128)(2,1)S(1)} %finish_rows.1), channel_id=1, source_target_pairs={{0,1},{1,0},{2,3},{3,2},{4,5},{5,4},{6,7},{7,6},{8,9},{9,8},{10,11... | collective-permute-start | bytes 786440 | tf_op jit(solution)/shard_map/ppermute | solution.py:17
  71.3 1.2 %collective-permute-done.15 = bf16[64,2048]{1,0:T(8,128)(2,1)S(1)} collective-permute-done((bf16[64,2048]{1,0:T(8,128)(2,1)S(1)}, bf16[64,2048]{1,0:T(8,128)(2,1)S(1)}, u32[]{:S(2)}, u32[]{:S(2)}) %collective-permute-start.15) | collective-permute-done | bytes 262176 | tf_op jit(solution)/shard_map/ppermute | solution.py:17
  72.4 0.9 %maximum_select_fusion = bf16[128,2048]{1,0:T(8,128)(2,1)} fusion(bf16[64,2048]{1,0:T(8,128)(2,1)S(1)} %collective-permute-done.15, bf16[64,2048]{1,0:T(8,128)(2,1)S(1)} %finish_rows.1, pred[]{:T(512)S(6)} %eq.7), kind=kLoop, calls=%fused_computation.11 | loop fusion | flops 2359296 | bytes 1048577 | tf_op jit(solution)/shard_map/jit(_where)/select_n | solution.py:257
  (136 shorter events, 6.3 us)
Async XLA Ops:
  3.7 63.3 %collective-permute-start.10 = (bf16[384,2048]{1,0:T(8,128)(2,1)}, bf16[384,2048]{1,0:T(8,128)(2,1)S(1)}, u32[]{:S(2)}, u32[]{:S(2)}) collective-permute-start(bf16[384,2048]{1,0:T(8,128)(2,1)} %constant_dynamic-update-slice_fusion.18), channel_id=1, source_target_pairs={{0,1},{1,0},{2,3},{3,2},{4,5},{5,4},{6,7},{7,6},{8,9},{9,8},{10,11... | collective-permute-start | bytes 4718600 | tf_op jit(solution)/shard_map/ppermute | solution.py:17
  4.4 49.2 %collective-permute-start.11 = (bf16[384,2048]{1,0:T(8,128)(2,1)}, bf16[384,2048]{1,0:T(8,128)(2,1)}, u32[]{:S(2)}, u32[]{:S(2)}) collective-permute-start(bf16[384,2048]{1,0:T(8,128)(2,1)} %constant_dynamic-update-slice_fusion.18), channel_id=1, source_target_pairs={{0,2},{1,3},{2,0},{3,1},{4,6},{5,7},{6,4},{7,5},{8,10},{9,11},{10,... | collective-permute-start | bytes 4718600 | tf_op jit(solution)/shard_map/ppermute | solution.py:17
  7.8 10.1 %collective-permute-start = (bf16[64,1024]{1,0:T(8,128)(2,1)S(1)}, bf16[64,1024]{1,0:T(8,128)(2,1)}, u32[]{:S(2)}, u32[]{:S(2)}) collective-permute-start(bf16[64,1024]{1,0:T(8,128)(2,1)S(1)} %dynamic_slice.19), channel_id=1, source_target_pairs={{0,8},{4,12},{8,0},{12,4},{1,9},{5,13},{9,1},{13,5},{2,10},{6,14},... | collective-permute-start | bytes 393224 | tf_op jit(solution)/shard_map/ppermute | solution.py:17
  10.3 25.9 %collective-permute-start.5 = (bf16[512,512]{1,0:T(8,128)(2,1)}, bf16[512,512]{1,0:T(8,128)(2,1)}, u32[]{:S(2)}, u32[]{:S(2)}) collective-permute-start(bf16[512,512]{1,0:T(8,128)(2,1)} %constant_dynamic-update-slice_fusion.16), channel_id=1, source_target_pairs={{0,4},{4,0},{8,12},{12,8},{1,5},{5,1},{9,13},{13,9},{2,6},{6,2},{1... | collective-permute-start | bytes 1572872 | tf_op jit(solution)/shard_map/ppermute | solution.py:17
  13.3 21.4 %collective-permute-start.2 = (bf16[512,384]{1,0:T(8,128)(2,1)S(1)}, bf16[512,384]{1,0:T(8,128)(2,1)}, u32[]{:S(2)}, u32[]{:S(2)}) collective-permute-start(bf16[512,384]{1,0:T(8,128)(2,1)S(1)} %constant_dynamic-update-slice_fusion), channel_id=1, source_target_pairs={{0,4},{4,0},{8,12},{12,8},{1,5},{5,1},{9,13},{13,9},{2,6},{6,2},{1... | collective-permute-start | bytes 1179656 | tf_op jit(solution)/shard_map/ppermute | solution.py:17
  18.0 2.5 %collective-permute-start.1 = (bf16[64,1024]{1,0:T(8,128)(2,1)}, bf16[64,1024]{1,0:T(8,128)(2,1)}, u32[]{:S(2)}, u32[]{:S(2)}) collective-permute-start(bf16[64,1024]{1,0:T(8,128)(2,1)} %collective-permute-done), channel_id=1, source_target_pairs={{0,1},{1,0},{2,3},{3,2},{4,5},{5,4},{6,7},{7,6},{8,9},{9,8},{10,11... | collective-permute-start | bytes 393224 | tf_op jit(solution)/shard_map/ppermute | solution.py:17
  20.5 41.6 %collective-permute-start.13 = (f32[2,256]{1,0:T(2,128)S(1)}, f32[2,256]{1,0:T(2,128)S(1)}, u32[]{:S(2)}, u32[]{:S(2)}) collective-permute-start(f32[2,256]{1,0:T(2,128)S(1)} %pad_maximum_fusion.5.gb0), channel_id=1, source_target_pairs={{0,1},{1,0},{2,3},{3,2},{4,5},{5,4},{6,7},{7,6},{8,9},{9,8},{10,11... | collective-permute-start | bytes 6152 | tf_op jit(solution)/shard_map/ppermute | solution.py:17
  36.1 13.2 %collective-permute-start.3 = (bf16[656,128]{1,0:T(8,128)(2,1)S(1)}, bf16[656,128]{1,0:T(8,128)(2,1)S(1)}, u32[]{:S(2)}, u32[]{:S(2)}) collective-permute-start(bf16[656,128]{1,0:T(8,128)(2,1)S(1)} %get-tuple-element.58), channel_id=1, source_target_pairs={{0,8},{4,12},{8,0},{12,4},{1,9},{5,13},{9,1},{13,5},{2,10},{6,14},... | collective-permute-start | bytes 503816 | tf_op jit(solution)/shard_map/ppermute | solution.py:17
  37.6 19.2 %copy-start.8 = (f32[1,256]{1,0:T(1,128)S(1)}, f32[1,256]{1,0:T(1,128)}, u32[]{:S(2)}) copy-start(f32[1,256]{1,0:T(1,128)} %get-tuple-element.25) | copy-start | bytes 3076
  37.6 19.2 %copy-start.9 = (f32[1,256]{1,0:T(1,128)S(1)}, f32[1,256]{1,0:T(1,128)}, u32[]{:S(2)}) copy-start(f32[1,256]{1,0:T(1,128)} %get-tuple-element.26) | copy-start | bytes 3076
  37.6 19.2 %copy-start.10 = (f32[1,256]{1,0:T(1,128)S(1)}, f32[1,256]{1,0:T(1,128)}, u32[]{:S(2)}) copy-start(f32[1,256]{1,0:T(1,128)} %get-tuple-element.27) | copy-start | bytes 3076
  37.6 19.2 %copy-start.11 = (f32[1,256]{1,0:T(1,128)S(1)}, f32[1,256]{1,0:T(1,128)}, u32[]{:S(2)}) copy-start(f32[1,256]{1,0:T(1,128)} %get-tuple-element.28) | copy-start | bytes 3076
  37.6 19.2 %copy-start.12 = (f32[1,256]{1,0:T(1,128)S(1)}, f32[1,256]{1,0:T(1,128)}, u32[]{:S(2)}) copy-start(f32[1,256]{1,0:T(1,128)} %get-tuple-element.29) | copy-start | bytes 3076
  37.6 19.2 %copy-start.13 = (f32[1,256]{1,0:T(1,128)S(1)}, f32[1,256]{1,0:T(1,128)}, u32[]{:S(2)}) copy-start(f32[1,256]{1,0:T(1,128)} %get-tuple-element.30) | copy-start | bytes 3076
  37.7 19.2 %copy-start.14 = (f32[1,256]{1,0:T(1,128)S(1)}, f32[1,256]{1,0:T(1,128)}, u32[]{:S(2)}) copy-start(f32[1,256]{1,0:T(1,128)} %get-tuple-element.31) | copy-start | bytes 3076
  37.7 19.2 %copy-start.15 = (f32[1,256]{1,0:T(1,128)S(1)}, f32[1,256]{1,0:T(1,128)}, u32[]{:S(2)}) copy-start(f32[1,256]{1,0:T(1,128)} %get-tuple-element.32) | copy-start | bytes 3076
  37.7 19.2 %copy-start.16 = (f32[1,256]{1,0:T(1,128)S(1)}, f32[1,256]{1,0:T(1,128)}, u32[]{:S(2)}) copy-start(f32[1,256]{1,0:T(1,128)} %get-tuple-element.33) | copy-start | bytes 3076
  37.7 19.2 %copy-start.17 = (f32[1,256]{1,0:T(1,128)S(1)}, f32[1,256]{1,0:T(1,128)}, u32[]{:S(2)}) copy-start(f32[1,256]{1,0:T(1,128)} %get-tuple-element.34) | copy-start | bytes 3076
  37.7 19.2 %copy-start.18 = (f32[1,256]{1,0:T(1,128)S(1)}, f32[1,256]{1,0:T(1,128)}, u32[]{:S(2)}) copy-start(f32[1,256]{1,0:T(1,128)} %get-tuple-element.35) | copy-start | bytes 3076
  37.7 19.2 %copy-start.19 = (f32[1,256]{1,0:T(1,128)S(1)}, f32[1,256]{1,0:T(1,128)}, u32[]{:S(2)}) copy-start(f32[1,256]{1,0:T(1,128)} %get-tuple-element.36) | copy-start | bytes 3076
  37.7 19.2 %copy-start.20 = (f32[1,256]{1,0:T(1,128)S(1)}, f32[1,256]{1,0:T(1,128)}, u32[]{:S(2)}) copy-start(f32[1,256]{1,0:T(1,128)} %get-tuple-element.37) | copy-start | bytes 3076
  37.7 19.2 %copy-start.21 = (f32[1,256]{1,0:T(1,128)S(1)}, f32[1,256]{1,0:T(1,128)}, u32[]{:S(2)}) copy-start(f32[1,256]{1,0:T(1,128)} %get-tuple-element.38) | copy-start | bytes 3076
  37.7 19.2 %copy-start.22 = (f32[1,256]{1,0:T(1,128)S(1)}, f32[1,256]{1,0:T(1,128)}, u32[]{:S(2)}) copy-start(f32[1,256]{1,0:T(1,128)} %get-tuple-element.39) | copy-start | bytes 3076
  37.7 19.2 %copy-start.23 = (f32[1,256]{1,0:T(1,128)S(1)}, f32[1,256]{1,0:T(1,128)}, u32[]{:S(2)}) copy-start(f32[1,256]{1,0:T(1,128)} %get-tuple-element.40) | copy-start | bytes 3076
  37.9 14.3 %collective-permute-start.6 = (bf16[128,512]{1,0:T(8,128)(2,1)S(1)}, bf16[128,512]{1,0:T(8,128)(2,1)S(1)}, u32[]{:S(2)}, u32[]{:S(2)}) collective-permute-start(bf16[128,512]{1,0:T(8,128)(2,1)S(1)} %slice.645), channel_id=1, source_target_pairs={{0,8},{4,12},{8,0},{12,4},{1,9},{5,13},{9,1},{13,5},{2,10},{6,14},... | collective-permute-start | bytes 393224 | tf_op jit(solution)/shard_map/ppermute | solution.py:17
  49.5 8.0 %collective-permute-start.4 = (bf16[528,128]{1,0:T(8,128)(2,1)S(1)}, bf16[528,128]{1,0:T(8,128)(2,1)S(1)}, u32[]{:S(2)}, u32[]{:S(2)}) collective-permute-start(bf16[528,128]{1,0:T(8,128)(2,1)S(1)} %get-tuple-element.15), channel_id=1, source_target_pairs={{0,4},{4,0},{8,12},{12,8},{1,5},{5,1},{9,13},{13,9},{2,6},{6,2},{1... | collective-permute-start | bytes 405512 | tf_op jit(solution)/shard_map/ppermute | solution.py:17
  52.3 4.5 %collective-permute-start.7 = (bf16[30,256]{1,0:T(8,128)(2,1)S(1)}, bf16[30,256]{1,0:T(8,128)(2,1)S(1)}, u32[]{:S(2)}, u32[]{:S(2)}) collective-permute-start(bf16[30,256]{1,0:T(8,128)(2,1)S(1)} %slice.410), channel_id=1, source_target_pairs={{0,4},{4,8},{8,12},{1,5},{5,9},{9,13},{2,6},{6,10},{10,14},{3,7},{... | collective-permute-start | bytes 46088 | tf_op jit(solution)/shard_map/ppermute | solution.py:23
  53.6 13.4 %collective-permute-start.12 = (bf16[384,2048]{1,0:T(8,128)(2,1)}, bf16[384,2048]{1,0:T(8,128)(2,1)S(1)}, u32[]{:S(2)}, u32[]{:S(2)}) collective-permute-start(bf16[384,2048]{1,0:T(8,128)(2,1)} %collective-permute-done.11.wx), channel_id=1, source_target_pairs={{0,1},{1,0},{2,3},{3,2},{4,5},{5,4},{6,7},{7,6},{8,9},{9,8},{10,11... | collective-permute-start | bytes 4718600 | tf_op jit(solution)/shard_map/ppermute | solution.py:17
  60.4 2.6 %collective-permute-start.8 = (bf16[64,384]{1,0:T(8,128)(2,1)S(1)}, bf16[64,384]{1,0:T(8,128)(2,1)S(1)}, u32[]{:S(2)}, u32[]{:S(2)}) collective-permute-start(bf16[64,384]{1,0:T(8,128)(2,1)S(1)} %get-tuple-element.22), channel_id=1, source_target_pairs={{0,1},{1,0},{2,3},{3,2},{4,5},{5,4},{6,7},{7,6},{8,9},{9,8},{10,11... | collective-permute-start | bytes 147464 | tf_op jit(solution)/shard_map/ppermute | solution.py:17
  62.1 2.5 %collective-permute-start.14 = (f32[4,256]{1,0:T(4,128)S(1)}, f32[4,256]{1,0:T(4,128)S(1)}, u32[]{:S(2)}, u32[]{:S(2)}) collective-permute-start(f32[4,256]{1,0:T(4,128)S(1)} %pad_maximum_fusion.4), channel_id=1, source_target_pairs={{0,2},{1,3},{2,0},{3,1},{4,6},{5,7},{6,4},{7,5},{8,10},{9,11},{10,... | collective-permute-start | bytes 12296 | tf_op jit(solution)/shard_map/ppermute | solution.py:17
  63.0 4.1 %collective-permute-start.9 = (bf16[2,64,384]{2,1,0:T(8,128)(2,1)S(1)}, bf16[2,64,384]{2,1,0:T(8,128)(2,1)S(1)}, u32[]{:S(2)}, u32[]{:S(2)}) collective-permute-start(bf16[2,64,384]{2,1,0:T(8,128)(2,1)S(1)} %pad_maximum_fusion.2), channel_id=1, source_target_pairs={{0,2},{1,3},{2,0},{3,1},{4,6},{5,7},{6,4},{7,5},{8,10},{9,11},{10,... | collective-permute-start | bytes 294920 | tf_op jit(solution)/shard_map/ppermute | solution.py:17
  70.0 2.4 %collective-permute-start.15 = (bf16[64,2048]{1,0:T(8,128)(2,1)S(1)}, bf16[64,2048]{1,0:T(8,128)(2,1)S(1)}, u32[]{:S(2)}, u32[]{:S(2)}) collective-permute-start(bf16[64,2048]{1,0:T(8,128)(2,1)S(1)} %finish_rows.1), channel_id=1, source_target_pairs={{0,1},{1,0},{2,3},{3,2},{4,5},{5,4},{6,7},{7,6},{8,9},{9,8},{10,11... | collective-permute-start | bytes 786440 | tf_op jit(solution)/shard_map/ppermute | solution.py:17
  (26 other events, 364.1 us)

commit v2 on v1

--- a/solution.py
+++ b/solution.py
@@ -123,41 +123,100 @@
     )(q, k, v, off, head_gain.reshape(1, width))
 
 
-def final_kernel(aw, cw, mine, core, far, wa, wc, wcore, wx, wxc, gb0, gb1, gb2, gb3, gain_ref, out_ref):
-    acts = [mine[...], core[...], far[0], far[1]]
-    convs = [a[:, aw:].astype(F32) for a in acts]
-    count = len(convs) * cw
+def norm_kernel(rows_out, x_ref, gain_ref, send_ref, own_ref, pair_ref, normed):
+    side, low = lax.axis_index("sp") // 2, lax.axis_index("sp") % 2
+    core = lax.axis_index("tp") % 2
+    block = own_ref.shape[1]
+    half = 2 * block
+    x = x_ref[...].astype(F32)
+    squares = jnp.mean(x * x, axis=1, keepdims=True)
+    normed[...] = (x * lax.rsqrt(squares + norm_eps) * gain_ref[...]).astype(BF16)
+    first = pl.multiple_of(core * rows_out, rows_out)
+    away = pl.multiple_of((1 - side) * half, half)
+    send_ref[...] = normed[pl.ds(first, rows_out), pl.ds(away, half)]
+    own_ref[...] = normed[:, pl.ds(pl.multiple_of(side * half + low * block, block), block)]
+    pair_ref[...] = normed[:, pl.ds(pl.multiple_of(side * half + (1 - low) * block, block), block)]
+
+
+def norm_parts(tokens, gain, block):
+    rows, features = tokens.shape
+    return pl.pallas_call(
+        functools.partial(norm_kernel, rows // 2),
+        out_shape=(
+            jax.ShapeDtypeStruct((rows // 2, 2 * block), BF16),
+            jax.ShapeDtypeStruct((rows, block), BF16),
+            jax.ShapeDtypeStruct((rows, block), BF16),
+        ),
+        in_specs=[pl.BlockSpec(memory_space=pltpu.VMEM)] * 2,
+        out_specs=[pl.BlockSpec(memory_space=pltpu.VMEM)] * 3,
+        scratch_shapes=[pltpu.VMEM((rows, features), BF16)],
+        cost_estimate=pl.CostEstimate(flops=2_000_000, bytes_accessed=1_000_000, transcendentals=128),
+        compiler_params=pltpu.CompilerParams(vmem_limit_bytes=16 * 1024 * 1024),
+        name="norm_parts",
+    )(tokens, gain.reshape(1, features))
+
+
+def assemble_kernel(own_ref, pair_ref, got_ref, other_ref, own_out, pair_out):
+    low = lax.axis_index("sp") % 2
+    core = lax.axis_index("tp") % 2
+    rows, block = own_ref.shape
+    half = got_ref.shape[0]
+    own_out[:rows, :] = own_ref[...]
+    pair_out[:rows, :] = pair_ref[...]
+    own_at = pl.multiple_of(low * block, block)
+    pair_at = pl.multiple_of((1 - low) * block, block)
+    for part, at in ((got_ref, core), (other_ref, 1 - core)):
+        first = pl.multiple_of(rows + at * half, half)
+        own_out[pl.ds(first, half), :] = part[:, pl.ds(own_at, block)]
+        pair_out[pl.ds(first, half), :] = part[:, pl.ds(pair_at, block)]
+
+
+def assemble(own, pair, got, other):
+    rows, block = own.shape
+    shape = jax.ShapeDtypeStruct((2 * rows, block), BF16)
+    return pl.pallas_call(
+        assemble_kernel,
+        out_shape=(shape, shape),
+        in_specs=[pl.BlockSpec(memory_space=pltpu.VMEM)] * 4,
+        out_specs=[pl.BlockSpec(memory_space=pltpu.VMEM)] * 2,
+        cost_estimate=pl.CostEstimate(flops=2_000_000, bytes_accessed=1_000_000, transcendentals=0),
+        compiler_params=pltpu.CompilerParams(vmem_limit_bytes=16 * 1024 * 1024),
+        name="assemble",
+    )(own, pair, got, other)
+
+
+def final_kernel(*refs):
+    att, conv, wa, wc, gb = (refs[n * 4 : (n + 1) * 4] for n in range(5))
+    gain_ref, out_ref = refs[20:]
+    convs = [c[...].astype(F32) for c in conv]
+    count = 4 * convs[0].shape[1]
     mean = sum(jnp.sum(v, axis=1, keepdims=True) for v in convs) / count
     centered = [v - mean for v in convs]
     spread = sum(jnp.sum(v * v, axis=1, keepdims=True) for v in centered) / count
     inverse = lax.rsqrt(spread + norm_eps)
+    acts = []
+    for slot in range(4):
+        y = centered[slot] * inverse * gb[slot][0:1, :] + gb[slot][1:2, :]
+        acts.append((y * jax.nn.sigmoid(y)).astype(BF16))
     total = None
-    for slot, (v, gb) in enumerate(zip(centered, (gb0, gb1, gb2, gb3))):
-        y = v * inverse * gb[0:1, :] + gb[1:2, :]
-        y = (y * jax.nn.sigmoid(y)).astype(BF16)
-        att = acts[slot][:, :aw]
-        if slot == 0:
-            part = dot_f32(att, wa[...]) + dot_f32(y, wc[...])
-        else:
-            w = (wcore, wx, wxc)[slot - 1]
-            part = dot_f32(jnp.concatenate([att, y], axis=1), w[...])
+    for slot in range(4):
+        part = dot_f32(att[slot][...], wa[slot][...]) + dot_f32(acts[slot], wc[slot][...])
         total = part if total is None else total + part
     squares = jnp.mean(total * total, axis=1, keepdims=True)
     out_ref[...] = (total * lax.rsqrt(squares + norm_eps) * gain_ref[...]).astype(BF16)
 
 
-def finish(mine, core, far, wa, wc, wcore, wx, wxc, gbs, out_gain):
-    rows = mine.shape[0]
-    width = wa.shape[1]
+def finish(att, conv, wa, wc, gb, out_gain):
+    rows, width = att[0].shape[0], wa[0].shape[1]
     return pl.pallas_call(
-        functools.partial(final_kernel, wa.shape[0], wc.shape[0]),
+        final_kernel,
         out_shape=jax.ShapeDtypeStruct((rows, width), BF16),
-        in_specs=[pl.BlockSpec(memory_space=pltpu.VMEM)] * 13,
+        in_specs=[pl.BlockSpec(memory_space=pltpu.VMEM)] * 21,
         out_specs=pl.BlockSpec(memory_space=pltpu.VMEM),
         cost_estimate=pl.CostEstimate(flops=800_000_000, bytes_accessed=7_000_000, transcendentals=70_000),
         compiler_params=pltpu.CompilerParams(vmem_limit_bytes=32 * 1024 * 1024),
         name="finish_rows",
-    )(mine, core, far, wa, wc, wcore, wx, wxc, *gbs, out_gain.reshape(1, width))
+    )(*att, *conv, *wa, *wc, *gb, out_gain.reshape(1, width))
 
 
 def depthwise(padded, conv_taps, rows):
@@ -184,50 +243,39 @@
     w_out_conv,
     out_gain,
 ):
-    rows, features = tokens.shape
-    half_rows, block = rows // 2, w_query.shape[0]
-    half = 2 * block
-    heads, hd = head_gain.shape
-    aw, cw = heads * hd, conv_taps.shape[1]
-    me_sp, me_tp = lax.axis_index("sp"), lax.axis_index("tp")
-    side, low = me_sp // 2, me_sp % 2
-    core = me_tp % 2
-
-    normed = row_norm(tokens.astype(F32), norm_gain).astype(BF16)
-    x_send = lax.dynamic_slice(normed, (core * half_rows, (1 - side) * half), (half_rows, half))
+    rows = tokens.shape[0]
+    heads, _ = head_gain.shape
+    x_send, mine_own, mine_pair = norm_parts(tokens, norm_gain, w_query.shape[0])
     x_got = exchange(x_send, "sp", 2)
-    w_attn = jnp.concatenate([w_query, w_key, w_value], axis=1)
-    w_attn_pair = exchange(w_attn, "sp", 1)
-    w_glu = jnp.concatenate([w_glu_value, w_glu_gate], axis=1)
-    w_glu_pair = exchange(w_glu, "sp", 1)
-    w_out = jnp.concatenate([w_out_attn, w_out_conv], axis=0)
-    w_out_x = exchange(w_out, "tp", 2)
-    w_out_core = exchange(w_out, "tp", 1)
+    wk_pair = exchange(w_key, "sp", 1)
+    wv_pair = exchange(w_value, "sp", 1)
+    gv_pair = exchange(w_glu_value, "sp", 1)
+    gg_pair = exchange(w_glu_gate, "sp", 1)
+    wq_pair = exchange(w_query, "sp", 1)
+    wa_x = exchange(w_out_attn, "tp", 2)
+    wc_x = exchange(w_out_conv, "tp", 2)
+    wa_core = exchange(w_out_attn, "tp", 1)
+    wc_core = exchange(w_out_conv, "tp", 1)
     gb = jnp.stack([channel_gain, channel_bias])
-    gb_core = exchange(gb, "tp", 1)
-    gb_x = exchange(jnp.concatenate([gb, gb_core]), "tp", 2)
+    gbs = [gb] + [exchange(gb, "tp", bit) for bit in (1, 2, 3)]
     x_other = exchange(x_got, "tp", 1)
-    w_out_xc = exchange(w_out_x, "tp", 1)
-
-    x_cross = jnp.where(
-        core == 0, jnp.concatenate([x_got, x_other]), jnp.concatenate([x_other, x_got])
-    )
-    x_mine = lax.dynamic_slice(normed, (0, side * half), (rows, half))
-    x_all = jnp.concatenate([x_mine, x_cross])
-    x_own = lax.dynamic_slice(x_all, (0, low * block), (2 * rows, block))
-    x_pair = lax.dynamic_slice(x_all, (0, (1 - low) * block), (2 * rows, block))
-
-    p = dot_f32(x_own, w_attn) + dot_f32(x_pair, w_attn_pair)
-    pq, pk, pv = (p[:, n * aw : (n + 1) * aw] for n in range(3))
+    wa_xc = exchange(wa_x, "tp", 1)
+    wc_xc = exchange(wc_x, "tp", 1)
+
+    x_own, x_pair = assemble(mine_own, mine_pair, x_got, x_other)
+
+    def project(own, pair):
+        return dot_f32(x_own, own) + dot_f32(x_pair, pair)
+
     off = jnp.pad(key_offset.T, ((0, 8 - heads), (0, 0)))
-    sent = jnp.concatenate([pq[rows:], pk[rows:], pv[rows:], pk[:rows], pv[:rows]]).astype(BF16)
-    got = exchange(jnp.concatenate([sent, off, off]), "sp", 2)
-    g = [got[n * rows : (n + 1) * rows].astype(F32) for n in range(5)]
-    q = (pq[:rows] + g[0]).astype(BF16)
-    k_two = jnp.concatenate([pk[:rows] + g[1], pk[rows:] + g[3]]).astype(BF16)
-    v_two = jnp.concatenate([pv[:rows] + g[2], pv[rows:] + g[4]]).astype(BF16)
-    off_two = jnp.concatenate([off, got[5 * rows : 5 * rows + 8]])
-    mine_two = jnp.concatenate([k_two, v_two, off_two])
+    pk = project(w_key, wk_pair)
+    k_got = exchange(jnp.concatenate([pk[rows:], pk[:rows]]).astype(BF16), "sp", 2)
+    pv = project(w_value, wv_pair)
+    v_sent = jnp.concatenate([pv[rows:], pv[:rows]]).astype(BF16)
+    v_got = exchange(jnp.concatenate([v_sent, off, off]), "sp", 2)
+    k_two = (pk + k_got.astype(F32)).astype(BF16)
+    v_two = (pv + v_got[: 2 * rows].astype(F32)).astype(BF16)
+    mine_two = jnp.concatenate([k_two, v_two, off, v_got[2 * rows : 2 * rows + 8]])
     pair_two = exchange(mine_two, "sp", 1)
 
     def slots(first, size):
@@ -236,25 +284,26 @@
 
     k_all, v_all, off_all = slots(0, rows), slots(2 * rows, rows), slots(4 * rows, 8)
 
-    pg = dot_f32(x_own, w_glu) + dot_f32(x_pair, w_glu_pair)
-    glu = pg[:rows] + exchange(pg[rows:].astype(BF16), "sp", 2).astype(F32)
-    gated = (glu[:, :cw] * jax.nn.sigmoid(glu[:, cw:])).astype(BF16)
+    pgv = project(w_glu_value, gv_pair)
+    gv = pgv[:rows] + exchange(pgv[rows:].astype(BF16), "sp", 2).astype(F32)
+    pgg = project(w_glu_gate, gg_pair)
+    gg = pgg[:rows] + exchange(pgg[rows:].astype(BF16), "sp", 2).astype(F32)
+    pq = project(w_query, wq_pair)
+    q = (pq[:rows] + exchange(pq[rows:].astype(BF16), "sp", 2).astype(F32)).astype(BF16)
+
+    gated = (gv * jax.nn.sigmoid(gg)).astype(BF16)
     reach = conv_taps.shape[0] - 1
     before = from_behind(gated[rows - reach :], "sp", 1)
+
+    attended, log_mass = attention(q, k_all, v_all, off_all, head_gain)
+    att = [attended] + [exchange(attended, "tp", bit) for bit in (1, 2, 3)]
+
     padded = jnp.concatenate([before, gated]).astype(F32)
     conv_out = depthwise(padded, conv_taps, rows).astype(BF16)
-
-    attended, log_mass = attention(q, k_all, v_all, off_all, head_gain)
-
-    act = jnp.concatenate([attended, conv_out], axis=1)
-    mine = lax.dynamic_slice(act, (core * half_rows, 0), (half_rows, aw + cw))
-    theirs = lax.dynamic_slice(act, ((1 - core) * half_rows, 0), (half_rows, aw + cw))
-    from_core = exchange(theirs, "tp", 1)
-    far = exchange(jnp.stack([mine, from_core]), "tp", 2)
-    gbs = (gb, gb_core, gb_x[:2], gb_x[2:])
-    done = finish(mine, from_core, far, w_out_attn, w_out_conv, w_out_core, w_out_x, w_out_xc, gbs, out_gain)
-    other = exchange(done, "tp", 1)
-    mixed = jnp.where(core == 0, jnp.concatenate([done, other]), jnp.concatenate([other, done]))
+    conv = [conv_out] + [exchange(conv_out, "tp", bit) for bit in (1, 2, 3)]
+    wa = (w_out_attn, wa_core, wa_x, wa_xc)
+    wc = (w_out_conv, wc_core, wc_x, wc_xc)
+    mixed = finish(att, conv, wa, wc, gbs, out_gain)
     return (mixed, log_mass)
 
 
@@ -347,7 +396,7 @@
         )
         return (head_mix, mass_sum + jnp.sum(weights, axis=3), carried + jnp.sum(log_not, axis=3))
 
-    head_mix, mass_sum, leftover = lax.fori_loop(
+    head_mix, mass_sum, _ = lax.fori_loop(
         0, last_block + 1, sweep, (zeros_mix, zeros_row, zeros_row)
     )
     log_mass = jnp.log(mass_sum).reshape(heads_local, row_count)

time: 73.9 us -> 89.5 us (1.21)
  starting transfers between devices: 13.5 us -> 35.3 us
  local copies, waits for them, and re-layouts: 13.6 us -> 4.06 us
  waiting for transfers between devices: 30.8 us -> 40 us
  other arithmetic: 3.88 us -> 1.21 us
  matrix products: 4.29 us -> 2.18 us
    ppermute x15 -> x28, starting transfers between devices: 12.2 us -> 34.1 us  [exchange(): return lax.ppermute(value, axis, [(s, s ^ bit) for s in range(count)])]
    ppermute x15 -> x28, waiting for transfers between devices: 28.3 us -> 36.9 us  [exchange(): return lax.ppermute(value, axis, [(s, s ^ bit) for s in range(count)])]
    concatenate x3 -> x0, local copies, waits for them, and re-layouts: 3.65 us -> none  [the longest x1 1.67 us: paired(): w_glu = jnp.concatenate([w_glu_value, w_glu_gate], axis=1)]
    slice x2, local copies, waits for them, and re-layouts: 3.26 us -> 0.02 us  [depthwise(): out = out + conv_taps[tap] * padded[tap:tap + rows]]
    dot_general x4 -> x10, matrix products: 4.29 us -> 2.18 us  [dot_f32(): return lax.dot_general(a, b, (dims, ((), ())), preferred_element_type=F32)]
    select_n x2 -> x0, other arithmetic: 2.06 us -> none  [the longest x1 1.16 us: paired(): jnp.where(core == 0, jnp.concatenate([x_got, x_other]), jnp.concatenate([...]
    dynamic_slice x2 -> x0, local copies, waits for them, and re-layouts: 1 us -> none  [the longest x1 0.98 us: paired(): lax.dynamic_slice(normed, (core * half_rows, (1 - side) * half), (half_ro...]
    unnamed x95 -> x26, local copies, waits for them, and re-layouts: 4.86 us -> 3.87 us
  transfers between devices with their start and end apart: 16 -> 29, of which waited for: 9 -> 16; matrix products, arithmetic and copies ran while one was open for 24% -> 4% of each run, Pallas kernels for 4% -> 3%
where the time goes in v2:
time: 89.5 us; the launch traced here: 89.3 us
  waiting for transfers between devices  40 us (45%)
  starting transfers between devices  35.3 us (39%)
  Pallas kernels  5.45 us (6%)
  local copies, waits for them, and re-layouts  4.06 us (5%)
  matrix products  2.18 us (2%)
  other arithmetic  1.21 us (1%)
  between operations  1.01 us (1%)
    ppermute x28, waiting for transfers between devices, exchange(): return lax.ppermute(value, axis, [(s, s ^ bit) for s in range(count)])  36.9 us
    ppermute x28, starting transfers between devices, exchange(): return lax.ppermute(value, axis, [(s, s ^ bit) for s in range(count)])  34.1 us
    unnamed x26, local copies, waits for them, and re-layouts  3.87 us
    ppermute x1, waiting for transfers between devices, from_behind(): lax.ppermute(value, axis, [(source, source + steps) for source in range(i...  3.11 us
    pallas_call x1, Pallas kernels, attention(): pl.pallas_call(functools.partial(attention_kernel, hd), out_shape=out_sha...  2.75 us
    pallas_call x1, Pallas kernels, finish(): pl.pallas_call(final_kernel, out_shape=jax.ShapeDtypeStruct((rows, width)...  2.41 us
    dot_general x10, matrix products, dot_f32(): return lax.dot_general(a, b, (dims, ((), ())), preferred_element_type=F32)  2.18 us
  transfers between devices with their start and end apart: 29, of which 16 were waited for; matrix products, arithmetic and copies ran while one was open for 4% of the time, Pallas kernels for 3%

profile of v2, /device:TPU:25, one launch (start us, length us, event | category | flops | bytes accessed | tf_op | source)
XLA Modules:
  0.0 89.3 jit_solution(6493672064796857894)
XLA Ops:
  1.4 1.2 %collective-permute-start.24 = (bf16[256,2048]{1,0:T(8,128)(2,1)}, bf16[256,2048]{1,0:T(8,128)(2,1)S(1)}, u32[]{:S(2)}, u32[]{:S(2)}) collective-permute-start(bf16[256,2048]{1,0:T(8,128)(2,1)} %refs_12_.1), channel_id=1, source_target_pairs={{0,2},{1,3},{2,0},{3,1},{4,6},{5,7},{6,4},{7,5},{8,10},{9,11},{10,... | collective-permute-start | bytes 3145736 | tf_op jit(solution)/shard_map/ppermute | solution.py:17
  4.0 1.0 %copy-done.2 = bf16[128,2048]{1,0:T(8,128)(2,1)S(1)} copy-done((bf16[128,2048]{1,0:T(8,128)(2,1)S(1)}, bf16[128,2048]{1,0:T(8,128)(2,1)}, u32[]{:S(2)}) %copy-start.2) | copy-done | bytes 524312
  6.7 5.8 %collective-permute-done.got_ref = bf16[64,1024]{1,0:T(8,128)(2,1)S(1)} collective-permute-done((bf16[64,1024]{1,0:T(8,128)(2,1)S(1)}, bf16[64,1024]{1,0:T(8,128)(2,1)S(1)}, u32[]{:S(2)}, u32[]{:S(2)}) %collective-permute-start) | collective-permute-done | bytes 131104 | tf_op jit(solution)/shard_map/ppermute | solution.py:17
  12.5 1.0 %collective-permute-start.1 = (bf16[64,1024]{1,0:T(8,128)(2,1)S(1)}, bf16[64,1024]{1,0:T(8,128)(2,1)S(1)}, u32[]{:S(2)}, u32[]{:S(2)}) collective-permute-start(bf16[64,1024]{1,0:T(8,128)(2,1)S(1)} %collective-permute-done.got_ref), channel_id=1, source_target_pairs={{0,1},{1,0},{2,3},{3,2},{4,5},{5,4},{6,7},{7,6},{8,9},{9,8},{10,11... | collective-permute-start | bytes 393224 | tf_op jit(solution)/shard_map/ppermute | solution.py:17
  14.5 2.1 %collective-permute-start.2 = (bf16[512,128]{1,0:T(8,128)(2,1)S(1)}, bf16[512,128]{1,0:T(8,128)(2,1)S(1)}, u32[]{:S(2)}, u32[]{:S(2)}) collective-permute-start(bf16[512,128]{1,0:T(8,128)(2,1)S(1)} %copy-done.7), channel_id=1, source_target_pairs={{0,4},{4,0},{8,12},{12,8},{1,5},{5,1},{9,13},{13,9},{2,6},{6,2},{1... | collective-permute-start | bytes 393224 | tf_op jit(solution)/shard_map/ppermute | solution.py:17
  17.7 2.4 %collective-permute-done.2 = bf16[512,128]{1,0:T(8,128)(2,1)S(1)} collective-permute-done((bf16[512,128]{1,0:T(8,128)(2,1)S(1)}, bf16[512,128]{1,0:T(8,128)(2,1)S(1)}, u32[]{:S(2)}, u32[]{:S(2)}) %collective-permute-start.2) | collective-permute-done | bytes 131104 | tf_op jit(solution)/shard_map/ppermute | solution.py:17
  20.1 1.2 %collective-permute-start.12 = (bf16[512,256]{1,0:T(8,128)(2,1)S(1)}, bf16[512,256]{1,0:T(8,128)(2,1)S(1)}, u32[]{:S(2)}, u32[]{:S(2)}) collective-permute-start(bf16[512,256]{1,0:T(8,128)(2,1)S(1)} %copy-done.6), channel_id=1, source_target_pairs={{0,4},{4,0},{8,12},{12,8},{1,5},{5,1},{9,13},{13,9},{2,6},{6,2},{1... | collective-permute-start | bytes 786440 | tf_op jit(solution)/shard_map/ppermute | solution.py:17
  22.7 5.0 %collective-permute-done.12 = bf16[512,256]{1,0:T(8,128)(2,1)S(1)} collective-permute-done((bf16[512,256]{1,0:T(8,128)(2,1)S(1)}, bf16[512,256]{1,0:T(8,128)(2,1)S(1)}, u32[]{:S(2)}, u32[]{:S(2)}) %collective-permute-start.12) | collective-permute-done | bytes 262176 | tf_op jit(solution)/shard_map/ppermute | solution.py:17
  27.8 1.2 %collective-permute-start.6 = (bf16[512,128]{1,0:T(8,128)(2,1)S(1)}, bf16[512,128]{1,0:T(8,128)(2,1)S(1)}, u32[]{:S(2)}, u32[]{:S(2)}) collective-permute-start(bf16[512,128]{1,0:T(8,128)(2,1)S(1)} %copy-done.9), channel_id=1, source_target_pairs={{0,4},{4,0},{8,12},{12,8},{1,5},{5,1},{9,13},{13,9},{2,6},{6,2},{1... | collective-permute-start | bytes 393224 | tf_op jit(solution)/shard_map/ppermute | solution.py:17
  29.4 1.4 %collective-permute-start.3 = (bf16[128,128]{1,0:T(8,128)(2,1)S(1)}, bf16[128,128]{1,0:T(8,128)(2,1)S(1)}, u32[]{:S(2)}, u32[]{:S(2)}) collective-permute-start(bf16[128,128]{1,0:T(8,128)(2,1)S(1)} %slice.595), channel_id=1, source_target_pairs={{0,8},{4,12},{8,0},{12,4},{1,9},{5,13},{9,1},{13,5},{2,10},{6,14},... | collective-permute-start | bytes 98312 | tf_op jit(solution)/shard_map/ppermute | solution.py:17
  32.1 2.3 %collective-permute-start.15 = (bf16[128,256]{1,0:T(8,128)(2,1)S(1)}, bf16[128,256]{1,0:T(8,128)(2,1)S(1)}, u32[]{:S(2)}, u32[]{:S(2)}) collective-permute-start(bf16[128,256]{1,0:T(8,128)(2,1)S(1)} %slice.593), channel_id=1, source_target_pairs={{0,8},{4,12},{8,0},{12,4},{1,9},{5,13},{9,1},{13,5},{2,10},{6,14},... | collective-permute-start | bytes 196616 | tf_op jit(solution)/shard_map/ppermute | solution.py:17
  34.6 3.0 %collective-permute-done.15 = bf16[128,256]{1,0:T(8,128)(2,1)S(1)} collective-permute-done((bf16[128,256]{1,0:T(8,128)(2,1)S(1)}, bf16[128,256]{1,0:T(8,128)(2,1)S(1)}, u32[]{:S(2)}, u32[]{:S(2)}) %collective-permute-start.15) | collective-permute-done | bytes 65568 | tf_op jit(solution)/shard_map/ppermute | solution.py:17
  37.6 1.2 %collective-permute-start.21 = (bf16[128,2048]{1,0:T(8,128)(2,1)S(1)}, bf16[128,2048]{1,0:T(8,128)(2,1)S(1)}, u32[]{:S(2)}, u32[]{:S(2)}) collective-permute-start(bf16[128,2048]{1,0:T(8,128)(2,1)S(1)} %copy-done.1), channel_id=1, source_target_pairs={{0,2},{1,3},{2,0},{3,1},{4,6},{5,7},{6,4},{7,5},{8,10},{9,11},{10,... | collective-permute-start | bytes 1572872 | tf_op jit(solution)/shard_map/ppermute | solution.py:17
  39.7 5.0 %collective-permute-done.5 = bf16[256,128]{1,0:T(8,128)(2,1)S(1)} collective-permute-done((bf16[256,128]{1,0:T(8,128)(2,1)S(1)}, bf16[256,128]{1,0:T(8,128)(2,1)S(1)}, u32[]{:S(2)}, u32[]{:S(2)}) %collective-permute-start.5) | collective-permute-done | bytes 65568 | tf_op jit(solution)/shard_map/ppermute | solution.py:17
  44.7 4.0 %collective-permute-done.7 = bf16[272,128]{1,0:T(8,128)(2,1)S(1)} collective-permute-done((bf16[272,128]{1,0:T(8,128)(2,1)S(1)}, bf16[272,128]{1,0:T(8,128)(2,1)S(1)}, u32[]{:S(2)}, u32[]{:S(2)}) %collective-permute-start.7) | collective-permute-done | bytes 69664 | tf_op jit(solution)/shard_map/ppermute | solution.py:17
  48.8 1.3 %collective-permute-start.16 = (bf16[30,256]{1,0:T(8,128)(2,1)S(1)}, bf16[30,256]{1,0:T(8,128)(2,1)S(1)}, u32[]{:S(2)}, u32[]{:S(2)}) collective-permute-start(bf16[30,256]{1,0:T(8,128)(2,1)S(1)} %slice.383), channel_id=1, source_target_pairs={{0,4},{4,8},{8,12},{1,5},{5,9},{9,13},{2,6},{6,10},{10,14},{3,7},{... | collective-permute-start | bytes 46088 | tf_op jit(solution)/shard_map/ppermute | solution.py:23
  50.1 3.1 %collective-permute-done.16 = bf16[30,256]{1,0:T(8,128)(2,1)S(1)} collective-permute-done((bf16[30,256]{1,0:T(8,128)(2,1)S(1)}, bf16[30,256]{1,0:T(8,128)(2,1)S(1)}, u32[]{:S(2)}, u32[]{:S(2)}) %collective-permute-start.16) | collective-permute-done | bytes 15392 | tf_op jit(solution)/shard_map/ppermute | solution.py:23
  53.8 7.8 %collective-permute-start.25 = (bf16[256,2048]{1,0:T(8,128)(2,1)S(1)}, bf16[256,2048]{1,0:T(8,128)(2,1)S(1)}, u32[]{:S(2)}, u32[]{:S(2)}) collective-permute-start(bf16[256,2048]{1,0:T(8,128)(2,1)S(1)} %collective-permute-done.24.refs_14_), channel_id=1, source_target_pairs={{0,1},{1,0},{2,3},{3,2},{4,5},{5,4},{6,7},{7,6},{8,9},{9,8},{10,11... | collective-permute-start | bytes 3145736 | tf_op jit(solution)/shard_map/ppermute | solution.py:17
  61.9 1.3 %collective-permute-start.27 = (f32[2,256]{1,0:T(2,128)S(1)}, f32[2,256]{1,0:T(2,128)S(1)}, u32[]{:S(2)}, u32[]{:S(2)}) collective-permute-start(f32[2,256]{1,0:T(2,128)S(1)} %pad_maximum_fusion.6.refs_16_), channel_id=1, source_target_pairs={{0,2},{1,3},{2,0},{3,1},{4,6},{5,7},{6,4},{7,5},{8,10},{9,11},{10,... | collective-permute-start | bytes 6152 | tf_op jit(solution)/shard_map/ppermute | solution.py:17
  63.2 3.3 %collective-permute-start.26 = (f32[2,256]{1,0:T(2,128)S(1)}, f32[2,256]{1,0:T(2,128)S(1)}, u32[]{:S(2)}, u32[]{:S(2)}) collective-permute-start(f32[2,256]{1,0:T(2,128)S(1)} %pad_maximum_fusion.6.refs_16_), channel_id=1, source_target_pairs={{0,1},{1,0},{2,3},{3,2},{4,5},{5,4},{6,7},{7,6},{8,9},{9,8},{10,11... | collective-permute-start | bytes 6152 | tf_op jit(solution)/shard_map/ppermute | solution.py:17
  67.3 1.4 %collective-permute-start.19 = (bf16[128,256]{1,0:T(8,128)(2,1)S(1)}, bf16[128,256]{1,0:T(8,128)(2,1)S(1)}, u32[]{:S(2)}, u32[]{:S(2)}) collective-permute-start(bf16[128,256]{1,0:T(8,128)(2,1)S(1)} %fusion.1.refs_4_), channel_id=1, source_target_pairs={{0,3},{1,2},{2,1},{3,0},{4,7},{5,6},{6,5},{7,4},{8,11},{9,10},{10,... | collective-permute-start | bytes 196616 | tf_op jit(solution)/shard_map/ppermute | solution.py:17
  68.9 2.4 %collective-permute-done.19.refs_7_ = bf16[128,256]{1,0:T(8,128)(2,1)S(1)} collective-permute-done((bf16[128,256]{1,0:T(8,128)(2,1)S(1)}, bf16[128,256]{1,0:T(8,128)(2,1)S(1)}, u32[]{:S(2)}, u32[]{:S(2)}) %collective-permute-start.19) | collective-permute-done | bytes 65568 | tf_op jit(solution)/shard_map/ppermute | solution.py:17
  71.3 1.2 %collective-permute-start.18 = (bf16[128,256]{1,0:T(8,128)(2,1)S(1)}, bf16[128,256]{1,0:T(8,128)(2,1)S(1)}, u32[]{:S(2)}, u32[]{:S(2)}) collective-permute-start(bf16[128,256]{1,0:T(8,128)(2,1)S(1)} %fusion.1.refs_4_), channel_id=1, source_target_pairs={{0,2},{1,3},{2,0},{3,1},{4,6},{5,7},{6,4},{7,5},{8,10},{9,11},{10,... | collective-permute-start | bytes 196616 | tf_op jit(solution)/shard_map/ppermute | solution.py:17
  72.5 1.9 %collective-permute-done.18.refs_6_ = bf16[128,256]{1,0:T(8,128)(2,1)S(1)} collective-permute-done((bf16[128,256]{1,0:T(8,128)(2,1)S(1)}, bf16[128,256]{1,0:T(8,128)(2,1)S(1)}, u32[]{:S(2)}, u32[]{:S(2)}) %collective-permute-start.18) | collective-permute-done | bytes 65568 | tf_op jit(solution)/shard_map/ppermute | solution.py:17
  74.4 1.5 %collective-permute-start.17 = (bf16[128,256]{1,0:T(8,128)(2,1)S(1)}, bf16[128,256]{1,0:T(8,128)(2,1)S(1)}, u32[]{:S(2)}, u32[]{:S(2)}) collective-permute-start(bf16[128,256]{1,0:T(8,128)(2,1)S(1)} %fusion.1.refs_4_), channel_id=1, source_target_pairs={{0,1},{1,0},{2,3},{3,2},{4,5},{5,4},{6,7},{7,6},{8,9},{9,8},{10,11... | collective-permute-start | bytes 196616 | tf_op jit(solution)/shard_map/ppermute | solution.py:17
  75.9 2.8 %stick_attention.1 = (bf16[128,128]{1,0:T(8,128)(2,1)S(1)}, f32[2,128]{1,0:T(2,128)}) custom-call(bf16[128,128]{1,0:T(8,128)(2,1)S(1)} %fusion.37.q_ref, bf16[512,128]{1,0:T(8,128)(2,1)S(1)} %get-tuple-element.65.k_ref, bf16[512,128]{1,0:T(8,128)(2,1)S(1)} %get-tuple-element.66.v_ref, bf16[32,128]{1,0:T(8,128)(2,1)S(1)} %pad_maximum_fusion.5.off_ref, ...), custom_call_target="tpu_custom_call" | custom-call | flops 400000000 | bytes 1000000 | tf_op jit(solution)/shard_map/stick_attention/pallas_call | solution.py:110
  78.7 1.1 %collective-permute-start.11 = (bf16[128,128]{1,0:T(8,128)(2,1)S(1)}, bf16[128,128]{1,0:T(8,128)(2,1)S(1)}, u32[]{:S(2)}, u32[]{:S(2)}) collective-permute-start(bf16[128,128]{1,0:T(8,128)(2,1)S(1)} %get-tuple-element.14.refs_0_), channel_id=1, source_target_pairs={{0,3},{1,2},{2,1},{3,0},{4,7},{5,6},{6,5},{7,4},{8,11},{9,10},{10,... | collective-permute-start | bytes 98312 | tf_op jit(solution)/shard_map/ppermute | solution.py:17
  79.8 2.2 %collective-permute-done.11.refs_3_ = bf16[128,128]{1,0:T(8,128)(2,1)S(1)} collective-permute-done((bf16[128,128]{1,0:T(8,128)(2,1)S(1)}, bf16[128,128]{1,0:T(8,128)(2,1)S(1)}, u32[]{:S(2)}, u32[]{:S(2)}) %collective-permute-start.11) | collective-permute-done | bytes 32800 | tf_op jit(solution)/shard_map/ppermute | solution.py:17
  82.0 1.2 %collective-permute-start.10 = (bf16[128,128]{1,0:T(8,128)(2,1)S(1)}, bf16[128,128]{1,0:T(8,128)(2,1)S(1)}, u32[]{:S(2)}, u32[]{:S(2)}) collective-permute-start(bf16[128,128]{1,0:T(8,128)(2,1)S(1)} %get-tuple-element.14.refs_0_), channel_id=1, source_target_pairs={{0,2},{1,3},{2,0},{3,1},{4,6},{5,7},{6,4},{7,5},{8,10},{9,11},{10,... | collective-permute-start | bytes 98312 | tf_op jit(solution)/shard_map/ppermute | solution.py:17
  83.2 1.5 %collective-permute-done.10.refs_2_ = bf16[128,128]{1,0:T(8,128)(2,1)S(1)} collective-permute-done((bf16[128,128]{1,0:T(8,128)(2,1)S(1)}, bf16[128,128]{1,0:T(8,128)(2,1)S(1)}, u32[]{:S(2)}, u32[]{:S(2)}) %collective-permute-start.10) | collective-permute-done | bytes 32800 | tf_op jit(solution)/shard_map/ppermute | solution.py:17
  84.8 1.2 %collective-permute-start.9 = (bf16[128,128]{1,0:T(8,128)(2,1)S(1)}, bf16[128,128]{1,0:T(8,128)(2,1)S(1)}, u32[]{:S(2)}, u32[]{:S(2)}) collective-permute-start(bf16[128,128]{1,0:T(8,128)(2,1)S(1)} %get-tuple-element.14.refs_0_), channel_id=1, source_target_pairs={{0,1},{1,0},{2,3},{3,2},{4,5},{5,4},{6,7},{7,6},{8,9},{9,8},{10,11... | collective-permute-start | bytes 98312 | tf_op jit(solution)/shard_map/ppermute | solution.py:17
  86.8 2.4 %finish_rows.1 = bf16[128,2048]{1,0:T(8,128)(2,1)} custom-call(bf16[128,128]{1,0:T(8,128)(2,1)S(1)} %get-tuple-element.14.refs_0_, bf16[128,128]{1,0:T(8,128)(2,1)S(1)} %collective-permute-done.9.refs_1_, bf16[128,128]{1,0:T(8,128)(2,1)S(1)} %collective-permute-done.10.refs_2_, bf16[128,128]{1,0:T(8,128)(2,1)S(1)} %collective-permute-done.11.refs_3_, ...), custom_call_target="tpu_custom_call" | custom-call | flops 800000000 | bytes 7000000 | tf_op jit(solution)/shard_map/finish_rows/pallas_call | solution.py:211
  (93 shorter events, 12.9 us)
Async XLA Ops:
  0.6 86.2 %collective-permute-start.23 = (bf16[256,2048]{1,0:T(8,128)(2,1)}, bf16[256,2048]{1,0:T(8,128)(2,1)S(1)}, u32[]{:S(2)}, u32[]{:S(2)}) collective-permute-start(bf16[256,2048]{1,0:T(8,128)(2,1)} %refs_12_.1), channel_id=1, source_target_pairs={{0,1},{1,0},{2,3},{3,2},{4,5},{5,4},{6,7},{7,6},{8,9},{9,8},{10,11... | collective-permute-start | bytes 3145736 | tf_op jit(solution)/shard_map/ppermute | solution.py:17
  1.4 52.4 %collective-permute-start.24 = (bf16[256,2048]{1,0:T(8,128)(2,1)}, bf16[256,2048]{1,0:T(8,128)(2,1)S(1)}, u32[]{:S(2)}, u32[]{:S(2)}) collective-permute-start(bf16[256,2048]{1,0:T(8,128)(2,1)} %refs_12_.1), channel_id=1, source_target_pairs={{0,2},{1,3},{2,0},{3,1},{4,6},{5,7},{6,4},{7,5},{8,10},{9,11},{10,... | collective-permute-start | bytes 3145736 | tf_op jit(solution)/shard_map/ppermute | solution.py:17
  3.3 58.6 %collective-permute-start.28 = (f32[2,256]{1,0:T(2,128)S(1)}, f32[2,256]{1,0:T(2,128)S(1)}, u32[]{:S(2)}, u32[]{:S(2)}) collective-permute-start(f32[2,256]{1,0:T(2,128)S(1)} %pad_maximum_fusion.6.refs_16_), channel_id=1, source_target_pairs={{0,3},{1,2},{2,1},{3,0},{4,7},{5,6},{6,5},{7,4},{8,11},{9,10},{10,... | collective-permute-start | bytes 6152 | tf_op jit(solution)/shard_map/ppermute | solution.py:17
  3.8 12.8 %collective-permute-start.14 = (bf16[512,256]{1,0:T(8,128)(2,1)}, bf16[512,256]{1,0:T(8,128)(2,1)S(1)}, u32[]{:S(2)}, u32[]{:S(2)}) collective-permute-start(bf16[512,256]{1,0:T(8,128)(2,1)} %param.21), channel_id=1, source_target_pairs={{0,4},{4,0},{8,12},{12,8},{1,5},{5,1},{9,13},{13,9},{2,6},{6,2},{1... | collective-permute-start | bytes 786440 | tf_op jit(solution)/shard_map/ppermute | solution.py:17
  5.0 9.5 %copy-start.7 = (bf16[512,128]{1,0:T(8,128)(2,1)S(1)}, bf16[512,128]{1,0:T(8,128)(2,1)}, u32[]{:S(2)}) copy-start(bf16[512,128]{1,0:T(8,128)(2,1)} %param.17) | copy-start | bytes 393220
  5.3 7.2 %collective-permute-start = (bf16[64,1024]{1,0:T(8,128)(2,1)S(1)}, bf16[64,1024]{1,0:T(8,128)(2,1)S(1)}, u32[]{:S(2)}, u32[]{:S(2)}) collective-permute-start(bf16[64,1024]{1,0:T(8,128)(2,1)S(1)} %get-tuple-element.11), channel_id=1, source_target_pairs={{0,8},{4,12},{8,0},{12,4},{1,9},{5,13},{9,1},{13,5},{2,10},{6,14},... | collective-permute-start | bytes 393224 | tf_op jit(solution)/shard_map/ppermute | solution.py:17
  12.5 2.0 %collective-permute-start.1 = (bf16[64,1024]{1,0:T(8,128)(2,1)S(1)}, bf16[64,1024]{1,0:T(8,128)(2,1)S(1)}, u32[]{:S(2)}, u32[]{:S(2)}) collective-permute-start(bf16[64,1024]{1,0:T(8,128)(2,1)S(1)} %collective-permute-done.got_ref), channel_id=1, source_target_pairs={{0,1},{1,0},{2,3},{3,2},{4,5},{5,4},{6,7},{7,6},{8,9},{9,8},{10,11... | collective-permute-start | bytes 393224 | tf_op jit(solution)/shard_map/ppermute | solution.py:17
  14.5 5.6 %collective-permute-start.2 = (bf16[512,128]{1,0:T(8,128)(2,1)S(1)}, bf16[512,128]{1,0:T(8,128)(2,1)S(1)}, u32[]{:S(2)}, u32[]{:S(2)}) collective-permute-start(bf16[512,128]{1,0:T(8,128)(2,1)S(1)} %copy-done.7), channel_id=1, source_target_pairs={{0,4},{4,0},{8,12},{12,8},{1,5},{5,1},{9,13},{13,9},{2,6},{6,2},{1... | collective-permute-start | bytes 393224 | tf_op jit(solution)/shard_map/ppermute | solution.py:17
  17.5 11.9 %collective-permute-start.4 = (bf16[512,128]{1,0:T(8,128)(2,1)S(1)}, bf16[512,128]{1,0:T(8,128)(2,1)S(1)}, u32[]{:S(2)}, u32[]{:S(2)}) collective-permute-start(bf16[512,128]{1,0:T(8,128)(2,1)S(1)} %copy-done.8), channel_id=1, source_target_pairs={{0,4},{4,0},{8,12},{12,8},{1,5},{5,1},{9,13},{13,9},{2,6},{6,2},{1... | collective-permute-start | bytes 393224 | tf_op jit(solution)/shard_map/ppermute | solution.py:17
  20.1 7.7 %collective-permute-start.12 = (bf16[512,256]{1,0:T(8,128)(2,1)S(1)}, bf16[512,256]{1,0:T(8,128)(2,1)S(1)}, u32[]{:S(2)}, u32[]{:S(2)}) collective-permute-start(bf16[512,256]{1,0:T(8,128)(2,1)S(1)} %copy-done.6), channel_id=1, source_target_pairs={{0,4},{4,0},{8,12},{12,8},{1,5},{5,1},{9,13},{13,9},{2,6},{6,2},{1... | collective-permute-start | bytes 786440 | tf_op jit(solution)/shard_map/ppermute | solution.py:17
  27.8 3.8 %collective-permute-start.6 = (bf16[512,128]{1,0:T(8,128)(2,1)S(1)}, bf16[512,128]{1,0:T(8,128)(2,1)S(1)}, u32[]{:S(2)}, u32[]{:S(2)}) collective-permute-start(bf16[512,128]{1,0:T(8,128)(2,1)S(1)} %copy-done.9), channel_id=1, source_target_pairs={{0,4},{4,0},{8,12},{12,8},{1,5},{5,1},{9,13},{13,9},{2,6},{6,2},{1... | collective-permute-start | bytes 393224 | tf_op jit(solution)/shard_map/ppermute | solution.py:17
  29.4 4.9 %collective-permute-start.3 = (bf16[128,128]{1,0:T(8,128)(2,1)S(1)}, bf16[128,128]{1,0:T(8,128)(2,1)S(1)}, u32[]{:S(2)}, u32[]{:S(2)}) collective-permute-start(bf16[128,128]{1,0:T(8,128)(2,1)S(1)} %slice.595), channel_id=1, source_target_pairs={{0,8},{4,12},{8,0},{12,4},{1,9},{5,13},{9,1},{13,5},{2,10},{6,14},... | collective-permute-start | bytes 98312 | tf_op jit(solution)/shard_map/ppermute | solution.py:17
  32.1 5.5 %collective-permute-start.15 = (bf16[128,256]{1,0:T(8,128)(2,1)S(1)}, bf16[128,256]{1,0:T(8,128)(2,1)S(1)}, u32[]{:S(2)}, u32[]{:S(2)}) collective-permute-start(bf16[128,256]{1,0:T(8,128)(2,1)S(1)} %slice.593), channel_id=1, source_target_pairs={{0,8},{4,12},{8,0},{12,4},{1,9},{5,13},{9,1},{13,5},{2,10},{6,14},... | collective-permute-start | bytes 196616 | tf_op jit(solution)/shard_map/ppermute | solution.py:17
  34.4 5.1 %collective-permute-start.13 = (bf16[128,256]{1,0:T(8,128)(2,1)S(1)}, bf16[128,256]{1,0:T(8,128)(2,1)S(1)}, u32[]{:S(2)}, u32[]{:S(2)}) collective-permute-start(bf16[128,256]{1,0:T(8,128)(2,1)S(1)} %slice.594), channel_id=1, source_target_pairs={{0,8},{4,12},{8,0},{12,4},{1,9},{5,13},{9,1},{13,5},{2,10},{6,14},... | collective-permute-start | bytes 196616 | tf_op jit(solution)/shard_map/ppermute | solution.py:17
  37.6 31.1 %collective-permute-start.21 = (bf16[128,2048]{1,0:T(8,128)(2,1)S(1)}, bf16[128,2048]{1,0:T(8,128)(2,1)S(1)}, u32[]{:S(2)}, u32[]{:S(2)}) collective-permute-start(bf16[128,2048]{1,0:T(8,128)(2,1)S(1)} %copy-done.1), channel_id=1, source_target_pairs={{0,2},{1,3},{2,0},{3,1},{4,6},{5,7},{6,4},{7,5},{8,10},{9,11},{10,... | collective-permute-start | bytes 1572872 | tf_op jit(solution)/shard_map/ppermute | solution.py:17
  39.5 5.2 %collective-permute-start.5 = (bf16[256,128]{1,0:T(8,128)(2,1)S(1)}, bf16[256,128]{1,0:T(8,128)(2,1)S(1)}, u32[]{:S(2)}, u32[]{:S(2)}) collective-permute-start(bf16[256,128]{1,0:T(8,128)(2,1)S(1)} %pad_maximum_fusion.4), channel_id=1, source_target_pairs={{0,8},{4,12},{8,0},{12,4},{1,9},{5,13},{9,1},{13,5},{2,10},{6,14},... | collective-permute-start | bytes 196616 | tf_op jit(solution)/shard_map/ppermute | solution.py:17
  44.7 4.1 %collective-permute-start.7 = (bf16[272,128]{1,0:T(8,128)(2,1)S(1)}, bf16[272,128]{1,0:T(8,128)(2,1)S(1)}, u32[]{:S(2)}, u32[]{:S(2)}) collective-permute-start(bf16[272,128]{1,0:T(8,128)(2,1)S(1)} %pad_maximum_fusion.3), channel_id=1, source_target_pairs={{0,8},{4,12},{8,0},{12,4},{1,9},{5,13},{9,1},{13,5},{2,10},{6,14},... | collective-permute-start | bytes 208904 | tf_op jit(solution)/shard_map/ppermute | solution.py:17
  48.8 4.5 %collective-permute-start.16 = (bf16[30,256]{1,0:T(8,128)(2,1)S(1)}, bf16[30,256]{1,0:T(8,128)(2,1)S(1)}, u32[]{:S(2)}, u32[]{:S(2)}) collective-permute-start(bf16[30,256]{1,0:T(8,128)(2,1)S(1)} %slice.383), channel_id=1, source_target_pairs={{0,4},{4,8},{8,12},{1,5},{5,9},{9,13},{2,6},{6,10},{10,14},{3,7},{... | collective-permute-start | bytes 46088 | tf_op jit(solution)/shard_map/ppermute | solution.py:23
  53.3 9.9 %collective-permute-start.8 = (bf16[528,128]{1,0:T(8,128)(2,1)S(1)}, bf16[528,128]{1,0:T(8,128)(2,1)S(1)}, u32[]{:S(2)}, u32[]{:S(2)}) collective-permute-start(bf16[528,128]{1,0:T(8,128)(2,1)S(1)} %pad_maximum_fusion), channel_id=1, source_target_pairs={{0,4},{4,0},{8,12},{12,8},{1,5},{5,1},{9,13},{13,9},{2,6},{6,2},{1... | collective-permute-start | bytes 405512 | tf_op jit(solution)/shard_map/ppermute | solution.py:17
  53.8 33.0 %collective-permute-start.25 = (bf16[256,2048]{1,0:T(8,128)(2,1)S(1)}, bf16[256,2048]{1,0:T(8,128)(2,1)S(1)}, u32[]{:S(2)}, u32[]{:S(2)}) collective-permute-start(bf16[256,2048]{1,0:T(8,128)(2,1)S(1)} %collective-permute-done.24.refs_14_), channel_id=1, source_target_pairs={{0,1},{1,0},{2,3},{3,2},{4,5},{5,4},{6,7},{7,6},{8,9},{9,8},{10,11... | collective-permute-start | bytes 3145736 | tf_op jit(solution)/shard_map/ppermute | solution.py:17
  61.9 4.6 %collective-permute-start.27 = (f32[2,256]{1,0:T(2,128)S(1)}, f32[2,256]{1,0:T(2,128)S(1)}, u32[]{:S(2)}, u32[]{:S(2)}) collective-permute-start(f32[2,256]{1,0:T(2,128)S(1)} %pad_maximum_fusion.6.refs_16_), channel_id=1, source_target_pairs={{0,2},{1,3},{2,0},{3,1},{4,6},{5,7},{6,4},{7,5},{8,10},{9,11},{10,... | collective-permute-start | bytes 6152 | tf_op jit(solution)/shard_map/ppermute | solution.py:17
  63.2 4.1 %collective-permute-start.26 = (f32[2,256]{1,0:T(2,128)S(1)}, f32[2,256]{1,0:T(2,128)S(1)}, u32[]{:S(2)}, u32[]{:S(2)}) collective-permute-start(f32[2,256]{1,0:T(2,128)S(1)} %pad_maximum_fusion.6.refs_16_), channel_id=1, source_target_pairs={{0,1},{1,0},{2,3},{3,2},{4,5},{5,4},{6,7},{7,6},{8,9},{9,8},{10,11... | collective-permute-start | bytes 6152 | tf_op jit(solution)/shard_map/ppermute | solution.py:17
  66.5 20.4 %copy-start = (bf16[256,2048]{1,0:T(8,128)(2,1)S(1)}, bf16[256,2048]{1,0:T(8,128)(2,1)}, u32[]{:S(2)}) copy-start(bf16[256,2048]{1,0:T(8,128)(2,1)} %refs_12_.1) | copy-start | bytes 3145732
  66.5 20.3 %collective-permute-start.20 = (bf16[128,2048]{1,0:T(8,128)(2,1)S(1)}, bf16[128,2048]{1,0:T(8,128)(2,1)S(1)}, u32[]{:S(2)}, u32[]{:S(2)}) collective-permute-start(bf16[128,2048]{1,0:T(8,128)(2,1)S(1)} %copy-done.1), channel_id=1, source_target_pairs={{0,1},{1,0},{2,3},{3,2},{4,5},{5,4},{6,7},{7,6},{8,9},{9,8},{10,11... | collective-permute-start | bytes 1572872 | tf_op jit(solution)/shard_map/ppermute | solution.py:17
  67.3 4.0 %collective-permute-start.19 = (bf16[128,256]{1,0:T(8,128)(2,1)S(1)}, bf16[128,256]{1,0:T(8,128)(2,1)S(1)}, u32[]{:S(2)}, u32[]{:S(2)}) collective-permute-start(bf16[128,256]{1,0:T(8,128)(2,1)S(1)} %fusion.1.refs_4_), channel_id=1, source_target_pairs={{0,3},{1,2},{2,1},{3,0},{4,7},{5,6},{6,5},{7,4},{8,11},{9,10},{10,... | collective-permute-start | bytes 196616 | tf_op jit(solution)/shard_map/ppermute | solution.py:17
  68.7 18.1 %collective-permute-start.22 = (bf16[128,2048]{1,0:T(8,128)(2,1)S(1)}, bf16[128,2048]{1,0:T(8,128)(2,1)S(1)}, u32[]{:S(2)}, u32[]{:S(2)}) collective-permute-start(bf16[128,2048]{1,0:T(8,128)(2,1)S(1)} %collective-permute-done.21.refs_10_), channel_id=1, source_target_pairs={{0,1},{1,0},{2,3},{3,2},{4,5},{5,4},{6,7},{7,6},{8,9},{9,8},{10,11... | collective-permute-start | bytes 1572872 | tf_op jit(solution)/shard_map/ppermute | solution.py:17
  71.3 3.1 %collective-permute-start.18 = (bf16[128,256]{1,0:T(8,128)(2,1)S(1)}, bf16[128,256]{1,0:T(8,128)(2,1)S(1)}, u32[]{:S(2)}, u32[]{:S(2)}) collective-permute-start(bf16[128,256]{1,0:T(8,128)(2,1)S(1)} %fusion.1.refs_4_), channel_id=1, source_target_pairs={{0,2},{1,3},{2,0},{3,1},{4,6},{5,7},{6,4},{7,5},{8,10},{9,11},{10,... | collective-permute-start | bytes 196616 | tf_op jit(solution)/shard_map/ppermute | solution.py:17
  74.4 4.2 %collective-permute-start.17 = (bf16[128,256]{1,0:T(8,128)(2,1)S(1)}, bf16[128,256]{1,0:T(8,128)(2,1)S(1)}, u32[]{:S(2)}, u32[]{:S(2)}) collective-permute-start(bf16[128,256]{1,0:T(8,128)(2,1)S(1)} %fusion.1.refs_4_), channel_id=1, source_target_pairs={{0,1},{1,0},{2,3},{3,2},{4,5},{5,4},{6,7},{7,6},{8,9},{9,8},{10,11... | collective-permute-start | bytes 196616 | tf_op jit(solution)/shard_map/ppermute | solution.py:17
  75.9 10.9 %copy-start.4 = (f32[2048]{0:T(1024)S(1)}, f32[2048]{0:T(1024)}, u32[]{:S(2)}) copy-start(f32[2048]{0:T(1024)} %param.29) | copy-start | bytes 24580
  78.7 3.3 %collective-permute-start.11 = (bf16[128,128]{1,0:T(8,128)(2,1)S(1)}, bf16[128,128]{1,0:T(8,128)(2,1)S(1)}, u32[]{:S(2)}, u32[]{:S(2)}) collective-permute-start(bf16[128,128]{1,0:T(8,128)(2,1)S(1)} %get-tuple-element.14.refs_0_), channel_id=1, source_target_pairs={{0,3},{1,2},{2,1},{3,0},{4,7},{5,6},{6,5},{7,4},{8,11},{9,10},{10,... | collective-permute-start | bytes 98312 | tf_op jit(solution)/shard_map/ppermute | solution.py:17
  82.0 2.8 %collective-permute-start.10 = (bf16[128,128]{1,0:T(8,128)(2,1)S(1)}, bf16[128,128]{1,0:T(8,128)(2,1)S(1)}, u32[]{:S(2)}, u32[]{:S(2)}) collective-permute-start(bf16[128,128]{1,0:T(8,128)(2,1)S(1)} %get-tuple-element.14.refs_0_), channel_id=1, source_target_pairs={{0,2},{1,3},{2,0},{3,1},{4,6},{5,7},{6,4},{7,5},{8,10},{9,11},{10,... | collective-permute-start | bytes 98312 | tf_op jit(solution)/shard_map/ppermute | solution.py:17
  84.8 2.0 %collective-permute-start.9 = (bf16[128,128]{1,0:T(8,128)(2,1)S(1)}, bf16[128,128]{1,0:T(8,128)(2,1)S(1)}, u32[]{:S(2)}, u32[]{:S(2)}) collective-permute-start(bf16[128,128]{1,0:T(8,128)(2,1)S(1)} %get-tuple-element.14.refs_0_), channel_id=1, source_target_pairs={{0,1},{1,0},{2,3},{3,2},{4,5},{5,4},{6,7},{7,6},{8,9},{9,8},{10,11... | collective-permute-start | bytes 98312 | tf_op jit(solution)/shard_map/ppermute | solution.py:17
  (10 other events, 21.6 us)

commit v3 on v1

--- a/solution.py
+++ b/solution.py
@@ -1,5 +1,3 @@
-import functools
-
 import jax
 import jax.numpy as jnp
 from jax import lax
@@ -32,12 +30,312 @@
     return lax.dot_general(a, b, (dims, ((), ())), preferred_element_type=F32)
 
 
-def attention_kernel(hd, q_ref, k_ref, v_ref, off_ref, gain_ref, out_ref, mass_ref, acc, mass, carry):
+FULL = 60
+
+
+def params(limit=16):
+    return pltpu.CompilerParams(vmem_limit_bytes=limit * 1024 * 1024)
+
+
+VM = pl.BlockSpec(memory_space=pltpu.VMEM)
+ANY = pl.BlockSpec(memory_space=pl.ANY)
+HBM = pl.BlockSpec(memory_space=pltpu.HBM)
+
+
+def shape(dims, dtype=BF16):
+    return jax.ShapeDtypeStruct(dims, dtype)
+
+
+def cost(flops, moved):
+    return pl.CostEstimate(flops=flops, bytes_accessed=moved, transcendentals=0)
+
+
+def norm_kernel(x_hbm, gain_hbm, *refs):
+    weights = refs[:3]
+    send_ref, own_ref, pair_ref, pack_ref, x_ref, gain_ref, normed, sems = refs[3:]
+    side, low = lax.axis_index("sp") // 2, lax.axis_index("sp") % 2
+    core = lax.axis_index("tp") % 2
+    block, width = weights[0].shape
+    half = 2 * block
+    half_rows = send_ref.shape[0]
+    part = block // 2
+    mine = pl.ds(pl.multiple_of(lax.axis_index("grp") * part, part), part)
+    copies = [
+        pltpu.make_async_copy(x_hbm, x_ref, sems.at[0]),
+        pltpu.make_async_copy(gain_hbm, gain_ref, sems.at[1]),
+    ]
+    for n, w in enumerate(weights):
+        at = slice(n * width, (n + 1) * width)
+        copies.append(pltpu.make_async_copy(w.at[mine, :], pack_ref.at[:, at], sems.at[2 + n]))
+    for copy in copies:
+        copy.start()
+    copies[0].wait()
+    copies[1].wait()
+    x = x_ref[...].astype(F32)
+    squares = jnp.mean(x * x, axis=1, keepdims=True)
+    normed[...] = (x * lax.rsqrt(squares + norm_eps) * gain_ref[...]).astype(BF16)
+    first = pl.multiple_of(core * half_rows, half_rows)
+    away = pl.multiple_of((1 - side) * half, half)
+    send_ref[...] = normed[pl.ds(first, half_rows), pl.ds(away, half)]
+    own_ref[...] = normed[:, pl.ds(pl.multiple_of(side * half + low * block, block), block)]
+    pair_ref[...] = normed[:, pl.ds(pl.multiple_of(side * half + (1 - low) * block, block), block)]
+    for copy in copies[2:]:
+        copy.wait()
+
+
+def norm_parts(tokens, gain, weights):
+    rows, features = tokens.shape
+    block, width = weights[0].shape
+    return pl.pallas_call(
+        norm_kernel,
+        out_shape=(
+            shape((rows // 2, 2 * block)),
+            shape((rows, block)),
+            shape((rows, block)),
+            shape((block // 2, 3 * width)),
+        ),
+        in_specs=[HBM] * 5,
+        out_specs=[VM] * 4,
+        scratch_shapes=[
+            pltpu.VMEM((rows, features), BF16),
+            pltpu.VMEM((1, features), F32),
+            pltpu.VMEM((rows, features), BF16),
+            pltpu.SemaphoreType.DMA((5,)),
+        ],
+        cost_estimate=cost(2_000_000, 1_000_000),
+        compiler_params=params(FULL),
+        name="norm_parts",
+    )(tokens, gain.reshape(1, features), *weights)
+
+
+def pack_kernel(gv_hbm, gg_hbm, wa_hbm, gain_hbm, bias_hbm, glu_ref, out_ref, gain_ref, bias_ref, sems):
+    cw, aw = gv_hbm.shape[1], wa_hbm.shape[0]
+    part = glu_ref.shape[0]
+    mine = pl.ds(pl.multiple_of(lax.axis_index("grp") * part, part), part)
+    copies = [
+        pltpu.make_async_copy(gv_hbm.at[mine, :], glu_ref.at[:, :cw], sems.at[0]),
+        pltpu.make_async_copy(gg_hbm.at[mine, :], glu_ref.at[:, cw:], sems.at[1]),
+        pltpu.make_async_copy(wa_hbm, out_ref.at[:aw, :], sems.at[2]),
+    ]
+    small = [
+        pltpu.make_async_copy(gain_hbm, gain_ref, sems.at[3]),
+        pltpu.make_async_copy(bias_hbm, bias_ref, sems.at[4]),
+    ]
+    for copy in small + copies:
+        copy.start()
+    for copy in small:
+        copy.wait()
+    extra = out_ref.shape[0] - aw
+    for n, ref in enumerate((gain_ref, bias_ref)):
+        rest = ref[...]
+        for piece in range(3):
+            part = rest.astype(BF16)
+            rest = rest - part.astype(F32)
+            first = (3 * n + piece) * cw
+            out_ref[aw:, first : first + cw] = jnp.broadcast_to(part, (extra, cw))
+    for copy in copies:
+        copy.wait()
+
+
+def pack(gv, gg, wa, gain, bias):
+    block, cw = gv.shape
+    aw, width = wa.shape
+    return pl.pallas_call(
+        pack_kernel,
+        out_shape=(shape((block // 2, 2 * cw)), shape((aw + 16, width))),
+        in_specs=[HBM] * 5,
+        out_specs=[VM] * 2,
+        scratch_shapes=[
+            pltpu.VMEM((1, cw), F32),
+            pltpu.VMEM((1, cw), F32),
+            pltpu.SemaphoreType.DMA((5,)),
+        ],
+        cost_estimate=cost(2_000_000, 2_000_000),
+        compiler_params=params(FULL),
+        name="pack",
+    )(gv, gg, wa, gain.reshape(1, cw), bias.reshape(1, cw))
+
+
+def assemble_kernel(own_ref, pair_ref, got_ref, other_ref, own_out, pair_out):
+    low = lax.axis_index("sp") % 2
+    core = lax.axis_index("tp") % 2
+    rows, block = own_ref.shape
+    half = got_ref.shape[0]
+    own_out[:rows, :] = own_ref[...]
+    pair_out[:rows, :] = pair_ref[...]
+    own_at = pl.multiple_of(low * block, block)
+    pair_at = pl.multiple_of((1 - low) * block, block)
+    for part, at in ((got_ref, core), (other_ref, 1 - core)):
+        first = pl.multiple_of(rows + at * half, half)
+        own_out[pl.ds(first, half), :] = part[:, pl.ds(own_at, block)]
+        pair_out[pl.ds(first, half), :] = part[:, pl.ds(pair_at, block)]
+
+
+def assemble(own, pair, got, other):
+    rows, block = own.shape
+    return pl.pallas_call(
+        assemble_kernel,
+        out_shape=(shape((2 * rows, block)),) * 2,
+        in_specs=[VM] * 4,
+        out_specs=[VM] * 2,
+        cost_estimate=cost(2_000_000, 1_000_000),
+        compiler_params=params(),
+        name="assemble",
+    )(own, pair, got, other)
+
+
+def far_dot(x_pair, same, other):
+    part = same.shape[0]
+    group = lax.axis_index("grp")
+    near = x_pair[:, pl.ds(pl.multiple_of(group * part, part), part)]
+    rest = x_pair[:, pl.ds(pl.multiple_of((1 - group) * part, part), part)]
+    return dot_f32(near, same[...]) + dot_f32(rest, other[...])
+
+
+def qkv_kernel(x_own, x_pair, wq, wk, wv, same, other, off_ref, keep_ref, send_ref):
+    rows = x_own.shape[0] // 2
+    width = wk.shape[1]
+    far = far_dot(x_pair, same, other)
+    for n, w in enumerate((wq, wk, wv)):
+        at = slice(n * width, (n + 1) * width)
+        part = dot_f32(x_own[...], w[...]) + far[:, at]
+        keep_ref[:, at] = part
+        first = 4 * rows if n == 0 else 2 * (n - 1) * rows
+        send_ref[first : first + rows, :] = part[rows:].astype(BF16)
+        if n > 0:
+            send_ref[first + rows : first + 2 * rows, :] = part[:rows].astype(BF16)
+    send_ref[5 * rows :, :] = jnp.zeros((send_ref.shape[0] - 5 * rows, width), BF16)
+    send_ref[5 * rows : 5 * rows + off_ref.shape[0], :] = off_ref[...]
+
+
+def project_qkv(x_own, x_pair, own, same, other, off):
+    rows, width = x_own.shape[0], own[0].shape[1]
+    return pl.pallas_call(
+        qkv_kernel,
+        out_shape=(shape((rows, 3 * width), F32), shape((5 * rows // 2 + 16, width))),
+        in_specs=[VM] * 8,
+        out_specs=[VM] * 2,
+        cost_estimate=cost(200_000_000, 1_000_000),
+        compiler_params=params(),
+        name="project_qkv",
+    )(x_own, x_pair, *own, same, other, off)
+
+
+def sum_kernel(keep_ref, got_ref, sent_ref, after, q_ref, out_ref):
+    rows, width = q_ref.shape
+
+    def got(n):
+        return got_ref[n * rows : (n + 1) * rows, :].astype(F32)
+
+    q_ref[...] = (keep_ref[:rows, :width] + got(4)).astype(BF16)
+    for n in range(4):
+        at = slice((1 + n // 2) * width, (2 + n // 2) * width)
+        part = keep_ref[(n % 2) * rows : (n % 2 + 1) * rows, at]
+        out_ref[n * rows : (n + 1) * rows, :] = (part + got(n)).astype(BF16)
+    first = 5 * rows
+    out_ref[4 * rows :, :] = jnp.concatenate([sent_ref[first : first + 8, :], got_ref[first : first + 8, :]])
+
+
+def sum_qkv(keep, got, sent, after):
+    rows, width = keep.shape[0] // 2, got.shape[1]
+    return pl.pallas_call(
+        sum_kernel,
+        out_shape=(shape((rows, width)), shape((4 * rows + 16, width))),
+        in_specs=[VM] * 3 + [ANY],
+        out_specs=[VM] * 2,
+        cost_estimate=cost(1_000_000, 1_000_000),
+        compiler_params=params(),
+        name="sum_qkv",
+    )(keep, got, sent, after)
+
+
+def glu_kernel(x_own, x_pair, gv, gg, same, other, after, keep_ref, send_ref):
+    rows = x_own.shape[0] // 2
+    cw = gv.shape[1]
+    far = far_dot(x_pair, same, other)
+    for n, w in enumerate((gv, gg)):
+        at = slice(n * cw, (n + 1) * cw)
+        part = dot_f32(x_own[...], w[...]) + far[:, at]
+        keep_ref[:, at] = part[:rows]
+        send_ref[:, at] = part[rows:].astype(BF16)
+
+
+def project_glu(x_own, x_pair, own, same, other, after):
+    rows, width = x_own.shape[0] // 2, same.shape[1]
+    return pl.pallas_call(
+        glu_kernel,
+        out_shape=(shape((rows, width), F32), shape((rows, width))),
+        in_specs=[VM] * 6 + [ANY],
+        out_specs=[VM] * 2,
+        cost_estimate=cost(270_000_000, 1_500_000),
+        compiler_params=params(),
+        name="project_glu",
+    )(x_own, x_pair, *own, same, other, after)
+
+
+def gate_kernel(keep_ref, got_ref, gated_ref, tail_ref):
+    rows, cw = gated_ref.shape
+    glu = keep_ref[...] + got_ref[...].astype(F32)
+    value = glu[:, :cw].astype(BF16).astype(F32)
+    gate = glu[:, cw:].astype(BF16).astype(F32)
+    gated = (value * jax.nn.sigmoid(gate)).astype(BF16)
+    gated_ref[...] = gated
+    tail_ref[...] = gated[rows - tail_ref.shape[0] :]
+
+
+def gate(keep, got, tail):
+    rows, cw = keep.shape[0], keep.shape[1] // 2
+    return pl.pallas_call(
+        gate_kernel,
+        out_shape=(shape((rows, cw)), shape((tail, cw))),
+        in_specs=[VM] * 2,
+        out_specs=[VM] * 2,
+        cost_estimate=cost(2_000_000, 500_000),
+        compiler_params=params(),
+        name="gate",
+    )(keep, got)
+
+
+def conv_kernel(gated_ref, before_ref, taps_ref, att_ref, act_ref, padded):
+    rows, aw = att_ref.shape
+    tail = before_ref.shape[0]
+    taps = taps_ref.shape[0]
+    padded[:tail, :] = before_ref[...].astype(F32)
+    padded[tail:, :] = gated_ref[...].astype(F32)
+    total = None
+    for tap in range(taps):
+        first = tail - (taps - 1) + tap
+        part = taps_ref[tap : tap + 1, :] * padded[first : first + rows, :]
+        total = part if total is None else total + part
+    act_ref[:, :aw] = att_ref[...]
+    act_ref[:, aw:] = total.astype(BF16)
+
+
+def conv(gated, before, taps, attended):
+    rows, cw = gated.shape
+    return pl.pallas_call(
+        conv_kernel,
+        out_shape=shape((rows, attended.shape[1] + cw)),
+        in_specs=[VM] * 4,
+        out_specs=VM,
+        scratch_shapes=[pltpu.VMEM((rows + before.shape[0], cw), F32)],
+        cost_estimate=cost(20_000_000, 500_000),
+        compiler_params=params(),
+        name="conv",
+    )(gated, before, taps, attended)
+
+
+def attention_kernel(q_ref, mine_ref, pair_ref, gain_ref, after, out_ref, mass_ref, kv, acc, mass, carry):
     me = lax.axis_index("sp")
     rows, width = q_ref.shape
-    heads = width // hd
+    heads, hd = gain_ref.shape
     lane = lax.broadcasted_iota(jnp.int32, (rows, width), 1) // hd
     keys = rows
+    for slot, (ref, n) in enumerate(((mine_ref, 0), (pair_ref, 0), (mine_ref, 1), (pair_ref, 1))):
+        kv[slot, :keys, :] = ref[n * keys : (n + 1) * keys, :]
+        kv[slot, keys : 2 * keys, :] = ref[(2 + n) * keys : (3 + n) * keys, :]
+        off = ref[4 * keys + 8 * n : 4 * keys + 8 * n + 8, :]
+        kv[slot, 2 * keys :, :] = jnp.concatenate([off, off])
     before = lax.broadcasted_iota(jnp.int32, (2 * keys, 2 * keys), 0) % keys
     column = lax.broadcasted_iota(jnp.int32, (2 * keys, 2 * keys), 1)
     suffix = jnp.where((column >= keys) | (before > column), 1.0, 0.0).astype(BF16)
@@ -45,10 +343,9 @@
     scale = hd ** (-0.5)
 
     def block(slot, first):
-        start = pl.multiple_of(slot * keys, keys)
-        k = k_ref[pl.ds(start, keys), :]
-        v = v_ref[pl.ds(start, keys), :]
-        off = off_ref[pl.ds(pl.multiple_of(slot * 8, 8), 8), :].astype(F32)
+        k = kv[slot, :keys, :]
+        v = kv[slot, keys : 2 * keys, :]
+        off = kv[slot, 2 * keys :, :].astype(F32)
         parts = []
         for h in range(heads):
             qh = jnp.where(lane == h, q, jnp.zeros_like(q))
@@ -98,73 +395,66 @@
     for h in range(heads):
         mean = jnp.sum(jnp.where(lane == h, squares, 0.0), axis=1, keepdims=True) / hd
         inverse = jnp.where(lane == h, lax.rsqrt(mean + norm_eps), inverse)
-    out_ref[...] = (mixed * inverse * gain_ref[...]).astype(BF16)
+    gain = jnp.concatenate([gain_ref[h : h + 1, :] for h in range(heads)], axis=1)
+    out_ref[...] = (mixed * inverse * gain).astype(BF16)
     for h in range(heads):
         mass_ref[h : h + 1, :] = jnp.log(jnp.sum(jnp.transpose(mass[h]), axis=0, keepdims=True))
 
 
-def attention(q, k, v, off, head_gain):
+def attention(q, mine, pair, head_gain, after):
     rows, width = q.shape
-    heads, hd = head_gain.shape
-    out_shape = (jax.ShapeDtypeStruct((rows, width), BF16), jax.ShapeDtypeStruct((heads, rows), F32))
-    return pl.pallas_call(
-        functools.partial(attention_kernel, hd),
-        out_shape=out_shape,
-        in_specs=[pl.BlockSpec(memory_space=pltpu.VMEM)] * 5,
-        out_specs=[pl.BlockSpec(memory_space=pltpu.VMEM)] * 2,
+    heads, _ = head_gain.shape
+    return pl.pallas_call(
+        attention_kernel,
+        out_shape=(shape((rows, width)), shape((heads, rows), F32)),
+        in_specs=[VM] * 4 + [ANY],
+        out_specs=[VM] * 2,
         scratch_shapes=[
+            pltpu.VMEM((4, 2 * rows + 16, width), BF16),
             pltpu.VMEM((rows, width), F32),
             pltpu.VMEM((heads, rows, rows), F32),
             pltpu.VMEM((heads, rows, rows), F32),
         ],
-        cost_estimate=pl.CostEstimate(flops=400_000_000, bytes_accessed=1_000_000, transcendentals=400_000),
-        compiler_params=pltpu.CompilerParams(vmem_limit_bytes=16 * 1024 * 1024),
+        cost_estimate=cost(400_000_000, 1_000_000),
+        compiler_params=params(),
         name="stick_attention",
-    )(q, k, v, off, head_gain.reshape(1, width))
-
-
-def final_kernel(aw, cw, mine, core, far, wa, wc, wcore, wx, wxc, gb0, gb1, gb2, gb3, gain_ref, out_ref):
-    acts = [mine[...], core[...], far[0], far[1]]
-    convs = [a[:, aw:].astype(F32) for a in acts]
-    count = len(convs) * cw
-    mean = sum(jnp.sum(v, axis=1, keepdims=True) for v in convs) / count
+    )(q, mine, pair, head_gain, after)
+
+
+def final_kernel(*refs):
+    act, wa, wc = (refs[n * 4 : (n + 1) * 4] for n in range(3))
+    gain_ref, out_ref = refs[12:]
+    cw = wc[0].shape[0]
+    aw = act[0].shape[1] - cw
+    convs = [c[:, aw:].astype(F32) for c in act]
+    mean = sum(jnp.sum(v, axis=1, keepdims=True) for v in convs) / (4 * cw)
     centered = [v - mean for v in convs]
-    spread = sum(jnp.sum(v * v, axis=1, keepdims=True) for v in centered) / count
+    spread = sum(jnp.sum(v * v, axis=1, keepdims=True) for v in centered) / (4 * cw)
     inverse = lax.rsqrt(spread + norm_eps)
     total = None
-    for slot, (v, gb) in enumerate(zip(centered, (gb0, gb1, gb2, gb3))):
-        y = v * inverse * gb[0:1, :] + gb[1:2, :]
+    for slot in range(4):
+        pieces = [wa[slot][aw : aw + 1, n * cw : (n + 1) * cw].astype(F32) for n in range(6)]
+        gain = pieces[0] + pieces[1] + pieces[2]
+        bias = pieces[3] + pieces[4] + pieces[5]
+        y = centered[slot] * inverse * gain + bias
         y = (y * jax.nn.sigmoid(y)).astype(BF16)
-        att = acts[slot][:, :aw]
-        if slot == 0:
-            part = dot_f32(att, wa[...]) + dot_f32(y, wc[...])
-        else:
-            w = (wcore, wx, wxc)[slot - 1]
-            part = dot_f32(jnp.concatenate([att, y], axis=1), w[...])
+        part = dot_f32(act[slot][:, :aw], wa[slot][:aw, :]) + dot_f32(y, wc[slot][...])
         total = part if total is None else total + part
     squares = jnp.mean(total * total, axis=1, keepdims=True)
     out_ref[...] = (total * lax.rsqrt(squares + norm_eps) * gain_ref[...]).astype(BF16)
 
 
-def finish(mine, core, far, wa, wc, wcore, wx, wxc, gbs, out_gain):
-    rows = mine.shape[0]
-    width = wa.shape[1]
-    return pl.pallas_call(
-        functools.partial(final_kernel, wa.shape[0], wc.shape[0]),
-        out_shape=jax.ShapeDtypeStruct((rows, width), BF16),
-        in_specs=[pl.BlockSpec(memory_space=pltpu.VMEM)] * 13,
-        out_specs=pl.BlockSpec(memory_space=pltpu.VMEM),
-        cost_estimate=pl.CostEstimate(flops=800_000_000, bytes_accessed=7_000_000, transcendentals=70_000),
-        compiler_params=pltpu.CompilerParams(vmem_limit_bytes=32 * 1024 * 1024),
+def finish(act, wa, wc, out_gain):
+    rows, width = act[0].shape[0], wa[0].shape[1]
+    return pl.pallas_call(
+        final_kernel,
+        out_shape=shape((rows, width)),
+        in_specs=[VM] * 13,
+        out_specs=VM,
+        cost_estimate=cost(800_000_000, 7_000_000),
+        compiler_params=params(32),
         name="finish_rows",
-    )(mine, core, far, wa, wc, wcore, wx, wxc, *gbs, out_gain.reshape(1, width))
-
-
-def depthwise(padded, conv_taps, rows):
-    out = jnp.zeros((rows, padded.shape[1]), F32)
-    for tap in range(conv_taps.shape[0]):
-        out = out + conv_taps[tap] * padded[tap : tap + rows]
-    return out
+    )(*act, *wa, *wc, out_gain.reshape(1, width))
 
 
 def paired(
@@ -184,77 +474,38 @@
     w_out_conv,
     out_gain,
 ):
-    rows, features = tokens.shape
-    half_rows, block = rows // 2, w_query.shape[0]
-    half = 2 * block
-    heads, hd = head_gain.shape
-    aw, cw = heads * hd, conv_taps.shape[1]
-    me_sp, me_tp = lax.axis_index("sp"), lax.axis_index("tp")
-    side, low = me_sp // 2, me_sp % 2
-    core = me_tp % 2
-
-    normed = row_norm(tokens.astype(F32), norm_gain).astype(BF16)
-    x_send = lax.dynamic_slice(normed, (core * half_rows, (1 - side) * half), (half_rows, half))
+    wc_x = exchange(w_out_conv, "tp", 2)
+    own_qkv = (w_query, w_key, w_value)
+    x_send, mine_own, mine_pair, w_qkv = norm_parts(tokens, norm_gain, own_qkv)
     x_got = exchange(x_send, "sp", 2)
-    w_attn = jnp.concatenate([w_query, w_key, w_value], axis=1)
-    w_attn_pair = exchange(w_attn, "sp", 1)
-    w_glu = jnp.concatenate([w_glu_value, w_glu_gate], axis=1)
-    w_glu_pair = exchange(w_glu, "sp", 1)
-    w_out = jnp.concatenate([w_out_attn, w_out_conv], axis=0)
-    w_out_x = exchange(w_out, "tp", 2)
-    w_out_core = exchange(w_out, "tp", 1)
-    gb = jnp.stack([channel_gain, channel_bias])
-    gb_core = exchange(gb, "tp", 1)
-    gb_x = exchange(jnp.concatenate([gb, gb_core]), "tp", 2)
+    qkv_same = exchange(w_qkv, "sp", 1)
+    w_glu, wa_mine = pack(w_glu_value, w_glu_gate, w_out_attn, channel_gain, channel_bias)
+    glu_same = exchange(w_glu, "sp", 1)
+    wa_x = exchange(wa_mine, "tp", 2)
     x_other = exchange(x_got, "tp", 1)
-    w_out_xc = exchange(w_out_x, "tp", 1)
-
-    x_cross = jnp.where(
-        core == 0, jnp.concatenate([x_got, x_other]), jnp.concatenate([x_other, x_got])
-    )
-    x_mine = lax.dynamic_slice(normed, (0, side * half), (rows, half))
-    x_all = jnp.concatenate([x_mine, x_cross])
-    x_own = lax.dynamic_slice(x_all, (0, low * block), (2 * rows, block))
-    x_pair = lax.dynamic_slice(x_all, (0, (1 - low) * block), (2 * rows, block))
-
-    p = dot_f32(x_own, w_attn) + dot_f32(x_pair, w_attn_pair)
-    pq, pk, pv = (p[:, n * aw : (n + 1) * aw] for n in range(3))
-    off = jnp.pad(key_offset.T, ((0, 8 - heads), (0, 0)))
-    sent = jnp.concatenate([pq[rows:], pk[rows:], pv[rows:], pk[:rows], pv[:rows]]).astype(BF16)
-    got = exchange(jnp.concatenate([sent, off, off]), "sp", 2)
-    g = [got[n * rows : (n + 1) * rows].astype(F32) for n in range(5)]
-    q = (pq[:rows] + g[0]).astype(BF16)
-    k_two = jnp.concatenate([pk[:rows] + g[1], pk[rows:] + g[3]]).astype(BF16)
-    v_two = jnp.concatenate([pv[:rows] + g[2], pv[rows:] + g[4]]).astype(BF16)
-    off_two = jnp.concatenate([off, got[5 * rows : 5 * rows + 8]])
-    mine_two = jnp.concatenate([k_two, v_two, off_two])
+    qkv_other = exchange(qkv_same, "grp", 1)
+    wc_core = exchange(w_out_conv, "tp", 1)
+    wa_core = exchange(wa_mine, "tp", 1)
+    glu_other = exchange(glu_same, "grp", 1)
+    wc_xc = exchange(wc_x, "tp", 1)
+    wa_xc = exchange(wa_x, "tp", 1)
+    x_own, x_pair = assemble(mine_own, mine_pair, x_got, x_other)
+
+    keep, sent = project_qkv(x_own, x_pair, own_qkv, qkv_same, qkv_other, key_offset.T)
+    got = exchange(sent, "sp", 2)
+    own_glu = (w_glu_value, w_glu_gate)
+    glu_keep, glu_sent = project_glu(x_own, x_pair, own_glu, glu_same, glu_other, sent)
+    glu_got = exchange(glu_sent, "sp", 2)
+    q, mine_two = sum_qkv(keep, got, sent, glu_sent)
     pair_two = exchange(mine_two, "sp", 1)
-
-    def slots(first, size):
-        a, b = mine_two[first : first + 2 * size], pair_two[first : first + 2 * size]
-        return jnp.concatenate([a[:size], b[:size], a[size:], b[size:]])
-
-    k_all, v_all, off_all = slots(0, rows), slots(2 * rows, rows), slots(4 * rows, 8)
-
-    pg = dot_f32(x_own, w_glu) + dot_f32(x_pair, w_glu_pair)
-    glu = pg[:rows] + exchange(pg[rows:].astype(BF16), "sp", 2).astype(F32)
-    gated = (glu[:, :cw] * jax.nn.sigmoid(glu[:, cw:])).astype(BF16)
-    reach = conv_taps.shape[0] - 1
-    before = from_behind(gated[rows - reach :], "sp", 1)
-    padded = jnp.concatenate([before, gated]).astype(F32)
-    conv_out = depthwise(padded, conv_taps, rows).astype(BF16)
-
-    attended, log_mass = attention(q, k_all, v_all, off_all, head_gain)
-
-    act = jnp.concatenate([attended, conv_out], axis=1)
-    mine = lax.dynamic_slice(act, (core * half_rows, 0), (half_rows, aw + cw))
-    theirs = lax.dynamic_slice(act, ((1 - core) * half_rows, 0), (half_rows, aw + cw))
-    from_core = exchange(theirs, "tp", 1)
-    far = exchange(jnp.stack([mine, from_core]), "tp", 2)
-    gbs = (gb, gb_core, gb_x[:2], gb_x[2:])
-    done = finish(mine, from_core, far, w_out_attn, w_out_conv, w_out_core, w_out_x, w_out_xc, gbs, out_gain)
-    other = exchange(done, "tp", 1)
-    mixed = jnp.where(core == 0, jnp.concatenate([done, other]), jnp.concatenate([other, done]))
+    gated, tail = gate(glu_keep, glu_got, -(-conv_taps.shape[0] // 16) * 16)
+    before = from_behind(tail, "sp", 1)
+    attended, log_mass = attention(q, mine_two, pair_two, head_gain, tail)
+    act_mine = conv(gated, before, conv_taps, attended)
+    act = [act_mine] + [exchange(act_mine, "tp", bit) for bit in (1, 2, 3)]
+    wa = (wa_mine, wa_core, wa_x, wa_xc)
+    wc = (w_out_conv, wc_core, wc_x, wc_xc)
+    mixed = finish(act, wa, wc, out_gain)
     return (mixed, log_mass)
 
 
@@ -347,7 +598,7 @@
         )
         return (head_mix, mass_sum + jnp.sum(weights, axis=3), carried + jnp.sum(log_not, axis=3))
 
-    head_mix, mass_sum, leftover = lax.fori_loop(
+    head_mix, mass_sum, _ = lax.fori_loop(
         0, last_block + 1, sweep, (zeros_mix, zeros_row, zeros_row)
     )
     log_mass = jnp.log(mass_sum).reshape(heads_local, row_count)
@@ -403,6 +654,6 @@
         P(),
     )
     out_specs = (P(("grp", "sp"), None), P("tp", ("grp", "sp")))
-    small = mesh.shape["sp"] == 4 and mesh.shape["tp"] == 4
+    small = mesh.shape["sp"] == 4 and mesh.shape["tp"] == 4 and mesh.shape["grp"] == 2
     local = paired if small else gathered
     return jax.shard_map(local, mesh=mesh, in_specs=in_specs, out_specs=out_specs, check_vma=False)

time: 73.9 us -> 81.6 us (1.10); the launches traced: 73.3 us -> 80.1 us
  waiting for transfers between devices: 30.8 us -> 48.9 us
  local copies, waits for them, and re-layouts: 13.6 us -> 0.8 us
  Pallas kernels: 5.68 us -> 11.2 us
  starting transfers between devices: 13.5 us -> 18.3 us
  matrix products: 4.29 us -> 0 us
  other arithmetic: 3.88 us -> 0 us
    ppermute x15 -> x18, waiting for transfers between devices: 28.3 us -> 48.5 us  [exchange(): return lax.ppermute(value, axis, [(s, s ^ bit) for s in range(count)])]
    pallas_call x2 -> x10, Pallas kernels: 5.68 us -> 11.2 us  [the longest x1 2.77 us: attention(): pl.pallas_call(attention_kernel, out_shape=(shape((rows, width)), shape((...]
    ppermute x15 -> x18, starting transfers between devices: 12.2 us -> 16.9 us  [exchange(): return lax.ppermute(value, axis, [(s, s ^ bit) for s in range(count)])]
    dot_general x4 -> x0, matrix products: 4.29 us -> none  [dot_f32(): return lax.dot_general(a, b, (dims, ((), ())), preferred_element_type=F32)]
    unnamed x95 -> x28, local copies, waits for them, and re-layouts: 4.86 us -> 0.8 us
    concatenate x3 -> x0, local copies, waits for them, and re-layouts: 3.65 us -> none  [the longest x1 1.67 us: paired(): w_glu = jnp.concatenate([w_glu_value, w_glu_gate], axis=1)]
    slice x8 -> x0, local copies, waits for them, and re-layouts: 3.32 us -> none  [the longest x2 3.26 us: depthwise(): out = out + conv_taps[tap] * padded[tap:tap + rows]]
    ppermute x1, waiting for transfers between devices: 2.59 us -> 0.38 us  [from_behind(): lax.ppermute(value, axis, [(source, source + steps) for source in range(i...]
  transfers between devices with their start and end apart: 16 -> 19, of which waited for: 9 -> 10; matrix products, arithmetic and copies ran while one was open for 24% -> 0% of each run, Pallas kernels for 4% -> 11%
where the time goes in v3:
time: 81.6 us; the launch traced here: 80.1 us
  waiting for transfers between devices  48.9 us (60%)
  starting transfers between devices  18.3 us (22%)
  Pallas kernels  11.2 us (14%)
    ppermute x18, waiting for transfers between devices, exchange(): return lax.ppermute(value, axis, [(s, s ^ bit) for s in range(count)])  48.5 us
    ppermute x18, starting transfers between devices, exchange(): return lax.ppermute(value, axis, [(s, s ^ bit) for s in range(count)])  16.9 us
    pallas_call x1, Pallas kernels, attention(): pl.pallas_call(attention_kernel, out_shape=(shape((rows, width)), shape((...  2.77 us
    pallas_call x1, Pallas kernels, finish(): pl.pallas_call(final_kernel, out_shape=shape((rows, width)), in_specs=[VM...  2.4 us
    pallas_call x1, Pallas kernels, pack(): pl.pallas_call(pack_kernel, out_shape=(shape((block // 2, 2 * cw)), shape...  2.21 us
    pallas_call x1, Pallas kernels, norm_parts(): pl.pallas_call(norm_kernel, out_shape=(shape((rows // 2, 2 * block)), sha...  2.19 us
  transfers between devices with their start and end apart: 19, of which 10 were waited for; matrix products, arithmetic and copies ran while one was open for 0% of the time, Pallas kernels for 11%

profile of v3, /device:TPU:25, one launch (start us, length us, event | category | flops | bytes accessed | tf_op | source)
XLA Modules:
  0.0 80.1 jit_solution(11894175577394262995)
XLA Ops:
  0.6 1.3 %collective-permute-start.17 = (bf16[256,2048]{1,0:T(8,128)(2,1)}, bf16[256,2048]{1,0:T(8,128)(2,1)S(1)}, u32[]{:S(2)}, u32[]{:S(2)}) collective-permute-start(bf16[256,2048]{1,0:T(8,128)(2,1)} %refs_8_.1), channel_id=1, source_target_pairs={{0,2},{1,3},{2,0},{3,1},{4,6},{5,7},{6,4},{7,5},{8,10},{9,11},{10,... | collective-permute-start | bytes 3145736 | tf_op jit(solution)/shard_map/ppermute | solution.py:15
  1.9 2.2 %norm_parts.1 = (bf16[64,1024]{1,0:T(8,128)(2,1)}, bf16[128,512]{1,0:T(8,128)(2,1)}, bf16[128,512]{1,0:T(8,128)(2,1)}, bf16[256,384]{1,0:T(8,128)(2,1)}) custom-call(bf16[128,2048]{1,0:T(8,128)(2,1)} %x_hbm.1, f32[1,2048]{1,0:T(1,128)} %bitcast.7, bf16[512,128]{1,0:T(8,128)(2,1)} %wq.1, bf16[512,128]{1,0:T(8,128)(2,1)} %wk.1, bf16[512,128]{1,0:T(8,128)(2,1)} %wv.1), custom_call_target="tpu_custom_call" | custom-call | flops 2000000 | bytes 1000000 | tf_op jit(solution)/shard_map/norm_parts/pallas_call | solution.py:89
  4.1 0.2 collective-permute-start.4
  4.4 2.2 %pack.1 = (bf16[256,512]{1,0:T(8,128)(2,1)}, bf16[144,2048]{1,0:T(8,128)(2,1)}) custom-call(bf16[512,256]{1,0:T(8,128)(2,1)} %gv.1, bf16[512,256]{1,0:T(8,128)(2,1)} %gg.1, bf16[128,2048]{1,0:T(8,128)(2,1)} %wa_hbm.1, f32[1,256]{1,0:T(1,128)} %bitcast.8, f32[1,256]{1,0:T(1,128)} %bitcast.9), custom_call_target="tpu_custom_call" | custom-call | flops 2000000 | bytes 2000000 | tf_op jit(solution)/shard_map/pack/pallas_call | solution.py:143
  6.6 1.4 %collective-permute-start.2 = (bf16[256,512]{1,0:T(8,128)(2,1)}, bf16[256,512]{1,0:T(8,128)(2,1)S(1)}, u32[]{:S(2)}, u32[]{:S(2)}) collective-permute-start(bf16[256,512]{1,0:T(8,128)(2,1)} %get-tuple-element.25), channel_id=1, source_target_pairs={{0,4},{4,0},{8,12},{12,8},{1,5},{5,1},{9,13},{13,9},{2,6},{6,2},{1... | collective-permute-start | bytes 786440 | tf_op jit(solution)/shard_map/ppermute | solution.py:15
  8.0 0.3 collective-permute-start.14
  8.3 8.4 %collective-permute-done.got_ref = bf16[64,1024]{1,0:T(8,128)(2,1)S(1)} collective-permute-done((bf16[64,1024]{1,0:T(8,128)(2,1)S(1)}, bf16[64,1024]{1,0:T(8,128)(2,1)S(1)}, u32[]{:S(2)}, u32[]{:S(2)}) %collective-permute-start) | collective-permute-done | bytes 131104 | tf_op jit(solution)/shard_map/ppermute | solution.py:15
  16.6 1.5 %collective-permute-start.16 = (bf16[256,2048]{1,0:T(8,128)(2,1)S(1)}, bf16[256,2048]{1,0:T(8,128)(2,1)S(1)}, u32[]{:S(2)}, u32[]{:S(2)}) collective-permute-start(bf16[256,2048]{1,0:T(8,128)(2,1)S(1)} %copy-done), channel_id=1, source_target_pairs={{0,1},{1,0},{2,3},{3,2},{4,5},{5,4},{6,7},{7,6},{8,9},{9,8},{10,11... | collective-permute-start | bytes 3145736 | tf_op jit(solution)/shard_map/ppermute | solution.py:15
  18.1 6.9 %collective-permute-done.17.refs_10_ = bf16[256,2048]{1,0:T(8,128)(2,1)S(1)} collective-permute-done((bf16[256,2048]{1,0:T(8,128)(2,1)}, bf16[256,2048]{1,0:T(8,128)(2,1)S(1)}, u32[]{:S(2)}, u32[]{:S(2)}) %collective-permute-start.17) | collective-permute-done | bytes 1048608 | tf_op jit(solution)/shard_map/ppermute | solution.py:15
  25.0 2.7 %collective-permute-start.18 = (bf16[256,2048]{1,0:T(8,128)(2,1)S(1)}, bf16[256,2048]{1,0:T(8,128)(2,1)S(1)}, u32[]{:S(2)}, u32[]{:S(2)}) collective-permute-start(bf16[256,2048]{1,0:T(8,128)(2,1)S(1)} %collective-permute-done.17.refs_10_), channel_id=1, source_target_pairs={{0,1},{1,0},{2,3},{3,2},{4,5},{5,4},{6,7},{7,6},{8,9},{9,8},{10,11... | collective-permute-start | bytes 3145736 | tf_op jit(solution)/shard_map/ppermute | solution.py:15
  27.6 1.3 %collective-permute-start.3 = (bf16[256,512]{1,0:T(8,128)(2,1)S(1)}, bf16[256,512]{1,0:T(8,128)(2,1)S(1)}, u32[]{:S(2)}, u32[]{:S(2)}) collective-permute-start(bf16[256,512]{1,0:T(8,128)(2,1)S(1)} %collective-permute-done.2.same), channel_id=1, source_target_pairs={{0,16},{16,0},{1,17},{17,1},{2,18},{18,2},{3,19},{19,3},{4,20},{20... | collective-permute-start | bytes 786440 | tf_op jit(solution)/shard_map/ppermute | solution.py:15
  28.9 1.2 %collective-permute-done.1.other_ref = bf16[64,1024]{1,0:T(8,128)(2,1)S(1)} collective-permute-done((bf16[64,1024]{1,0:T(8,128)(2,1)S(1)}, bf16[64,1024]{1,0:T(8,128)(2,1)S(1)}, u32[]{:S(2)}, u32[]{:S(2)}) %collective-permute-start.1) | collective-permute-done | bytes 131104 | tf_op jit(solution)/shard_map/ppermute | solution.py:15
  30.1 1.2 %collective-permute-start.5 = (bf16[256,384]{1,0:T(8,128)(2,1)S(1)}, bf16[256,384]{1,0:T(8,128)(2,1)S(1)}, u32[]{:S(2)}, u32[]{:S(2)}) collective-permute-start(bf16[256,384]{1,0:T(8,128)(2,1)S(1)} %collective-permute-done.4.same), channel_id=1, source_target_pairs={{0,16},{16,0},{1,17},{17,1},{2,18},{18,2},{3,19},{19,3},{4,20},{20... | collective-permute-start | bytes 589832 | tf_op jit(solution)/shard_map/ppermute | solution.py:15
  31.4 7.9 %collective-permute-done.5.other = bf16[256,384]{1,0:T(8,128)(2,1)S(1)} collective-permute-done((bf16[256,384]{1,0:T(8,128)(2,1)S(1)}, bf16[256,384]{1,0:T(8,128)(2,1)S(1)}, u32[]{:S(2)}, u32[]{:S(2)}) %collective-permute-start.5) | collective-permute-done | bytes 196640 | tf_op jit(solution)/shard_map/ppermute | solution.py:15
  39.3 1.3 %collective-permute-start.13 = (bf16[144,2048]{1,0:T(8,128)(2,1)}, bf16[144,2048]{1,0:T(8,128)(2,1)S(1)}, u32[]{:S(2)}, u32[]{:S(2)}) collective-permute-start(bf16[144,2048]{1,0:T(8,128)(2,1)} %get-tuple-element.36.refs_4_), channel_id=1, source_target_pairs={{0,1},{1,0},{2,3},{3,2},{4,5},{5,4},{6,7},{7,6},{8,9},{9,8},{10,11... | collective-permute-start | bytes 1769480 | tf_op jit(solution)/shard_map/ppermute | solution.py:15
  40.6 0.6 copy-done.11
  41.3 0.5 project_qkv.1
  41.9 0.3 collective-permute-start.15
  42.3 0.4 project_glu.1
  42.8 9.8 %collective-permute-done.8.got_ref = bf16[656,128]{1,0:T(8,128)(2,1)S(1)} collective-permute-done((bf16[656,128]{1,0:T(8,128)(2,1)S(1)}, bf16[656,128]{1,0:T(8,128)(2,1)S(1)}, u32[]{:S(2)}, u32[]{:S(2)}) %collective-permute-start.8) | collective-permute-done | bytes 167968 | tf_op jit(solution)/shard_map/ppermute | solution.py:15
  52.6 5.9 %collective-permute-done.6.got_ref = bf16[128,512]{1,0:T(8,128)(2,1)S(1)} collective-permute-done((bf16[128,512]{1,0:T(8,128)(2,1)S(1)}, bf16[128,512]{1,0:T(8,128)(2,1)S(1)}, u32[]{:S(2)}, u32[]{:S(2)}) %collective-permute-start.6) | collective-permute-done | bytes 131104 | tf_op jit(solution)/shard_map/ppermute | solution.py:15
  58.5 3.8 %collective-permute-done.9.pair_ref = bf16[528,128]{1,0:T(8,128)(2,1)S(1)} collective-permute-done((bf16[528,128]{1,0:T(8,128)(2,1)S(1)}, bf16[528,128]{1,0:T(8,128)(2,1)S(1)}, u32[]{:S(2)}, u32[]{:S(2)}) %collective-permute-start.9) | collective-permute-done | bytes 135200 | tf_op jit(solution)/shard_map/ppermute | solution.py:15
  62.3 1.4 %collective-permute-start.7 = (bf16[32,256]{1,0:T(8,128)(2,1)S(1)}, bf16[32,256]{1,0:T(8,128)(2,1)S(1)}, u32[]{:S(2)}, u32[]{:S(2)}) collective-permute-start(bf16[32,256]{1,0:T(8,128)(2,1)S(1)} %get-tuple-element.31.after), channel_id=1, source_target_pairs={{0,4},{4,8},{8,12},{1,5},{5,9},{9,13},{2,6},{6,10},{10,14},{3,7},{... | collective-permute-start | bytes 49160 | tf_op jit(solution)/shard_map/ppermute | solution.py:21
  63.7 2.8 %stick_attention.1 = (bf16[128,128]{1,0:T(8,128)(2,1)S(1)}, f32[2,128]{1,0:T(2,128)}) custom-call(bf16[128,128]{1,0:T(8,128)(2,1)S(1)} %get-tuple-element.33.q_ref, bf16[528,128]{1,0:T(8,128)(2,1)S(1)} %get-tuple-element.34.mine_ref, bf16[528,128]{1,0:T(8,128)(2,1)S(1)} %collective-permute-done.9.pair_ref, f32[2,64]{1,0:T(2,128)S(1)} %copy-done.12, ...), custom_call_target="tpu_custom_call" | custom-call | flops 400000000 | bytes 1000000 | tf_op jit(solution)/shard_map/stick_attention/pallas_call | solution.py:407
  66.5 0.4 collective-permute-done.7.before_ref
  66.9 0.6 conv.1.refs_0_
  67.5 4.4 %collective-permute-start.12 = (bf16[128,384]{1,0:T(8,128)(2,1)S(1)}, bf16[128,384]{1,0:T(8,128)(2,1)S(1)}, u32[]{:S(2)}, u32[]{:S(2)}) collective-permute-start(bf16[128,384]{1,0:T(8,128)(2,1)S(1)} %conv.1.refs_0_), channel_id=1, source_target_pairs={{0,3},{1,2},{2,1},{3,0},{4,7},{5,6},{6,5},{7,4},{8,11},{9,10},{10,... | collective-permute-start | bytes 294920 | tf_op jit(solution)/shard_map/ppermute | solution.py:15
  71.9 0.4 collective-permute-start.11
  72.3 3.2 %collective-permute-done.12.refs_3_ = bf16[128,384]{1,0:T(8,128)(2,1)S(1)} collective-permute-done((bf16[128,384]{1,0:T(8,128)(2,1)S(1)}, bf16[128,384]{1,0:T(8,128)(2,1)S(1)}, u32[]{:S(2)}, u32[]{:S(2)}) %collective-permute-start.12) | collective-permute-done | bytes 98336 | tf_op jit(solution)/shard_map/ppermute | solution.py:15
  75.5 0.5 collective-permute-start.10
  76.0 1.6 %collective-permute-done.11.refs_2_ = bf16[128,384]{1,0:T(8,128)(2,1)S(1)} collective-permute-done((bf16[128,384]{1,0:T(8,128)(2,1)S(1)}, bf16[128,384]{1,0:T(8,128)(2,1)S(1)}, u32[]{:S(2)}, u32[]{:S(2)}) %collective-permute-start.11) | collective-permute-done | bytes 98336 | tf_op jit(solution)/shard_map/ppermute | solution.py:15
  77.7 2.4 %finish_rows.1 = bf16[128,2048]{1,0:T(8,128)(2,1)} custom-call(bf16[128,384]{1,0:T(8,128)(2,1)S(1)} %conv.1.refs_0_, bf16[128,384]{1,0:T(8,128)(2,1)S(1)} %collective-permute-done.10.refs_1_, bf16[128,384]{1,0:T(8,128)(2,1)S(1)} %collective-permute-done.11.refs_2_, bf16[128,384]{1,0:T(8,128)(2,1)S(1)} %collective-permute-done.12.refs_3_, ...), custom_call_target="tpu_custom_call" | custom-call | flops 800000000 | bytes 7000000 | tf_op jit(solution)/shard_map/finish_rows/pallas_call | solution.py:449
  (44 shorter events, 0.5 us)
Async XLA Ops:
  0.6 16.0 %copy-start = (bf16[256,2048]{1,0:T(8,128)(2,1)S(1)}, bf16[256,2048]{1,0:T(8,128)(2,1)}, u32[]{:S(2)}) copy-start(bf16[256,2048]{1,0:T(8,128)(2,1)} %refs_8_.1) | copy-start | bytes 3145732
  0.6 24.3 %collective-permute-start.17 = (bf16[256,2048]{1,0:T(8,128)(2,1)}, bf16[256,2048]{1,0:T(8,128)(2,1)S(1)}, u32[]{:S(2)}, u32[]{:S(2)}) collective-permute-start(bf16[256,2048]{1,0:T(8,128)(2,1)} %refs_8_.1), channel_id=1, source_target_pairs={{0,2},{1,3},{2,0},{3,1},{4,6},{5,7},{6,4},{7,5},{8,10},{9,11},{10,... | collective-permute-start | bytes 3145736 | tf_op jit(solution)/shard_map/ppermute | solution.py:15
  4.1 23.5 %collective-permute-start.4 = (bf16[256,384]{1,0:T(8,128)(2,1)}, bf16[256,384]{1,0:T(8,128)(2,1)S(1)}, u32[]{:S(2)}, u32[]{:S(2)}) collective-permute-start(bf16[256,384]{1,0:T(8,128)(2,1)} %get-tuple-element.26), channel_id=1, source_target_pairs={{0,4},{4,0},{8,12},{12,8},{1,5},{5,1},{9,13},{13,9},{2,6},{6,2},{1... | collective-permute-start | bytes 589832 | tf_op jit(solution)/shard_map/ppermute | solution.py:15
  4.4 3.6 %copy-start.13 = (bf16[64,1024]{1,0:T(8,128)(2,1)S(1)}, bf16[64,1024]{1,0:T(8,128)(2,1)}, u32[]{:S(2)}) copy-start(bf16[64,1024]{1,0:T(8,128)(2,1)} %get-tuple-element.22) | copy-start | bytes 393220
  4.4 27.0 %copy-start.7 = (bf16[128,512]{1,0:T(8,128)(2,1)S(1)}, bf16[128,512]{1,0:T(8,128)(2,1)}, u32[]{:S(2)}) copy-start(bf16[128,512]{1,0:T(8,128)(2,1)} %get-tuple-element.20.own_ref) | copy-start | bytes 393220
  4.4 27.0 %copy-start.8 = (bf16[128,512]{1,0:T(8,128)(2,1)S(1)}, bf16[128,512]{1,0:T(8,128)(2,1)}, u32[]{:S(2)}) copy-start(bf16[128,512]{1,0:T(8,128)(2,1)} %get-tuple-element.21.pair_ref) | copy-start | bytes 393220
  6.6 21.1 %collective-permute-start.2 = (bf16[256,512]{1,0:T(8,128)(2,1)}, bf16[256,512]{1,0:T(8,128)(2,1)S(1)}, u32[]{:S(2)}, u32[]{:S(2)}) collective-permute-start(bf16[256,512]{1,0:T(8,128)(2,1)} %get-tuple-element.25), channel_id=1, source_target_pairs={{0,4},{4,0},{8,12},{12,8},{1,5},{5,1},{9,13},{13,9},{2,6},{6,2},{1... | collective-permute-start | bytes 786440 | tf_op jit(solution)/shard_map/ppermute | solution.py:15
  7.9 8.7 %collective-permute-start = (bf16[64,1024]{1,0:T(8,128)(2,1)S(1)}, bf16[64,1024]{1,0:T(8,128)(2,1)S(1)}, u32[]{:S(2)}, u32[]{:S(2)}) collective-permute-start(bf16[64,1024]{1,0:T(8,128)(2,1)S(1)} %copy-done.13), channel_id=1, source_target_pairs={{0,8},{4,12},{8,0},{12,4},{1,9},{5,13},{9,1},{13,5},{2,10},{6,14},... | collective-permute-start | bytes 393224 | tf_op jit(solution)/shard_map/ppermute | solution.py:15
  8.0 33.9 %collective-permute-start.14 = (bf16[144,2048]{1,0:T(8,128)(2,1)}, bf16[144,2048]{1,0:T(8,128)(2,1)S(1)}, u32[]{:S(2)}, u32[]{:S(2)}) collective-permute-start(bf16[144,2048]{1,0:T(8,128)(2,1)} %get-tuple-element.36.refs_4_), channel_id=1, source_target_pairs={{0,2},{1,3},{2,0},{3,1},{4,6},{5,7},{6,4},{7,5},{8,10},{9,11},{10,... | collective-permute-start | bytes 1769480 | tf_op jit(solution)/shard_map/ppermute | solution.py:15
  16.6 61.0 %collective-permute-start.16 = (bf16[256,2048]{1,0:T(8,128)(2,1)S(1)}, bf16[256,2048]{1,0:T(8,128)(2,1)S(1)}, u32[]{:S(2)}, u32[]{:S(2)}) collective-permute-start(bf16[256,2048]{1,0:T(8,128)(2,1)S(1)} %copy-done), channel_id=1, source_target_pairs={{0,1},{1,0},{2,3},{3,2},{4,5},{5,4},{6,7},{7,6},{8,9},{9,8},{10,11... | collective-permute-start | bytes 3145736 | tf_op jit(solution)/shard_map/ppermute | solution.py:15
  25.0 52.7 %collective-permute-start.18 = (bf16[256,2048]{1,0:T(8,128)(2,1)S(1)}, bf16[256,2048]{1,0:T(8,128)(2,1)S(1)}, u32[]{:S(2)}, u32[]{:S(2)}) collective-permute-start(bf16[256,2048]{1,0:T(8,128)(2,1)S(1)} %collective-permute-done.17.refs_10_), channel_id=1, source_target_pairs={{0,1},{1,0},{2,3},{3,2},{4,5},{5,4},{6,7},{7,6},{8,9},{9,8},{10,11... | collective-permute-start | bytes 3145736 | tf_op jit(solution)/shard_map/ppermute | solution.py:15
  27.6 2.5 %collective-permute-start.1 = (bf16[64,1024]{1,0:T(8,128)(2,1)S(1)}, bf16[64,1024]{1,0:T(8,128)(2,1)S(1)}, u32[]{:S(2)}, u32[]{:S(2)}) collective-permute-start(bf16[64,1024]{1,0:T(8,128)(2,1)S(1)} %collective-permute-done.got_ref), channel_id=1, source_target_pairs={{0,1},{1,0},{2,3},{3,2},{4,5},{5,4},{6,7},{7,6},{8,9},{9,8},{10,11... | collective-permute-start | bytes 393224 | tf_op jit(solution)/shard_map/ppermute | solution.py:15
  27.6 14.2 %collective-permute-start.3 = (bf16[256,512]{1,0:T(8,128)(2,1)S(1)}, bf16[256,512]{1,0:T(8,128)(2,1)S(1)}, u32[]{:S(2)}, u32[]{:S(2)}) collective-permute-start(bf16[256,512]{1,0:T(8,128)(2,1)S(1)} %collective-permute-done.2.same), channel_id=1, source_target_pairs={{0,16},{16,0},{1,17},{17,1},{2,18},{18,2},{3,19},{19,3},{4,20},{20... | collective-permute-start | bytes 786440 | tf_op jit(solution)/shard_map/ppermute | solution.py:15
  30.1 9.2 %collective-permute-start.5 = (bf16[256,384]{1,0:T(8,128)(2,1)S(1)}, bf16[256,384]{1,0:T(8,128)(2,1)S(1)}, u32[]{:S(2)}, u32[]{:S(2)}) collective-permute-start(bf16[256,384]{1,0:T(8,128)(2,1)S(1)} %collective-permute-done.4.same), channel_id=1, source_target_pairs={{0,16},{16,0},{1,17},{17,1},{2,18},{18,2},{3,19},{19,3},{4,20},{20... | collective-permute-start | bytes 589832 | tf_op jit(solution)/shard_map/ppermute | solution.py:15
  31.3 9.3 %copy-start.4 = (bf16[512,128]{1,0:T(8,128)(2,1)S(1)}, bf16[512,128]{1,0:T(8,128)(2,1)}, u32[]{:S(2)}) copy-start(bf16[512,128]{1,0:T(8,128)(2,1)} %wq.1) | copy-start | bytes 393220
  31.3 9.3 %copy-start.5 = (bf16[512,128]{1,0:T(8,128)(2,1)S(1)}, bf16[512,128]{1,0:T(8,128)(2,1)}, u32[]{:S(2)}) copy-start(bf16[512,128]{1,0:T(8,128)(2,1)} %wk.1) | copy-start | bytes 393220
  31.4 9.3 %copy-start.6 = (bf16[512,128]{1,0:T(8,128)(2,1)S(1)}, bf16[512,128]{1,0:T(8,128)(2,1)}, u32[]{:S(2)}) copy-start(bf16[512,128]{1,0:T(8,128)(2,1)} %wv.1) | copy-start | bytes 393220
  39.3 32.6 %collective-permute-start.13 = (bf16[144,2048]{1,0:T(8,128)(2,1)}, bf16[144,2048]{1,0:T(8,128)(2,1)S(1)}, u32[]{:S(2)}, u32[]{:S(2)}) collective-permute-start(bf16[144,2048]{1,0:T(8,128)(2,1)} %get-tuple-element.36.refs_4_), channel_id=1, source_target_pairs={{0,1},{1,0},{2,3},{3,2},{4,5},{5,4},{6,7},{7,6},{8,9},{9,8},{10,11... | collective-permute-start | bytes 1769480 | tf_op jit(solution)/shard_map/ppermute | solution.py:15
  41.3 0.9 %copy-start.1 = (bf16[512,256]{1,0:T(8,128)(2,1)S(1)}, bf16[512,256]{1,0:T(8,128)(2,1)}, u32[]{:S(2)}) copy-start(bf16[512,256]{1,0:T(8,128)(2,1)} %gv.1) | copy-start | bytes 786436
  41.3 1.0 %copy-start.2 = (bf16[512,256]{1,0:T(8,128)(2,1)S(1)}, bf16[512,256]{1,0:T(8,128)(2,1)}, u32[]{:S(2)}) copy-start(bf16[512,256]{1,0:T(8,128)(2,1)} %gg.1) | copy-start | bytes 786436
  41.8 10.7 %collective-permute-start.8 = (bf16[656,128]{1,0:T(8,128)(2,1)S(1)}, bf16[656,128]{1,0:T(8,128)(2,1)S(1)}, u32[]{:S(2)}, u32[]{:S(2)}) collective-permute-start(bf16[656,128]{1,0:T(8,128)(2,1)S(1)} %get-tuple-element.27.after.sent_ref), channel_id=1, source_target_pairs={{0,8},{4,12},{8,0},{12,4},{1,9},{5,13},{9,1},{13,5},{2,10},{6,14},... | collective-permute-start | bytes 503816 | tf_op jit(solution)/shard_map/ppermute | solution.py:15
  41.9 35.7 %collective-permute-start.15 = (bf16[144,2048]{1,0:T(8,128)(2,1)S(1)}, bf16[144,2048]{1,0:T(8,128)(2,1)S(1)}, u32[]{:S(2)}, u32[]{:S(2)}) collective-permute-start(bf16[144,2048]{1,0:T(8,128)(2,1)S(1)} %collective-permute-done.14.refs_6_), channel_id=1, source_target_pairs={{0,1},{1,0},{2,3},{3,2},{4,5},{5,4},{6,7},{7,6},{8,9},{9,8},{10,11... | collective-permute-start | bytes 1769480 | tf_op jit(solution)/shard_map/ppermute | solution.py:15
  52.5 5.9 %collective-permute-start.6 = (bf16[128,512]{1,0:T(8,128)(2,1)S(1)}, bf16[128,512]{1,0:T(8,128)(2,1)S(1)}, u32[]{:S(2)}, u32[]{:S(2)}) collective-permute-start(bf16[128,512]{1,0:T(8,128)(2,1)S(1)} %get-tuple-element.29.after), channel_id=1, source_target_pairs={{0,8},{4,12},{8,0},{12,4},{1,9},{5,13},{9,1},{13,5},{2,10},{6,14},... | collective-permute-start | bytes 393224 | tf_op jit(solution)/shard_map/ppermute | solution.py:15
  58.4 3.9 %collective-permute-start.9 = (bf16[528,128]{1,0:T(8,128)(2,1)S(1)}, bf16[528,128]{1,0:T(8,128)(2,1)S(1)}, u32[]{:S(2)}, u32[]{:S(2)}) collective-permute-start(bf16[528,128]{1,0:T(8,128)(2,1)S(1)} %get-tuple-element.34.mine_ref), channel_id=1, source_target_pairs={{0,4},{4,0},{8,12},{12,8},{1,5},{5,1},{9,13},{13,9},{2,6},{6,2},{1... | collective-permute-start | bytes 405512 | tf_op jit(solution)/shard_map/ppermute | solution.py:15
  62.3 1.4 %copy-start.12 = (f32[2,64]{1,0:T(2,128)S(1)}, f32[2,64]{1,0:T(2,128)}, u32[]{:S(2)}) copy-start(f32[2,64]{1,0:T(2,128)} %gain_ref.1) | copy-start | bytes 1540
  62.3 4.6 %collective-permute-start.7 = (bf16[32,256]{1,0:T(8,128)(2,1)S(1)}, bf16[32,256]{1,0:T(8,128)(2,1)S(1)}, u32[]{:S(2)}, u32[]{:S(2)}) collective-permute-start(bf16[32,256]{1,0:T(8,128)(2,1)S(1)} %get-tuple-element.31.after), channel_id=1, source_target_pairs={{0,4},{4,8},{8,12},{1,5},{5,9},{9,13},{2,6},{6,10},{10,14},{3,7},{... | collective-permute-start | bytes 49160 | tf_op jit(solution)/shard_map/ppermute | solution.py:21
  63.7 3.2 %copy-start.9 = (f32[31,256]{1,0:T(8,128)S(1)}, f32[31,256]{1,0:T(8,128)}, u32[]{:S(2)}) copy-start(f32[31,256]{1,0:T(8,128)} %taps_ref.1) | copy-start | bytes 95236
  63.7 13.9 %copy-start.3 = (bf16[144,2048]{1,0:T(8,128)(2,1)S(1)}, bf16[144,2048]{1,0:T(8,128)(2,1)}, u32[]{:S(2)}) copy-start(bf16[144,2048]{1,0:T(8,128)(2,1)} %get-tuple-element.36.refs_4_) | copy-start | bytes 1769476
  66.9 10.8 %copy-start.10 = (f32[2048]{0:T(1024)S(1)}, f32[2048]{0:T(1024)}, u32[]{:S(2)}) copy-start(f32[2048]{0:T(1024)} %param.29) | copy-start | bytes 24580
  67.5 8.0 %collective-permute-start.12 = (bf16[128,384]{1,0:T(8,128)(2,1)S(1)}, bf16[128,384]{1,0:T(8,128)(2,1)S(1)}, u32[]{:S(2)}, u32[]{:S(2)}) collective-permute-start(bf16[128,384]{1,0:T(8,128)(2,1)S(1)} %conv.1.refs_0_), channel_id=1, source_target_pairs={{0,3},{1,2},{2,1},{3,0},{4,7},{5,6},{6,5},{7,4},{8,11},{9,10},{10,... | collective-permute-start | bytes 294920 | tf_op jit(solution)/shard_map/ppermute | solution.py:15
  71.9 5.7 %collective-permute-start.11 = (bf16[128,384]{1,0:T(8,128)(2,1)S(1)}, bf16[128,384]{1,0:T(8,128)(2,1)S(1)}, u32[]{:S(2)}, u32[]{:S(2)}) collective-permute-start(bf16[128,384]{1,0:T(8,128)(2,1)S(1)} %conv.1.refs_0_), channel_id=1, source_target_pairs={{0,2},{1,3},{2,0},{3,1},{4,6},{5,7},{6,4},{7,5},{8,10},{9,11},{10,... | collective-permute-start | bytes 294920 | tf_op jit(solution)/shard_map/ppermute | solution.py:15
  75.5 2.1 %collective-permute-start.10 = (bf16[128,384]{1,0:T(8,128)(2,1)S(1)}, bf16[128,384]{1,0:T(8,128)(2,1)S(1)}, u32[]{:S(2)}, u32[]{:S(2)}) collective-permute-start(bf16[128,384]{1,0:T(8,128)(2,1)S(1)} %conv.1.refs_0_), channel_id=1, source_target_pairs={{0,1},{1,0},{2,3},{3,2},{4,5},{5,4},{6,7},{7,6},{8,9},{9,8},{10,11... | collective-permute-start | bytes 294920 | tf_op jit(solution)/shard_map/ppermute | solution.py:15
  (1 other events, 0.7 us)

commit v4 on v3

--- a/solution.py
+++ b/solution.py
@@ -30,9 +30,6 @@
     return lax.dot_general(a, b, (dims, ((), ())), preferred_element_type=F32)
 
 
-FULL = 60
-
-
 def params(limit=16):
     return pltpu.CompilerParams(vmem_limit_bytes=limit * 1024 * 1024)
 
@@ -50,27 +47,52 @@
     return pl.CostEstimate(flops=flops, bytes_accessed=moved, transcendentals=0)
 
 
-def norm_kernel(x_hbm, gain_hbm, *refs):
-    weights = refs[:3]
-    send_ref, own_ref, pair_ref, pack_ref, x_ref, gain_ref, normed, sems = refs[3:]
+def in_hbm(*values):
+    return [pltpu.with_memory_space_constraint(v, pltpu.HBM) for v in values]
+
+
+def pack_qkv_kernel(wq, wk, wv, pack_ref, sems):
+    part = pack_ref.shape[0]
+    width = wq.shape[1]
+    mine = pl.ds(pl.multiple_of(lax.axis_index("grp") * part, part), part)
+    copies = []
+    for n, w in enumerate((wq, wk, wv)):
+        at = slice(n * width, (n + 1) * width)
+        copies.append(pltpu.make_async_copy(w.at[mine, :], pack_ref.at[:, at], sems.at[n]))
+    for copy in copies:
+        copy.start()
+    for copy in copies:
+        copy.wait()
+
+
+def pack_qkv(weights):
+    block, width = weights[0].shape
+    return pl.pallas_call(
+        pack_qkv_kernel,
+        out_shape=shape((block // 2, 3 * width)),
+        in_specs=[HBM] * 3,
+        out_specs=VM,
+        scratch_shapes=[pltpu.SemaphoreType.DMA((3,))],
+        cost_estimate=cost(2_000_000, 400_000),
+        compiler_params=params(),
+        name="pack_qkv",
+    )(*in_hbm(*weights))
+
+
+def norm_kernel(x_hbm, gain_hbm, send_ref, own_ref, pair_ref, x_ref, gain_ref, normed, sems):
     side, low = lax.axis_index("sp") // 2, lax.axis_index("sp") % 2
     core = lax.axis_index("tp") % 2
-    block, width = weights[0].shape
+    block = own_ref.shape[1]
     half = 2 * block
     half_rows = send_ref.shape[0]
-    part = block // 2
-    mine = pl.ds(pl.multiple_of(lax.axis_index("grp") * part, part), part)
     copies = [
         pltpu.make_async_copy(x_hbm, x_ref, sems.at[0]),
         pltpu.make_async_copy(gain_hbm, gain_ref, sems.at[1]),
     ]
-    for n, w in enumerate(weights):
-        at = slice(n * width, (n + 1) * width)
-        copies.append(pltpu.make_async_copy(w.at[mine, :], pack_ref.at[:, at], sems.at[2 + n]))
     for copy in copies:
         copy.start()
-    copies[0].wait()
-    copies[1].wait()
+    for copy in copies:
+        copy.wait()
     x = x_ref[...].astype(F32)
     squares = jnp.mean(x * x, axis=1, keepdims=True)
     normed[...] = (x * lax.rsqrt(squares + norm_eps) * gain_ref[...]).astype(BF16)
@@ -79,42 +101,32 @@
     send_ref[...] = normed[pl.ds(first, half_rows), pl.ds(away, half)]
     own_ref[...] = normed[:, pl.ds(pl.multiple_of(side * half + low * block, block), block)]
     pair_ref[...] = normed[:, pl.ds(pl.multiple_of(side * half + (1 - low) * block, block), block)]
-    for copy in copies[2:]:
-        copy.wait()
-
-
-def norm_parts(tokens, gain, weights):
+
+
+def norm_parts(tokens, gain, block):
     rows, features = tokens.shape
-    block, width = weights[0].shape
     return pl.pallas_call(
         norm_kernel,
-        out_shape=(
-            shape((rows // 2, 2 * block)),
-            shape((rows, block)),
-            shape((rows, block)),
-            shape((block // 2, 3 * width)),
-        ),
-        in_specs=[HBM] * 5,
-        out_specs=[VM] * 4,
+        out_shape=(shape((rows // 2, 2 * block)), shape((rows, block)), shape((rows, block))),
+        in_specs=[HBM] * 2,
+        out_specs=[VM] * 3,
         scratch_shapes=[
             pltpu.VMEM((rows, features), BF16),
             pltpu.VMEM((1, features), F32),
             pltpu.VMEM((rows, features), BF16),
-            pltpu.SemaphoreType.DMA((5,)),
+            pltpu.SemaphoreType.DMA((2,)),
         ],
         cost_estimate=cost(2_000_000, 1_000_000),
-        compiler_params=params(FULL),
+        compiler_params=params(),
         name="norm_parts",
-    )(tokens, gain.reshape(1, features), *weights)
+    )(*in_hbm(tokens, gain.reshape(1, features)))
 
 
 def pack_kernel(gv_hbm, gg_hbm, wa_hbm, gain_hbm, bias_hbm, glu_ref, out_ref, gain_ref, bias_ref, sems):
     cw, aw = gv_hbm.shape[1], wa_hbm.shape[0]
-    part = glu_ref.shape[0]
-    mine = pl.ds(pl.multiple_of(lax.axis_index("grp") * part, part), part)
     copies = [
-        pltpu.make_async_copy(gv_hbm.at[mine, :], glu_ref.at[:, :cw], sems.at[0]),
-        pltpu.make_async_copy(gg_hbm.at[mine, :], glu_ref.at[:, cw:], sems.at[1]),
+        pltpu.make_async_copy(gv_hbm, glu_ref.at[:, :cw], sems.at[0]),
+        pltpu.make_async_copy(gg_hbm, glu_ref.at[:, cw:], sems.at[1]),
         pltpu.make_async_copy(wa_hbm, out_ref.at[:aw, :], sems.at[2]),
     ]
     small = [
@@ -142,7 +154,7 @@
     aw, width = wa.shape
     return pl.pallas_call(
         pack_kernel,
-        out_shape=(shape((block // 2, 2 * cw)), shape((aw + 16, width))),
+        out_shape=(shape((block, 2 * cw)), shape((aw + 16, width))),
         in_specs=[HBM] * 5,
         out_specs=[VM] * 2,
         scratch_shapes=[
@@ -151,9 +163,9 @@
             pltpu.SemaphoreType.DMA((5,)),
         ],
         cost_estimate=cost(2_000_000, 2_000_000),
-        compiler_params=params(FULL),
+        compiler_params=params(),
         name="pack",
-    )(gv, gg, wa, gain.reshape(1, cw), bias.reshape(1, cw))
+    )(*in_hbm(gv, gg, wa, gain.reshape(1, cw), bias.reshape(1, cw)))
 
 
 def assemble_kernel(own_ref, pair_ref, got_ref, other_ref, own_out, pair_out):
@@ -249,10 +261,10 @@
     )(keep, got, sent, after)
 
 
-def glu_kernel(x_own, x_pair, gv, gg, same, other, after, keep_ref, send_ref):
+def glu_kernel(x_own, x_pair, gv, gg, w_pair, after, keep_ref, send_ref):
     rows = x_own.shape[0] // 2
     cw = gv.shape[1]
-    far = far_dot(x_pair, same, other)
+    far = dot_f32(x_pair[...], w_pair[...])
     for n, w in enumerate((gv, gg)):
         at = slice(n * cw, (n + 1) * cw)
         part = dot_f32(x_own[...], w[...]) + far[:, at]
@@ -260,17 +272,17 @@
         send_ref[:, at] = part[rows:].astype(BF16)
 
 
-def project_glu(x_own, x_pair, own, same, other, after):
-    rows, width = x_own.shape[0] // 2, same.shape[1]
+def project_glu(x_own, x_pair, own, w_pair, after):
+    rows, width = x_own.shape[0] // 2, w_pair.shape[1]
     return pl.pallas_call(
         glu_kernel,
         out_shape=(shape((rows, width), F32), shape((rows, width))),
-        in_specs=[VM] * 6 + [ANY],
+        in_specs=[VM] * 5 + [ANY],
         out_specs=[VM] * 2,
         cost_estimate=cost(270_000_000, 1_500_000),
         compiler_params=params(),
         name="project_glu",
-    )(x_own, x_pair, *own, same, other, after)
+    )(x_own, x_pair, *own, w_pair, after)
 
 
 def gate_kernel(keep_ref, got_ref, gated_ref, tail_ref):
@@ -474,19 +486,18 @@
     w_out_conv,
     out_gain,
 ):
+    own_qkv = (w_query, w_key, w_value)
+    qkv_same = exchange(pack_qkv(own_qkv), "sp", 1)
     wc_x = exchange(w_out_conv, "tp", 2)
-    own_qkv = (w_query, w_key, w_value)
-    x_send, mine_own, mine_pair, w_qkv = norm_parts(tokens, norm_gain, own_qkv)
+    x_send, mine_own, mine_pair = norm_parts(tokens, norm_gain, w_query.shape[0])
     x_got = exchange(x_send, "sp", 2)
-    qkv_same = exchange(w_qkv, "sp", 1)
     w_glu, wa_mine = pack(w_glu_value, w_glu_gate, w_out_attn, channel_gain, channel_bias)
-    glu_same = exchange(w_glu, "sp", 1)
+    glu_pair = exchange(w_glu, "sp", 1)
+    qkv_other = exchange(qkv_same, "grp", 1)
+    x_other = exchange(x_got, "tp", 1)
     wa_x = exchange(wa_mine, "tp", 2)
-    x_other = exchange(x_got, "tp", 1)
-    qkv_other = exchange(qkv_same, "grp", 1)
     wc_core = exchange(w_out_conv, "tp", 1)
     wa_core = exchange(wa_mine, "tp", 1)
-    glu_other = exchange(glu_same, "grp", 1)
     wc_xc = exchange(wc_x, "tp", 1)
     wa_xc = exchange(wa_x, "tp", 1)
     x_own, x_pair = assemble(mine_own, mine_pair, x_got, x_other)
@@ -494,7 +505,7 @@
     keep, sent = project_qkv(x_own, x_pair, own_qkv, qkv_same, qkv_other, key_offset.T)
     got = exchange(sent, "sp", 2)
     own_glu = (w_glu_value, w_glu_gate)
-    glu_keep, glu_sent = project_glu(x_own, x_pair, own_glu, glu_same, glu_other, sent)
+    glu_keep, glu_sent = project_glu(x_own, x_pair, own_glu, glu_pair, sent)
     glu_got = exchange(glu_sent, "sp", 2)
     q, mine_two = sum_qkv(keep, got, sent, glu_sent)
     pair_two = exchange(mine_two, "sp", 1)

time: 81.6 us -> 78.4 us (0.961)
  the two profiles are of different devices: /device:TPU:25 before, /device:TPU:0 now
where the time goes in v4:
time: 78.4 us; the launch traced here: 78.2 us
  waiting for transfers between devices  50.3 us (64%)
  starting transfers between devices  17.6 us (22%)
  Pallas kernels  8.84 us (11%)
  between operations  0.8 us (1%)
    ppermute x17, waiting for transfers between devices, exchange(): return lax.ppermute(value, axis, [(s, s ^ bit) for s in range(count)])  50.1 us
    ppermute x17, starting transfers between devices, exchange(): return lax.ppermute(value, axis, [(s, s ^ bit) for s in range(count)])  15.6 us
    pallas_call x1, Pallas kernels, finish(): pl.pallas_call(final_kernel, out_shape=shape((rows, width)), in_specs=[VM...  2.41 us
    ppermute x1, starting transfers between devices, from_behind(): lax.ppermute(value, axis, [(source, source + steps) for source in range(i...  2.03 us
  transfers between devices with their start and end apart: 18, of which 10 were waited for; matrix products, arithmetic and copies ran while one was open for 0% of the time, Pallas kernels for 8%

profile of v4, /device:TPU:0, one launch (start us, length us, event | category | flops | bytes accessed | tf_op | source)
XLA Modules:
  0.0 78.2 jit_solution(15206426506892570336)
XLA Ops:
  0.6 3.0 %collective-permute-start.16 = (bf16[256,2048]{1,0:T(8,128)(2,1)}, bf16[256,2048]{1,0:T(8,128)(2,1)S(1)}, u32[]{:S(2)}, u32[]{:S(2)}) collective-permute-start(bf16[256,2048]{1,0:T(8,128)(2,1)} %refs_8_.1), channel_id=1, source_target_pairs={{0,2},{1,3},{2,0},{3,1},{4,6},{5,7},{6,4},{7,5},{8,10},{9,11},{10,... | collective-permute-start | bytes 3145736 | tf_op jit(solution)/shard_map/ppermute | solution.py:15
  3.7 0.9 %pack_qkv.1 = bf16[256,384]{1,0:T(8,128)(2,1)S(1)} custom-call(bf16[512,128]{1,0:T(8,128)(2,1)} %wq.3, bf16[512,128]{1,0:T(8,128)(2,1)} %wk.3, bf16[512,128]{1,0:T(8,128)(2,1)} %wv.3), custom_call_target="tpu_custom_call" | custom-call | flops 2000000 | bytes 400000 | tf_op jit(solution)/shard_map/pack_qkv/pallas_call | solution.py:70
  4.6 1.6 %collective-permute-start.3 = (bf16[256,384]{1,0:T(8,128)(2,1)S(1)}, bf16[256,384]{1,0:T(8,128)(2,1)S(1)}, u32[]{:S(2)}, u32[]{:S(2)}) collective-permute-start(bf16[256,384]{1,0:T(8,128)(2,1)S(1)} %pack_qkv.1), channel_id=1, source_target_pairs={{0,4},{4,0},{8,12},{12,8},{1,5},{5,1},{9,13},{13,9},{2,6},{6,2},{1... | collective-permute-start | bytes 589832 | tf_op jit(solution)/shard_map/ppermute | solution.py:15
  6.2 1.3 %pack.1 = (bf16[512,512]{1,0:T(8,128)(2,1)S(1)}, bf16[144,2048]{1,0:T(8,128)(2,1)S(1)}) custom-call(bf16[512,256]{1,0:T(8,128)(2,1)} %gv.1, bf16[512,256]{1,0:T(8,128)(2,1)} %gg.1, bf16[128,2048]{1,0:T(8,128)(2,1)} %wa_hbm.1, f32[1,256]{1,0:T(1,128)} %bitcast.8, f32[1,256]{1,0:T(1,128)} %bitcast.9), custom_call_target="tpu_custom_call" | custom-call | flops 2000000 | bytes 2000000 | tf_op jit(solution)/shard_map/pack/pallas_call | solution.py:155
  7.5 0.5 collective-permute-start.2
  8.0 1.3 %norm_parts.1 = (bf16[64,1024]{1,0:T(8,128)(2,1)S(1)}, bf16[128,512]{1,0:T(8,128)(2,1)S(1)}, bf16[128,512]{1,0:T(8,128)(2,1)S(1)}) custom-call(bf16[128,2048]{1,0:T(8,128)(2,1)} %x_hbm.1, f32[1,2048]{1,0:T(1,128)} %bitcast.7), custom_call_target="tpu_custom_call" | custom-call | flops 2000000 | bytes 1000000 | tf_op jit(solution)/shard_map/norm_parts/pallas_call | solution.py:108
  9.4 2.7 %collective-permute-start = (bf16[64,1024]{1,0:T(8,128)(2,1)S(1)}, bf16[64,1024]{1,0:T(8,128)(2,1)S(1)}, u32[]{:S(2)}, u32[]{:S(2)}) collective-permute-start(bf16[64,1024]{1,0:T(8,128)(2,1)S(1)} %get-tuple-element.21), channel_id=1, source_target_pairs={{0,8},{4,12},{8,0},{12,4},{1,9},{5,13},{9,1},{13,5},{2,10},{6,14},... | collective-permute-start | bytes 393224 | tf_op jit(solution)/shard_map/ppermute | solution.py:15
  12.0 0.5 collective-permute-start.13
  12.6 11.6 %collective-permute-done.got_ref = bf16[64,1024]{1,0:T(8,128)(2,1)S(1)} collective-permute-done((bf16[64,1024]{1,0:T(8,128)(2,1)S(1)}, bf16[64,1024]{1,0:T(8,128)(2,1)S(1)}, u32[]{:S(2)}, u32[]{:S(2)}) %collective-permute-start) | collective-permute-done | bytes 131104 | tf_op jit(solution)/shard_map/ppermute | solution.py:15
  24.2 3.7 %collective-permute-done.16.refs_10_ = bf16[256,2048]{1,0:T(8,128)(2,1)S(1)} collective-permute-done((bf16[256,2048]{1,0:T(8,128)(2,1)}, bf16[256,2048]{1,0:T(8,128)(2,1)S(1)}, u32[]{:S(2)}, u32[]{:S(2)}) %collective-permute-start.16) | collective-permute-done | bytes 1048608 | tf_op jit(solution)/shard_map/ppermute | solution.py:15
  27.9 0.5 collective-permute-start.1
  28.4 2.3 %collective-permute-done.1.other_ref = bf16[64,1024]{1,0:T(8,128)(2,1)S(1)} collective-permute-done((bf16[64,1024]{1,0:T(8,128)(2,1)S(1)}, bf16[64,1024]{1,0:T(8,128)(2,1)S(1)}, u32[]{:S(2)}, u32[]{:S(2)}) %collective-permute-start.1) | collective-permute-done | bytes 131104 | tf_op jit(solution)/shard_map/ppermute | solution.py:15
  30.7 2.0 %collective-permute-start.4 = (bf16[256,384]{1,0:T(8,128)(2,1)S(1)}, bf16[256,384]{1,0:T(8,128)(2,1)S(1)}, u32[]{:S(2)}, u32[]{:S(2)}) collective-permute-start(bf16[256,384]{1,0:T(8,128)(2,1)S(1)} %collective-permute-done.3.same), channel_id=1, source_target_pairs={{0,16},{16,0},{1,17},{17,1},{2,18},{18,2},{3,19},{19,3},{4,20},{20... | collective-permute-start | bytes 589832 | tf_op jit(solution)/shard_map/ppermute | solution.py:15
  32.8 5.2 %collective-permute-done.4.other = bf16[256,384]{1,0:T(8,128)(2,1)S(1)} collective-permute-done((bf16[256,384]{1,0:T(8,128)(2,1)S(1)}, bf16[256,384]{1,0:T(8,128)(2,1)S(1)}, u32[]{:S(2)}, u32[]{:S(2)}) %collective-permute-start.4) | collective-permute-done | bytes 196640 | tf_op jit(solution)/shard_map/ppermute | solution.py:15
  38.0 0.6 copy-done.8
  38.7 0.5 project_qkv.1
  39.2 2.9 %collective-permute-start.7 = (bf16[656,128]{1,0:T(8,128)(2,1)S(1)}, bf16[656,128]{1,0:T(8,128)(2,1)S(1)}, u32[]{:S(2)}, u32[]{:S(2)}) collective-permute-start(bf16[656,128]{1,0:T(8,128)(2,1)S(1)} %get-tuple-element.25.after.sent_ref), channel_id=1, source_target_pairs={{0,8},{4,12},{8,0},{12,4},{1,9},{5,13},{9,1},{13,5},{2,10},{6,14},... | collective-permute-start | bytes 503816 | tf_op jit(solution)/shard_map/ppermute | solution.py:15
  42.0 0.2 collective-permute-start.14
  42.3 0.4 project_glu.1
  42.7 7.9 %collective-permute-done.7.got_ref = bf16[656,128]{1,0:T(8,128)(2,1)S(1)} collective-permute-done((bf16[656,128]{1,0:T(8,128)(2,1)S(1)}, bf16[656,128]{1,0:T(8,128)(2,1)S(1)}, u32[]{:S(2)}, u32[]{:S(2)}) %collective-permute-start.7) | collective-permute-done | bytes 167968 | tf_op jit(solution)/shard_map/ppermute | solution.py:15
  50.7 8.9 %collective-permute-done.5.got_ref = bf16[128,512]{1,0:T(8,128)(2,1)S(1)} collective-permute-done((bf16[128,512]{1,0:T(8,128)(2,1)S(1)}, bf16[128,512]{1,0:T(8,128)(2,1)S(1)}, u32[]{:S(2)}, u32[]{:S(2)}) %collective-permute-start.5) | collective-permute-done | bytes 131104 | tf_op jit(solution)/shard_map/ppermute | solution.py:15
  59.5 0.1 gate.1
  59.6 5.0 %collective-permute-done.8.pair_ref = bf16[528,128]{1,0:T(8,128)(2,1)S(1)} collective-permute-done((bf16[528,128]{1,0:T(8,128)(2,1)S(1)}, bf16[528,128]{1,0:T(8,128)(2,1)S(1)}, u32[]{:S(2)}, u32[]{:S(2)}) %collective-permute-start.8) | collective-permute-done | bytes 135200 | tf_op jit(solution)/shard_map/ppermute | solution.py:15
  64.6 2.0 %collective-permute-start.6 = (bf16[32,256]{1,0:T(8,128)(2,1)S(1)}, bf16[32,256]{1,0:T(8,128)(2,1)S(1)}, u32[]{:S(2)}, u32[]{:S(2)}) collective-permute-start(bf16[32,256]{1,0:T(8,128)(2,1)S(1)} %get-tuple-element.29.after), channel_id=1, source_target_pairs={{0,4},{4,8},{8,12},{1,5},{5,9},{9,13},{2,6},{6,10},{10,14},{3,7},{... | collective-permute-start | bytes 49160 | tf_op jit(solution)/shard_map/ppermute | solution.py:21
  66.6 1.3 %stick_attention.1 = (bf16[128,128]{1,0:T(8,128)(2,1)S(1)}, f32[2,128]{1,0:T(2,128)}) custom-call(bf16[128,128]{1,0:T(8,128)(2,1)S(1)} %get-tuple-element.31.q_ref, bf16[528,128]{1,0:T(8,128)(2,1)S(1)} %get-tuple-element.32.mine_ref, bf16[528,128]{1,0:T(8,128)(2,1)S(1)} %collective-permute-done.8.pair_ref, f32[2,64]{1,0:T(2,128)S(1)} %copy-done.9, ...), custom_call_target="tpu_custom_call" | custom-call | flops 400000000 | bytes 1000000 | tf_op jit(solution)/shard_map/stick_attention/pallas_call | solution.py:419
  67.9 0.1 collective-permute-done.6.before_ref
  68.0 0.6 conv.1.refs_0_
  68.6 0.1 collective-permute-start.11
  68.7 1.4 %collective-permute-start.10 = (bf16[128,384]{1,0:T(8,128)(2,1)S(1)}, bf16[128,384]{1,0:T(8,128)(2,1)S(1)}, u32[]{:S(2)}, u32[]{:S(2)}) collective-permute-start(bf16[128,384]{1,0:T(8,128)(2,1)S(1)} %conv.1.refs_0_), channel_id=1, source_target_pairs={{0,2},{1,3},{2,0},{3,1},{4,6},{5,7},{6,4},{7,5},{8,10},{9,11},{10,... | collective-permute-start | bytes 294920 | tf_op jit(solution)/shard_map/ppermute | solution.py:15
  70.1 3.6 %collective-permute-done.11.refs_3_ = bf16[128,384]{1,0:T(8,128)(2,1)S(1)} collective-permute-done((bf16[128,384]{1,0:T(8,128)(2,1)S(1)}, bf16[128,384]{1,0:T(8,128)(2,1)S(1)}, u32[]{:S(2)}, u32[]{:S(2)}) %collective-permute-start.11) | collective-permute-done | bytes 98336 | tf_op jit(solution)/shard_map/ppermute | solution.py:15
  73.8 1.9 %collective-permute-done.10.refs_2_ = bf16[128,384]{1,0:T(8,128)(2,1)S(1)} collective-permute-done((bf16[128,384]{1,0:T(8,128)(2,1)S(1)}, bf16[128,384]{1,0:T(8,128)(2,1)S(1)}, u32[]{:S(2)}, u32[]{:S(2)}) %collective-permute-start.10) | collective-permute-done | bytes 98336 | tf_op jit(solution)/shard_map/ppermute | solution.py:15
  75.8 2.4 %finish_rows.1 = bf16[128,2048]{1,0:T(8,128)(2,1)} custom-call(bf16[128,384]{1,0:T(8,128)(2,1)S(1)} %conv.1.refs_0_, bf16[128,384]{1,0:T(8,128)(2,1)S(1)} %collective-permute-done.9.refs_1_, bf16[128,384]{1,0:T(8,128)(2,1)S(1)} %collective-permute-done.10.refs_2_, bf16[128,384]{1,0:T(8,128)(2,1)S(1)} %collective-permute-done.11.refs_3_, ...), custom_call_target="tpu_custom_call" | custom-call | flops 800000000 | bytes 7000000 | tf_op jit(solution)/shard_map/finish_rows/pallas_call | solution.py:461
  (35 shorter events, 0.2 us)
Async XLA Ops:
  0.6 23.5 %copy-start = (bf16[256,2048]{1,0:T(8,128)(2,1)S(1)}, bf16[256,2048]{1,0:T(8,128)(2,1)}, u32[]{:S(2)}) copy-start(bf16[256,2048]{1,0:T(8,128)(2,1)} %refs_8_.1) | copy-start | bytes 3145732
  0.6 27.3 %collective-permute-start.16 = (bf16[256,2048]{1,0:T(8,128)(2,1)}, bf16[256,2048]{1,0:T(8,128)(2,1)S(1)}, u32[]{:S(2)}, u32[]{:S(2)}) collective-permute-start(bf16[256,2048]{1,0:T(8,128)(2,1)} %refs_8_.1), channel_id=1, source_target_pairs={{0,2},{1,3},{2,0},{3,1},{4,6},{5,7},{6,4},{7,5},{8,10},{9,11},{10,... | collective-permute-start | bytes 3145736 | tf_op jit(solution)/shard_map/ppermute | solution.py:15
  4.6 23.3 %collective-permute-start.3 = (bf16[256,384]{1,0:T(8,128)(2,1)S(1)}, bf16[256,384]{1,0:T(8,128)(2,1)S(1)}, u32[]{:S(2)}, u32[]{:S(2)}) collective-permute-start(bf16[256,384]{1,0:T(8,128)(2,1)S(1)} %pack_qkv.1), channel_id=1, source_target_pairs={{0,4},{4,0},{8,12},{12,8},{1,5},{5,1},{9,13},{13,9},{2,6},{6,2},{1... | collective-permute-start | bytes 589832 | tf_op jit(solution)/shard_map/ppermute | solution.py:15
  7.5 31.6 %collective-permute-start.2 = (bf16[512,512]{1,0:T(8,128)(2,1)S(1)}, bf16[512,512]{1,0:T(8,128)(2,1)S(1)}, u32[]{:S(2)}, u32[]{:S(2)}) collective-permute-start(bf16[512,512]{1,0:T(8,128)(2,1)S(1)} %get-tuple-element.24), channel_id=1, source_target_pairs={{0,4},{4,0},{8,12},{12,8},{1,5},{5,1},{9,13},{13,9},{2,6},{6,2},{1... | collective-permute-start | bytes 1572872 | tf_op jit(solution)/shard_map/ppermute | solution.py:15
  9.4 14.8 %collective-permute-start = (bf16[64,1024]{1,0:T(8,128)(2,1)S(1)}, bf16[64,1024]{1,0:T(8,128)(2,1)S(1)}, u32[]{:S(2)}, u32[]{:S(2)}) collective-permute-start(bf16[64,1024]{1,0:T(8,128)(2,1)S(1)} %get-tuple-element.21), channel_id=1, source_target_pairs={{0,8},{4,12},{8,0},{12,4},{1,9},{5,13},{9,1},{13,5},{2,10},{6,14},... | collective-permute-start | bytes 393224 | tf_op jit(solution)/shard_map/ppermute | solution.py:15
  12.0 30.0 %collective-permute-start.13 = (bf16[144,2048]{1,0:T(8,128)(2,1)S(1)}, bf16[144,2048]{1,0:T(8,128)(2,1)S(1)}, u32[]{:S(2)}, u32[]{:S(2)}) collective-permute-start(bf16[144,2048]{1,0:T(8,128)(2,1)S(1)} %get-tuple-element.34.refs_4_), channel_id=1, source_target_pairs={{0,2},{1,3},{2,0},{3,1},{4,6},{5,7},{6,4},{7,5},{8,10},{9,11},{10,... | collective-permute-start | bytes 1769480 | tf_op jit(solution)/shard_map/ppermute | solution.py:15
  24.2 51.6 %collective-permute-start.15 = (bf16[256,2048]{1,0:T(8,128)(2,1)S(1)}, bf16[256,2048]{1,0:T(8,128)(2,1)S(1)}, u32[]{:S(2)}, u32[]{:S(2)}) collective-permute-start(bf16[256,2048]{1,0:T(8,128)(2,1)S(1)} %copy-done), channel_id=1, source_target_pairs={{0,1},{1,0},{2,3},{3,2},{4,5},{5,4},{6,7},{7,6},{8,9},{9,8},{10,11... | collective-permute-start | bytes 3145736 | tf_op jit(solution)/shard_map/ppermute | solution.py:15
  27.9 47.8 %collective-permute-start.17 = (bf16[256,2048]{1,0:T(8,128)(2,1)S(1)}, bf16[256,2048]{1,0:T(8,128)(2,1)S(1)}, u32[]{:S(2)}, u32[]{:S(2)}) collective-permute-start(bf16[256,2048]{1,0:T(8,128)(2,1)S(1)} %collective-permute-done.16.refs_10_), channel_id=1, source_target_pairs={{0,1},{1,0},{2,3},{3,2},{4,5},{5,4},{6,7},{7,6},{8,9},{9,8},{10,11... | collective-permute-start | bytes 3145736 | tf_op jit(solution)/shard_map/ppermute | solution.py:15
  27.9 2.8 %collective-permute-start.1 = (bf16[64,1024]{1,0:T(8,128)(2,1)S(1)}, bf16[64,1024]{1,0:T(8,128)(2,1)S(1)}, u32[]{:S(2)}, u32[]{:S(2)}) collective-permute-start(bf16[64,1024]{1,0:T(8,128)(2,1)S(1)} %collective-permute-done.got_ref), channel_id=1, source_target_pairs={{0,1},{1,0},{2,3},{3,2},{4,5},{5,4},{6,7},{7,6},{8,9},{9,8},{10,11... | collective-permute-start | bytes 393224 | tf_op jit(solution)/shard_map/ppermute | solution.py:15
  30.7 7.2 %collective-permute-start.4 = (bf16[256,384]{1,0:T(8,128)(2,1)S(1)}, bf16[256,384]{1,0:T(8,128)(2,1)S(1)}, u32[]{:S(2)}, u32[]{:S(2)}) collective-permute-start(bf16[256,384]{1,0:T(8,128)(2,1)S(1)} %collective-permute-done.3.same), channel_id=1, source_target_pairs={{0,16},{16,0},{1,17},{17,1},{2,18},{18,2},{3,19},{19,3},{4,20},{20... | collective-permute-start | bytes 589832 | tf_op jit(solution)/shard_map/ppermute | solution.py:15
  32.8 5.2 %copy-start.3 = (bf16[512,128]{1,0:T(8,128)(2,1)S(1)}, bf16[512,128]{1,0:T(8,128)(2,1)}, u32[]{:S(2)}) copy-start(bf16[512,128]{1,0:T(8,128)(2,1)} %wq.3) | copy-start | bytes 393220
  32.8 5.2 %copy-start.4 = (bf16[512,128]{1,0:T(8,128)(2,1)S(1)}, bf16[512,128]{1,0:T(8,128)(2,1)}, u32[]{:S(2)}) copy-start(bf16[512,128]{1,0:T(8,128)(2,1)} %wk.3) | copy-start | bytes 393220
  32.8 5.2 %copy-start.5 = (bf16[512,128]{1,0:T(8,128)(2,1)S(1)}, bf16[512,128]{1,0:T(8,128)(2,1)}, u32[]{:S(2)}) copy-start(bf16[512,128]{1,0:T(8,128)(2,1)} %wv.3) | copy-start | bytes 393220
  38.0 30.7 %collective-permute-start.12 = (bf16[144,2048]{1,0:T(8,128)(2,1)S(1)}, bf16[144,2048]{1,0:T(8,128)(2,1)S(1)}, u32[]{:S(2)}, u32[]{:S(2)}) collective-permute-start(bf16[144,2048]{1,0:T(8,128)(2,1)S(1)} %get-tuple-element.34.refs_4_), channel_id=1, source_target_pairs={{0,1},{1,0},{2,3},{3,2},{4,5},{5,4},{6,7},{7,6},{8,9},{9,8},{10,11... | collective-permute-start | bytes 1769480 | tf_op jit(solution)/shard_map/ppermute | solution.py:15
  38.0 0.7 copy-start.8
  38.6 3.6 %copy-start.1 = (bf16[512,256]{1,0:T(8,128)(2,1)S(1)}, bf16[512,256]{1,0:T(8,128)(2,1)}, u32[]{:S(2)}) copy-start(bf16[512,256]{1,0:T(8,128)(2,1)} %gv.1) | copy-start | bytes 786436
  38.7 3.6 %copy-start.2 = (bf16[512,256]{1,0:T(8,128)(2,1)S(1)}, bf16[512,256]{1,0:T(8,128)(2,1)}, u32[]{:S(2)}) copy-start(bf16[512,256]{1,0:T(8,128)(2,1)} %gg.1) | copy-start | bytes 786436
  39.2 11.4 %collective-permute-start.7 = (bf16[656,128]{1,0:T(8,128)(2,1)S(1)}, bf16[656,128]{1,0:T(8,128)(2,1)S(1)}, u32[]{:S(2)}, u32[]{:S(2)}) collective-permute-start(bf16[656,128]{1,0:T(8,128)(2,1)S(1)} %get-tuple-element.25.after.sent_ref), channel_id=1, source_target_pairs={{0,8},{4,12},{8,0},{12,4},{1,9},{5,13},{9,1},{13,5},{2,10},{6,14},... | collective-permute-start | bytes 503816 | tf_op jit(solution)/shard_map/ppermute | solution.py:15
  42.0 33.7 %collective-permute-start.14 = (bf16[144,2048]{1,0:T(8,128)(2,1)S(1)}, bf16[144,2048]{1,0:T(8,128)(2,1)S(1)}, u32[]{:S(2)}, u32[]{:S(2)}) collective-permute-start(bf16[144,2048]{1,0:T(8,128)(2,1)S(1)} %collective-permute-done.13.refs_6_), channel_id=1, source_target_pairs={{0,1},{1,0},{2,3},{3,2},{4,5},{5,4},{6,7},{7,6},{8,9},{9,8},{10,11... | collective-permute-start | bytes 1769480 | tf_op jit(solution)/shard_map/ppermute | solution.py:15
  50.6 8.9 %collective-permute-start.5 = (bf16[128,512]{1,0:T(8,128)(2,1)S(1)}, bf16[128,512]{1,0:T(8,128)(2,1)S(1)}, u32[]{:S(2)}, u32[]{:S(2)}) collective-permute-start(bf16[128,512]{1,0:T(8,128)(2,1)S(1)} %get-tuple-element.27.after), channel_id=1, source_target_pairs={{0,8},{4,12},{8,0},{12,4},{1,9},{5,13},{9,1},{13,5},{2,10},{6,14},... | collective-permute-start | bytes 393224 | tf_op jit(solution)/shard_map/ppermute | solution.py:15
  59.5 5.0 %collective-permute-start.8 = (bf16[528,128]{1,0:T(8,128)(2,1)S(1)}, bf16[528,128]{1,0:T(8,128)(2,1)S(1)}, u32[]{:S(2)}, u32[]{:S(2)}) collective-permute-start(bf16[528,128]{1,0:T(8,128)(2,1)S(1)} %get-tuple-element.32.mine_ref), channel_id=1, source_target_pairs={{0,4},{4,0},{8,12},{12,8},{1,5},{5,1},{9,13},{13,9},{2,6},{6,2},{1... | collective-permute-start | bytes 405512 | tf_op jit(solution)/shard_map/ppermute | solution.py:15
  64.5 2.0 %copy-start.9 = (f32[2,64]{1,0:T(2,128)S(1)}, f32[2,64]{1,0:T(2,128)}, u32[]{:S(2)}) copy-start(f32[2,64]{1,0:T(2,128)} %gain_ref.1) | copy-start | bytes 1540
  64.6 3.5 %collective-permute-start.6 = (bf16[32,256]{1,0:T(8,128)(2,1)S(1)}, bf16[32,256]{1,0:T(8,128)(2,1)S(1)}, u32[]{:S(2)}, u32[]{:S(2)}) collective-permute-start(bf16[32,256]{1,0:T(8,128)(2,1)S(1)} %get-tuple-element.29.after), channel_id=1, source_target_pairs={{0,4},{4,8},{8,12},{1,5},{5,9},{9,13},{2,6},{6,10},{10,14},{3,7},{... | collective-permute-start | bytes 49160 | tf_op jit(solution)/shard_map/ppermute | solution.py:21
  66.6 1.4 %copy-start.6 = (f32[31,256]{1,0:T(8,128)S(1)}, f32[31,256]{1,0:T(8,128)}, u32[]{:S(2)}) copy-start(f32[31,256]{1,0:T(8,128)} %taps_ref.1) | copy-start | bytes 95236
  68.0 7.7 %copy-start.7 = (f32[2048]{0:T(1024)S(1)}, f32[2048]{0:T(1024)}, u32[]{:S(2)}) copy-start(f32[2048]{0:T(1024)} %param.29) | copy-start | bytes 24580
  68.6 5.2 %collective-permute-start.11 = (bf16[128,384]{1,0:T(8,128)(2,1)S(1)}, bf16[128,384]{1,0:T(8,128)(2,1)S(1)}, u32[]{:S(2)}, u32[]{:S(2)}) collective-permute-start(bf16[128,384]{1,0:T(8,128)(2,1)S(1)} %conv.1.refs_0_), channel_id=1, source_target_pairs={{0,3},{1,2},{2,1},{3,0},{4,7},{5,6},{6,5},{7,4},{8,11},{9,10},{10,... | collective-permute-start | bytes 294920 | tf_op jit(solution)/shard_map/ppermute | solution.py:15
  68.7 7.0 %collective-permute-start.10 = (bf16[128,384]{1,0:T(8,128)(2,1)S(1)}, bf16[128,384]{1,0:T(8,128)(2,1)S(1)}, u32[]{:S(2)}, u32[]{:S(2)}) collective-permute-start(bf16[128,384]{1,0:T(8,128)(2,1)S(1)} %conv.1.refs_0_), channel_id=1, source_target_pairs={{0,2},{1,3},{2,0},{3,1},{4,6},{5,7},{6,4},{7,5},{8,10},{9,11},{10,... | collective-permute-start | bytes 294920 | tf_op jit(solution)/shard_map/ppermute | solution.py:15
  73.8 1.9 %collective-permute-start.9 = (bf16[128,384]{1,0:T(8,128)(2,1)S(1)}, bf16[128,384]{1,0:T(8,128)(2,1)S(1)}, u32[]{:S(2)}, u32[]{:S(2)}) collective-permute-start(bf16[128,384]{1,0:T(8,128)(2,1)S(1)} %conv.1.refs_0_), channel_id=1, source_target_pairs={{0,1},{1,0},{2,3},{3,2},{4,5},{5,4},{6,7},{7,6},{8,9},{9,8},{10,11... | collective-permute-start | bytes 294920 | tf_op jit(solution)/shard_map/ppermute | solution.py:15

commit v5 on v4

--- a/solution.py
+++ b/solution.py
@@ -51,17 +51,18 @@
     return [pltpu.with_memory_space_constraint(v, pltpu.HBM) for v in values]
 
 
-def pack_qkv_kernel(wq, wk, wv, pack_ref, sems):
-    part = pack_ref.shape[0]
+def pack_qkv_kernel(wq, wk, wv, all_ref, send_ref, sems):
+    part = send_ref.shape[0]
     width = wq.shape[1]
     mine = pl.ds(pl.multiple_of(lax.axis_index("grp") * part, part), part)
-    copies = []
+    first, rest = [], []
     for n, w in enumerate((wq, wk, wv)):
         at = slice(n * width, (n + 1) * width)
-        copies.append(pltpu.make_async_copy(w.at[mine, :], pack_ref.at[:, at], sems.at[n]))
-    for copy in copies:
+        first.append(pltpu.make_async_copy(w.at[mine, :], send_ref.at[:, at], sems.at[n]))
+        rest.append(pltpu.make_async_copy(w, all_ref.at[:, at], sems.at[3 + n]))
+    for copy in first + rest:
         copy.start()
-    for copy in copies:
+    for copy in first + rest:
         copy.wait()
 
 
@@ -69,10 +70,10 @@
     block, width = weights[0].shape
     return pl.pallas_call(
         pack_qkv_kernel,
-        out_shape=shape((block // 2, 3 * width)),
+        out_shape=(shape((block, 3 * width)), shape((block // 2, 3 * width))),
         in_specs=[HBM] * 3,
-        out_specs=VM,
-        scratch_shapes=[pltpu.SemaphoreType.DMA((3,))],
+        out_specs=[VM] * 2,
+        scratch_shapes=[pltpu.SemaphoreType.DMA((6,))],
         cost_estimate=cost(2_000_000, 400_000),
         compiler_params=params(),
         name="pack_qkv",
@@ -122,12 +123,13 @@
     )(*in_hbm(tokens, gain.reshape(1, features)))
 
 
-def pack_kernel(gv_hbm, gg_hbm, wa_hbm, gain_hbm, bias_hbm, glu_ref, out_ref, gain_ref, bias_ref, sems):
+def pack_kernel(gv_hbm, gg_hbm, wa_hbm, off_hbm, gain_hbm, bias_hbm, glu_ref, out_ref, off_ref, gain_ref, bias_ref, sems):
     cw, aw = gv_hbm.shape[1], wa_hbm.shape[0]
     copies = [
         pltpu.make_async_copy(gv_hbm, glu_ref.at[:, :cw], sems.at[0]),
         pltpu.make_async_copy(gg_hbm, glu_ref.at[:, cw:], sems.at[1]),
         pltpu.make_async_copy(wa_hbm, out_ref.at[:aw, :], sems.at[2]),
+        pltpu.make_async_copy(off_hbm, off_ref, sems.at[5]),
     ]
     small = [
         pltpu.make_async_copy(gain_hbm, gain_ref, sems.at[3]),
@@ -149,23 +151,23 @@
         copy.wait()
 
 
-def pack(gv, gg, wa, gain, bias):
+def pack(gv, gg, wa, off, gain, bias):
     block, cw = gv.shape
     aw, width = wa.shape
     return pl.pallas_call(
         pack_kernel,
-        out_shape=(shape((block, 2 * cw)), shape((aw + 16, width))),
-        in_specs=[HBM] * 5,
-        out_specs=[VM] * 2,
+        out_shape=(shape((block, 2 * cw)), shape((aw + 16, width)), shape(off.shape)),
+        in_specs=[HBM] * 6,
+        out_specs=[VM] * 3,
         scratch_shapes=[
             pltpu.VMEM((1, cw), F32),
             pltpu.VMEM((1, cw), F32),
-            pltpu.SemaphoreType.DMA((5,)),
+            pltpu.SemaphoreType.DMA((6,)),
         ],
         cost_estimate=cost(2_000_000, 2_000_000),
         compiler_params=params(),
         name="pack",
-    )(*in_hbm(gv, gg, wa, gain.reshape(1, cw), bias.reshape(1, cw)))
+    )(*in_hbm(gv, gg, wa, off, gain.reshape(1, cw), bias.reshape(1, cw)))
 
 
 def assemble_kernel(own_ref, pair_ref, got_ref, other_ref, own_out, pair_out):
@@ -204,33 +206,32 @@
     return dot_f32(near, same[...]) + dot_f32(rest, other[...])
 
 
-def qkv_kernel(x_own, x_pair, wq, wk, wv, same, other, off_ref, keep_ref, send_ref):
+def qkv_kernel(x_own, x_pair, own, same, other, off_ref, keep_ref, send_ref):
     rows = x_own.shape[0] // 2
-    width = wk.shape[1]
-    far = far_dot(x_pair, same, other)
-    for n, w in enumerate((wq, wk, wv)):
-        at = slice(n * width, (n + 1) * width)
-        part = dot_f32(x_own[...], w[...]) + far[:, at]
-        keep_ref[:, at] = part
+    width = send_ref.shape[1]
+    total = dot_f32(x_own[...], own[...]) + far_dot(x_pair, same, other)
+    keep_ref[...] = total
+    for n in range(3):
+        part = total[:, n * width : (n + 1) * width].astype(BF16)
         first = 4 * rows if n == 0 else 2 * (n - 1) * rows
-        send_ref[first : first + rows, :] = part[rows:].astype(BF16)
+        send_ref[first : first + rows, :] = part[rows:]
         if n > 0:
-            send_ref[first + rows : first + 2 * rows, :] = part[:rows].astype(BF16)
+            send_ref[first + rows : first + 2 * rows, :] = part[:rows]
     send_ref[5 * rows :, :] = jnp.zeros((send_ref.shape[0] - 5 * rows, width), BF16)
     send_ref[5 * rows : 5 * rows + off_ref.shape[0], :] = off_ref[...]
 
 
 def project_qkv(x_own, x_pair, own, same, other, off):
-    rows, width = x_own.shape[0], own[0].shape[1]
+    rows, width = x_own.shape[0], own.shape[1] // 3
     return pl.pallas_call(
         qkv_kernel,
         out_shape=(shape((rows, 3 * width), F32), shape((5 * rows // 2 + 16, width))),
-        in_specs=[VM] * 8,
+        in_specs=[VM] * 6,
         out_specs=[VM] * 2,
         cost_estimate=cost(200_000_000, 1_000_000),
         compiler_params=params(),
         name="project_qkv",
-    )(x_own, x_pair, *own, same, other, off)
+    )(x_own, x_pair, own, same, other, off)
 
 
 def sum_kernel(keep_ref, got_ref, sent_ref, after, q_ref, out_ref):
@@ -261,28 +262,24 @@
     )(keep, got, sent, after)
 
 
-def glu_kernel(x_own, x_pair, gv, gg, w_pair, after, keep_ref, send_ref):
+def glu_kernel(x_own, x_pair, own, pair, after, keep_ref, send_ref):
     rows = x_own.shape[0] // 2
-    cw = gv.shape[1]
-    far = dot_f32(x_pair[...], w_pair[...])
-    for n, w in enumerate((gv, gg)):
-        at = slice(n * cw, (n + 1) * cw)
-        part = dot_f32(x_own[...], w[...]) + far[:, at]
-        keep_ref[:, at] = part[:rows]
-        send_ref[:, at] = part[rows:].astype(BF16)
-
-
-def project_glu(x_own, x_pair, own, w_pair, after):
-    rows, width = x_own.shape[0] // 2, w_pair.shape[1]
+    total = dot_f32(x_own[...], own[...]) + dot_f32(x_pair[...], pair[...])
+    keep_ref[...] = total[:rows]
+    send_ref[...] = total[rows:].astype(BF16)
+
+
+def project_glu(x_own, x_pair, own, pair, after):
+    rows, width = x_own.shape[0] // 2, pair.shape[1]
     return pl.pallas_call(
         glu_kernel,
         out_shape=(shape((rows, width), F32), shape((rows, width))),
-        in_specs=[VM] * 5 + [ANY],
+        in_specs=[VM] * 4 + [ANY],
         out_specs=[VM] * 2,
         cost_estimate=cost(270_000_000, 1_500_000),
         compiler_params=params(),
         name="project_glu",
-    )(x_own, x_pair, *own, w_pair, after)
+    )(x_own, x_pair, own, pair, after)
 
 
 def gate_kernel(keep_ref, got_ref, gated_ref, tail_ref):
@@ -337,67 +334,120 @@
     )(gated, before, taps, attended)
 
 
-def attention_kernel(q_ref, mine_ref, pair_ref, gain_ref, after, out_ref, mass_ref, kv, acc, mass, carry):
+def suffix_matrix(keys):
+    before = lax.broadcasted_iota(jnp.int32, (2 * keys, 2 * keys), 0) % keys
+    column = lax.broadcasted_iota(jnp.int32, (2 * keys, 2 * keys), 1)
+    return jnp.where((column >= keys) | (before > column), 1.0, 0.0).astype(BF16)
+
+
+def stick_block(q, k, v, off, hd, suffix, carry, diagonal):
+    rows, width = q.shape
+    keys = k.shape[0]
+    lane = lax.broadcasted_iota(jnp.int32, (rows, width), 1) // hd
+    offsets = off.astype(F32)
+    weights, totals, values = [], [], []
+    for h in range(width // hd):
+        qh = jnp.where(lane == h, q, jnp.zeros_like(q))
+        s = dot_f32(qh, k, ((1,), (1,))) * hd ** (-0.5) + offsets[h : h + 1, :]
+        soft = jnp.maximum(s, 0.0) + jnp.log(1.0 + jnp.exp(-jnp.abs(s)))
+        log_not = -soft
+        if diagonal:
+            allowed = lax.broadcasted_iota(jnp.int32, (rows, keys), 1) <= lax.broadcasted_iota(
+                jnp.int32, (rows, keys), 0
+            )
+            log_not = jnp.where(allowed, log_not, 0.0)
+        high = log_not.astype(BF16)
+        low = (log_not - high.astype(F32)).astype(BF16)
+        sums = dot_f32(jnp.concatenate([high, low], axis=1), suffix)
+        later = sums[:, :keys]
+        if carry is not None:
+            later = later + carry[h]
+        w = jnp.exp(s - soft + later)
+        if diagonal:
+            w = jnp.where(allowed, w, 0.0)
+        weights.append(w)
+        totals.append(sums[:, keys:])
+        values.append(jnp.where(lane == h, v, jnp.zeros_like(v)))
+    mix = dot_f32(
+        jnp.concatenate([w.astype(BF16) for w in weights], axis=1), jnp.concatenate(values, axis=0)
+    )
+    return mix, weights, totals
+
+
+def near_kernel(q_ref, mine_ref, gain_ref, after, mix_ref, mass_ref, carry_ref):
+    rows = q_ref.shape[0]
+    heads, hd = gain_ref.shape
+    suffix = suffix_matrix(rows)
+    for n in range(2):
+        k = mine_ref[n * rows : (n + 1) * rows, :]
+        v = mine_ref[(2 + n) * rows : (3 + n) * rows, :]
+        off = mine_ref[4 * rows + 8 * n : 4 * rows + 8 * n + 8, :]
+        mix, weights, totals = stick_block(q_ref[...], k, v, off, hd, suffix, None, n == 0)
+        mix_ref[n] = mix
+        for h in range(heads):
+            mass_ref[n * heads + h] = weights[h]
+            carry_ref[n * heads + h] = totals[h]
+
+
+def near_attention(q, mine, head_gain, after):
+    rows, width = q.shape
+    heads = head_gain.shape[0]
+    return pl.pallas_call(
+        near_kernel,
+        out_shape=(
+            shape((2, rows, width), F32),
+            shape((2 * heads, rows, rows), F32),
+            shape((2 * heads, rows, rows), F32),
+        ),
+        in_specs=[VM] * 3 + [ANY],
+        out_specs=[VM] * 3,
+        cost_estimate=cost(200_000_000, 1_000_000),
+        compiler_params=params(),
+        name="near_attention",
+    )(q, mine, head_gain, after)
+
+
+def attention_kernel(q_ref, pair_ref, gain_ref, mix_ref, mass_ref, carry_ref, after, out_ref, log_ref, acc, mass, carry):
     me = lax.axis_index("sp")
     rows, width = q_ref.shape
     heads, hd = gain_ref.shape
     lane = lax.broadcasted_iota(jnp.int32, (rows, width), 1) // hd
-    keys = rows
-    for slot, (ref, n) in enumerate(((mine_ref, 0), (pair_ref, 0), (mine_ref, 1), (pair_ref, 1))):
-        kv[slot, :keys, :] = ref[n * keys : (n + 1) * keys, :]
-        kv[slot, keys : 2 * keys, :] = ref[(2 + n) * keys : (3 + n) * keys, :]
-        off = ref[4 * keys + 8 * n : 4 * keys + 8 * n + 8, :]
-        kv[slot, 2 * keys :, :] = jnp.concatenate([off, off])
-    before = lax.broadcasted_iota(jnp.int32, (2 * keys, 2 * keys), 0) % keys
-    column = lax.broadcasted_iota(jnp.int32, (2 * keys, 2 * keys), 1)
-    suffix = jnp.where((column >= keys) | (before > column), 1.0, 0.0).astype(BF16)
-    q = q_ref[...]
-    scale = hd ** (-0.5)
-
-    def block(slot, first):
-        k = kv[slot, :keys, :]
-        v = kv[slot, keys : 2 * keys, :]
-        off = kv[slot, 2 * keys :, :].astype(F32)
-        parts = []
-        for h in range(heads):
-            qh = jnp.where(lane == h, q, jnp.zeros_like(q))
-            s = dot_f32(qh, k, ((1,), (1,))) * scale + off[h : h + 1, :]
-            soft = jnp.maximum(s, 0.0) + jnp.log(1.0 + jnp.exp(-jnp.abs(s)))
-            if first:
-                allowed = lax.broadcasted_iota(jnp.int32, (rows, keys), 1) <= lax.broadcasted_iota(
-                    jnp.int32, (rows, keys), 0
-                )
-                log_not = jnp.where(allowed, -soft, 0.0)
-            else:
-                log_not = -soft
-            high = log_not.astype(BF16)
-            low = (log_not - high.astype(F32)).astype(BF16)
-            sums = dot_f32(jnp.concatenate([high, low], axis=1), suffix)
-            later, total = sums[:, :keys], sums[:, keys:]
-            if not first:
-                later = later + carry[h]
-            w = jnp.exp(s - soft + later)
-            if first:
-                w = jnp.where(allowed, w, 0.0)
-                mass[h] = w
-                carry[h] = total
-            else:
-                mass[h] = mass[h] + w
-                carry[h] = carry[h] + total
-            parts.append((w.astype(BF16), jnp.where(lane == h, v, jnp.zeros_like(v))))
-        mix = dot_f32(
-            jnp.concatenate([w for w, _ in parts], axis=1),
-            jnp.concatenate([v for _, v in parts], axis=0),
-        )
-        if first:
-            acc[...] = mix
-        else:
+    suffix = suffix_matrix(rows)
+    acc[...] = mix_ref[0]
+    for h in range(heads):
+        mass[h] = mass_ref[h]
+        carry[h] = carry_ref[h]
+
+    def earlier(t, _):
+        slot = jnp.bitwise_xor(me - t, me)
+
+        @pl.when(slot == 2)
+        def _():
+            scale = jnp.zeros_like(acc)
+            for h in range(heads):
+                left = jnp.exp(carry[h])
+                mass[h] = mass[h] + left * mass_ref[heads + h]
+                scale = jnp.where(lane == h, left, scale)
+                carry[h] = carry[h] + carry_ref[heads + h]
+            acc[...] = acc[...] + scale * mix_ref[1]
+
+        @pl.when(slot != 2)
+        def _():
+            n = slot // 2
+            k = pair_ref[pl.ds(pl.multiple_of(n * rows, rows), rows), :]
+            v = pair_ref[pl.ds(pl.multiple_of((2 + n) * rows, rows), rows), :]
+            off = jnp.where(
+                n == 0,
+                pair_ref[4 * rows : 4 * rows + 8, :].astype(F32),
+                pair_ref[4 * rows + 8 : 4 * rows + 16, :].astype(F32),
+            )
+            so_far = [carry[h] for h in range(heads)]
+            mix, weights, totals = stick_block(q_ref[...], k, v, off, hd, suffix, so_far, False)
             acc[...] = acc[...] + mix
-
-    block(0, True)
-
-    def earlier(t, _):
-        block(jnp.bitwise_xor(me - t, me), False)
+            for h in range(heads):
+                mass[h] = mass[h] + weights[h]
+                carry[h] = so_far[h] + totals[h]
+
         return 0
 
     lax.fori_loop(1, me + 1, earlier, 0)
@@ -410,19 +460,18 @@
     gain = jnp.concatenate([gain_ref[h : h + 1, :] for h in range(heads)], axis=1)
     out_ref[...] = (mixed * inverse * gain).astype(BF16)
     for h in range(heads):
-        mass_ref[h : h + 1, :] = jnp.log(jnp.sum(jnp.transpose(mass[h]), axis=0, keepdims=True))
-
-
-def attention(q, mine, pair, head_gain, after):
+        log_ref[h : h + 1, :] = jnp.log(jnp.sum(jnp.transpose(mass[h]), axis=0, keepdims=True))
+
+
+def attention(q, pair, head_gain, near, after):
     rows, width = q.shape
-    heads, _ = head_gain.shape
+    heads = head_gain.shape[0]
     return pl.pallas_call(
         attention_kernel,
         out_shape=(shape((rows, width)), shape((heads, rows), F32)),
-        in_specs=[VM] * 4 + [ANY],
+        in_specs=[VM] * 6 + [ANY],
         out_specs=[VM] * 2,
         scratch_shapes=[
-            pltpu.VMEM((4, 2 * rows + 16, width), BF16),
             pltpu.VMEM((rows, width), F32),
             pltpu.VMEM((heads, rows, rows), F32),
             pltpu.VMEM((heads, rows, rows), F32),
@@ -430,7 +479,7 @@
         cost_estimate=cost(400_000_000, 1_000_000),
         compiler_params=params(),
         name="stick_attention",
-    )(q, mine, pair, head_gain, after)
+    )(q, pair, head_gain, *near, after)
 
 
 def final_kernel(*refs):
@@ -486,13 +535,15 @@
     w_out_conv,
     out_gain,
 ):
-    own_qkv = (w_query, w_key, w_value)
-    qkv_same = exchange(pack_qkv(own_qkv), "sp", 1)
+    own_qkv, half_qkv = pack_qkv((w_query, w_key, w_value))
+    qkv_same = exchange(half_qkv, "sp", 1)
     wc_x = exchange(w_out_conv, "tp", 2)
     x_send, mine_own, mine_pair = norm_parts(tokens, norm_gain, w_query.shape[0])
     x_got = exchange(x_send, "sp", 2)
-    w_glu, wa_mine = pack(w_glu_value, w_glu_gate, w_out_attn, channel_gain, channel_bias)
-    glu_pair = exchange(w_glu, "sp", 1)
+    own_glu, wa_mine, off = pack(
+        w_glu_value, w_glu_gate, w_out_attn, key_offset.T, channel_gain, channel_bias
+    )
+    glu_pair = exchange(own_glu, "sp", 1)
     qkv_other = exchange(qkv_same, "grp", 1)
     x_other = exchange(x_got, "tp", 1)
     wa_x = exchange(wa_mine, "tp", 2)
@@ -502,16 +553,16 @@
     wa_xc = exchange(wa_x, "tp", 1)
     x_own, x_pair = assemble(mine_own, mine_pair, x_got, x_other)
 
-    keep, sent = project_qkv(x_own, x_pair, own_qkv, qkv_same, qkv_other, key_offset.T)
+    keep, sent = project_qkv(x_own, x_pair, own_qkv, qkv_same, qkv_other, off)
     got = exchange(sent, "sp", 2)
-    own_glu = (w_glu_value, w_glu_gate)
     glu_keep, glu_sent = project_glu(x_own, x_pair, own_glu, glu_pair, sent)
     glu_got = exchange(glu_sent, "sp", 2)
     q, mine_two = sum_qkv(keep, got, sent, glu_sent)
     pair_two = exchange(mine_two, "sp", 1)
+    near = near_attention(q, mine_two, head_gain, mine_two)
     gated, tail = gate(glu_keep, glu_got, -(-conv_taps.shape[0] // 16) * 16)
     before = from_behind(tail, "sp", 1)
-    attended, log_mass = attention(q, mine_two, pair_two, head_gain, tail)
+    attended, log_mass = attention(q, pair_two, head_gain, near, tail)
     act_mine = conv(gated, before, conv_taps, attended)
     act = [act_mine] + [exchange(act_mine, "tp", bit) for bit in (1, 2, 3)]
     wa = (wa_mine, wa_core, wa_x, wa_xc)

time: 78.4 us -> 76.9 us (0.981)
  waiting for transfers between devices: 50.3 us -> 48.6 us
    ppermute x17, waiting for transfers between devices: 50.1 us -> 48 us  [exchange(): return lax.ppermute(value, axis, [(s, s ^ bit) for s in range(count)])]
    pallas_call x1 -> x2, Pallas kernels: 0.93 us -> 1.9 us  [the longest x1 1.18 us: pack_qkv(): pl.pallas_call(pack_qkv_kernel, out_shape=(shape((block, 3 * width)), sha...]
  transfers between devices with their start and end apart: 18 -> 18, of which waited for: 10 -> 10; matrix products, arithmetic and copies ran while one was open for 0% -> 0% of each run, Pallas kernels for 8% -> 9%
where the time goes in v5:
time: 76.9 us; the launch traced here: 76.7 us
  waiting for transfers between devices  48.6 us (63%)
  starting transfers between devices  17.4 us (23%)
  Pallas kernels  9.25 us (12%)
    ppermute x17, waiting for transfers between devices, exchange(): return lax.ppermute(value, axis, [(s, s ^ bit) for s in range(count)])  48 us
    ppermute x17, starting transfers between devices, exchange(): return lax.ppermute(value, axis, [(s, s ^ bit) for s in range(count)])  15.5 us
    pallas_call x1, Pallas kernels, finish(): pl.pallas_call(final_kernel, out_shape=shape((rows, width)), in_specs=[VM...  2.41 us
    ppermute x1, starting transfers between devices, from_behind(): lax.ppermute(value, axis, [(source, source + steps) for source in range(i...  1.9 us
  transfers between devices with their start and end apart: 18, of which 10 were waited for; matrix products, arithmetic and copies ran while one was open for 0% of the time, Pallas kernels for 9%

profile of v5, /device:TPU:0, one launch (start us, length us, event | category | flops | bytes accessed | tf_op | source)
XLA Modules:
  0.0 76.7 jit_solution(8223547797720387302)
XLA Ops:
  0.6 3.0 %collective-permute-start.16 = (bf16[256,2048]{1,0:T(8,128)(2,1)}, bf16[256,2048]{1,0:T(8,128)(2,1)S(1)}, u32[]{:S(2)}, u32[]{:S(2)}) collective-permute-start(bf16[256,2048]{1,0:T(8,128)(2,1)} %refs_8_.1), channel_id=1, source_target_pairs={{0,2},{1,3},{2,0},{3,1},{4,6},{5,7},{6,4},{7,5},{8,10},{9,11},{10,... | collective-permute-start | bytes 3145736 | tf_op jit(solution)/shard_map/ppermute | solution.py:15
  3.7 1.2 %pack_qkv.1 = (bf16[512,384]{1,0:T(8,128)(2,1)S(1)}, bf16[256,384]{1,0:T(8,128)(2,1)S(1)}) custom-call(bf16[512,128]{1,0:T(8,128)(2,1)} %wq.1, bf16[512,128]{1,0:T(8,128)(2,1)} %wk.1, bf16[512,128]{1,0:T(8,128)(2,1)} %wv.1), custom_call_target="tpu_custom_call" | custom-call | flops 2000000 | bytes 400000 | tf_op jit(solution)/shard_map/pack_qkv/pallas_call | solution.py:71
  4.9 1.6 %collective-permute-start.3 = (bf16[256,384]{1,0:T(8,128)(2,1)S(1)}, bf16[256,384]{1,0:T(8,128)(2,1)S(1)}, u32[]{:S(2)}, u32[]{:S(2)}) collective-permute-start(bf16[256,384]{1,0:T(8,128)(2,1)S(1)} %get-tuple-element.32), channel_id=1, source_target_pairs={{0,4},{4,0},{8,12},{12,8},{1,5},{5,1},{9,13},{13,9},{2,6},{6,2},{1... | collective-permute-start | bytes 589832 | tf_op jit(solution)/shard_map/ppermute | solution.py:15
  6.5 1.3 %pack.1 = (bf16[512,512]{1,0:T(8,128)(2,1)S(1)}, bf16[144,2048]{1,0:T(8,128)(2,1)S(1)}, bf16[2,128]{1,0:T(2,128)(2,1)S(1)}) custom-call(bf16[512,256]{1,0:T(8,128)(2,1)} %gv_hbm.1, bf16[512,256]{1,0:T(8,128)(2,1)} %gg_hbm.1, bf16[128,2048]{1,0:T(8,128)(2,1)} %wa_hbm.1, bf16[2,128]{1,0:T(2,128)(2,1)} %bitcast.9, f32[1,256]{1,0:T(1,128)} %bitcast.7, ...), custom_call_target="tpu_custom_call" | custom-call | flops 2000000 | bytes 2000000 | tf_op jit(solution)/shard_map/pack/pallas_call | solution.py:157
  7.8 0.5 collective-permute-start.2
  8.3 1.3 %norm_parts.1 = (bf16[64,1024]{1,0:T(8,128)(2,1)S(1)}, bf16[128,512]{1,0:T(8,128)(2,1)S(1)}, bf16[128,512]{1,0:T(8,128)(2,1)S(1)}) custom-call(bf16[128,2048]{1,0:T(8,128)(2,1)} %x_hbm.1, f32[1,2048]{1,0:T(1,128)} %bitcast.6), custom_call_target="tpu_custom_call" | custom-call | flops 2000000 | bytes 1000000 | tf_op jit(solution)/shard_map/norm_parts/pallas_call | solution.py:109
  9.6 2.7 %collective-permute-start = (bf16[64,1024]{1,0:T(8,128)(2,1)S(1)}, bf16[64,1024]{1,0:T(8,128)(2,1)S(1)}, u32[]{:S(2)}, u32[]{:S(2)}) collective-permute-start(bf16[64,1024]{1,0:T(8,128)(2,1)S(1)} %get-tuple-element.27), channel_id=1, source_target_pairs={{0,8},{4,12},{8,0},{12,4},{1,9},{5,13},{9,1},{13,5},{2,10},{6,14},... | collective-permute-start | bytes 393224 | tf_op jit(solution)/shard_map/ppermute | solution.py:15
  12.3 0.5 collective-permute-start.13
  12.8 11.6 %collective-permute-done.got_ref = bf16[64,1024]{1,0:T(8,128)(2,1)S(1)} collective-permute-done((bf16[64,1024]{1,0:T(8,128)(2,1)S(1)}, bf16[64,1024]{1,0:T(8,128)(2,1)S(1)}, u32[]{:S(2)}, u32[]{:S(2)}) %collective-permute-start) | collective-permute-done | bytes 131104 | tf_op jit(solution)/shard_map/ppermute | solution.py:15
  24.4 3.5 %collective-permute-done.16.refs_10_ = bf16[256,2048]{1,0:T(8,128)(2,1)S(1)} collective-permute-done((bf16[256,2048]{1,0:T(8,128)(2,1)}, bf16[256,2048]{1,0:T(8,128)(2,1)S(1)}, u32[]{:S(2)}, u32[]{:S(2)}) %collective-permute-start.16) | collective-permute-done | bytes 1048608 | tf_op jit(solution)/shard_map/ppermute | solution.py:15
  27.9 0.5 collective-permute-start.1
  28.4 2.3 %collective-permute-done.1.other_ref = bf16[64,1024]{1,0:T(8,128)(2,1)S(1)} collective-permute-done((bf16[64,1024]{1,0:T(8,128)(2,1)S(1)}, bf16[64,1024]{1,0:T(8,128)(2,1)S(1)}, u32[]{:S(2)}, u32[]{:S(2)}) %collective-permute-start.1) | collective-permute-done | bytes 131104 | tf_op jit(solution)/shard_map/ppermute | solution.py:15
  30.7 2.0 %collective-permute-start.4 = (bf16[256,384]{1,0:T(8,128)(2,1)S(1)}, bf16[256,384]{1,0:T(8,128)(2,1)S(1)}, u32[]{:S(2)}, u32[]{:S(2)}) collective-permute-start(bf16[256,384]{1,0:T(8,128)(2,1)S(1)} %collective-permute-done.3.same), channel_id=1, source_target_pairs={{0,16},{16,0},{1,17},{17,1},{2,18},{18,2},{3,19},{19,3},{4,20},{20... | collective-permute-start | bytes 589832 | tf_op jit(solution)/shard_map/ppermute | solution.py:15
  32.8 5.2 %collective-permute-done.4.other = bf16[256,384]{1,0:T(8,128)(2,1)S(1)} collective-permute-done((bf16[256,384]{1,0:T(8,128)(2,1)S(1)}, bf16[256,384]{1,0:T(8,128)(2,1)S(1)}, u32[]{:S(2)}, u32[]{:S(2)}) %collective-permute-start.4) | collective-permute-done | bytes 196640 | tf_op jit(solution)/shard_map/ppermute | solution.py:15
  38.0 0.4 project_qkv.1
  38.4 2.9 %collective-permute-start.7 = (bf16[656,128]{1,0:T(8,128)(2,1)S(1)}, bf16[656,128]{1,0:T(8,128)(2,1)S(1)}, u32[]{:S(2)}, u32[]{:S(2)}) collective-permute-start(bf16[656,128]{1,0:T(8,128)(2,1)S(1)} %get-tuple-element.34.after.sent_ref), channel_id=1, source_target_pairs={{0,8},{4,12},{8,0},{12,4},{1,9},{5,13},{9,1},{13,5},{2,10},{6,14},... | collective-permute-start | bytes 503816 | tf_op jit(solution)/shard_map/ppermute | solution.py:15
  41.3 0.2 collective-permute-start.14
  41.5 0.4 project_glu.1
  42.0 7.9 %collective-permute-done.7.got_ref = bf16[656,128]{1,0:T(8,128)(2,1)S(1)} collective-permute-done((bf16[656,128]{1,0:T(8,128)(2,1)S(1)}, bf16[656,128]{1,0:T(8,128)(2,1)S(1)}, u32[]{:S(2)}, u32[]{:S(2)}) %collective-permute-start.7) | collective-permute-done | bytes 167968 | tf_op jit(solution)/shard_map/ppermute | solution.py:15
  49.9 8.9 %collective-permute-done.5.got_ref = bf16[128,512]{1,0:T(8,128)(2,1)S(1)} collective-permute-done((bf16[128,512]{1,0:T(8,128)(2,1)S(1)}, bf16[128,512]{1,0:T(8,128)(2,1)S(1)}, u32[]{:S(2)}, u32[]{:S(2)}) %collective-permute-start.5) | collective-permute-done | bytes 131104 | tf_op jit(solution)/shard_map/ppermute | solution.py:15
  58.8 0.7 copy-done.3
  59.5 0.7 near_attention.1
  60.2 0.1 gate.1
  60.3 3.5 %collective-permute-done.8.pair_ref = bf16[528,128]{1,0:T(8,128)(2,1)S(1)} collective-permute-done((bf16[528,128]{1,0:T(8,128)(2,1)S(1)}, bf16[528,128]{1,0:T(8,128)(2,1)S(1)}, u32[]{:S(2)}, u32[]{:S(2)}) %collective-permute-start.8) | collective-permute-done | bytes 135200 | tf_op jit(solution)/shard_map/ppermute | solution.py:15
  63.8 1.9 %collective-permute-start.6 = (bf16[32,256]{1,0:T(8,128)(2,1)S(1)}, bf16[32,256]{1,0:T(8,128)(2,1)S(1)}, u32[]{:S(2)}, u32[]{:S(2)}) collective-permute-start(bf16[32,256]{1,0:T(8,128)(2,1)S(1)} %get-tuple-element.38.after), channel_id=1, source_target_pairs={{0,4},{4,8},{8,12},{1,5},{5,9},{9,13},{2,6},{6,10},{10,14},{3,7},{... | collective-permute-start | bytes 49160 | tf_op jit(solution)/shard_map/ppermute | solution.py:21
  65.7 0.8 %stick_attention.1 = (bf16[128,128]{1,0:T(8,128)(2,1)S(1)}, f32[2,128]{1,0:T(2,128)}) custom-call(bf16[128,128]{1,0:T(8,128)(2,1)S(1)} %get-tuple-element.40.q_ref, bf16[528,128]{1,0:T(8,128)(2,1)S(1)} %collective-permute-done.8.pair_ref, f32[2,64]{1,0:T(2,128)S(1)} %copy-done.3, f32[2,128,128]{2,1,0:T(8,128)S(1)} %get-tuple-element.42.mix_ref, ...), custom_call_target="tpu_custom_call" | custom-call | flops 400000000 | bytes 1000000 | tf_op jit(solution)/shard_map/stick_attention/pallas_call | solution.py:469
  66.5 0.6 collective-permute-done.6.before_ref
  67.2 0.6 conv.1.refs_0_
  67.8 1.4 %collective-permute-start.10 = (bf16[128,384]{1,0:T(8,128)(2,1)S(1)}, bf16[128,384]{1,0:T(8,128)(2,1)S(1)}, u32[]{:S(2)}, u32[]{:S(2)}) collective-permute-start(bf16[128,384]{1,0:T(8,128)(2,1)S(1)} %conv.1.refs_0_), channel_id=1, source_target_pairs={{0,2},{1,3},{2,0},{3,1},{4,6},{5,7},{6,4},{7,5},{8,10},{9,11},{10,... | collective-permute-start | bytes 294920 | tf_op jit(solution)/shard_map/ppermute | solution.py:15
  69.2 3.5 %collective-permute-done.10.refs_2_ = bf16[128,384]{1,0:T(8,128)(2,1)S(1)} collective-permute-done((bf16[128,384]{1,0:T(8,128)(2,1)S(1)}, bf16[128,384]{1,0:T(8,128)(2,1)S(1)}, u32[]{:S(2)}, u32[]{:S(2)}) %collective-permute-start.10) | collective-permute-done | bytes 98336 | tf_op jit(solution)/shard_map/ppermute | solution.py:15
  72.7 1.6 %collective-permute-done.11.refs_3_ = bf16[128,384]{1,0:T(8,128)(2,1)S(1)} collective-permute-done((bf16[128,384]{1,0:T(8,128)(2,1)S(1)}, bf16[128,384]{1,0:T(8,128)(2,1)S(1)}, u32[]{:S(2)}, u32[]{:S(2)}) %collective-permute-start.11) | collective-permute-done | bytes 98336 | tf_op jit(solution)/shard_map/ppermute | solution.py:15
  74.3 2.4 %finish_rows.1 = bf16[128,2048]{1,0:T(8,128)(2,1)} custom-call(bf16[128,384]{1,0:T(8,128)(2,1)S(1)} %conv.1.refs_0_, bf16[128,384]{1,0:T(8,128)(2,1)S(1)} %collective-permute-done.9.refs_1_, bf16[128,384]{1,0:T(8,128)(2,1)S(1)} %collective-permute-done.10.refs_2_, bf16[128,384]{1,0:T(8,128)(2,1)S(1)} %collective-permute-done.11.refs_3_, ...), custom_call_target="tpu_custom_call" | custom-call | flops 800000000 | bytes 7000000 | tf_op jit(solution)/shard_map/finish_rows/pallas_call | solution.py:510
  (24 shorter events, 0.1 us)
Async XLA Ops:
  0.6 23.8 %copy-start = (bf16[256,2048]{1,0:T(8,128)(2,1)S(1)}, bf16[256,2048]{1,0:T(8,128)(2,1)}, u32[]{:S(2)}) copy-start(bf16[256,2048]{1,0:T(8,128)(2,1)} %refs_8_.1) | copy-start | bytes 3145732
  0.6 27.3 %collective-permute-start.16 = (bf16[256,2048]{1,0:T(8,128)(2,1)}, bf16[256,2048]{1,0:T(8,128)(2,1)S(1)}, u32[]{:S(2)}, u32[]{:S(2)}) collective-permute-start(bf16[256,2048]{1,0:T(8,128)(2,1)} %refs_8_.1), channel_id=1, source_target_pairs={{0,2},{1,3},{2,0},{3,1},{4,6},{5,7},{6,4},{7,5},{8,10},{9,11},{10,... | collective-permute-start | bytes 3145736 | tf_op jit(solution)/shard_map/ppermute | solution.py:15
  4.9 23.0 %collective-permute-start.3 = (bf16[256,384]{1,0:T(8,128)(2,1)S(1)}, bf16[256,384]{1,0:T(8,128)(2,1)S(1)}, u32[]{:S(2)}, u32[]{:S(2)}) collective-permute-start(bf16[256,384]{1,0:T(8,128)(2,1)S(1)} %get-tuple-element.32), channel_id=1, source_target_pairs={{0,4},{4,0},{8,12},{12,8},{1,5},{5,1},{9,13},{13,9},{2,6},{6,2},{1... | collective-permute-start | bytes 589832 | tf_op jit(solution)/shard_map/ppermute | solution.py:15
  7.8 30.6 %collective-permute-start.2 = (bf16[512,512]{1,0:T(8,128)(2,1)S(1)}, bf16[512,512]{1,0:T(8,128)(2,1)S(1)}, u32[]{:S(2)}, u32[]{:S(2)}) collective-permute-start(bf16[512,512]{1,0:T(8,128)(2,1)S(1)} %get-tuple-element.30.own), channel_id=1, source_target_pairs={{0,4},{4,0},{8,12},{12,8},{1,5},{5,1},{9,13},{13,9},{2,6},{6,2},{1... | collective-permute-start | bytes 1572872 | tf_op jit(solution)/shard_map/ppermute | solution.py:15
  9.6 14.8 %collective-permute-start = (bf16[64,1024]{1,0:T(8,128)(2,1)S(1)}, bf16[64,1024]{1,0:T(8,128)(2,1)S(1)}, u32[]{:S(2)}, u32[]{:S(2)}) collective-permute-start(bf16[64,1024]{1,0:T(8,128)(2,1)S(1)} %get-tuple-element.27), channel_id=1, source_target_pairs={{0,8},{4,12},{8,0},{12,4},{1,9},{5,13},{9,1},{13,5},{2,10},{6,14},... | collective-permute-start | bytes 393224 | tf_op jit(solution)/shard_map/ppermute | solution.py:15
  12.3 29.0 %collective-permute-start.13 = (bf16[144,2048]{1,0:T(8,128)(2,1)S(1)}, bf16[144,2048]{1,0:T(8,128)(2,1)S(1)}, u32[]{:S(2)}, u32[]{:S(2)}) collective-permute-start(bf16[144,2048]{1,0:T(8,128)(2,1)S(1)} %get-tuple-element.46.refs_4_), channel_id=1, source_target_pairs={{0,2},{1,3},{2,0},{3,1},{4,6},{5,7},{6,4},{7,5},{8,10},{9,11},{10,... | collective-permute-start | bytes 1769480 | tf_op jit(solution)/shard_map/ppermute | solution.py:15
  24.4 49.9 %collective-permute-start.15 = (bf16[256,2048]{1,0:T(8,128)(2,1)S(1)}, bf16[256,2048]{1,0:T(8,128)(2,1)S(1)}, u32[]{:S(2)}, u32[]{:S(2)}) collective-permute-start(bf16[256,2048]{1,0:T(8,128)(2,1)S(1)} %copy-done), channel_id=1, source_target_pairs={{0,1},{1,0},{2,3},{3,2},{4,5},{5,4},{6,7},{7,6},{8,9},{9,8},{10,11... | collective-permute-start | bytes 3145736 | tf_op jit(solution)/shard_map/ppermute | solution.py:15
  27.9 46.4 %collective-permute-start.17 = (bf16[256,2048]{1,0:T(8,128)(2,1)S(1)}, bf16[256,2048]{1,0:T(8,128)(2,1)S(1)}, u32[]{:S(2)}, u32[]{:S(2)}) collective-permute-start(bf16[256,2048]{1,0:T(8,128)(2,1)S(1)} %collective-permute-done.16.refs_10_), channel_id=1, source_target_pairs={{0,1},{1,0},{2,3},{3,2},{4,5},{5,4},{6,7},{7,6},{8,9},{9,8},{10,11... | collective-permute-start | bytes 3145736 | tf_op jit(solution)/shard_map/ppermute | solution.py:15
  27.9 2.8 %collective-permute-start.1 = (bf16[64,1024]{1,0:T(8,128)(2,1)S(1)}, bf16[64,1024]{1,0:T(8,128)(2,1)S(1)}, u32[]{:S(2)}, u32[]{:S(2)}) collective-permute-start(bf16[64,1024]{1,0:T(8,128)(2,1)S(1)} %collective-permute-done.got_ref), channel_id=1, source_target_pairs={{0,1},{1,0},{2,3},{3,2},{4,5},{5,4},{6,7},{7,6},{8,9},{9,8},{10,11... | collective-permute-start | bytes 393224 | tf_op jit(solution)/shard_map/ppermute | solution.py:15
  30.7 7.2 %collective-permute-start.4 = (bf16[256,384]{1,0:T(8,128)(2,1)S(1)}, bf16[256,384]{1,0:T(8,128)(2,1)S(1)}, u32[]{:S(2)}, u32[]{:S(2)}) collective-permute-start(bf16[256,384]{1,0:T(8,128)(2,1)S(1)} %collective-permute-done.3.same), channel_id=1, source_target_pairs={{0,16},{16,0},{1,17},{17,1},{2,18},{18,2},{3,19},{19,3},{4,20},{20... | collective-permute-start | bytes 589832 | tf_op jit(solution)/shard_map/ppermute | solution.py:15
  38.0 31.2 %collective-permute-start.12 = (bf16[144,2048]{1,0:T(8,128)(2,1)S(1)}, bf16[144,2048]{1,0:T(8,128)(2,1)S(1)}, u32[]{:S(2)}, u32[]{:S(2)}) collective-permute-start(bf16[144,2048]{1,0:T(8,128)(2,1)S(1)} %get-tuple-element.46.refs_4_), channel_id=1, source_target_pairs={{0,1},{1,0},{2,3},{3,2},{4,5},{5,4},{6,7},{7,6},{8,9},{9,8},{10,11... | collective-permute-start | bytes 1769480 | tf_op jit(solution)/shard_map/ppermute | solution.py:15
  38.4 11.4 %collective-permute-start.7 = (bf16[656,128]{1,0:T(8,128)(2,1)S(1)}, bf16[656,128]{1,0:T(8,128)(2,1)S(1)}, u32[]{:S(2)}, u32[]{:S(2)}) collective-permute-start(bf16[656,128]{1,0:T(8,128)(2,1)S(1)} %get-tuple-element.34.after.sent_ref), channel_id=1, source_target_pairs={{0,8},{4,12},{8,0},{12,4},{1,9},{5,13},{9,1},{13,5},{2,10},{6,14},... | collective-permute-start | bytes 503816 | tf_op jit(solution)/shard_map/ppermute | solution.py:15
  41.3 33.0 %collective-permute-start.14 = (bf16[144,2048]{1,0:T(8,128)(2,1)S(1)}, bf16[144,2048]{1,0:T(8,128)(2,1)S(1)}, u32[]{:S(2)}, u32[]{:S(2)}) collective-permute-start(bf16[144,2048]{1,0:T(8,128)(2,1)S(1)} %collective-permute-done.13.refs_6_), channel_id=1, source_target_pairs={{0,1},{1,0},{2,3},{3,2},{4,5},{5,4},{6,7},{7,6},{8,9},{9,8},{10,11... | collective-permute-start | bytes 1769480 | tf_op jit(solution)/shard_map/ppermute | solution.py:15
  49.9 8.9 %collective-permute-start.5 = (bf16[128,512]{1,0:T(8,128)(2,1)S(1)}, bf16[128,512]{1,0:T(8,128)(2,1)S(1)}, u32[]{:S(2)}, u32[]{:S(2)}) collective-permute-start(bf16[128,512]{1,0:T(8,128)(2,1)S(1)} %get-tuple-element.36.after), channel_id=1, source_target_pairs={{0,8},{4,12},{8,0},{12,4},{1,9},{5,13},{9,1},{13,5},{2,10},{6,14},... | collective-permute-start | bytes 393224 | tf_op jit(solution)/shard_map/ppermute | solution.py:15
  58.8 0.7 copy-start.3
  58.8 5.0 %collective-permute-start.8 = (bf16[528,128]{1,0:T(8,128)(2,1)S(1)}, bf16[528,128]{1,0:T(8,128)(2,1)S(1)}, u32[]{:S(2)}, u32[]{:S(2)}) collective-permute-start(bf16[528,128]{1,0:T(8,128)(2,1)S(1)} %get-tuple-element.41.mine_ref.after), channel_id=1, source_target_pairs={{0,4},{4,0},{8,12},{12,8},{1,5},{5,1},{9,13},{13,9},{2,6},{6,2},{1... | collective-permute-start | bytes 405512 | tf_op jit(solution)/shard_map/ppermute | solution.py:15
  63.8 3.3 %collective-permute-start.6 = (bf16[32,256]{1,0:T(8,128)(2,1)S(1)}, bf16[32,256]{1,0:T(8,128)(2,1)S(1)}, u32[]{:S(2)}, u32[]{:S(2)}) collective-permute-start(bf16[32,256]{1,0:T(8,128)(2,1)S(1)} %get-tuple-element.38.after), channel_id=1, source_target_pairs={{0,4},{4,8},{8,12},{1,5},{5,9},{9,13},{2,6},{6,10},{10,14},{3,7},{... | collective-permute-start | bytes 49160 | tf_op jit(solution)/shard_map/ppermute | solution.py:21
  65.7 1.4 %copy-start.1 = (f32[31,256]{1,0:T(8,128)S(1)}, f32[31,256]{1,0:T(8,128)}, u32[]{:S(2)}) copy-start(f32[31,256]{1,0:T(8,128)} %taps_ref.1) | copy-start | bytes 95236
  67.1 7.2 %copy-start.2 = (f32[2048]{0:T(1024)S(1)}, f32[2048]{0:T(1024)}, u32[]{:S(2)}) copy-start(f32[2048]{0:T(1024)} %param.29) | copy-start | bytes 24580
  67.8 4.9 %collective-permute-start.10 = (bf16[128,384]{1,0:T(8,128)(2,1)S(1)}, bf16[128,384]{1,0:T(8,128)(2,1)S(1)}, u32[]{:S(2)}, u32[]{:S(2)}) collective-permute-start(bf16[128,384]{1,0:T(8,128)(2,1)S(1)} %conv.1.refs_0_), channel_id=1, source_target_pairs={{0,2},{1,3},{2,0},{3,1},{4,6},{5,7},{6,4},{7,5},{8,10},{9,11},{10,... | collective-permute-start | bytes 294920 | tf_op jit(solution)/shard_map/ppermute | solution.py:15
  69.2 5.1 %collective-permute-start.11 = (bf16[128,384]{1,0:T(8,128)(2,1)S(1)}, bf16[128,384]{1,0:T(8,128)(2,1)S(1)}, u32[]{:S(2)}, u32[]{:S(2)}) collective-permute-start(bf16[128,384]{1,0:T(8,128)(2,1)S(1)} %conv.1.refs_0_), channel_id=1, source_target_pairs={{0,3},{1,2},{2,1},{3,0},{4,7},{5,6},{6,5},{7,4},{8,11},{9,10},{10,... | collective-permute-start | bytes 294920 | tf_op jit(solution)/shard_map/ppermute | solution.py:15
  72.7 1.6 %collective-permute-start.9 = (bf16[128,384]{1,0:T(8,128)(2,1)S(1)}, bf16[128,384]{1,0:T(8,128)(2,1)S(1)}, u32[]{:S(2)}, u32[]{:S(2)}) collective-permute-start(bf16[128,384]{1,0:T(8,128)(2,1)S(1)} %conv.1.refs_0_), channel_id=1, source_target_pairs={{0,1},{1,0},{2,3},{3,2},{4,5},{5,4},{6,7},{7,6},{8,9},{9,8},{10,11... | collective-permute-start | bytes 294920 | tf_op jit(solution)/shard_map/ppermute | solution.py:15

commit v6 on v5

--- a/solution.py
+++ b/solution.py
@@ -51,33 +51,40 @@
     return [pltpu.with_memory_space_constraint(v, pltpu.HBM) for v in values]
 
 
-def pack_qkv_kernel(wq, wk, wv, all_ref, send_ref, sems):
-    part = send_ref.shape[0]
-    width = wq.shape[1]
-    mine = pl.ds(pl.multiple_of(lax.axis_index("grp") * part, part), part)
+def pack_qkv_kernel(wq, wk, wv, wc, all_ref, send_ref, wc_ref, sems):
+    part, width = send_ref.shape[0], wq.shape[1]
+    group = lax.axis_index("grp")
+    mine = pl.ds(pl.multiple_of(group * part, part), part)
+    columns = wc_ref.shape[1]
     first, rest = [], []
     for n, w in enumerate((wq, wk, wv)):
         at = slice(n * width, (n + 1) * width)
         first.append(pltpu.make_async_copy(w.at[mine, :], send_ref.at[:, at], sems.at[n]))
         rest.append(pltpu.make_async_copy(w, all_ref.at[:, at], sems.at[3 + n]))
+    half = wc.at[:, pl.ds(pl.multiple_of(group * columns, columns), columns)]
+    rest.append(pltpu.make_async_copy(half, wc_ref, sems.at[6]))
     for copy in first + rest:
         copy.start()
     for copy in first + rest:
         copy.wait()
 
 
-def pack_qkv(weights):
+def pack_qkv(weights, wc):
     block, width = weights[0].shape
     return pl.pallas_call(
         pack_qkv_kernel,
-        out_shape=(shape((block, 3 * width)), shape((block // 2, 3 * width))),
-        in_specs=[HBM] * 3,
-        out_specs=[VM] * 2,
-        scratch_shapes=[pltpu.SemaphoreType.DMA((6,))],
+        out_shape=(
+            shape((block, 3 * width)),
+            shape((block // 2, 3 * width)),
+            shape((wc.shape[0], wc.shape[1] // 2)),
+        ),
+        in_specs=[HBM] * 4,
+        out_specs=[VM] * 3,
+        scratch_shapes=[pltpu.SemaphoreType.DMA((7,))],
         cost_estimate=cost(2_000_000, 400_000),
         compiler_params=params(),
         name="pack_qkv",
-    )(*in_hbm(*weights))
+    )(*in_hbm(*weights, wc))
 
 
 def norm_kernel(x_hbm, gain_hbm, send_ref, own_ref, pair_ref, x_ref, gain_ref, normed, sems):
@@ -123,21 +130,25 @@
     )(*in_hbm(tokens, gain.reshape(1, features)))
 
 
-def pack_kernel(gv_hbm, gg_hbm, wa_hbm, off_hbm, gain_hbm, bias_hbm, glu_ref, out_ref, off_ref, gain_ref, bias_ref, sems):
+def pack_kernel(
+    gv_hbm, gg_hbm, wa_hbm, off_hbm, gain_hbm, bias_hbm, gv_ref, gv_send, gg_ref, out_ref, off_ref, gain_ref, bias_ref, sems
+):
     cw, aw = gv_hbm.shape[1], wa_hbm.shape[0]
-    copies = [
-        pltpu.make_async_copy(gv_hbm, glu_ref.at[:, :cw], sems.at[0]),
-        pltpu.make_async_copy(gg_hbm, glu_ref.at[:, cw:], sems.at[1]),
-        pltpu.make_async_copy(wa_hbm, out_ref.at[:aw, :], sems.at[2]),
-        pltpu.make_async_copy(off_hbm, off_ref, sems.at[5]),
-    ]
-    small = [
-        pltpu.make_async_copy(gain_hbm, gain_ref, sems.at[3]),
-        pltpu.make_async_copy(bias_hbm, bias_ref, sems.at[4]),
-    ]
-    for copy in small + copies:
+    part = gv_send.shape[0]
+    mine = pl.ds(pl.multiple_of(lax.axis_index("grp") * part, part), part)
+    pairs = (
+        (gain_hbm, gain_ref),
+        (bias_hbm, bias_ref),
+        (gv_hbm.at[mine, :], gv_send),
+        (gg_hbm, gg_ref),
+        (wa_hbm, out_ref.at[:aw, :]),
+        (off_hbm, off_ref),
+        (gv_hbm, gv_ref),
+    )
+    copies = [pltpu.make_async_copy(a, b, sems.at[n]) for n, (a, b) in enumerate(pairs)]
+    for copy in copies:
         copy.start()
-    for copy in small:
+    for copy in copies[:2]:
         copy.wait()
     extra = out_ref.shape[0] - aw
     for n, ref in enumerate((gain_ref, bias_ref)):
@@ -147,7 +158,7 @@
             rest = rest - part.astype(F32)
             first = (3 * n + piece) * cw
             out_ref[aw:, first : first + cw] = jnp.broadcast_to(part, (extra, cw))
-    for copy in copies:
+    for copy in copies[2:]:
         copy.wait()
 
 
@@ -156,13 +167,19 @@
     aw, width = wa.shape
     return pl.pallas_call(
         pack_kernel,
-        out_shape=(shape((block, 2 * cw)), shape((aw + 16, width)), shape(off.shape)),
+        out_shape=(
+            shape((block, cw)),
+            shape((block // 2, cw)),
+            shape((block, cw)),
+            shape((aw + 16, width)),
+            shape(off.shape),
+        ),
         in_specs=[HBM] * 6,
-        out_specs=[VM] * 3,
+        out_specs=[VM] * 5,
         scratch_shapes=[
             pltpu.VMEM((1, cw), F32),
             pltpu.VMEM((1, cw), F32),
-            pltpu.SemaphoreType.DMA((6,)),
+            pltpu.SemaphoreType.DMA((7,)),
         ],
         cost_estimate=cost(2_000_000, 2_000_000),
         compiler_params=params(),
@@ -206,26 +223,39 @@
     return dot_f32(near, same[...]) + dot_f32(rest, other[...])
 
 
+def pick(second, a, b):
+    return jnp.where(second == 1, b, a)
+
+
 def qkv_kernel(x_own, x_pair, own, same, other, off_ref, keep_ref, send_ref):
     rows = x_own.shape[0] // 2
     width = send_ref.shape[1]
+    hd = width // 2
+    side = lax.axis_index("sp") // 2
     total = dot_f32(x_own[...], own[...]) + far_dot(x_pair, same, other)
-    keep_ref[...] = total
-    for n in range(3):
-        part = total[:, n * width : (n + 1) * width].astype(BF16)
-        first = 4 * rows if n == 0 else 2 * (n - 1) * rows
-        send_ref[first : first + rows, :] = part[rows:]
-        if n > 0:
-            send_ref[first + rows : first + 2 * rows, :] = part[:rows]
-    send_ref[5 * rows :, :] = jnp.zeros((send_ref.shape[0] - 5 * rows, width), BF16)
-    send_ref[5 * rows : 5 * rows + off_ref.shape[0], :] = off_ref[...]
+    q, k, v = (total[:, n * width : (n + 1) * width] for n in range(3))
+    heads = [slice(0, hd), slice(hd, width)]
+    kvs = [jnp.concatenate([k[:, at], v[:, at]], axis=1) for at in heads]
+    ordered = [jnp.concatenate([q[:rows, at], q[rows:, at]], axis=1) for at in heads]
+    swapped = [jnp.concatenate([q[rows:, at], q[:rows, at]], axis=1) for at in heads]
+    mine = pick(side, kvs[0], kvs[1])
+    theirs = pick(side, kvs[1], kvs[0]).astype(BF16)
+    for n, block in enumerate((side, 1 - side)):
+        at = pl.ds(pl.multiple_of(block * rows, rows), rows)
+        keep_ref[at, :] = mine[n * rows : (n + 1) * rows]
+        send_ref[at, :] = theirs[n * rows : (n + 1) * rows]
+    keep_ref[2 * rows :, :] = pick(side, ordered[0], swapped[1])
+    send_ref[2 * rows : 3 * rows, :] = pick(side, ordered[1], swapped[0]).astype(BF16)
+    offsets = off_ref[...].astype(F32)
+    off = pick(side, offsets[1:2], offsets[0:1]).astype(BF16)
+    send_ref[3 * rows :, :] = jnp.broadcast_to(off, (send_ref.shape[0] - 3 * rows, width))
 
 
 def project_qkv(x_own, x_pair, own, same, other, off):
-    rows, width = x_own.shape[0], own.shape[1] // 3
+    rows, width = x_own.shape[0] // 2, own.shape[1] // 3
     return pl.pallas_call(
         qkv_kernel,
-        out_shape=(shape((rows, 3 * width), F32), shape((5 * rows // 2 + 16, width))),
+        out_shape=(shape((3 * rows, width), F32), shape((3 * rows + 16, width))),
         in_specs=[VM] * 6,
         out_specs=[VM] * 2,
         cost_estimate=cost(200_000_000, 1_000_000),
@@ -234,81 +264,86 @@
     )(x_own, x_pair, own, same, other, off)
 
 
-def sum_kernel(keep_ref, got_ref, sent_ref, after, q_ref, out_ref):
-    rows, width = q_ref.shape
-
-    def got(n):
-        return got_ref[n * rows : (n + 1) * rows, :].astype(F32)
-
-    q_ref[...] = (keep_ref[:rows, :width] + got(4)).astype(BF16)
-    for n in range(4):
-        at = slice((1 + n // 2) * width, (2 + n // 2) * width)
-        part = keep_ref[(n % 2) * rows : (n % 2 + 1) * rows, at]
-        out_ref[n * rows : (n + 1) * rows, :] = (part + got(n)).astype(BF16)
-    first = 5 * rows
-    out_ref[4 * rows :, :] = jnp.concatenate([sent_ref[first : first + 8, :], got_ref[first : first + 8, :]])
-
-
-def sum_qkv(keep, got, sent, after):
-    rows, width = keep.shape[0] // 2, got.shape[1]
+def sum_kernel(keep_ref, got_ref, off_ref, after, q_ref, kv_ref):
+    rows, width = keep_ref.shape[0] // 3, keep_ref.shape[1]
+    hd = width // 2
+    side = lax.axis_index("sp") // 2
+    kv_ref[: 2 * rows, :] = (keep_ref[: 2 * rows, :] + got_ref[: 2 * rows, :].astype(F32)).astype(BF16)
+    q = keep_ref[2 * rows :, :] + got_ref[2 * rows : 3 * rows, :].astype(F32)
+    none = jnp.zeros((rows, hd), F32)
+    q_ref[:rows, :] = jnp.concatenate([q[:, :hd], none], axis=1).astype(BF16)
+    q_ref[rows:, :] = jnp.concatenate([q[:, hd:], none], axis=1).astype(BF16)
+    offsets = off_ref[...].astype(F32)
+    mine = jnp.broadcast_to(pick(side, offsets[0:1], offsets[1:2]), (8, width))
+    theirs = got_ref[3 * rows : 3 * rows + 8, :].astype(F32)
+    both = jnp.concatenate([pick(side, mine, theirs), pick(side, theirs, mine)])
+    kv_ref[2 * rows :, :] = both.astype(BF16)
+
+
+def sum_qkv(keep, got, off, after):
+    rows, width = keep.shape[0] // 3, got.shape[1]
     return pl.pallas_call(
         sum_kernel,
-        out_shape=(shape((rows, width)), shape((4 * rows + 16, width))),
+        out_shape=(shape((2 * rows, width)), shape((2 * rows + 16, width))),
         in_specs=[VM] * 3 + [ANY],
         out_specs=[VM] * 2,
         cost_estimate=cost(1_000_000, 1_000_000),
         compiler_params=params(),
         name="sum_qkv",
-    )(keep, got, sent, after)
-
-
-def glu_kernel(x_own, x_pair, own, pair, after, keep_ref, send_ref):
+    )(keep, got, off, after)
+
+
+def glu_kernel(x_own, x_pair, gv, gg, gv_same, gv_other, gg_pair, after, keep_ref, send_ref):
     rows = x_own.shape[0] // 2
-    total = dot_f32(x_own[...], own[...]) + dot_f32(x_pair[...], pair[...])
-    keep_ref[...] = total[:rows]
-    send_ref[...] = total[rows:].astype(BF16)
+    cw = gv.shape[1]
+    for n in range(2):
+        own = (gv, gg)[n]
+        far = far_dot(x_pair, gv_same, gv_other) if n == 0 else dot_f32(x_pair[...], gg_pair[...])
+        total = dot_f32(x_own[...], own[...]) + far
+        at = slice(n * cw, (n + 1) * cw)
+        keep_ref[:, at] = total[:rows]
+        send_ref[:, at] = total[rows:].astype(BF16)
 
 
 def project_glu(x_own, x_pair, own, pair, after):
-    rows, width = x_own.shape[0] // 2, pair.shape[1]
+    rows, width = x_own.shape[0] // 2, 2 * own[0].shape[1]
     return pl.pallas_call(
         glu_kernel,
         out_shape=(shape((rows, width), F32), shape((rows, width))),
-        in_specs=[VM] * 4 + [ANY],
+        in_specs=[VM] * 7 + [ANY],
         out_specs=[VM] * 2,
-        cost_estimate=cost(270_000_000, 1_500_000),
+        cost_estimate=cost(270_000_000, 1_000_000),
         compiler_params=params(),
         name="project_glu",
-    )(x_own, x_pair, own, pair, after)
-
-
-def gate_kernel(keep_ref, got_ref, gated_ref, tail_ref):
+    )(x_own, x_pair, *own, *pair, after)
+
+
+def gate_kernel(keep_ref, got_ref, after, gated_ref, tail_ref):
     rows, cw = gated_ref.shape
     glu = keep_ref[...] + got_ref[...].astype(F32)
     value = glu[:, :cw].astype(BF16).astype(F32)
-    gate = glu[:, cw:].astype(BF16).astype(F32)
-    gated = (value * jax.nn.sigmoid(gate)).astype(BF16)
+    gated = (value * jax.nn.sigmoid(glu[:, cw:].astype(BF16).astype(F32))).astype(BF16)
     gated_ref[...] = gated
     tail_ref[...] = gated[rows - tail_ref.shape[0] :]
 
 
-def gate(keep, got, tail):
+def gate(keep, got, tail, after):
     rows, cw = keep.shape[0], keep.shape[1] // 2
     return pl.pallas_call(
         gate_kernel,
         out_shape=(shape((rows, cw)), shape((tail, cw))),
-        in_specs=[VM] * 2,
+        in_specs=[VM] * 2 + [ANY],
         out_specs=[VM] * 2,
         cost_estimate=cost(2_000_000, 500_000),
         compiler_params=params(),
         name="gate",
-    )(keep, got)
-
-
-def conv_kernel(gated_ref, before_ref, taps_ref, att_ref, act_ref, padded):
+    )(keep, got, after)
+
+
+def conv_kernel(gated_ref, before_ref, taps_ref, att_ref, got_ref, own_log, act_ref, log_ref, padded):
     rows, aw = att_ref.shape
-    tail = before_ref.shape[0]
-    taps = taps_ref.shape[0]
+    tail, taps, hd = before_ref.shape[0], taps_ref.shape[0], aw // 2
+    side = lax.axis_index("sp") // 2
     padded[:tail, :] = before_ref[...].astype(F32)
     padded[tail:, :] = gated_ref[...].astype(F32)
     total = None
@@ -316,22 +351,32 @@
         first = tail - (taps - 1) + tap
         part = taps_ref[tap : tap + 1, :] * padded[first : first + rows, :]
         total = part if total is None else total + part
-    act_ref[:, :aw] = att_ref[...]
     act_ref[:, aw:] = total.astype(BF16)
-
-
-def conv(gated, before, taps, attended):
+    half = rows // 2
+    both = got_ref[:half, :].astype(F32)
+    theirs = jnp.concatenate([both[:, :hd], both[:, hd:]], axis=0)
+    none = jnp.zeros_like(theirs)
+    placed = pick(side, jnp.concatenate([none, theirs], axis=1), jnp.concatenate([theirs, none], axis=1))
+    act_ref[:, :aw] = (att_ref[...].astype(F32) + placed).astype(BF16)
+    pieces = [got_ref[half + 16 * n : half + 16 * n + 1, :].astype(F32) for n in range(3)]
+    far_log = pieces[0] + pieces[1] + pieces[2]
+    near_log = own_log[0:1, :]
+    log_ref[0:1, :] = pick(side, near_log, far_log)
+    log_ref[1:2, :] = pick(side, far_log, near_log)
+
+
+def conv(gated, before, taps, attended, att_got, own_log):
     rows, cw = gated.shape
     return pl.pallas_call(
         conv_kernel,
-        out_shape=shape((rows, attended.shape[1] + cw)),
-        in_specs=[VM] * 4,
-        out_specs=VM,
+        out_shape=(shape((rows, attended.shape[1] + cw)), shape((2, rows), F32)),
+        in_specs=[VM] * 6,
+        out_specs=[VM] * 2,
         scratch_shapes=[pltpu.VMEM((rows + before.shape[0], cw), F32)],
         cost_estimate=cost(20_000_000, 500_000),
         compiler_params=params(),
         name="conv",
-    )(gated, before, taps, attended)
+    )(gated, before, taps, attended, att_got, own_log)
 
 
 def suffix_matrix(keys):
@@ -340,141 +385,124 @@
     return jnp.where((column >= keys) | (before > column), 1.0, 0.0).astype(BF16)
 
 
-def stick_block(q, k, v, off, hd, suffix, carry, diagonal):
-    rows, width = q.shape
-    keys = k.shape[0]
-    lane = lax.broadcasted_iota(jnp.int32, (rows, width), 1) // hd
-    offsets = off.astype(F32)
-    weights, totals, values = [], [], []
-    for h in range(width // hd):
-        qh = jnp.where(lane == h, q, jnp.zeros_like(q))
-        s = dot_f32(qh, k, ((1,), (1,))) * hd ** (-0.5) + offsets[h : h + 1, :]
-        soft = jnp.maximum(s, 0.0) + jnp.log(1.0 + jnp.exp(-jnp.abs(s)))
-        log_not = -soft
-        if diagonal:
-            allowed = lax.broadcasted_iota(jnp.int32, (rows, keys), 1) <= lax.broadcasted_iota(
-                jnp.int32, (rows, keys), 0
-            )
-            log_not = jnp.where(allowed, log_not, 0.0)
-        high = log_not.astype(BF16)
-        low = (log_not - high.astype(F32)).astype(BF16)
-        sums = dot_f32(jnp.concatenate([high, low], axis=1), suffix)
-        later = sums[:, :keys]
-        if carry is not None:
-            later = later + carry[h]
-        w = jnp.exp(s - soft + later)
-        if diagonal:
-            w = jnp.where(allowed, w, 0.0)
-        weights.append(w)
-        totals.append(sums[:, keys:])
-        values.append(jnp.where(lane == h, v, jnp.zeros_like(v)))
-    mix = dot_f32(
-        jnp.concatenate([w.astype(BF16) for w in weights], axis=1), jnp.concatenate(values, axis=0)
-    )
-    return mix, weights, totals
-
-
-def near_kernel(q_ref, mine_ref, gain_ref, after, mix_ref, mass_ref, carry_ref):
-    rows = q_ref.shape[0]
-    heads, hd = gain_ref.shape
+def stick_block(q, kv, off, suffix, carry, diagonal):
+    rows, keys = q.shape[0], kv.shape[0]
+    s = dot_f32(q, kv, ((1,), (1,))) * (q.shape[1] // 2) ** (-0.5) + off
+    soft = jnp.maximum(s, 0.0) + jnp.log(1.0 + jnp.exp(-jnp.abs(s)))
+    log_not = -soft
+    if diagonal:
+        column = lax.broadcasted_iota(jnp.int32, (rows, keys), 1)
+        allowed = column <= lax.broadcasted_iota(jnp.int32, (rows, keys), 0)
+        log_not = jnp.where(allowed, log_not, 0.0)
+    high = log_not.astype(BF16)
+    low = (log_not - high.astype(F32)).astype(BF16)
+    sums = dot_f32(jnp.concatenate([high, low], axis=1), suffix)
+    later = sums[:, :keys]
+    if carry is not None:
+        later = later + carry
+    w = jnp.exp(s - soft + later)
+    if diagonal:
+        w = jnp.where(allowed, w, 0.0)
+    return w, sums[:, keys:]
+
+
+def block_of(ref, n):
+    rows = (ref.shape[0] - 16) // 2
+    return ref[n * rows : (n + 1) * rows, :], ref[2 * rows + 8 * n : 2 * rows + 8 * n + 8, :].astype(F32)[0:1]
+
+
+def near_kernel(q_ref, kv_ref, after, mix_ref, mass_ref, carry_ref):
+    rows = q_ref.shape[0] // 2
     suffix = suffix_matrix(rows)
-    for n in range(2):
-        k = mine_ref[n * rows : (n + 1) * rows, :]
-        v = mine_ref[(2 + n) * rows : (3 + n) * rows, :]
-        off = mine_ref[4 * rows + 8 * n : 4 * rows + 8 * n + 8, :]
-        mix, weights, totals = stick_block(q_ref[...], k, v, off, hd, suffix, None, n == 0)
-        mix_ref[n] = mix
-        for h in range(heads):
-            mass_ref[n * heads + h] = weights[h]
-            carry_ref[n * heads + h] = totals[h]
-
-
-def near_attention(q, mine, head_gain, after):
-    rows, width = q.shape
-    heads = head_gain.shape[0]
+    for n, (query, key) in enumerate(((0, 0), (1, 1), (1, 0))):
+        kv, off = block_of(kv_ref, key)
+        q = q_ref[query * rows : (query + 1) * rows, :]
+        w, total = stick_block(q, kv, off, suffix, None, query == key)
+        mix_ref[n] = dot_f32(w.astype(BF16), kv)
+        mass_ref[n] = w
+        carry_ref[n] = total
+
+
+def near_attention(q, kv, after):
+    rows, width = q.shape[0] // 2, q.shape[1]
+    out = shape((3, rows, rows), F32)
     return pl.pallas_call(
         near_kernel,
-        out_shape=(
-            shape((2, rows, width), F32),
-            shape((2 * heads, rows, rows), F32),
-            shape((2 * heads, rows, rows), F32),
-        ),
-        in_specs=[VM] * 3 + [ANY],
+        out_shape=(shape((3, rows, width), F32), out, out),
+        in_specs=[VM] * 2 + [ANY],
         out_specs=[VM] * 3,
         cost_estimate=cost(200_000_000, 1_000_000),
         compiler_params=params(),
         name="near_attention",
-    )(q, mine, head_gain, after)
-
-
-def attention_kernel(q_ref, pair_ref, gain_ref, mix_ref, mass_ref, carry_ref, after, out_ref, log_ref, acc, mass, carry):
-    me = lax.axis_index("sp")
-    rows, width = q_ref.shape
-    heads, hd = gain_ref.shape
-    lane = lax.broadcasted_iota(jnp.int32, (rows, width), 1) // hd
+    )(q, kv, after)
+
+
+def attention_kernel(
+    q_ref, pair_ref, gain_ref, mix_ref, mass_ref, carry_ref, after, own_ref, send_ref, log_ref, acc, mass, carry
+):
+    side, odd = lax.axis_index("sp") // 2, lax.axis_index("sp") % 2
+    rows, width = q_ref.shape[0] // 2, q_ref.shape[1]
+    hd = width // 2
     suffix = suffix_matrix(rows)
-    acc[...] = mix_ref[0]
-    for h in range(heads):
-        mass[h] = mass_ref[h]
-        carry[h] = carry_ref[h]
-
-    def earlier(t, _):
-        slot = jnp.bitwise_xor(me - t, me)
-
-        @pl.when(slot == 2)
-        def _():
-            scale = jnp.zeros_like(acc)
-            for h in range(heads):
-                left = jnp.exp(carry[h])
-                mass[h] = mass[h] + left * mass_ref[heads + h]
-                scale = jnp.where(lane == h, left, scale)
-                carry[h] = carry[h] + carry_ref[heads + h]
-            acc[...] = acc[...] + scale * mix_ref[1]
-
-        @pl.when(slot != 2)
-        def _():
-            n = slot // 2
-            k = pair_ref[pl.ds(pl.multiple_of(n * rows, rows), rows), :]
-            v = pair_ref[pl.ds(pl.multiple_of((2 + n) * rows, rows), rows), :]
-            off = jnp.where(
-                n == 0,
-                pair_ref[4 * rows : 4 * rows + 8, :].astype(F32),
-                pair_ref[4 * rows + 8 : 4 * rows + 16, :].astype(F32),
-            )
-            so_far = [carry[h] for h in range(heads)]
-            mix, weights, totals = stick_block(q_ref[...], k, v, off, hd, suffix, so_far, False)
-            acc[...] = acc[...] + mix
-            for h in range(heads):
-                mass[h] = mass[h] + weights[h]
-                carry[h] = so_far[h] + totals[h]
-
-        return 0
-
-    lax.fori_loop(1, me + 1, earlier, 0)
+    acc[:rows, :] = mix_ref[0]
+    acc[rows:, :] = mix_ref[1]
+    mass[:rows, :] = mass_ref[0]
+    mass[rows:, :] = mass_ref[1]
+    carry[...] = carry_ref[1]
+
+    @pl.when(odd == 1)
+    def _():
+        kv, off = block_of(pair_ref, 1)
+        w, total = stick_block(q_ref[rows:, :], kv, off, suffix, carry[...], False)
+        acc[rows:, :] = acc[rows:, :] + dot_f32(w.astype(BF16), kv)
+        mass[rows:, :] = mass[rows:, :] + w
+        carry[...] = carry[...] + total
+
+    share = odd.astype(F32)
+    so_far = carry[...]
+    kv, off = block_of(pair_ref, 0)
+    both = jnp.concatenate([carry_ref[0], so_far + share * carry_ref[2]])
+    w, total = stick_block(q_ref[...], kv, off, suffix, both, False)
+    w = jnp.concatenate([share * w[:rows], w[rows:]])
+    scale = jnp.exp(so_far + (1.0 - share) * total[rows:])
+    acc[...] = acc[...] + dot_f32(w.astype(BF16), kv)
+    acc[rows:, :] = acc[rows:, :] + scale * mix_ref[2]
+    mass[...] = mass[...] + w
+    mass[rows:, :] = mass[rows:, :] + scale * mass_ref[2]
+
     mixed = acc[...]
-    squares = mixed * mixed
-    inverse = jnp.zeros_like(mixed)
-    for h in range(heads):
-        mean = jnp.sum(jnp.where(lane == h, squares, 0.0), axis=1, keepdims=True) / hd
-        inverse = jnp.where(lane == h, lax.rsqrt(mean + norm_eps), inverse)
-    gain = jnp.concatenate([gain_ref[h : h + 1, :] for h in range(heads)], axis=1)
-    out_ref[...] = (mixed * inverse * gain).astype(BF16)
-    for h in range(heads):
-        log_ref[h : h + 1, :] = jnp.log(jnp.sum(jnp.transpose(mass[h]), axis=0, keepdims=True))
+    lane = lax.broadcasted_iota(jnp.int32, (rows, width), 1)
+    squares = jnp.where(lax.broadcasted_iota(jnp.int32, mixed.shape, 1) >= hd, mixed * mixed, 0.0)
+    mean = jnp.sum(squares, axis=1, keepdims=True) / hd
+    gain = pick(side, gain_ref[0:1, :], gain_ref[1:2, :])
+    att = mixed * lax.rsqrt(mean + norm_eps) * jnp.concatenate([gain, gain], axis=1)
+    own = pick(side, att[:rows], att[rows:])
+    cross = pick(side, att[rows:], att[:rows])
+    swapped = jnp.concatenate([own[:, hd:], own[:, :hd]], axis=1)
+    own = pick(side, jnp.where(lane < hd, swapped, 0.0), jnp.where(lane >= hd, own, 0.0))
+    own_ref[...] = own.astype(BF16)
+    half = rows // 2
+    send_ref[:half, :] = jnp.concatenate([cross[:half, hd:], cross[half:, hd:]], axis=1).astype(BF16)
+    logs = [jnp.log(jnp.sum(jnp.transpose(mass[n * rows : (n + 1) * rows]), axis=0, keepdims=True)) for n in range(2)]
+    log_ref[...] = jnp.broadcast_to(pick(side, logs[0], logs[1]), log_ref.shape)
+    rest = pick(side, logs[1], logs[0])
+    for n in range(3):
+        part = rest.astype(BF16)
+        rest = rest - part.astype(F32)
+        send_ref[half + 16 * n : half + 16 * (n + 1), :] = jnp.broadcast_to(part, (16, width))
 
 
 def attention(q, pair, head_gain, near, after):
-    rows, width = q.shape
-    heads = head_gain.shape[0]
+    rows, width = q.shape[0] // 2, q.shape[1]
     return pl.pallas_call(
         attention_kernel,
-        out_shape=(shape((rows, width)), shape((heads, rows), F32)),
+        out_shape=(shape((rows, width)), shape((rows // 2 + 48, width)), shape((8, rows), F32)),
         in_specs=[VM] * 6 + [ANY],
-        out_specs=[VM] * 2,
+        out_specs=[VM] * 3,
         scratch_shapes=[
-            pltpu.VMEM((rows, width), F32),
-            pltpu.VMEM((heads, rows, rows), F32),
-            pltpu.VMEM((heads, rows, rows), F32),
+            pltpu.VMEM((2 * rows, width), F32),
+            pltpu.VMEM((2 * rows, rows), F32),
+            pltpu.VMEM((rows, rows), F32),
         ],
         cost_estimate=cost(400_000_000, 1_000_000),
         compiler_params=params(),
@@ -483,8 +511,7 @@
 
 
 def final_kernel(*refs):
-    act, wa, wc = (refs[n * 4 : (n + 1) * 4] for n in range(3))
-    gain_ref, out_ref = refs[12:]
+    act, wa, wc, gain_ref, out_ref = refs[:4], refs[4:8], refs[8:14], refs[14], refs[15]
     cw = wc[0].shape[0]
     aw = act[0].shape[1] - cw
     convs = [c[:, aw:].astype(F32) for c in act]
@@ -493,14 +520,22 @@
     spread = sum(jnp.sum(v * v, axis=1, keepdims=True) for v in centered) / (4 * cw)
     inverse = lax.rsqrt(spread + norm_eps)
     total = None
+    ys = []
     for slot in range(4):
         pieces = [wa[slot][aw : aw + 1, n * cw : (n + 1) * cw].astype(F32) for n in range(6)]
         gain = pieces[0] + pieces[1] + pieces[2]
         bias = pieces[3] + pieces[4] + pieces[5]
         y = centered[slot] * inverse * gain + bias
         y = (y * jax.nn.sigmoid(y)).astype(BF16)
-        part = dot_f32(act[slot][:, :aw], wa[slot][:aw, :]) + dot_f32(y, wc[slot][...])
+        part = dot_f32(act[slot][:, :aw], wa[slot][:aw, :])
+        if slot < 2:
+            part = part + dot_f32(y, wc[slot][...])
         total = part if total is None else total + part
+        ys.append(y)
+    same = dot_f32(ys[2], wc[2][...]) + dot_f32(ys[3], wc[4][...])
+    other = dot_f32(ys[2], wc[3][...]) + dot_f32(ys[3], wc[5][...])
+    swap = lax.axis_index("grp") == 1
+    total = total + jnp.concatenate([jnp.where(swap, other, same), jnp.where(swap, same, other)], axis=1)
     squares = jnp.mean(total * total, axis=1, keepdims=True)
     out_ref[...] = (total * lax.rsqrt(squares + norm_eps) * gain_ref[...]).astype(BF16)
 
@@ -510,7 +545,7 @@
     return pl.pallas_call(
         final_kernel,
         out_shape=shape((rows, width)),
-        in_specs=[VM] * 13,
+        in_specs=[VM] * 15,
         out_specs=VM,
         cost_estimate=cost(800_000_000, 7_000_000),
         compiler_params=params(32),
@@ -535,38 +570,47 @@
     w_out_conv,
     out_gain,
 ):
-    own_qkv, half_qkv = pack_qkv((w_query, w_key, w_value))
+    own_qkv, half_qkv, wc_half = pack_qkv((w_query, w_key, w_value), w_out_conv)
     qkv_same = exchange(half_qkv, "sp", 1)
-    wc_x = exchange(w_out_conv, "tp", 2)
+    wc_x = exchange(wc_half, "tp", 2)
     x_send, mine_own, mine_pair = norm_parts(tokens, norm_gain, w_query.shape[0])
     x_got = exchange(x_send, "sp", 2)
-    own_glu, wa_mine, off = pack(
+    own_gv, half_gv, own_gg, wa_mine, off = pack(
         w_glu_value, w_glu_gate, w_out_attn, key_offset.T, channel_gain, channel_bias
     )
-    glu_pair = exchange(own_glu, "sp", 1)
     qkv_other = exchange(qkv_same, "grp", 1)
+    gv_same = exchange(half_gv, "sp", 1)
+    gg_pair = exchange(own_gg, "sp", 1)
     x_other = exchange(x_got, "tp", 1)
     wa_x = exchange(wa_mine, "tp", 2)
     wc_core = exchange(w_out_conv, "tp", 1)
     wa_core = exchange(wa_mine, "tp", 1)
+    gv_other = exchange(gv_same, "grp", 1)
+    wc_y = exchange(wc_x, "grp", 1)
     wc_xc = exchange(wc_x, "tp", 1)
     wa_xc = exchange(wa_x, "tp", 1)
+    wc_yc = exchange(wc_y, "tp", 1)
     x_own, x_pair = assemble(mine_own, mine_pair, x_got, x_other)
 
     keep, sent = project_qkv(x_own, x_pair, own_qkv, qkv_same, qkv_other, off)
     got = exchange(sent, "sp", 2)
-    glu_keep, glu_sent = project_glu(x_own, x_pair, own_glu, glu_pair, sent)
+    glu_keep, glu_sent = project_glu(
+        x_own, x_pair, (own_gv, own_gg), (gv_same, gv_other, gg_pair), sent
+    )
     glu_got = exchange(glu_sent, "sp", 2)
-    q, mine_two = sum_qkv(keep, got, sent, glu_sent)
-    pair_two = exchange(mine_two, "sp", 1)
-    near = near_attention(q, mine_two, head_gain, mine_two)
-    gated, tail = gate(glu_keep, glu_got, -(-conv_taps.shape[0] // 16) * 16)
+    q, kv_mine = sum_qkv(keep, got, off, glu_sent)
+    kv_pair = exchange(kv_mine, "sp", 1)
+    near = near_attention(q, kv_mine, kv_mine)
+    attended, att_sent, own_log = attention(q, kv_pair, head_gain, near, kv_mine)
+    att_got = exchange(att_sent, "sp", 2)
+    gated, tail = gate(glu_keep, glu_got, -(-conv_taps.shape[0] // 16) * 16, att_sent)
     before = from_behind(tail, "sp", 1)
-    attended, log_mass = attention(q, pair_two, head_gain, near, tail)
-    act_mine = conv(gated, before, conv_taps, attended)
-    act = [act_mine] + [exchange(act_mine, "tp", bit) for bit in (1, 2, 3)]
+    act_mine, log_mass = conv(gated, before, conv_taps, attended, att_got, own_log)
+    act_x = exchange(act_mine, "tp", 2)
+    act_core = exchange(act_mine, "tp", 1)
+    act = (act_mine, act_core, act_x, exchange(act_x, "tp", 1))
     wa = (wa_mine, wa_core, wa_x, wa_xc)
-    wc = (w_out_conv, wc_core, wc_x, wc_xc)
+    wc = (w_out_conv, wc_core, wc_x, wc_y, wc_xc, wc_yc)
     mixed = finish(act, wa, wc, out_gain)
     return (mixed, log_mass)
 

time: 76.9 us -> 69.6 us (0.905)
  the two profiles are of different devices: /device:TPU:0 before, /device:TPU:25 now
where the time goes in v6:
time: 69.6 us; the launch traced here: 68.7 us
  waiting for transfers between devices  33.7 us (48%)
  starting transfers between devices  22.6 us (32%)
  Pallas kernels  10.9 us (16%)
  between operations  0.78 us (1%)
    ppermute x22, waiting for transfers between devices, exchange(): return lax.ppermute(value, axis, [(s, s ^ bit) for s in range(count)])  30.6 us
    ppermute x22, starting transfers between devices, exchange(): return lax.ppermute(value, axis, [(s, s ^ bit) for s in range(count)])  21.4 us
    ppermute x1, waiting for transfers between devices, from_behind(): lax.ppermute(value, axis, [(source, source + steps) for source in range(i...  3.18 us
    pallas_call x1, Pallas kernels, finish(): pl.pallas_call(final_kernel, out_shape=shape((rows, width)), in_specs=[VM...  2.49 us
    pallas_call x1, Pallas kernels, pack_qkv(): pl.pallas_call(pack_qkv_kernel, out_shape=(shape((block, 3 * width)), sha...  1.42 us
  transfers between devices with their start and end apart: 23, of which 11 were waited for; matrix products, arithmetic and copies ran while one was open for 0% of the time, Pallas kernels for 10%

profile of v6, /device:TPU:25, one launch (start us, length us, event | category | flops | bytes accessed | tf_op | source)
XLA Modules:
  0.0 68.7 jit_solution(15205027707009126367)
XLA Ops:
  0.6 1.4 %pack_qkv.1 = (bf16[512,384]{1,0:T(8,128)(2,1)S(1)}, bf16[256,384]{1,0:T(8,128)(2,1)S(1)}, bf16[256,1024]{1,0:T(8,128)(2,1)S(1)}) custom-call(bf16[512,128]{1,0:T(8,128)(2,1)} %wq.1, bf16[512,128]{1,0:T(8,128)(2,1)} %wk.1, bf16[512,128]{1,0:T(8,128)(2,1)} %wv.1, bf16[256,2048]{1,0:T(8,128)(2,1)} %refs_8_.1), custom_call_target="tpu_custom_call" | custom-call | flops 2000000 | bytes 400000 | tf_op jit(solution)/shard_map/pack_qkv/pallas_call | solution.py:74
  2.1 1.3 %collective-permute-start.19 = (bf16[256,1024]{1,0:T(8,128)(2,1)S(1)}, bf16[256,1024]{1,0:T(8,128)(2,1)S(1)}, u32[]{:S(2)}, u32[]{:S(2)}) collective-permute-start(bf16[256,1024]{1,0:T(8,128)(2,1)S(1)} %get-tuple-element.58), channel_id=1, source_target_pairs={{0,2},{1,3},{2,0},{3,1},{4,6},{5,7},{6,4},{7,5},{8,10},{9,11},{10,... | collective-permute-start | bytes 1572872 | tf_op jit(solution)/shard_map/ppermute | solution.py:15
  3.3 1.3 %norm_parts.1 = (bf16[64,1024]{1,0:T(8,128)(2,1)S(1)}, bf16[128,512]{1,0:T(8,128)(2,1)S(1)}, bf16[128,512]{1,0:T(8,128)(2,1)S(1)}) custom-call(bf16[128,2048]{1,0:T(8,128)(2,1)} %x_hbm.1, f32[1,2048]{1,0:T(1,128)} %bitcast.6), custom_call_target="tpu_custom_call" | custom-call | flops 2000000 | bytes 1000000 | tf_op jit(solution)/shard_map/norm_parts/pallas_call | solution.py:116
  5.0 1.4 %pack.1 = (bf16[512,256]{1,0:T(8,128)(2,1)S(1)}, bf16[256,256]{1,0:T(8,128)(2,1)S(1)}, bf16[512,256]{1,0:T(8,128)(2,1)S(1)}, bf16[144,2048]{1,0:T(8,128)(2,1)S(1)}, bf16[2,128]{1,0:T(2,128)(2,1)S(1)}) custom-call(bf16[512,256]{1,0:T(8,128)(2,1)} %gv_hbm.1, bf16[512,256]{1,0:T(8,128)(2,1)} %gg_hbm.1, bf16[128,2048]{1,0:T(8,128)(2,1)} %wa_hbm.1, ...), custom_call_target="tpu_custom_call" | custom-call | flops 2000000 | bytes 2000000 | tf_op jit(solution)/shard_map/pack/pallas_call | solution.py:168
  6.3 1.4 %collective-permute-start.2 = (bf16[256,256]{1,0:T(8,128)(2,1)S(1)}, bf16[256,256]{1,0:T(8,128)(2,1)S(1)}, u32[]{:S(2)}, u32[]{:S(2)}) collective-permute-start(bf16[256,256]{1,0:T(8,128)(2,1)S(1)} %get-tuple-element.38), channel_id=1, source_target_pairs={{0,4},{4,0},{8,12},{12,8},{1,5},{5,1},{9,13},{13,9},{2,6},{6,2},{1... | collective-permute-start | bytes 393224 | tf_op jit(solution)/shard_map/ppermute | solution.py:15
  7.7 6.1 %collective-permute-done.got_ref = bf16[64,1024]{1,0:T(8,128)(2,1)S(1)} collective-permute-done((bf16[64,1024]{1,0:T(8,128)(2,1)S(1)}, bf16[64,1024]{1,0:T(8,128)(2,1)S(1)}, u32[]{:S(2)}, u32[]{:S(2)}) %collective-permute-start) | collective-permute-done | bytes 131104 | tf_op jit(solution)/shard_map/ppermute | solution.py:15
  14.6 1.2 %collective-permute-done.2.gv_same = bf16[256,256]{1,0:T(8,128)(2,1)S(1)} collective-permute-done((bf16[256,256]{1,0:T(8,128)(2,1)S(1)}, bf16[256,256]{1,0:T(8,128)(2,1)S(1)}, u32[]{:S(2)}, u32[]{:S(2)}) %collective-permute-start.2) | collective-permute-done | bytes 131104 | tf_op jit(solution)/shard_map/ppermute | solution.py:15
  15.7 1.2 %collective-permute-start.3 = (bf16[256,256]{1,0:T(8,128)(2,1)S(1)}, bf16[256,256]{1,0:T(8,128)(2,1)S(1)}, u32[]{:S(2)}, u32[]{:S(2)}) collective-permute-start(bf16[256,256]{1,0:T(8,128)(2,1)S(1)} %collective-permute-done.2.gv_same), channel_id=1, source_target_pairs={{0,16},{16,0},{1,17},{17,1},{2,18},{18,2},{3,19},{19,3},{4,20},{20... | collective-permute-start | bytes 393224 | tf_op jit(solution)/shard_map/ppermute | solution.py:15
  17.5 2.4 %collective-permute-done.3.gv_other = bf16[256,256]{1,0:T(8,128)(2,1)S(1)} collective-permute-done((bf16[256,256]{1,0:T(8,128)(2,1)S(1)}, bf16[256,256]{1,0:T(8,128)(2,1)S(1)}, u32[]{:S(2)}, u32[]{:S(2)}) %collective-permute-start.3) | collective-permute-done | bytes 131104 | tf_op jit(solution)/shard_map/ppermute | solution.py:15
  19.9 4.0 %collective-permute-start.18 = (bf16[256,2048]{1,0:T(8,128)(2,1)S(1)}, bf16[256,2048]{1,0:T(8,128)(2,1)S(1)}, u32[]{:S(2)}, u32[]{:S(2)}) collective-permute-start(bf16[256,2048]{1,0:T(8,128)(2,1)S(1)} %copy-done), channel_id=1, source_target_pairs={{0,1},{1,0},{2,3},{3,2},{4,5},{5,4},{6,7},{7,6},{8,9},{9,8},{10,11... | collective-permute-start | bytes 3145736 | tf_op jit(solution)/shard_map/ppermute | solution.py:15
  23.9 1.1 %collective-permute-start.20 = (bf16[256,1024]{1,0:T(8,128)(2,1)S(1)}, bf16[256,1024]{1,0:T(8,128)(2,1)S(1)}, u32[]{:S(2)}, u32[]{:S(2)}) collective-permute-start(bf16[256,1024]{1,0:T(8,128)(2,1)S(1)} %collective-permute-done.19.refs_10_), channel_id=1, source_target_pairs={{0,16},{16,0},{1,17},{17,1},{2,18},{18,2},{3,19},{19,3},{4,20},{20... | collective-permute-start | bytes 1572872 | tf_op jit(solution)/shard_map/ppermute | solution.py:15
  25.1 0.9 %collective-permute-start.15 = (bf16[144,2048]{1,0:T(8,128)(2,1)S(1)}, bf16[144,2048]{1,0:T(8,128)(2,1)S(1)}, u32[]{:S(2)}, u32[]{:S(2)}) collective-permute-start(bf16[144,2048]{1,0:T(8,128)(2,1)S(1)} %get-tuple-element.57.refs_4_), channel_id=1, source_target_pairs={{0,1},{1,0},{2,3},{3,2},{4,5},{5,4},{6,7},{7,6},{8,9},{9,8},{10,11... | collective-permute-start | bytes 1769480 | tf_op jit(solution)/shard_map/ppermute | solution.py:15
  26.5 1.3 %collective-permute-start.8 = (bf16[400,128]{1,0:T(8,128)(2,1)S(1)}, bf16[400,128]{1,0:T(8,128)(2,1)S(1)}, u32[]{:S(2)}, u32[]{:S(2)}) collective-permute-start(bf16[400,128]{1,0:T(8,128)(2,1)S(1)} %get-tuple-element.42.after), channel_id=1, source_target_pairs={{0,8},{4,12},{8,0},{12,4},{1,9},{5,13},{9,1},{13,5},{2,10},{6,14},... | collective-permute-start | bytes 307208 | tf_op jit(solution)/shard_map/ppermute | solution.py:15
  28.3 5.8 %collective-permute-done.8.got_ref = bf16[400,128]{1,0:T(8,128)(2,1)S(1)} collective-permute-done((bf16[400,128]{1,0:T(8,128)(2,1)S(1)}, bf16[400,128]{1,0:T(8,128)(2,1)S(1)}, u32[]{:S(2)}, u32[]{:S(2)}) %collective-permute-start.8) | collective-permute-done | bytes 102432 | tf_op jit(solution)/shard_map/ppermute | solution.py:15
  34.3 3.4 %collective-permute-done.9.pair_ref = bf16[272,128]{1,0:T(8,128)(2,1)S(1)} collective-permute-done((bf16[272,128]{1,0:T(8,128)(2,1)S(1)}, bf16[272,128]{1,0:T(8,128)(2,1)S(1)}, u32[]{:S(2)}, u32[]{:S(2)}) %collective-permute-start.9) | collective-permute-done | bytes 69664 | tf_op jit(solution)/shard_map/ppermute | solution.py:15
  37.7 1.1 %collective-permute-start.7 = (bf16[128,512]{1,0:T(8,128)(2,1)S(1)}, bf16[128,512]{1,0:T(8,128)(2,1)S(1)}, u32[]{:S(2)}, u32[]{:S(2)}) collective-permute-start(bf16[128,512]{1,0:T(8,128)(2,1)S(1)} %get-tuple-element.44.after), channel_id=1, source_target_pairs={{0,8},{4,12},{8,0},{12,4},{1,9},{5,13},{9,1},{13,5},{2,10},{6,14},... | collective-permute-start | bytes 393224 | tf_op jit(solution)/shard_map/ppermute | solution.py:15
  38.8 0.8 %near_attention.1 = (f32[3,128,128]{2,1,0:T(8,128)S(1)}, f32[3,128,128]{2,1,0:T(8,128)S(1)}, f32[3,128,128]{2,1,0:T(8,128)S(1)}) custom-call(bf16[256,128]{1,0:T(8,128)(2,1)S(1)} %get-tuple-element.46.q_ref, bf16[272,128]{1,0:T(8,128)(2,1)S(1)} %get-tuple-element.47.kv_ref.after, bf16[272,128]{1,0:T(8,128)(2,1)S(1)} %get-tuple-element.47.kv_ref.after), custom_call_target="tpu_custom_call" | custom-call | flops 200000000 | bytes 1000000 | tf_op jit(solution)/shard_map/near_attention/pallas_call | solution.py:429
  39.6 1.5 %collective-permute-start.17 = (bf16[144,2048]{1,0:T(8,128)(2,1)S(1)}, bf16[144,2048]{1,0:T(8,128)(2,1)S(1)}, u32[]{:S(2)}, u32[]{:S(2)}) collective-permute-start(bf16[144,2048]{1,0:T(8,128)(2,1)S(1)} %collective-permute-done.16.refs_6_), channel_id=1, source_target_pairs={{0,1},{1,0},{2,3},{3,2},{4,5},{5,4},{6,7},{7,6},{8,9},{9,8},{10,11... | collective-permute-start | bytes 1769480 | tf_op jit(solution)/shard_map/ppermute | solution.py:15
  41.1 0.7 copy-done.3
  41.8 1.1 %stick_attention.1 = (bf16[128,128]{1,0:T(8,128)(2,1)S(1)}, bf16[112,128]{1,0:T(8,128)(2,1)S(1)}, f32[8,128]{1,0:T(8,128)S(1)}) custom-call(bf16[256,128]{1,0:T(8,128)(2,1)S(1)} %get-tuple-element.46.q_ref, bf16[272,128]{1,0:T(8,128)(2,1)S(1)} %collective-permute-done.9.pair_ref, f32[2,64]{1,0:T(2,128)S(1)} %copy-done.3, ...), custom_call_target="tpu_custom_call" | custom-call | flops 400000000 | bytes 1000000 | tf_op jit(solution)/shard_map/stick_attention/pallas_call | solution.py:497
  43.0 3.2 %collective-permute-done.7.got_ref = bf16[128,512]{1,0:T(8,128)(2,1)S(1)} collective-permute-done((bf16[128,512]{1,0:T(8,128)(2,1)S(1)}, bf16[128,512]{1,0:T(8,128)(2,1)S(1)}, u32[]{:S(2)}, u32[]{:S(2)}) %collective-permute-start.7) | collective-permute-done | bytes 131104 | tf_op jit(solution)/shard_map/ppermute | solution.py:15
  46.2 1.3 %collective-permute-start.10 = (bf16[32,256]{1,0:T(8,128)(2,1)S(1)}, bf16[32,256]{1,0:T(8,128)(2,1)S(1)}, u32[]{:S(2)}, u32[]{:S(2)}) collective-permute-start(bf16[32,256]{1,0:T(8,128)(2,1)S(1)} %get-tuple-element.53), channel_id=1, source_target_pairs={{0,4},{4,8},{8,12},{1,5},{5,9},{9,13},{2,6},{6,10},{10,14},{3,7},{... | collective-permute-start | bytes 49160 | tf_op jit(solution)/shard_map/ppermute | solution.py:21
  47.5 3.2 %collective-permute-done.10.before_ref = bf16[32,256]{1,0:T(8,128)(2,1)S(1)} collective-permute-done((bf16[32,256]{1,0:T(8,128)(2,1)S(1)}, bf16[32,256]{1,0:T(8,128)(2,1)S(1)}, u32[]{:S(2)}, u32[]{:S(2)}) %collective-permute-start.10) | collective-permute-done | bytes 16416 | tf_op jit(solution)/shard_map/ppermute | solution.py:21
  50.7 0.7 collective-permute-start.11
  51.4 3.0 %collective-permute-done.11.got_ref = bf16[112,128]{1,0:T(8,128)(2,1)S(1)} collective-permute-done((bf16[112,128]{1,0:T(8,128)(2,1)S(1)}, bf16[112,128]{1,0:T(8,128)(2,1)S(1)}, u32[]{:S(2)}, u32[]{:S(2)}) %collective-permute-start.11) | collective-permute-done | bytes 28704 | tf_op jit(solution)/shard_map/ppermute | solution.py:15
  54.3 3.2 %collective-permute-start.21 = (bf16[256,1024]{1,0:T(8,128)(2,1)S(1)}, bf16[256,1024]{1,0:T(8,128)(2,1)S(1)}, u32[]{:S(2)}, u32[]{:S(2)}) collective-permute-start(bf16[256,1024]{1,0:T(8,128)(2,1)S(1)} %collective-permute-done.19.refs_10_), channel_id=1, source_target_pairs={{0,1},{1,0},{2,3},{3,2},{4,5},{5,4},{6,7},{7,6},{8,9},{9,8},{10,11... | collective-permute-start | bytes 1572872 | tf_op jit(solution)/shard_map/ppermute | solution.py:15
  57.5 1.2 %conv.1 = (bf16[128,384]{1,0:T(8,128)(2,1)S(1)}, f32[2,128]{1,0:T(2,128)}) custom-call(bf16[128,256]{1,0:T(8,128)(2,1)S(1)} %get-tuple-element.52.gated_ref, bf16[32,256]{1,0:T(8,128)(2,1)S(1)} %collective-permute-done.10.before_ref, f32[31,256]{1,0:T(8,128)S(1)} %copy-done.1, bf16[128,128]{1,0:T(8,128)(2,1)S(1)} %get-tuple-element.54.att_ref, ...), custom_call_target="tpu_custom_call" | custom-call | flops 20000000 | bytes 500000 | tf_op jit(solution)/shard_map/conv/pallas_call | solution.py:370
  59.0 3.6 %collective-permute-done.13.refs_2_ = bf16[128,384]{1,0:T(8,128)(2,1)S(1)} collective-permute-done((bf16[128,384]{1,0:T(8,128)(2,1)S(1)}, bf16[128,384]{1,0:T(8,128)(2,1)S(1)}, u32[]{:S(2)}, u32[]{:S(2)}) %collective-permute-start.13) | collective-permute-done | bytes 98336 | tf_op jit(solution)/shard_map/ppermute | solution.py:15
  62.6 1.3 %collective-permute-start.12 = (bf16[128,384]{1,0:T(8,128)(2,1)S(1)}, bf16[128,384]{1,0:T(8,128)(2,1)S(1)}, u32[]{:S(2)}, u32[]{:S(2)}) collective-permute-start(bf16[128,384]{1,0:T(8,128)(2,1)S(1)} %get-tuple-element.56.refs_0_), channel_id=1, source_target_pairs={{0,1},{1,0},{2,3},{3,2},{4,5},{5,4},{6,7},{7,6},{8,9},{9,8},{10,11... | collective-permute-start | bytes 294920 | tf_op jit(solution)/shard_map/ppermute | solution.py:15
  63.9 0.9 %collective-permute-done.12.refs_1_ = bf16[128,384]{1,0:T(8,128)(2,1)S(1)} collective-permute-done((bf16[128,384]{1,0:T(8,128)(2,1)S(1)}, bf16[128,384]{1,0:T(8,128)(2,1)S(1)}, u32[]{:S(2)}, u32[]{:S(2)}) %collective-permute-start.12) | collective-permute-done | bytes 98336 | tf_op jit(solution)/shard_map/ppermute | solution.py:15
  65.2 0.9 %collective-permute-done.14.refs_3_ = bf16[128,384]{1,0:T(8,128)(2,1)S(1)} collective-permute-done((bf16[128,384]{1,0:T(8,128)(2,1)S(1)}, bf16[128,384]{1,0:T(8,128)(2,1)S(1)}, u32[]{:S(2)}, u32[]{:S(2)}) %collective-permute-start.14) | collective-permute-done | bytes 98336 | tf_op jit(solution)/shard_map/ppermute | solution.py:15
  66.2 2.5 %finish_rows.1 = bf16[128,2048]{1,0:T(8,128)(2,1)} custom-call(bf16[128,384]{1,0:T(8,128)(2,1)S(1)} %get-tuple-element.56.refs_0_, bf16[128,384]{1,0:T(8,128)(2,1)S(1)} %collective-permute-done.12.refs_1_, bf16[128,384]{1,0:T(8,128)(2,1)S(1)} %collective-permute-done.13.refs_2_, bf16[128,384]{1,0:T(8,128)(2,1)S(1)} %collective-permute-done.14.refs_3_, ...), custom_call_target="tpu_custom_call" | custom-call | flops 800000000 | bytes 7000000 | tf_op jit(solution)/shard_map/finish_rows/pallas_call | solution.py:545
  (34 shorter events, 3.5 us)
Async XLA Ops:
  2.1 17.8 %copy-start = (bf16[256,2048]{1,0:T(8,128)(2,1)S(1)}, bf16[256,2048]{1,0:T(8,128)(2,1)}, u32[]{:S(2)}) copy-start(bf16[256,2048]{1,0:T(8,128)(2,1)} %refs_8_.1) | copy-start | bytes 3145732
  2.1 21.8 %collective-permute-start.19 = (bf16[256,1024]{1,0:T(8,128)(2,1)S(1)}, bf16[256,1024]{1,0:T(8,128)(2,1)S(1)}, u32[]{:S(2)}, u32[]{:S(2)}) collective-permute-start(bf16[256,1024]{1,0:T(8,128)(2,1)S(1)} %get-tuple-element.58), channel_id=1, source_target_pairs={{0,2},{1,3},{2,0},{3,1},{4,6},{5,7},{6,4},{7,5},{8,10},{9,11},{10,... | collective-permute-start | bytes 1572872 | tf_op jit(solution)/shard_map/ppermute | solution.py:15
  4.7 9.1 %collective-permute-start = (bf16[64,1024]{1,0:T(8,128)(2,1)S(1)}, bf16[64,1024]{1,0:T(8,128)(2,1)S(1)}, u32[]{:S(2)}, u32[]{:S(2)}) collective-permute-start(bf16[64,1024]{1,0:T(8,128)(2,1)S(1)} %get-tuple-element.33), channel_id=1, source_target_pairs={{0,8},{4,12},{8,0},{12,4},{1,9},{5,13},{9,1},{13,5},{2,10},{6,14},... | collective-permute-start | bytes 393224 | tf_op jit(solution)/shard_map/ppermute | solution.py:15
  4.8 12.2 %collective-permute-start.5 = (bf16[256,384]{1,0:T(8,128)(2,1)S(1)}, bf16[256,384]{1,0:T(8,128)(2,1)S(1)}, u32[]{:S(2)}, u32[]{:S(2)}) collective-permute-start(bf16[256,384]{1,0:T(8,128)(2,1)S(1)} %get-tuple-element.40), channel_id=1, source_target_pairs={{0,4},{4,0},{8,12},{12,8},{1,5},{5,1},{9,13},{13,9},{2,6},{6,2},{1... | collective-permute-start | bytes 589832 | tf_op jit(solution)/shard_map/ppermute | solution.py:15
  6.3 9.4 %collective-permute-start.2 = (bf16[256,256]{1,0:T(8,128)(2,1)S(1)}, bf16[256,256]{1,0:T(8,128)(2,1)S(1)}, u32[]{:S(2)}, u32[]{:S(2)}) collective-permute-start(bf16[256,256]{1,0:T(8,128)(2,1)S(1)} %get-tuple-element.38), channel_id=1, source_target_pairs={{0,4},{4,0},{8,12},{12,8},{1,5},{5,1},{9,13},{13,9},{2,6},{6,2},{1... | collective-permute-start | bytes 393224 | tf_op jit(solution)/shard_map/ppermute | solution.py:15
  13.8 3.5 %collective-permute-start.1 = (bf16[64,1024]{1,0:T(8,128)(2,1)S(1)}, bf16[64,1024]{1,0:T(8,128)(2,1)S(1)}, u32[]{:S(2)}, u32[]{:S(2)}) collective-permute-start(bf16[64,1024]{1,0:T(8,128)(2,1)S(1)} %collective-permute-done.got_ref), channel_id=1, source_target_pairs={{0,1},{1,0},{2,3},{3,2},{4,5},{5,4},{6,7},{7,6},{8,9},{9,8},{10,11... | collective-permute-start | bytes 393224 | tf_op jit(solution)/shard_map/ppermute | solution.py:15
  14.3 25.3 %collective-permute-start.16 = (bf16[144,2048]{1,0:T(8,128)(2,1)S(1)}, bf16[144,2048]{1,0:T(8,128)(2,1)S(1)}, u32[]{:S(2)}, u32[]{:S(2)}) collective-permute-start(bf16[144,2048]{1,0:T(8,128)(2,1)S(1)} %get-tuple-element.57.refs_4_), channel_id=1, source_target_pairs={{0,2},{1,3},{2,0},{3,1},{4,6},{5,7},{6,4},{7,5},{8,10},{9,11},{10,... | collective-permute-start | bytes 1769480 | tf_op jit(solution)/shard_map/ppermute | solution.py:15
  15.7 4.1 %collective-permute-start.3 = (bf16[256,256]{1,0:T(8,128)(2,1)S(1)}, bf16[256,256]{1,0:T(8,128)(2,1)S(1)}, u32[]{:S(2)}, u32[]{:S(2)}) collective-permute-start(bf16[256,256]{1,0:T(8,128)(2,1)S(1)} %collective-permute-done.2.gv_same), channel_id=1, source_target_pairs={{0,16},{16,0},{1,17},{17,1},{2,18},{18,2},{3,19},{19,3},{4,20},{20... | collective-permute-start | bytes 393224 | tf_op jit(solution)/shard_map/ppermute | solution.py:15
  17.0 9.5 %collective-permute-start.4 = (bf16[512,256]{1,0:T(8,128)(2,1)S(1)}, bf16[512,256]{1,0:T(8,128)(2,1)S(1)}, u32[]{:S(2)}, u32[]{:S(2)}) collective-permute-start(bf16[512,256]{1,0:T(8,128)(2,1)S(1)} %get-tuple-element.37.gg), channel_id=1, source_target_pairs={{0,4},{4,0},{8,12},{12,8},{1,5},{5,1},{9,13},{13,9},{2,6},{6,2},{1... | collective-permute-start | bytes 786440 | tf_op jit(solution)/shard_map/ppermute | solution.py:15
  17.2 7.8 %collective-permute-start.6 = (bf16[256,384]{1,0:T(8,128)(2,1)S(1)}, bf16[256,384]{1,0:T(8,128)(2,1)S(1)}, u32[]{:S(2)}, u32[]{:S(2)}) collective-permute-start(bf16[256,384]{1,0:T(8,128)(2,1)S(1)} %collective-permute-done.5.same), channel_id=1, source_target_pairs={{0,16},{16,0},{1,17},{17,1},{2,18},{18,2},{3,19},{19,3},{4,20},{20... | collective-permute-start | bytes 589832 | tf_op jit(solution)/shard_map/ppermute | solution.py:15
  19.9 46.3 %collective-permute-start.18 = (bf16[256,2048]{1,0:T(8,128)(2,1)S(1)}, bf16[256,2048]{1,0:T(8,128)(2,1)S(1)}, u32[]{:S(2)}, u32[]{:S(2)}) collective-permute-start(bf16[256,2048]{1,0:T(8,128)(2,1)S(1)} %copy-done), channel_id=1, source_target_pairs={{0,1},{1,0},{2,3},{3,2},{4,5},{5,4},{6,7},{7,6},{8,9},{9,8},{10,11... | collective-permute-start | bytes 3145736 | tf_op jit(solution)/shard_map/ppermute | solution.py:15
  23.9 33.6 %collective-permute-start.20 = (bf16[256,1024]{1,0:T(8,128)(2,1)S(1)}, bf16[256,1024]{1,0:T(8,128)(2,1)S(1)}, u32[]{:S(2)}, u32[]{:S(2)}) collective-permute-start(bf16[256,1024]{1,0:T(8,128)(2,1)S(1)} %collective-permute-done.19.refs_10_), channel_id=1, source_target_pairs={{0,16},{16,0},{1,17},{17,1},{2,18},{18,2},{3,19},{19,3},{4,20},{20... | collective-permute-start | bytes 1572872 | tf_op jit(solution)/shard_map/ppermute | solution.py:15
  25.1 33.7 %collective-permute-start.15 = (bf16[144,2048]{1,0:T(8,128)(2,1)S(1)}, bf16[144,2048]{1,0:T(8,128)(2,1)S(1)}, u32[]{:S(2)}, u32[]{:S(2)}) collective-permute-start(bf16[144,2048]{1,0:T(8,128)(2,1)S(1)} %get-tuple-element.57.refs_4_), channel_id=1, source_target_pairs={{0,1},{1,0},{2,3},{3,2},{4,5},{5,4},{6,7},{7,6},{8,9},{9,8},{10,11... | collective-permute-start | bytes 1769480 | tf_op jit(solution)/shard_map/ppermute | solution.py:15
  26.5 7.6 %collective-permute-start.8 = (bf16[400,128]{1,0:T(8,128)(2,1)S(1)}, bf16[400,128]{1,0:T(8,128)(2,1)S(1)}, u32[]{:S(2)}, u32[]{:S(2)}) collective-permute-start(bf16[400,128]{1,0:T(8,128)(2,1)S(1)} %get-tuple-element.42.after), channel_id=1, source_target_pairs={{0,8},{4,12},{8,0},{12,4},{1,9},{5,13},{9,1},{13,5},{2,10},{6,14},... | collective-permute-start | bytes 307208 | tf_op jit(solution)/shard_map/ppermute | solution.py:15
  34.2 3.5 %collective-permute-start.9 = (bf16[272,128]{1,0:T(8,128)(2,1)S(1)}, bf16[272,128]{1,0:T(8,128)(2,1)S(1)}, u32[]{:S(2)}, u32[]{:S(2)}) collective-permute-start(bf16[272,128]{1,0:T(8,128)(2,1)S(1)} %get-tuple-element.47.kv_ref.after), channel_id=1, source_target_pairs={{0,4},{4,0},{8,12},{12,8},{1,5},{5,1},{9,13},{13,9},{2,6},{6,2},{1... | collective-permute-start | bytes 208904 | tf_op jit(solution)/shard_map/ppermute | solution.py:15
  37.7 8.4 %collective-permute-start.7 = (bf16[128,512]{1,0:T(8,128)(2,1)S(1)}, bf16[128,512]{1,0:T(8,128)(2,1)S(1)}, u32[]{:S(2)}, u32[]{:S(2)}) collective-permute-start(bf16[128,512]{1,0:T(8,128)(2,1)S(1)} %get-tuple-element.44.after), channel_id=1, source_target_pairs={{0,8},{4,12},{8,0},{12,4},{1,9},{5,13},{9,1},{13,5},{2,10},{6,14},... | collective-permute-start | bytes 393224 | tf_op jit(solution)/shard_map/ppermute | solution.py:15
  39.6 26.6 %collective-permute-start.17 = (bf16[144,2048]{1,0:T(8,128)(2,1)S(1)}, bf16[144,2048]{1,0:T(8,128)(2,1)S(1)}, u32[]{:S(2)}, u32[]{:S(2)}) collective-permute-start(bf16[144,2048]{1,0:T(8,128)(2,1)S(1)} %collective-permute-done.16.refs_6_), channel_id=1, source_target_pairs={{0,1},{1,0},{2,3},{3,2},{4,5},{5,4},{6,7},{7,6},{8,9},{9,8},{10,11... | collective-permute-start | bytes 1769480 | tf_op jit(solution)/shard_map/ppermute | solution.py:15
  41.1 0.7 copy-start.3
  46.2 11.4 %copy-start.1 = (f32[31,256]{1,0:T(8,128)S(1)}, f32[31,256]{1,0:T(8,128)}, u32[]{:S(2)}) copy-start(f32[31,256]{1,0:T(8,128)} %taps_ref.1) | copy-start | bytes 95236
  46.2 4.5 %collective-permute-start.10 = (bf16[32,256]{1,0:T(8,128)(2,1)S(1)}, bf16[32,256]{1,0:T(8,128)(2,1)S(1)}, u32[]{:S(2)}, u32[]{:S(2)}) collective-permute-start(bf16[32,256]{1,0:T(8,128)(2,1)S(1)} %get-tuple-element.53), channel_id=1, source_target_pairs={{0,4},{4,8},{8,12},{1,5},{5,9},{9,13},{2,6},{6,10},{10,14},{3,7},{... | collective-permute-start | bytes 49160 | tf_op jit(solution)/shard_map/ppermute | solution.py:21
  50.7 3.6 %collective-permute-start.11 = (bf16[112,128]{1,0:T(8,128)(2,1)S(1)}, bf16[112,128]{1,0:T(8,128)(2,1)S(1)}, u32[]{:S(2)}, u32[]{:S(2)}) collective-permute-start(bf16[112,128]{1,0:T(8,128)(2,1)S(1)} %get-tuple-element.51.after), channel_id=1, source_target_pairs={{0,8},{4,12},{8,0},{12,4},{1,9},{5,13},{9,1},{13,5},{2,10},{6,14},... | collective-permute-start | bytes 86024 | tf_op jit(solution)/shard_map/ppermute | solution.py:15
  54.3 11.9 %collective-permute-start.21 = (bf16[256,1024]{1,0:T(8,128)(2,1)S(1)}, bf16[256,1024]{1,0:T(8,128)(2,1)S(1)}, u32[]{:S(2)}, u32[]{:S(2)}) collective-permute-start(bf16[256,1024]{1,0:T(8,128)(2,1)S(1)} %collective-permute-done.19.refs_10_), channel_id=1, source_target_pairs={{0,1},{1,0},{2,3},{3,2},{4,5},{5,4},{6,7},{7,6},{8,9},{9,8},{10,11... | collective-permute-start | bytes 1572872 | tf_op jit(solution)/shard_map/ppermute | solution.py:15
  57.5 8.7 %collective-permute-start.22 = (bf16[256,1024]{1,0:T(8,128)(2,1)S(1)}, bf16[256,1024]{1,0:T(8,128)(2,1)S(1)}, u32[]{:S(2)}, u32[]{:S(2)}) collective-permute-start(bf16[256,1024]{1,0:T(8,128)(2,1)S(1)} %collective-permute-done.20.refs_11_), channel_id=1, source_target_pairs={{0,1},{1,0},{2,3},{3,2},{4,5},{5,4},{6,7},{7,6},{8,9},{9,8},{10,11... | collective-permute-start | bytes 1572872 | tf_op jit(solution)/shard_map/ppermute | solution.py:15
  57.5 8.7 %copy-start.2 = (f32[2048]{0:T(1024)S(1)}, f32[2048]{0:T(1024)}, u32[]{:S(2)}) copy-start(f32[2048]{0:T(1024)} %param.29) | copy-start | bytes 24580
  58.7 3.9 %collective-permute-start.13 = (bf16[128,384]{1,0:T(8,128)(2,1)S(1)}, bf16[128,384]{1,0:T(8,128)(2,1)S(1)}, u32[]{:S(2)}, u32[]{:S(2)}) collective-permute-start(bf16[128,384]{1,0:T(8,128)(2,1)S(1)} %get-tuple-element.56.refs_0_), channel_id=1, source_target_pairs={{0,2},{1,3},{2,0},{3,1},{4,6},{5,7},{6,4},{7,5},{8,10},{9,11},{10,... | collective-permute-start | bytes 294920 | tf_op jit(solution)/shard_map/ppermute | solution.py:15
  62.6 2.3 %collective-permute-start.12 = (bf16[128,384]{1,0:T(8,128)(2,1)S(1)}, bf16[128,384]{1,0:T(8,128)(2,1)S(1)}, u32[]{:S(2)}, u32[]{:S(2)}) collective-permute-start(bf16[128,384]{1,0:T(8,128)(2,1)S(1)} %get-tuple-element.56.refs_0_), channel_id=1, source_target_pairs={{0,1},{1,0},{2,3},{3,2},{4,5},{5,4},{6,7},{7,6},{8,9},{9,8},{10,11... | collective-permute-start | bytes 294920 | tf_op jit(solution)/shard_map/ppermute | solution.py:15
  64.9 1.3 %collective-permute-start.14 = (bf16[128,384]{1,0:T(8,128)(2,1)S(1)}, bf16[128,384]{1,0:T(8,128)(2,1)S(1)}, u32[]{:S(2)}, u32[]{:S(2)}) collective-permute-start(bf16[128,384]{1,0:T(8,128)(2,1)S(1)} %collective-permute-done.13.refs_2_), channel_id=1, source_target_pairs={{0,1},{1,0},{2,3},{3,2},{4,5},{5,4},{6,7},{7,6},{8,9},{9,8},{10,11... | collective-permute-start | bytes 294920 | tf_op jit(solution)/shard_map/ppermute | solution.py:15

commit v7 on v5

--- a/solution.py
+++ b/solution.py
@@ -51,33 +51,40 @@
     return [pltpu.with_memory_space_constraint(v, pltpu.HBM) for v in values]
 
 
-def pack_qkv_kernel(wq, wk, wv, all_ref, send_ref, sems):
-    part = send_ref.shape[0]
-    width = wq.shape[1]
-    mine = pl.ds(pl.multiple_of(lax.axis_index("grp") * part, part), part)
+def pack_qkv_kernel(wq, wk, wv, wc, all_ref, send_ref, wc_ref, sems):
+    part, width = send_ref.shape[0], wq.shape[1]
+    group = lax.axis_index("grp")
+    mine = pl.ds(pl.multiple_of(group * part, part), part)
+    columns = wc_ref.shape[1]
     first, rest = [], []
     for n, w in enumerate((wq, wk, wv)):
         at = slice(n * width, (n + 1) * width)
         first.append(pltpu.make_async_copy(w.at[mine, :], send_ref.at[:, at], sems.at[n]))
         rest.append(pltpu.make_async_copy(w, all_ref.at[:, at], sems.at[3 + n]))
+    half = wc.at[:, pl.ds(pl.multiple_of(group * columns, columns), columns)]
+    rest.append(pltpu.make_async_copy(half, wc_ref, sems.at[6]))
     for copy in first + rest:
         copy.start()
     for copy in first + rest:
         copy.wait()
 
 
-def pack_qkv(weights):
+def pack_qkv(weights, wc):
     block, width = weights[0].shape
     return pl.pallas_call(
         pack_qkv_kernel,
-        out_shape=(shape((block, 3 * width)), shape((block // 2, 3 * width))),
-        in_specs=[HBM] * 3,
-        out_specs=[VM] * 2,
-        scratch_shapes=[pltpu.SemaphoreType.DMA((6,))],
+        out_shape=(
+            shape((block, 3 * width)),
+            shape((block // 2, 3 * width)),
+            shape((wc.shape[0], wc.shape[1] // 2)),
+        ),
+        in_specs=[HBM] * 4,
+        out_specs=[VM] * 3,
+        scratch_shapes=[pltpu.SemaphoreType.DMA((7,))],
         cost_estimate=cost(2_000_000, 400_000),
         compiler_params=params(),
         name="pack_qkv",
-    )(*in_hbm(*weights))
+    )(*in_hbm(*weights, wc))
 
 
 def norm_kernel(x_hbm, gain_hbm, send_ref, own_ref, pair_ref, x_ref, gain_ref, normed, sems):
@@ -123,21 +130,27 @@
     )(*in_hbm(tokens, gain.reshape(1, features)))
 
 
-def pack_kernel(gv_hbm, gg_hbm, wa_hbm, off_hbm, gain_hbm, bias_hbm, glu_ref, out_ref, off_ref, gain_ref, bias_ref, sems):
+def pack_kernel(
+    gv_hbm, gg_hbm, wa_hbm, off_hbm, head_hbm, gain_hbm, bias_hbm, *refs
+):
+    gv_ref, gv_send, gg_ref, out_ref, off_ref, head_ref, gain_ref, bias_ref, sems = refs
     cw, aw = gv_hbm.shape[1], wa_hbm.shape[0]
-    copies = [
-        pltpu.make_async_copy(gv_hbm, glu_ref.at[:, :cw], sems.at[0]),
-        pltpu.make_async_copy(gg_hbm, glu_ref.at[:, cw:], sems.at[1]),
-        pltpu.make_async_copy(wa_hbm, out_ref.at[:aw, :], sems.at[2]),
-        pltpu.make_async_copy(off_hbm, off_ref, sems.at[5]),
-    ]
-    small = [
-        pltpu.make_async_copy(gain_hbm, gain_ref, sems.at[3]),
-        pltpu.make_async_copy(bias_hbm, bias_ref, sems.at[4]),
-    ]
-    for copy in small + copies:
+    part = gv_send.shape[0]
+    mine = pl.ds(pl.multiple_of(lax.axis_index("grp") * part, part), part)
+    pairs = (
+        (gain_hbm, gain_ref),
+        (bias_hbm, bias_ref),
+        (gv_hbm.at[mine, :], gv_send),
+        (gg_hbm, gg_ref),
+        (wa_hbm, out_ref.at[:aw, :]),
+        (off_hbm, off_ref),
+        (head_hbm, head_ref),
+        (gv_hbm, gv_ref),
+    )
+    copies = [pltpu.make_async_copy(a, b, sems.at[n]) for n, (a, b) in enumerate(pairs)]
+    for copy in copies:
         copy.start()
-    for copy in small:
+    for copy in copies[:2]:
         copy.wait()
     extra = out_ref.shape[0] - aw
     for n, ref in enumerate((gain_ref, bias_ref)):
@@ -147,27 +160,34 @@
             rest = rest - part.astype(F32)
             first = (3 * n + piece) * cw
             out_ref[aw:, first : first + cw] = jnp.broadcast_to(part, (extra, cw))
-    for copy in copies:
+    for copy in copies[2:]:
         copy.wait()
 
 
-def pack(gv, gg, wa, off, gain, bias):
+def pack(gv, gg, wa, off, head_gain, gain, bias):
     block, cw = gv.shape
     aw, width = wa.shape
     return pl.pallas_call(
         pack_kernel,
-        out_shape=(shape((block, 2 * cw)), shape((aw + 16, width)), shape(off.shape)),
-        in_specs=[HBM] * 6,
-        out_specs=[VM] * 3,
+        out_shape=(
+            shape((block, cw)),
+            shape((block // 2, cw)),
+            shape((block, cw)),
+            shape((aw + 16, width)),
+            shape(off.shape),
+            shape(head_gain.shape, F32),
+        ),
+        in_specs=[HBM] * 7,
+        out_specs=[VM] * 6,
         scratch_shapes=[
             pltpu.VMEM((1, cw), F32),
             pltpu.VMEM((1, cw), F32),
-            pltpu.SemaphoreType.DMA((6,)),
+            pltpu.SemaphoreType.DMA((8,)),
         ],
         cost_estimate=cost(2_000_000, 2_000_000),
         compiler_params=params(),
         name="pack",
-    )(*in_hbm(gv, gg, wa, off, gain.reshape(1, cw), bias.reshape(1, cw)))
+    )(*in_hbm(gv, gg, wa, off, head_gain, gain.reshape(1, cw), bias.reshape(1, cw)))
 
 
 def assemble_kernel(own_ref, pair_ref, got_ref, other_ref, own_out, pair_out):
@@ -262,24 +282,29 @@
     )(keep, got, sent, after)
 
 
-def glu_kernel(x_own, x_pair, own, pair, after, keep_ref, send_ref):
+def glu_kernel(x_own, x_pair, gv, gg, gv_same, gv_other, gg_pair, after, keep_ref, send_ref):
     rows = x_own.shape[0] // 2
-    total = dot_f32(x_own[...], own[...]) + dot_f32(x_pair[...], pair[...])
-    keep_ref[...] = total[:rows]
-    send_ref[...] = total[rows:].astype(BF16)
+    cw = gv.shape[1]
+    for n in range(2):
+        own = (gv, gg)[n]
+        far = far_dot(x_pair, gv_same, gv_other) if n == 0 else dot_f32(x_pair[...], gg_pair[...])
+        total = dot_f32(x_own[...], own[...]) + far
+        at = slice(n * cw, (n + 1) * cw)
+        keep_ref[:, at] = total[:rows]
+        send_ref[:, at] = total[rows:].astype(BF16)
 
 
 def project_glu(x_own, x_pair, own, pair, after):
-    rows, width = x_own.shape[0] // 2, pair.shape[1]
+    rows, width = x_own.shape[0] // 2, 2 * own[0].shape[1]
     return pl.pallas_call(
         glu_kernel,
         out_shape=(shape((rows, width), F32), shape((rows, width))),
-        in_specs=[VM] * 4 + [ANY],
+        in_specs=[VM] * 7 + [ANY],
         out_specs=[VM] * 2,
-        cost_estimate=cost(270_000_000, 1_500_000),
+        cost_estimate=cost(270_000_000, 1_000_000),
         compiler_params=params(),
         name="project_glu",
-    )(x_own, x_pair, own, pair, after)
+    )(x_own, x_pair, *own, *pair, after)
 
 
 def gate_kernel(keep_ref, got_ref, gated_ref, tail_ref):
@@ -483,8 +508,7 @@
 
 
 def final_kernel(*refs):
-    act, wa, wc = (refs[n * 4 : (n + 1) * 4] for n in range(3))
-    gain_ref, out_ref = refs[12:]
+    act, wa, wc, gain_ref, out_ref = refs[:4], refs[4:8], refs[8:14], refs[14], refs[15]
     cw = wc[0].shape[0]
     aw = act[0].shape[1] - cw
     convs = [c[:, aw:].astype(F32) for c in act]
@@ -493,14 +517,22 @@
     spread = sum(jnp.sum(v * v, axis=1, keepdims=True) for v in centered) / (4 * cw)
     inverse = lax.rsqrt(spread + norm_eps)
     total = None
+    ys = []
     for slot in range(4):
         pieces = [wa[slot][aw : aw + 1, n * cw : (n + 1) * cw].astype(F32) for n in range(6)]
         gain = pieces[0] + pieces[1] + pieces[2]
         bias = pieces[3] + pieces[4] + pieces[5]
         y = centered[slot] * inverse * gain + bias
         y = (y * jax.nn.sigmoid(y)).astype(BF16)
-        part = dot_f32(act[slot][:, :aw], wa[slot][:aw, :]) + dot_f32(y, wc[slot][...])
+        part = dot_f32(act[slot][:, :aw], wa[slot][:aw, :])
+        if slot < 2:
+            part = part + dot_f32(y, wc[slot][...])
         total = part if total is None else total + part
+        ys.append(y)
+    same = dot_f32(ys[2], wc[2][...]) + dot_f32(ys[3], wc[4][...])
+    other = dot_f32(ys[2], wc[3][...]) + dot_f32(ys[3], wc[5][...])
+    swap = lax.axis_index("grp") == 1
+    total = total + jnp.concatenate([jnp.where(swap, other, same), jnp.where(swap, same, other)], axis=1)
     squares = jnp.mean(total * total, axis=1, keepdims=True)
     out_ref[...] = (total * lax.rsqrt(squares + norm_eps) * gain_ref[...]).astype(BF16)
 
@@ -510,7 +542,7 @@
     return pl.pallas_call(
         final_kernel,
         out_shape=shape((rows, width)),
-        in_specs=[VM] * 13,
+        in_specs=[VM] * 15,
         out_specs=VM,
         cost_estimate=cost(800_000_000, 7_000_000),
         compiler_params=params(32),
@@ -535,15 +567,20 @@
     w_out_conv,
     out_gain,
 ):
-    own_qkv, half_qkv = pack_qkv((w_query, w_key, w_value))
+    own_qkv, half_qkv, wc_half = pack_qkv((w_query, w_key, w_value), w_out_conv)
     qkv_same = exchange(half_qkv, "sp", 1)
-    wc_x = exchange(w_out_conv, "tp", 2)
+    wc_x = exchange(wc_half, "tp", 2)
+    wc_y = exchange(wc_x, "grp", 1)
+    wc_yc = exchange(wc_y, "tp", 1)
     x_send, mine_own, mine_pair = norm_parts(tokens, norm_gain, w_query.shape[0])
     x_got = exchange(x_send, "sp", 2)
-    own_glu, wa_mine, off = pack(
-        w_glu_value, w_glu_gate, w_out_attn, key_offset.T, channel_gain, channel_bias
-    )
-    glu_pair = exchange(own_glu, "sp", 1)
+    own_gv, half_gv, own_gg, wa_mine, off, head_rows = pack(
+        w_glu_value, w_glu_gate, w_out_attn, key_offset.T, head_gain, channel_gain, channel_bias
+    )
+    qkv_same, half_gv = lax.optimization_barrier((qkv_same, half_gv))
+    gv_same = exchange(half_gv, "sp", 1)
+    gg_pair = exchange(own_gg, "sp", 1)
+    gv_other = exchange(gv_same, "grp", 1)
     qkv_other = exchange(qkv_same, "grp", 1)
     x_other = exchange(x_got, "tp", 1)
     wa_x = exchange(wa_mine, "tp", 2)
@@ -555,18 +592,22 @@
 
     keep, sent = project_qkv(x_own, x_pair, own_qkv, qkv_same, qkv_other, off)
     got = exchange(sent, "sp", 2)
-    glu_keep, glu_sent = project_glu(x_own, x_pair, own_glu, glu_pair, sent)
+    glu_keep, glu_sent = project_glu(
+        x_own, x_pair, (own_gv, own_gg), (gv_same, gv_other, gg_pair), sent
+    )
     glu_got = exchange(glu_sent, "sp", 2)
     q, mine_two = sum_qkv(keep, got, sent, glu_sent)
     pair_two = exchange(mine_two, "sp", 1)
-    near = near_attention(q, mine_two, head_gain, mine_two)
+    near = near_attention(q, mine_two, head_rows, mine_two)
     gated, tail = gate(glu_keep, glu_got, -(-conv_taps.shape[0] // 16) * 16)
     before = from_behind(tail, "sp", 1)
-    attended, log_mass = attention(q, pair_two, head_gain, near, tail)
+    attended, log_mass = attention(q, pair_two, head_rows, near, tail)
     act_mine = conv(gated, before, conv_taps, attended)
-    act = [act_mine] + [exchange(act_mine, "tp", bit) for bit in (1, 2, 3)]
+    act_x = exchange(act_mine, "tp", 2)
+    act_core = exchange(act_mine, "tp", 1)
+    act = (act_mine, act_core, act_x, exchange(act_x, "tp", 1))
     wa = (wa_mine, wa_core, wa_x, wa_xc)
-    wc = (w_out_conv, wc_core, wc_x, wc_xc)
+    wc = (w_out_conv, wc_core, wc_x, wc_y, wc_xc, wc_yc)
     mixed = finish(act, wa, wc, out_gain)
     return (mixed, log_mass)
 

time: 76.9 us -> 75.1 us (0.977)
  the two profiles are of different devices: /device:TPU:0 before, /device:TPU:25 now
where the time goes in v7:
time: 75.1 us; the launch traced here: 74 us
  waiting for transfers between devices  49.2 us (66%)
  starting transfers between devices  13.3 us (18%)
  Pallas kernels  10.8 us (14%)
  between operations  0.82 us (1%)
    ppermute x21, waiting for transfers between devices, exchange(): return lax.ppermute(value, axis, [(s, s ^ bit) for s in range(count)])  45.5 us
    ppermute x21, starting transfers between devices, exchange(): return lax.ppermute(value, axis, [(s, s ^ bit) for s in range(count)])  12 us
    ppermute x1, waiting for transfers between devices, from_behind(): lax.ppermute(value, axis, [(source, source + steps) for source in range(i...  3.69 us
    pallas_call x1, Pallas kernels, finish(): pl.pallas_call(final_kernel, out_shape=shape((rows, width)), in_specs=[VM...  2.49 us
    pallas_call x1, Pallas kernels, attention(): pl.pallas_call(attention_kernel, out_shape=(shape((rows, width)), shape((...  1.87 us
  transfers between devices with their start and end apart: 22, of which 8 were waited for; matrix products, arithmetic and copies ran while one was open for 0% of the time, Pallas kernels for 9%

profile of v7, /device:TPU:25, one launch (start us, length us, event | category | flops | bytes accessed | tf_op | source)
XLA Modules:
  0.0 74.0 jit_solution(603784633763286540)
XLA Ops:
  0.6 1.4 %pack_qkv.1 = (bf16[512,384]{1,0:T(8,128)(2,1)S(1)}, bf16[256,384]{1,0:T(8,128)(2,1)S(1)}, bf16[256,1024]{1,0:T(8,128)(2,1)S(1)}) custom-call(bf16[512,128]{1,0:T(8,128)(2,1)} %wq.1, bf16[512,128]{1,0:T(8,128)(2,1)} %wk.1, bf16[512,128]{1,0:T(8,128)(2,1)} %wv.1, bf16[256,2048]{1,0:T(8,128)(2,1)} %refs_8_.1), custom_call_target="tpu_custom_call" | custom-call | flops 2000000 | bytes 400000 | tf_op jit(solution)/shard_map/pack_qkv/pallas_call | solution.py:74
  2.1 1.3 %collective-permute-start.18 = (bf16[256,1024]{1,0:T(8,128)(2,1)S(1)}, bf16[256,1024]{1,0:T(8,128)(2,1)S(1)}, u32[]{:S(2)}, u32[]{:S(2)}) collective-permute-start(bf16[256,1024]{1,0:T(8,128)(2,1)S(1)} %get-tuple-element.58), channel_id=1, source_target_pairs={{0,2},{1,3},{2,0},{3,1},{4,6},{5,7},{6,4},{7,5},{8,10},{9,11},{10,... | collective-permute-start | bytes 1572872 | tf_op jit(solution)/shard_map/ppermute | solution.py:15
  3.3 1.3 %norm_parts.1 = (bf16[64,1024]{1,0:T(8,128)(2,1)S(1)}, bf16[128,512]{1,0:T(8,128)(2,1)S(1)}, bf16[128,512]{1,0:T(8,128)(2,1)S(1)}) custom-call(bf16[128,2048]{1,0:T(8,128)(2,1)} %x_hbm.1, f32[1,2048]{1,0:T(1,128)} %bitcast.6), custom_call_target="tpu_custom_call" | custom-call | flops 2000000 | bytes 1000000 | tf_op jit(solution)/shard_map/norm_parts/pallas_call | solution.py:116
  5.0 8.8 %collective-permute-done.got_ref = bf16[64,1024]{1,0:T(8,128)(2,1)S(1)} collective-permute-done((bf16[64,1024]{1,0:T(8,128)(2,1)S(1)}, bf16[64,1024]{1,0:T(8,128)(2,1)S(1)}, u32[]{:S(2)}, u32[]{:S(2)}) %collective-permute-start) | collective-permute-done | bytes 131104 | tf_op jit(solution)/shard_map/ppermute | solution.py:15
  13.8 0.5 collective-permute-start.1
  14.3 1.4 %pack.1 = (bf16[512,256]{1,0:T(8,128)(2,1)S(1)}, bf16[256,256]{1,0:T(8,128)(2,1)S(1)}, bf16[512,256]{1,0:T(8,128)(2,1)S(1)}, bf16[144,2048]{1,0:T(8,128)(2,1)S(1...) custom-call(bf16[512,256]{1,0:T(8,128)(2,1)} %gv_hbm.1, bf16[512,256]{1,0:T(8,128)(2,1)} %gg_hbm.1, ...), custom_call_target="tpu_custom_call" | custom-call | flops 2000000 | bytes 2000000 | tf_op jit(solution)/shard_map/pack/pallas_call | solution.py:170
  15.8 1.3 %collective-permute-start.6 = (bf16[256,384]{1,0:T(8,128)(2,1)S(1)}, bf16[256,384]{1,0:T(8,128)(2,1)S(1)}, u32[]{:S(2)}, u32[]{:S(2)}) collective-permute-start(bf16[256,384]{1,0:T(8,128)(2,1)S(1)} %collective-permute-done.2.same), channel_id=1, source_target_pairs={{0,16},{16,0},{1,17},{17,1},{2,18},{18,2},{3,19},{19,3},{4,20},{20... | collective-permute-start | bytes 589832 | tf_op jit(solution)/shard_map/ppermute | solution.py:15
  17.1 0.3 collective-permute-start.15
  17.4 1.4 %collective-permute-start.3 = (bf16[256,256]{1,0:T(8,128)(2,1)S(1)}, bf16[256,256]{1,0:T(8,128)(2,1)S(1)}, u32[]{:S(2)}, u32[]{:S(2)}) collective-permute-start(bf16[256,256]{1,0:T(8,128)(2,1)S(1)} %get-tuple-element.40), channel_id=1, source_target_pairs={{0,4},{4,0},{8,12},{12,8},{1,5},{5,1},{9,13},{13,9},{2,6},{6,2},{1... | collective-permute-start | bytes 393224 | tf_op jit(solution)/shard_map/ppermute | solution.py:15
  18.8 7.7 %collective-permute-done.3.gv_same = bf16[256,256]{1,0:T(8,128)(2,1)S(1)} collective-permute-done((bf16[256,256]{1,0:T(8,128)(2,1)S(1)}, bf16[256,256]{1,0:T(8,128)(2,1)S(1)}, u32[]{:S(2)}, u32[]{:S(2)}) %collective-permute-start.3) | collective-permute-done | bytes 131104 | tf_op jit(solution)/shard_map/ppermute | solution.py:15
  26.5 0.9 %collective-permute-start.17 = (bf16[256,2048]{1,0:T(8,128)(2,1)S(1)}, bf16[256,2048]{1,0:T(8,128)(2,1)S(1)}, u32[]{:S(2)}, u32[]{:S(2)}) collective-permute-start(bf16[256,2048]{1,0:T(8,128)(2,1)S(1)} %copy-done), channel_id=1, source_target_pairs={{0,1},{1,0},{2,3},{3,2},{4,5},{5,4},{6,7},{7,6},{8,9},{9,8},{10,11... | collective-permute-start | bytes 3145736 | tf_op jit(solution)/shard_map/ppermute | solution.py:15
  27.3 1.2 %collective-permute-start.19 = (bf16[256,1024]{1,0:T(8,128)(2,1)S(1)}, bf16[256,1024]{1,0:T(8,128)(2,1)S(1)}, u32[]{:S(2)}, u32[]{:S(2)}) collective-permute-start(bf16[256,1024]{1,0:T(8,128)(2,1)S(1)} %collective-permute-done.18.refs_10_), channel_id=1, source_target_pairs={{0,16},{16,0},{1,17},{17,1},{2,18},{18,2},{3,19},{19,3},{4,20},{20... | collective-permute-start | bytes 1572872 | tf_op jit(solution)/shard_map/ppermute | solution.py:15
  28.6 0.2 collective-permute-start.4
  28.8 0.4 project_qkv.1
  29.4 14.2 %collective-permute-done.4.gv_other = bf16[256,256]{1,0:T(8,128)(2,1)S(1)} collective-permute-done((bf16[256,256]{1,0:T(8,128)(2,1)S(1)}, bf16[256,256]{1,0:T(8,128)(2,1)S(1)}, u32[]{:S(2)}, u32[]{:S(2)}) %collective-permute-start.4) | collective-permute-done | bytes 131104 | tf_op jit(solution)/shard_map/ppermute | solution.py:15
  43.5 0.9 %collective-permute-start.14 = (bf16[144,2048]{1,0:T(8,128)(2,1)S(1)}, bf16[144,2048]{1,0:T(8,128)(2,1)S(1)}, u32[]{:S(2)}, u32[]{:S(2)}) collective-permute-start(bf16[144,2048]{1,0:T(8,128)(2,1)S(1)} %get-tuple-element.57.refs_4_), channel_id=1, source_target_pairs={{0,1},{1,0},{2,3},{3,2},{4,5},{5,4},{6,7},{7,6},{8,9},{9,8},{10,11... | collective-permute-start | bytes 1769480 | tf_op jit(solution)/shard_map/ppermute | solution.py:15
  44.5 0.4 project_glu.1
  45.0 8.8 %collective-permute-done.7.got_ref = bf16[128,512]{1,0:T(8,128)(2,1)S(1)} collective-permute-done((bf16[128,512]{1,0:T(8,128)(2,1)S(1)}, bf16[128,512]{1,0:T(8,128)(2,1)S(1)}, u32[]{:S(2)}, u32[]{:S(2)}) %collective-permute-start.7) | collective-permute-done | bytes 131104 | tf_op jit(solution)/shard_map/ppermute | solution.py:15
  54.0 1.3 %collective-permute-start.8 = (bf16[32,256]{1,0:T(8,128)(2,1)S(1)}, bf16[32,256]{1,0:T(8,128)(2,1)S(1)}, u32[]{:S(2)}, u32[]{:S(2)}) collective-permute-start(bf16[32,256]{1,0:T(8,128)(2,1)S(1)} %get-tuple-element.48.after), channel_id=1, source_target_pairs={{0,4},{4,8},{8,12},{1,5},{5,9},{9,13},{2,6},{6,10},{10,14},{3,7},{... | collective-permute-start | bytes 49160 | tf_op jit(solution)/shard_map/ppermute | solution.py:21
  55.3 3.7 %collective-permute-done.8.before_ref = bf16[32,256]{1,0:T(8,128)(2,1)S(1)} collective-permute-done((bf16[32,256]{1,0:T(8,128)(2,1)S(1)}, bf16[32,256]{1,0:T(8,128)(2,1)S(1)}, u32[]{:S(2)}, u32[]{:S(2)}) %collective-permute-start.8) | collective-permute-done | bytes 16416 | tf_op jit(solution)/shard_map/ppermute | solution.py:21
  59.0 1.3 %collective-permute-start.16 = (bf16[144,2048]{1,0:T(8,128)(2,1)S(1)}, bf16[144,2048]{1,0:T(8,128)(2,1)S(1)}, u32[]{:S(2)}, u32[]{:S(2)}) collective-permute-start(bf16[144,2048]{1,0:T(8,128)(2,1)S(1)} %collective-permute-done.15.refs_6_), channel_id=1, source_target_pairs={{0,1},{1,0},{2,3},{3,2},{4,5},{5,4},{6,7},{7,6},{8,9},{9,8},{10,11... | collective-permute-start | bytes 1769480 | tf_op jit(solution)/shard_map/ppermute | solution.py:15
  60.3 0.5 collective-permute-start.21
  60.8 0.7 near_attention.1
  61.5 1.9 %stick_attention.1 = (bf16[128,128]{1,0:T(8,128)(2,1)S(1)}, f32[2,128]{1,0:T(2,128)}) custom-call(bf16[128,128]{1,0:T(8,128)(2,1)S(1)} %get-tuple-element.50.q_ref, bf16[528,128]{1,0:T(8,128)(2,1)S(1)} %collective-permute-done.10.pair_ref, f32[2,64]{1,0:T(2,128)S(1)} %get-tuple-element.52.gain_ref, f32[2,128,128]{2,1,0:T(8,128)S(1)} %get-tuple-element.53.mix_ref, ...), custom_call_target="tpu_custom_call" | custom-call | flops 400000000 | bytes 1000000 | tf_op jit(solution)/shard_map/stick_attention/pallas_call | solution.py:494
  63.4 0.6 conv.1.refs_0_
  64.0 0.3 collective-permute-start.12
  64.3 4.0 %collective-permute-done.12.refs_2_ = bf16[128,384]{1,0:T(8,128)(2,1)S(1)} collective-permute-done((bf16[128,384]{1,0:T(8,128)(2,1)S(1)}, bf16[128,384]{1,0:T(8,128)(2,1)S(1)}, u32[]{:S(2)}, u32[]{:S(2)}) %collective-permute-start.12) | collective-permute-done | bytes 98336 | tf_op jit(solution)/shard_map/ppermute | solution.py:15
  68.3 0.9 %collective-permute-start.11 = (bf16[128,384]{1,0:T(8,128)(2,1)S(1)}, bf16[128,384]{1,0:T(8,128)(2,1)S(1)}, u32[]{:S(2)}, u32[]{:S(2)}) collective-permute-start(bf16[128,384]{1,0:T(8,128)(2,1)S(1)} %conv.1.refs_0_), channel_id=1, source_target_pairs={{0,1},{1,0},{2,3},{3,2},{4,5},{5,4},{6,7},{7,6},{8,9},{9,8},{10,11... | collective-permute-start | bytes 294920 | tf_op jit(solution)/shard_map/ppermute | solution.py:15
  69.3 0.9 %collective-permute-done.11.refs_1_ = bf16[128,384]{1,0:T(8,128)(2,1)S(1)} collective-permute-done((bf16[128,384]{1,0:T(8,128)(2,1)S(1)}, bf16[128,384]{1,0:T(8,128)(2,1)S(1)}, u32[]{:S(2)}, u32[]{:S(2)}) %collective-permute-start.11) | collective-permute-done | bytes 98336 | tf_op jit(solution)/shard_map/ppermute | solution.py:15
  70.2 0.4 collective-permute-start.13
  70.6 0.9 %collective-permute-done.13.refs_3_ = bf16[128,384]{1,0:T(8,128)(2,1)S(1)} collective-permute-done((bf16[128,384]{1,0:T(8,128)(2,1)S(1)}, bf16[128,384]{1,0:T(8,128)(2,1)S(1)}, u32[]{:S(2)}, u32[]{:S(2)}) %collective-permute-start.13) | collective-permute-done | bytes 98336 | tf_op jit(solution)/shard_map/ppermute | solution.py:15
  71.5 2.5 %finish_rows.1 = bf16[128,2048]{1,0:T(8,128)(2,1)} custom-call(bf16[128,384]{1,0:T(8,128)(2,1)S(1)} %conv.1.refs_0_, bf16[128,384]{1,0:T(8,128)(2,1)S(1)} %collective-permute-done.11.refs_1_, bf16[128,384]{1,0:T(8,128)(2,1)S(1)} %collective-permute-done.12.refs_2_, bf16[128,384]{1,0:T(8,128)(2,1)S(1)} %collective-permute-done.13.refs_3_, ...), custom_call_target="tpu_custom_call" | custom-call | flops 800000000 | bytes 7000000 | tf_op jit(solution)/shard_map/finish_rows/pallas_call | solution.py:542
  (30 shorter events, 0.7 us)
Async XLA Ops:
  2.1 24.4 %copy-start = (bf16[256,2048]{1,0:T(8,128)(2,1)S(1)}, bf16[256,2048]{1,0:T(8,128)(2,1)}, u32[]{:S(2)}) copy-start(bf16[256,2048]{1,0:T(8,128)(2,1)} %refs_8_.1) | copy-start | bytes 3145732
  2.1 25.3 %collective-permute-start.18 = (bf16[256,1024]{1,0:T(8,128)(2,1)S(1)}, bf16[256,1024]{1,0:T(8,128)(2,1)S(1)}, u32[]{:S(2)}, u32[]{:S(2)}) collective-permute-start(bf16[256,1024]{1,0:T(8,128)(2,1)S(1)} %get-tuple-element.58), channel_id=1, source_target_pairs={{0,2},{1,3},{2,0},{3,1},{4,6},{5,7},{6,4},{7,5},{8,10},{9,11},{10,... | collective-permute-start | bytes 1572872 | tf_op jit(solution)/shard_map/ppermute | solution.py:15
  4.7 9.1 %collective-permute-start = (bf16[64,1024]{1,0:T(8,128)(2,1)S(1)}, bf16[64,1024]{1,0:T(8,128)(2,1)S(1)}, u32[]{:S(2)}, u32[]{:S(2)}) collective-permute-start(bf16[64,1024]{1,0:T(8,128)(2,1)S(1)} %get-tuple-element.33), channel_id=1, source_target_pairs={{0,8},{4,12},{8,0},{12,4},{1,9},{5,13},{9,1},{13,5},{2,10},{6,14},... | collective-permute-start | bytes 393224 | tf_op jit(solution)/shard_map/ppermute | solution.py:15
  4.8 11.0 %collective-permute-start.2 = (bf16[256,384]{1,0:T(8,128)(2,1)S(1)}, bf16[256,384]{1,0:T(8,128)(2,1)S(1)}, u32[]{:S(2)}, u32[]{:S(2)}) collective-permute-start(bf16[256,384]{1,0:T(8,128)(2,1)S(1)} %get-tuple-element.38), channel_id=1, source_target_pairs={{0,4},{4,0},{8,12},{12,8},{1,5},{5,1},{9,13},{13,9},{2,6},{6,2},{1... | collective-permute-start | bytes 589832 | tf_op jit(solution)/shard_map/ppermute | solution.py:15
  13.8 3.6 %collective-permute-start.1 = (bf16[64,1024]{1,0:T(8,128)(2,1)S(1)}, bf16[64,1024]{1,0:T(8,128)(2,1)S(1)}, u32[]{:S(2)}, u32[]{:S(2)}) collective-permute-start(bf16[64,1024]{1,0:T(8,128)(2,1)S(1)} %collective-permute-done.got_ref), channel_id=1, source_target_pairs={{0,1},{1,0},{2,3},{3,2},{4,5},{5,4},{6,7},{7,6},{8,9},{9,8},{10,11... | collective-permute-start | bytes 393224 | tf_op jit(solution)/shard_map/ppermute | solution.py:15
  15.7 13.5 %collective-permute-start.5 = (bf16[512,256]{1,0:T(8,128)(2,1)S(1)}, bf16[512,256]{1,0:T(8,128)(2,1)S(1)}, u32[]{:S(2)}, u32[]{:S(2)}) collective-permute-start(bf16[512,256]{1,0:T(8,128)(2,1)S(1)} %get-tuple-element.37.gg), channel_id=1, source_target_pairs={{0,4},{4,0},{8,12},{12,8},{1,5},{5,1},{9,13},{13,9},{2,6},{6,2},{1... | collective-permute-start | bytes 786440 | tf_op jit(solution)/shard_map/ppermute | solution.py:15
  15.8 12.8 %collective-permute-start.6 = (bf16[256,384]{1,0:T(8,128)(2,1)S(1)}, bf16[256,384]{1,0:T(8,128)(2,1)S(1)}, u32[]{:S(2)}, u32[]{:S(2)}) collective-permute-start(bf16[256,384]{1,0:T(8,128)(2,1)S(1)} %collective-permute-done.2.same), channel_id=1, source_target_pairs={{0,16},{16,0},{1,17},{17,1},{2,18},{18,2},{3,19},{19,3},{4,20},{20... | collective-permute-start | bytes 589832 | tf_op jit(solution)/shard_map/ppermute | solution.py:15
  17.1 36.8 %collective-permute-start.15 = (bf16[144,2048]{1,0:T(8,128)(2,1)S(1)}, bf16[144,2048]{1,0:T(8,128)(2,1)S(1)}, u32[]{:S(2)}, u32[]{:S(2)}) collective-permute-start(bf16[144,2048]{1,0:T(8,128)(2,1)S(1)} %get-tuple-element.57.refs_4_), channel_id=1, source_target_pairs={{0,2},{1,3},{2,0},{3,1},{4,6},{5,7},{6,4},{7,5},{8,10},{9,11},{10,... | collective-permute-start | bytes 1769480 | tf_op jit(solution)/shard_map/ppermute | solution.py:15
  17.4 9.1 %collective-permute-start.3 = (bf16[256,256]{1,0:T(8,128)(2,1)S(1)}, bf16[256,256]{1,0:T(8,128)(2,1)S(1)}, u32[]{:S(2)}, u32[]{:S(2)}) collective-permute-start(bf16[256,256]{1,0:T(8,128)(2,1)S(1)} %get-tuple-element.40), channel_id=1, source_target_pairs={{0,4},{4,0},{8,12},{12,8},{1,5},{5,1},{9,13},{13,9},{2,6},{6,2},{1... | collective-permute-start | bytes 393224 | tf_op jit(solution)/shard_map/ppermute | solution.py:15
  26.5 45.0 %collective-permute-start.17 = (bf16[256,2048]{1,0:T(8,128)(2,1)S(1)}, bf16[256,2048]{1,0:T(8,128)(2,1)S(1)}, u32[]{:S(2)}, u32[]{:S(2)}) collective-permute-start(bf16[256,2048]{1,0:T(8,128)(2,1)S(1)} %copy-done), channel_id=1, source_target_pairs={{0,1},{1,0},{2,3},{3,2},{4,5},{5,4},{6,7},{7,6},{8,9},{9,8},{10,11... | collective-permute-start | bytes 3145736 | tf_op jit(solution)/shard_map/ppermute | solution.py:15
  27.3 32.9 %collective-permute-start.19 = (bf16[256,1024]{1,0:T(8,128)(2,1)S(1)}, bf16[256,1024]{1,0:T(8,128)(2,1)S(1)}, u32[]{:S(2)}, u32[]{:S(2)}) collective-permute-start(bf16[256,1024]{1,0:T(8,128)(2,1)S(1)} %collective-permute-done.18.refs_10_), channel_id=1, source_target_pairs={{0,16},{16,0},{1,17},{17,1},{2,18},{18,2},{3,19},{19,3},{4,20},{20... | collective-permute-start | bytes 1572872 | tf_op jit(solution)/shard_map/ppermute | solution.py:15
  28.6 15.0 %collective-permute-start.4 = (bf16[256,256]{1,0:T(8,128)(2,1)S(1)}, bf16[256,256]{1,0:T(8,128)(2,1)S(1)}, u32[]{:S(2)}, u32[]{:S(2)}) collective-permute-start(bf16[256,256]{1,0:T(8,128)(2,1)S(1)} %collective-permute-done.3.gv_same), channel_id=1, source_target_pairs={{0,16},{16,0},{1,17},{17,1},{2,18},{18,2},{3,19},{19,3},{4,20},{20... | collective-permute-start | bytes 393224 | tf_op jit(solution)/shard_map/ppermute | solution.py:15
  29.3 15.6 %collective-permute-start.9 = (bf16[656,128]{1,0:T(8,128)(2,1)S(1)}, bf16[656,128]{1,0:T(8,128)(2,1)S(1)}, u32[]{:S(2)}, u32[]{:S(2)}) collective-permute-start(bf16[656,128]{1,0:T(8,128)(2,1)S(1)} %get-tuple-element.44.after.sent_ref), channel_id=1, source_target_pairs={{0,8},{4,12},{8,0},{12,4},{1,9},{5,13},{9,1},{13,5},{2,10},{6,14},... | collective-permute-start | bytes 503816 | tf_op jit(solution)/shard_map/ppermute | solution.py:15
  43.5 20.4 %collective-permute-start.14 = (bf16[144,2048]{1,0:T(8,128)(2,1)S(1)}, bf16[144,2048]{1,0:T(8,128)(2,1)S(1)}, u32[]{:S(2)}, u32[]{:S(2)}) collective-permute-start(bf16[144,2048]{1,0:T(8,128)(2,1)S(1)} %get-tuple-element.57.refs_4_), channel_id=1, source_target_pairs={{0,1},{1,0},{2,3},{3,2},{4,5},{5,4},{6,7},{7,6},{8,9},{9,8},{10,11... | collective-permute-start | bytes 1769480 | tf_op jit(solution)/shard_map/ppermute | solution.py:15
  44.9 9.0 %collective-permute-start.7 = (bf16[128,512]{1,0:T(8,128)(2,1)S(1)}, bf16[128,512]{1,0:T(8,128)(2,1)S(1)}, u32[]{:S(2)}, u32[]{:S(2)}) collective-permute-start(bf16[128,512]{1,0:T(8,128)(2,1)S(1)} %get-tuple-element.46.after), channel_id=1, source_target_pairs={{0,8},{4,12},{8,0},{12,4},{1,9},{5,13},{9,1},{13,5},{2,10},{6,14},... | collective-permute-start | bytes 393224 | tf_op jit(solution)/shard_map/ppermute | solution.py:15
  53.9 6.4 %collective-permute-start.10 = (bf16[528,128]{1,0:T(8,128)(2,1)S(1)}, bf16[528,128]{1,0:T(8,128)(2,1)S(1)}, u32[]{:S(2)}, u32[]{:S(2)}) collective-permute-start(bf16[528,128]{1,0:T(8,128)(2,1)S(1)} %get-tuple-element.51.mine_ref.after), channel_id=1, source_target_pairs={{0,4},{4,0},{8,12},{12,8},{1,5},{5,1},{9,13},{13,9},{2,6},{6,2},{1... | collective-permute-start | bytes 405512 | tf_op jit(solution)/shard_map/ppermute | solution.py:15
  54.0 5.0 %collective-permute-start.8 = (bf16[32,256]{1,0:T(8,128)(2,1)S(1)}, bf16[32,256]{1,0:T(8,128)(2,1)S(1)}, u32[]{:S(2)}, u32[]{:S(2)}) collective-permute-start(bf16[32,256]{1,0:T(8,128)(2,1)S(1)} %get-tuple-element.48.after), channel_id=1, source_target_pairs={{0,4},{4,8},{8,12},{1,5},{5,9},{9,13},{2,6},{6,10},{10,14},{3,7},{... | collective-permute-start | bytes 49160 | tf_op jit(solution)/shard_map/ppermute | solution.py:21
  59.0 12.6 %collective-permute-start.16 = (bf16[144,2048]{1,0:T(8,128)(2,1)S(1)}, bf16[144,2048]{1,0:T(8,128)(2,1)S(1)}, u32[]{:S(2)}, u32[]{:S(2)}) collective-permute-start(bf16[144,2048]{1,0:T(8,128)(2,1)S(1)} %collective-permute-done.15.refs_6_), channel_id=1, source_target_pairs={{0,1},{1,0},{2,3},{3,2},{4,5},{5,4},{6,7},{7,6},{8,9},{9,8},{10,11... | collective-permute-start | bytes 1769480 | tf_op jit(solution)/shard_map/ppermute | solution.py:15
  60.3 11.3 %collective-permute-start.20 = (bf16[256,1024]{1,0:T(8,128)(2,1)S(1)}, bf16[256,1024]{1,0:T(8,128)(2,1)S(1)}, u32[]{:S(2)}, u32[]{:S(2)}) collective-permute-start(bf16[256,1024]{1,0:T(8,128)(2,1)S(1)} %collective-permute-done.18.refs_10_), channel_id=1, source_target_pairs={{0,1},{1,0},{2,3},{3,2},{4,5},{5,4},{6,7},{7,6},{8,9},{9,8},{10,11... | collective-permute-start | bytes 1572872 | tf_op jit(solution)/shard_map/ppermute | solution.py:15
  60.3 11.3 %collective-permute-start.21 = (bf16[256,1024]{1,0:T(8,128)(2,1)S(1)}, bf16[256,1024]{1,0:T(8,128)(2,1)S(1)}, u32[]{:S(2)}, u32[]{:S(2)}) collective-permute-start(bf16[256,1024]{1,0:T(8,128)(2,1)S(1)} %collective-permute-done.19.refs_11_), channel_id=1, source_target_pairs={{0,1},{1,0},{2,3},{3,2},{4,5},{5,4},{6,7},{7,6},{8,9},{9,8},{10,11... | collective-permute-start | bytes 1572872 | tf_op jit(solution)/shard_map/ppermute | solution.py:15
  61.5 1.9 %copy-start.1 = (f32[31,256]{1,0:T(8,128)S(1)}, f32[31,256]{1,0:T(8,128)}, u32[]{:S(2)}) copy-start(f32[31,256]{1,0:T(8,128)} %taps_ref.1) | copy-start | bytes 95236
  63.4 8.2 %copy-start.2 = (f32[2048]{0:T(1024)S(1)}, f32[2048]{0:T(1024)}, u32[]{:S(2)}) copy-start(f32[2048]{0:T(1024)} %param.29) | copy-start | bytes 24580
  64.0 4.3 %collective-permute-start.12 = (bf16[128,384]{1,0:T(8,128)(2,1)S(1)}, bf16[128,384]{1,0:T(8,128)(2,1)S(1)}, u32[]{:S(2)}, u32[]{:S(2)}) collective-permute-start(bf16[128,384]{1,0:T(8,128)(2,1)S(1)} %conv.1.refs_0_), channel_id=1, source_target_pairs={{0,2},{1,3},{2,0},{3,1},{4,6},{5,7},{6,4},{7,5},{8,10},{9,11},{10,... | collective-permute-start | bytes 294920 | tf_op jit(solution)/shard_map/ppermute | solution.py:15
  68.3 1.9 %collective-permute-start.11 = (bf16[128,384]{1,0:T(8,128)(2,1)S(1)}, bf16[128,384]{1,0:T(8,128)(2,1)S(1)}, u32[]{:S(2)}, u32[]{:S(2)}) collective-permute-start(bf16[128,384]{1,0:T(8,128)(2,1)S(1)} %conv.1.refs_0_), channel_id=1, source_target_pairs={{0,1},{1,0},{2,3},{3,2},{4,5},{5,4},{6,7},{7,6},{8,9},{9,8},{10,11... | collective-permute-start | bytes 294920 | tf_op jit(solution)/shard_map/ppermute | solution.py:15
  70.2 1.3 %collective-permute-start.13 = (bf16[128,384]{1,0:T(8,128)(2,1)S(1)}, bf16[128,384]{1,0:T(8,128)(2,1)S(1)}, u32[]{:S(2)}, u32[]{:S(2)}) collective-permute-start(bf16[128,384]{1,0:T(8,128)(2,1)S(1)} %collective-permute-done.12.refs_2_), channel_id=1, source_target_pairs={{0,1},{1,0},{2,3},{3,2},{4,5},{5,4},{6,7},{7,6},{8,9},{9,8},{10,11... | collective-permute-start | bytes 294920 | tf_op jit(solution)/shard_map/ppermute | solution.py:15

commit v8 on v7

--- a/solution.py
+++ b/solution.py
@@ -508,7 +508,7 @@
 
 
 def final_kernel(*refs):
-    act, wa, wc, gain_ref, out_ref = refs[:4], refs[4:8], refs[8:14], refs[14], refs[15]
+    act, wa, wc, gain_ref, out_ref, mix = refs[:4], refs[4:8], refs[8:14], refs[14], refs[15], refs[16]
     cw = wc[0].shape[0]
     aw = act[0].shape[1] - cw
     convs = [c[:, aw:].astype(F32) for c in act]
@@ -516,25 +516,39 @@
     centered = [v - mean for v in convs]
     spread = sum(jnp.sum(v * v, axis=1, keepdims=True) for v in centered) / (4 * cw)
     inverse = lax.rsqrt(spread + norm_eps)
-    total = None
     ys = []
     for slot in range(4):
         pieces = [wa[slot][aw : aw + 1, n * cw : (n + 1) * cw].astype(F32) for n in range(6)]
         gain = pieces[0] + pieces[1] + pieces[2]
         bias = pieces[3] + pieces[4] + pieces[5]
         y = centered[slot] * inverse * gain + bias
-        y = (y * jax.nn.sigmoid(y)).astype(BF16)
-        part = dot_f32(act[slot][:, :aw], wa[slot][:aw, :])
-        if slot < 2:
-            part = part + dot_f32(y, wc[slot][...])
-        total = part if total is None else total + part
-        ys.append(y)
-    same = dot_f32(ys[2], wc[2][...]) + dot_f32(ys[3], wc[4][...])
-    other = dot_f32(ys[2], wc[3][...]) + dot_f32(ys[3], wc[5][...])
+        ys.append((y * jax.nn.sigmoid(y)).astype(BF16))
     swap = lax.axis_index("grp") == 1
-    total = total + jnp.concatenate([jnp.where(swap, other, same), jnp.where(swap, same, other)], axis=1)
-    squares = jnp.mean(total * total, axis=1, keepdims=True)
-    out_ref[...] = (total * lax.rsqrt(squares + norm_eps) * gain_ref[...]).astype(BF16)
+    rows, width = mix.shape
+    half = width // 2
+    squares = jnp.zeros((rows, 1), F32)
+    for first in range(0, width, CHUNK):
+        at = slice(first, first + CHUNK)
+        part = None
+        for slot in range(4):
+            if slot < 2:
+                w = wc[slot][:, at]
+            else:
+                pair = wc[2 * slot - 2], wc[2 * slot - 1]
+                near, far = pair if first < half else pair[::-1]
+                inner = slice(first % half, first % half + CHUNK)
+                w = jnp.where(swap, far[:, inner], near[:, inner])
+            one = dot_f32(ys[slot], w)
+            part = one if part is None else part + one
+        for slot in (0, 2):
+            w = jnp.concatenate([wa[slot][:aw, at], wa[slot + 1][:aw, at]], axis=0)
+            part = part + dot_f32(jnp.concatenate([act[slot][:, :aw], act[slot + 1][:, :aw]], axis=1), w)
+        mix[:, at] = part
+        squares = squares + jnp.sum(part * part, axis=1, keepdims=True)
+    out_ref[...] = (mix[...] * lax.rsqrt(squares / width + norm_eps) * gain_ref[...]).astype(BF16)
+
+
+CHUNK = 256
 
 
 def finish(act, wa, wc, out_gain):
@@ -544,6 +558,7 @@
         out_shape=shape((rows, width)),
         in_specs=[VM] * 15,
         out_specs=VM,
+        scratch_shapes=[pltpu.VMEM((rows, width), F32)],
         cost_estimate=cost(800_000_000, 7_000_000),
         compiler_params=params(32),
         name="finish_rows",

time: 75.1 us -> 74.8 us (level)
  no operation moved by 1% of the time
where the time goes in v8:
time: 74.8 us; the launch traced here: 73.7 us
  waiting for transfers between devices  49.2 us (66%)
  starting transfers between devices  13.3 us (18%)
  Pallas kernels  10.4 us (14%)
  between operations  0.82 us (1%)
    ppermute x21, waiting for transfers between devices, exchange(): return lax.ppermute(value, axis, [(s, s ^ bit) for s in range(count)])  45.5 us
    ppermute x21, starting transfers between devices, exchange(): return lax.ppermute(value, axis, [(s, s ^ bit) for s in range(count)])  12 us
    ppermute x1, waiting for transfers between devices, from_behind(): lax.ppermute(value, axis, [(source, source + steps) for source in range(i...  3.69 us
    pallas_call x1, Pallas kernels, finish(): pl.pallas_call(final_kernel, out_shape=shape((rows, width)), in_specs=[VM...  2.18 us
    pallas_call x1, Pallas kernels, attention(): pl.pallas_call(attention_kernel, out_shape=(shape((rows, width)), shape((...  1.87 us
  transfers between devices with their start and end apart: 22, of which 8 were waited for; matrix products, arithmetic and copies ran while one was open for 0% of the time, Pallas kernels for 9%

profile of v8, /device:TPU:25, one launch (start us, length us, event | category | flops | bytes accessed | tf_op | source)
XLA Modules:
  0.0 73.7 jit_solution(17484274621903126767)
XLA Ops:
  0.6 1.4 %pack_qkv.1 = (bf16[512,384]{1,0:T(8,128)(2,1)S(1)}, bf16[256,384]{1,0:T(8,128)(2,1)S(1)}, bf16[256,1024]{1,0:T(8,128)(2,1)S(1)}) custom-call(bf16[512,128]{1,0:T(8,128)(2,1)} %wq.1, bf16[512,128]{1,0:T(8,128)(2,1)} %wk.1, bf16[512,128]{1,0:T(8,128)(2,1)} %wv.1, bf16[256,2048]{1,0:T(8,128)(2,1)} %refs_8_.1), custom_call_target="tpu_custom_call" | custom-call | flops 2000000 | bytes 400000 | tf_op jit(solution)/shard_map/pack_qkv/pallas_call | solution.py:74
  2.1 1.3 %collective-permute-start.18 = (bf16[256,1024]{1,0:T(8,128)(2,1)S(1)}, bf16[256,1024]{1,0:T(8,128)(2,1)S(1)}, u32[]{:S(2)}, u32[]{:S(2)}) collective-permute-start(bf16[256,1024]{1,0:T(8,128)(2,1)S(1)} %get-tuple-element.58), channel_id=1, source_target_pairs={{0,2},{1,3},{2,0},{3,1},{4,6},{5,7},{6,4},{7,5},{8,10},{9,11},{10,... | collective-permute-start | bytes 1572872 | tf_op jit(solution)/shard_map/ppermute | solution.py:15
  3.3 1.3 %norm_parts.1 = (bf16[64,1024]{1,0:T(8,128)(2,1)S(1)}, bf16[128,512]{1,0:T(8,128)(2,1)S(1)}, bf16[128,512]{1,0:T(8,128)(2,1)S(1)}) custom-call(bf16[128,2048]{1,0:T(8,128)(2,1)} %x_hbm.1, f32[1,2048]{1,0:T(1,128)} %bitcast.6), custom_call_target="tpu_custom_call" | custom-call | flops 2000000 | bytes 1000000 | tf_op jit(solution)/shard_map/norm_parts/pallas_call | solution.py:116
  5.0 8.8 %collective-permute-done.got_ref = bf16[64,1024]{1,0:T(8,128)(2,1)S(1)} collective-permute-done((bf16[64,1024]{1,0:T(8,128)(2,1)S(1)}, bf16[64,1024]{1,0:T(8,128)(2,1)S(1)}, u32[]{:S(2)}, u32[]{:S(2)}) %collective-permute-start) | collective-permute-done | bytes 131104 | tf_op jit(solution)/shard_map/ppermute | solution.py:15
  13.8 0.5 collective-permute-start.1
  14.3 1.4 %pack.1 = (bf16[512,256]{1,0:T(8,128)(2,1)S(1)}, bf16[256,256]{1,0:T(8,128)(2,1)S(1)}, bf16[512,256]{1,0:T(8,128)(2,1)S(1)}, bf16[144,2048]{1,0:T(8,128)(2,1)S(1...) custom-call(bf16[512,256]{1,0:T(8,128)(2,1)} %gv_hbm.1, bf16[512,256]{1,0:T(8,128)(2,1)} %gg_hbm.1, ...), custom_call_target="tpu_custom_call" | custom-call | flops 2000000 | bytes 2000000 | tf_op jit(solution)/shard_map/pack/pallas_call | solution.py:170
  15.8 1.3 %collective-permute-start.6 = (bf16[256,384]{1,0:T(8,128)(2,1)S(1)}, bf16[256,384]{1,0:T(8,128)(2,1)S(1)}, u32[]{:S(2)}, u32[]{:S(2)}) collective-permute-start(bf16[256,384]{1,0:T(8,128)(2,1)S(1)} %collective-permute-done.2.same), channel_id=1, source_target_pairs={{0,16},{16,0},{1,17},{17,1},{2,18},{18,2},{3,19},{19,3},{4,20},{20... | collective-permute-start | bytes 589832 | tf_op jit(solution)/shard_map/ppermute | solution.py:15
  17.1 0.3 collective-permute-start.15
  17.4 1.4 %collective-permute-start.3 = (bf16[256,256]{1,0:T(8,128)(2,1)S(1)}, bf16[256,256]{1,0:T(8,128)(2,1)S(1)}, u32[]{:S(2)}, u32[]{:S(2)}) collective-permute-start(bf16[256,256]{1,0:T(8,128)(2,1)S(1)} %get-tuple-element.40), channel_id=1, source_target_pairs={{0,4},{4,0},{8,12},{12,8},{1,5},{5,1},{9,13},{13,9},{2,6},{6,2},{1... | collective-permute-start | bytes 393224 | tf_op jit(solution)/shard_map/ppermute | solution.py:15
  18.8 7.7 %collective-permute-done.3.gv_same = bf16[256,256]{1,0:T(8,128)(2,1)S(1)} collective-permute-done((bf16[256,256]{1,0:T(8,128)(2,1)S(1)}, bf16[256,256]{1,0:T(8,128)(2,1)S(1)}, u32[]{:S(2)}, u32[]{:S(2)}) %collective-permute-start.3) | collective-permute-done | bytes 131104 | tf_op jit(solution)/shard_map/ppermute | solution.py:15
  26.5 0.9 %collective-permute-start.17 = (bf16[256,2048]{1,0:T(8,128)(2,1)S(1)}, bf16[256,2048]{1,0:T(8,128)(2,1)S(1)}, u32[]{:S(2)}, u32[]{:S(2)}) collective-permute-start(bf16[256,2048]{1,0:T(8,128)(2,1)S(1)} %copy-done), channel_id=1, source_target_pairs={{0,1},{1,0},{2,3},{3,2},{4,5},{5,4},{6,7},{7,6},{8,9},{9,8},{10,11... | collective-permute-start | bytes 3145736 | tf_op jit(solution)/shard_map/ppermute | solution.py:15
  27.3 1.2 %collective-permute-start.19 = (bf16[256,1024]{1,0:T(8,128)(2,1)S(1)}, bf16[256,1024]{1,0:T(8,128)(2,1)S(1)}, u32[]{:S(2)}, u32[]{:S(2)}) collective-permute-start(bf16[256,1024]{1,0:T(8,128)(2,1)S(1)} %collective-permute-done.18.refs_10_), channel_id=1, source_target_pairs={{0,16},{16,0},{1,17},{17,1},{2,18},{18,2},{3,19},{19,3},{4,20},{20... | collective-permute-start | bytes 1572872 | tf_op jit(solution)/shard_map/ppermute | solution.py:15
  28.6 0.2 collective-permute-start.4
  28.8 0.4 project_qkv.1
  29.4 14.2 %collective-permute-done.4.gv_other = bf16[256,256]{1,0:T(8,128)(2,1)S(1)} collective-permute-done((bf16[256,256]{1,0:T(8,128)(2,1)S(1)}, bf16[256,256]{1,0:T(8,128)(2,1)S(1)}, u32[]{:S(2)}, u32[]{:S(2)}) %collective-permute-start.4) | collective-permute-done | bytes 131104 | tf_op jit(solution)/shard_map/ppermute | solution.py:15
  43.5 0.9 %collective-permute-start.14 = (bf16[144,2048]{1,0:T(8,128)(2,1)S(1)}, bf16[144,2048]{1,0:T(8,128)(2,1)S(1)}, u32[]{:S(2)}, u32[]{:S(2)}) collective-permute-start(bf16[144,2048]{1,0:T(8,128)(2,1)S(1)} %get-tuple-element.57.refs_4_), channel_id=1, source_target_pairs={{0,1},{1,0},{2,3},{3,2},{4,5},{5,4},{6,7},{7,6},{8,9},{9,8},{10,11... | collective-permute-start | bytes 1769480 | tf_op jit(solution)/shard_map/ppermute | solution.py:15
  44.5 0.4 project_glu.1
  45.0 8.8 %collective-permute-done.7.got_ref = bf16[128,512]{1,0:T(8,128)(2,1)S(1)} collective-permute-done((bf16[128,512]{1,0:T(8,128)(2,1)S(1)}, bf16[128,512]{1,0:T(8,128)(2,1)S(1)}, u32[]{:S(2)}, u32[]{:S(2)}) %collective-permute-start.7) | collective-permute-done | bytes 131104 | tf_op jit(solution)/shard_map/ppermute | solution.py:15
  54.0 1.3 %collective-permute-start.8 = (bf16[32,256]{1,0:T(8,128)(2,1)S(1)}, bf16[32,256]{1,0:T(8,128)(2,1)S(1)}, u32[]{:S(2)}, u32[]{:S(2)}) collective-permute-start(bf16[32,256]{1,0:T(8,128)(2,1)S(1)} %get-tuple-element.48.after), channel_id=1, source_target_pairs={{0,4},{4,8},{8,12},{1,5},{5,9},{9,13},{2,6},{6,10},{10,14},{3,7},{... | collective-permute-start | bytes 49160 | tf_op jit(solution)/shard_map/ppermute | solution.py:21
  55.3 3.7 %collective-permute-done.8.before_ref = bf16[32,256]{1,0:T(8,128)(2,1)S(1)} collective-permute-done((bf16[32,256]{1,0:T(8,128)(2,1)S(1)}, bf16[32,256]{1,0:T(8,128)(2,1)S(1)}, u32[]{:S(2)}, u32[]{:S(2)}) %collective-permute-start.8) | collective-permute-done | bytes 16416 | tf_op jit(solution)/shard_map/ppermute | solution.py:21
  59.0 1.3 %collective-permute-start.16 = (bf16[144,2048]{1,0:T(8,128)(2,1)S(1)}, bf16[144,2048]{1,0:T(8,128)(2,1)S(1)}, u32[]{:S(2)}, u32[]{:S(2)}) collective-permute-start(bf16[144,2048]{1,0:T(8,128)(2,1)S(1)} %collective-permute-done.15.refs_6_), channel_id=1, source_target_pairs={{0,1},{1,0},{2,3},{3,2},{4,5},{5,4},{6,7},{7,6},{8,9},{9,8},{10,11... | collective-permute-start | bytes 1769480 | tf_op jit(solution)/shard_map/ppermute | solution.py:15
  60.3 0.5 collective-permute-start.21
  60.8 0.7 near_attention.1
  61.5 1.9 %stick_attention.1 = (bf16[128,128]{1,0:T(8,128)(2,1)S(1)}, f32[2,128]{1,0:T(2,128)}) custom-call(bf16[128,128]{1,0:T(8,128)(2,1)S(1)} %get-tuple-element.50.q_ref, bf16[528,128]{1,0:T(8,128)(2,1)S(1)} %collective-permute-done.10.pair_ref, f32[2,64]{1,0:T(2,128)S(1)} %get-tuple-element.52.gain_ref, f32[2,128,128]{2,1,0:T(8,128)S(1)} %get-tuple-element.53.mix_ref, ...), custom_call_target="tpu_custom_call" | custom-call | flops 400000000 | bytes 1000000 | tf_op jit(solution)/shard_map/stick_attention/pallas_call | solution.py:494
  63.4 0.6 conv.1.refs_0_
  64.0 0.3 collective-permute-start.12
  64.3 4.0 %collective-permute-done.12.refs_2_ = bf16[128,384]{1,0:T(8,128)(2,1)S(1)} collective-permute-done((bf16[128,384]{1,0:T(8,128)(2,1)S(1)}, bf16[128,384]{1,0:T(8,128)(2,1)S(1)}, u32[]{:S(2)}, u32[]{:S(2)}) %collective-permute-start.12) | collective-permute-done | bytes 98336 | tf_op jit(solution)/shard_map/ppermute | solution.py:15
  68.3 0.9 %collective-permute-start.11 = (bf16[128,384]{1,0:T(8,128)(2,1)S(1)}, bf16[128,384]{1,0:T(8,128)(2,1)S(1)}, u32[]{:S(2)}, u32[]{:S(2)}) collective-permute-start(bf16[128,384]{1,0:T(8,128)(2,1)S(1)} %conv.1.refs_0_), channel_id=1, source_target_pairs={{0,1},{1,0},{2,3},{3,2},{4,5},{5,4},{6,7},{7,6},{8,9},{9,8},{10,11... | collective-permute-start | bytes 294920 | tf_op jit(solution)/shard_map/ppermute | solution.py:15
  69.3 0.9 %collective-permute-done.11.refs_1_ = bf16[128,384]{1,0:T(8,128)(2,1)S(1)} collective-permute-done((bf16[128,384]{1,0:T(8,128)(2,1)S(1)}, bf16[128,384]{1,0:T(8,128)(2,1)S(1)}, u32[]{:S(2)}, u32[]{:S(2)}) %collective-permute-start.11) | collective-permute-done | bytes 98336 | tf_op jit(solution)/shard_map/ppermute | solution.py:15
  70.2 0.4 collective-permute-start.13
  70.6 0.9 %collective-permute-done.13.refs_3_ = bf16[128,384]{1,0:T(8,128)(2,1)S(1)} collective-permute-done((bf16[128,384]{1,0:T(8,128)(2,1)S(1)}, bf16[128,384]{1,0:T(8,128)(2,1)S(1)}, u32[]{:S(2)}, u32[]{:S(2)}) %collective-permute-start.13) | collective-permute-done | bytes 98336 | tf_op jit(solution)/shard_map/ppermute | solution.py:15
  71.5 2.2 %finish_rows.1 = bf16[128,2048]{1,0:T(8,128)(2,1)} custom-call(bf16[128,384]{1,0:T(8,128)(2,1)S(1)} %conv.1.refs_0_, bf16[128,384]{1,0:T(8,128)(2,1)S(1)} %collective-permute-done.11.refs_1_, bf16[128,384]{1,0:T(8,128)(2,1)S(1)} %collective-permute-done.12.refs_2_, bf16[128,384]{1,0:T(8,128)(2,1)S(1)} %collective-permute-done.13.refs_3_, ...), custom_call_target="tpu_custom_call" | custom-call | flops 800000000 | bytes 7000000 | tf_op jit(solution)/shard_map/finish_rows/pallas_call | solution.py:556
  (30 shorter events, 0.7 us)
Async XLA Ops:
  2.1 24.4 %copy-start = (bf16[256,2048]{1,0:T(8,128)(2,1)S(1)}, bf16[256,2048]{1,0:T(8,128)(2,1)}, u32[]{:S(2)}) copy-start(bf16[256,2048]{1,0:T(8,128)(2,1)} %refs_8_.1) | copy-start | bytes 3145732
  2.1 25.3 %collective-permute-start.18 = (bf16[256,1024]{1,0:T(8,128)(2,1)S(1)}, bf16[256,1024]{1,0:T(8,128)(2,1)S(1)}, u32[]{:S(2)}, u32[]{:S(2)}) collective-permute-start(bf16[256,1024]{1,0:T(8,128)(2,1)S(1)} %get-tuple-element.58), channel_id=1, source_target_pairs={{0,2},{1,3},{2,0},{3,1},{4,6},{5,7},{6,4},{7,5},{8,10},{9,11},{10,... | collective-permute-start | bytes 1572872 | tf_op jit(solution)/shard_map/ppermute | solution.py:15
  4.7 9.1 %collective-permute-start = (bf16[64,1024]{1,0:T(8,128)(2,1)S(1)}, bf16[64,1024]{1,0:T(8,128)(2,1)S(1)}, u32[]{:S(2)}, u32[]{:S(2)}) collective-permute-start(bf16[64,1024]{1,0:T(8,128)(2,1)S(1)} %get-tuple-element.33), channel_id=1, source_target_pairs={{0,8},{4,12},{8,0},{12,4},{1,9},{5,13},{9,1},{13,5},{2,10},{6,14},... | collective-permute-start | bytes 393224 | tf_op jit(solution)/shard_map/ppermute | solution.py:15
  4.8 11.0 %collective-permute-start.2 = (bf16[256,384]{1,0:T(8,128)(2,1)S(1)}, bf16[256,384]{1,0:T(8,128)(2,1)S(1)}, u32[]{:S(2)}, u32[]{:S(2)}) collective-permute-start(bf16[256,384]{1,0:T(8,128)(2,1)S(1)} %get-tuple-element.38), channel_id=1, source_target_pairs={{0,4},{4,0},{8,12},{12,8},{1,5},{5,1},{9,13},{13,9},{2,6},{6,2},{1... | collective-permute-start | bytes 589832 | tf_op jit(solution)/shard_map/ppermute | solution.py:15
  13.8 3.6 %collective-permute-start.1 = (bf16[64,1024]{1,0:T(8,128)(2,1)S(1)}, bf16[64,1024]{1,0:T(8,128)(2,1)S(1)}, u32[]{:S(2)}, u32[]{:S(2)}) collective-permute-start(bf16[64,1024]{1,0:T(8,128)(2,1)S(1)} %collective-permute-done.got_ref), channel_id=1, source_target_pairs={{0,1},{1,0},{2,3},{3,2},{4,5},{5,4},{6,7},{7,6},{8,9},{9,8},{10,11... | collective-permute-start | bytes 393224 | tf_op jit(solution)/shard_map/ppermute | solution.py:15
  15.7 13.5 %collective-permute-start.5 = (bf16[512,256]{1,0:T(8,128)(2,1)S(1)}, bf16[512,256]{1,0:T(8,128)(2,1)S(1)}, u32[]{:S(2)}, u32[]{:S(2)}) collective-permute-start(bf16[512,256]{1,0:T(8,128)(2,1)S(1)} %get-tuple-element.37.gg), channel_id=1, source_target_pairs={{0,4},{4,0},{8,12},{12,8},{1,5},{5,1},{9,13},{13,9},{2,6},{6,2},{1... | collective-permute-start | bytes 786440 | tf_op jit(solution)/shard_map/ppermute | solution.py:15
  15.8 12.8 %collective-permute-start.6 = (bf16[256,384]{1,0:T(8,128)(2,1)S(1)}, bf16[256,384]{1,0:T(8,128)(2,1)S(1)}, u32[]{:S(2)}, u32[]{:S(2)}) collective-permute-start(bf16[256,384]{1,0:T(8,128)(2,1)S(1)} %collective-permute-done.2.same), channel_id=1, source_target_pairs={{0,16},{16,0},{1,17},{17,1},{2,18},{18,2},{3,19},{19,3},{4,20},{20... | collective-permute-start | bytes 589832 | tf_op jit(solution)/shard_map/ppermute | solution.py:15
  17.1 36.8 %collective-permute-start.15 = (bf16[144,2048]{1,0:T(8,128)(2,1)S(1)}, bf16[144,2048]{1,0:T(8,128)(2,1)S(1)}, u32[]{:S(2)}, u32[]{:S(2)}) collective-permute-start(bf16[144,2048]{1,0:T(8,128)(2,1)S(1)} %get-tuple-element.57.refs_4_), channel_id=1, source_target_pairs={{0,2},{1,3},{2,0},{3,1},{4,6},{5,7},{6,4},{7,5},{8,10},{9,11},{10,... | collective-permute-start | bytes 1769480 | tf_op jit(solution)/shard_map/ppermute | solution.py:15
  17.4 9.1 %collective-permute-start.3 = (bf16[256,256]{1,0:T(8,128)(2,1)S(1)}, bf16[256,256]{1,0:T(8,128)(2,1)S(1)}, u32[]{:S(2)}, u32[]{:S(2)}) collective-permute-start(bf16[256,256]{1,0:T(8,128)(2,1)S(1)} %get-tuple-element.40), channel_id=1, source_target_pairs={{0,4},{4,0},{8,12},{12,8},{1,5},{5,1},{9,13},{13,9},{2,6},{6,2},{1... | collective-permute-start | bytes 393224 | tf_op jit(solution)/shard_map/ppermute | solution.py:15
  26.5 45.0 %collective-permute-start.17 = (bf16[256,2048]{1,0:T(8,128)(2,1)S(1)}, bf16[256,2048]{1,0:T(8,128)(2,1)S(1)}, u32[]{:S(2)}, u32[]{:S(2)}) collective-permute-start(bf16[256,2048]{1,0:T(8,128)(2,1)S(1)} %copy-done), channel_id=1, source_target_pairs={{0,1},{1,0},{2,3},{3,2},{4,5},{5,4},{6,7},{7,6},{8,9},{9,8},{10,11... | collective-permute-start | bytes 3145736 | tf_op jit(solution)/shard_map/ppermute | solution.py:15
  27.3 32.9 %collective-permute-start.19 = (bf16[256,1024]{1,0:T(8,128)(2,1)S(1)}, bf16[256,1024]{1,0:T(8,128)(2,1)S(1)}, u32[]{:S(2)}, u32[]{:S(2)}) collective-permute-start(bf16[256,1024]{1,0:T(8,128)(2,1)S(1)} %collective-permute-done.18.refs_10_), channel_id=1, source_target_pairs={{0,16},{16,0},{1,17},{17,1},{2,18},{18,2},{3,19},{19,3},{4,20},{20... | collective-permute-start | bytes 1572872 | tf_op jit(solution)/shard_map/ppermute | solution.py:15
  28.6 15.0 %collective-permute-start.4 = (bf16[256,256]{1,0:T(8,128)(2,1)S(1)}, bf16[256,256]{1,0:T(8,128)(2,1)S(1)}, u32[]{:S(2)}, u32[]{:S(2)}) collective-permute-start(bf16[256,256]{1,0:T(8,128)(2,1)S(1)} %collective-permute-done.3.gv_same), channel_id=1, source_target_pairs={{0,16},{16,0},{1,17},{17,1},{2,18},{18,2},{3,19},{19,3},{4,20},{20... | collective-permute-start | bytes 393224 | tf_op jit(solution)/shard_map/ppermute | solution.py:15
  29.3 15.6 %collective-permute-start.9 = (bf16[656,128]{1,0:T(8,128)(2,1)S(1)}, bf16[656,128]{1,0:T(8,128)(2,1)S(1)}, u32[]{:S(2)}, u32[]{:S(2)}) collective-permute-start(bf16[656,128]{1,0:T(8,128)(2,1)S(1)} %get-tuple-element.44.after.sent_ref), channel_id=1, source_target_pairs={{0,8},{4,12},{8,0},{12,4},{1,9},{5,13},{9,1},{13,5},{2,10},{6,14},... | collective-permute-start | bytes 503816 | tf_op jit(solution)/shard_map/ppermute | solution.py:15
  43.5 20.4 %collective-permute-start.14 = (bf16[144,2048]{1,0:T(8,128)(2,1)S(1)}, bf16[144,2048]{1,0:T(8,128)(2,1)S(1)}, u32[]{:S(2)}, u32[]{:S(2)}) collective-permute-start(bf16[144,2048]{1,0:T(8,128)(2,1)S(1)} %get-tuple-element.57.refs_4_), channel_id=1, source_target_pairs={{0,1},{1,0},{2,3},{3,2},{4,5},{5,4},{6,7},{7,6},{8,9},{9,8},{10,11... | collective-permute-start | bytes 1769480 | tf_op jit(solution)/shard_map/ppermute | solution.py:15
  44.9 9.0 %collective-permute-start.7 = (bf16[128,512]{1,0:T(8,128)(2,1)S(1)}, bf16[128,512]{1,0:T(8,128)(2,1)S(1)}, u32[]{:S(2)}, u32[]{:S(2)}) collective-permute-start(bf16[128,512]{1,0:T(8,128)(2,1)S(1)} %get-tuple-element.46.after), channel_id=1, source_target_pairs={{0,8},{4,12},{8,0},{12,4},{1,9},{5,13},{9,1},{13,5},{2,10},{6,14},... | collective-permute-start | bytes 393224 | tf_op jit(solution)/shard_map/ppermute | solution.py:15
  53.9 6.4 %collective-permute-start.10 = (bf16[528,128]{1,0:T(8,128)(2,1)S(1)}, bf16[528,128]{1,0:T(8,128)(2,1)S(1)}, u32[]{:S(2)}, u32[]{:S(2)}) collective-permute-start(bf16[528,128]{1,0:T(8,128)(2,1)S(1)} %get-tuple-element.51.mine_ref.after), channel_id=1, source_target_pairs={{0,4},{4,0},{8,12},{12,8},{1,5},{5,1},{9,13},{13,9},{2,6},{6,2},{1... | collective-permute-start | bytes 405512 | tf_op jit(solution)/shard_map/ppermute | solution.py:15
  54.0 5.0 %collective-permute-start.8 = (bf16[32,256]{1,0:T(8,128)(2,1)S(1)}, bf16[32,256]{1,0:T(8,128)(2,1)S(1)}, u32[]{:S(2)}, u32[]{:S(2)}) collective-permute-start(bf16[32,256]{1,0:T(8,128)(2,1)S(1)} %get-tuple-element.48.after), channel_id=1, source_target_pairs={{0,4},{4,8},{8,12},{1,5},{5,9},{9,13},{2,6},{6,10},{10,14},{3,7},{... | collective-permute-start | bytes 49160 | tf_op jit(solution)/shard_map/ppermute | solution.py:21
  59.0 12.6 %collective-permute-start.16 = (bf16[144,2048]{1,0:T(8,128)(2,1)S(1)}, bf16[144,2048]{1,0:T(8,128)(2,1)S(1)}, u32[]{:S(2)}, u32[]{:S(2)}) collective-permute-start(bf16[144,2048]{1,0:T(8,128)(2,1)S(1)} %collective-permute-done.15.refs_6_), channel_id=1, source_target_pairs={{0,1},{1,0},{2,3},{3,2},{4,5},{5,4},{6,7},{7,6},{8,9},{9,8},{10,11... | collective-permute-start | bytes 1769480 | tf_op jit(solution)/shard_map/ppermute | solution.py:15
  60.3 11.3 %collective-permute-start.20 = (bf16[256,1024]{1,0:T(8,128)(2,1)S(1)}, bf16[256,1024]{1,0:T(8,128)(2,1)S(1)}, u32[]{:S(2)}, u32[]{:S(2)}) collective-permute-start(bf16[256,1024]{1,0:T(8,128)(2,1)S(1)} %collective-permute-done.18.refs_10_), channel_id=1, source_target_pairs={{0,1},{1,0},{2,3},{3,2},{4,5},{5,4},{6,7},{7,6},{8,9},{9,8},{10,11... | collective-permute-start | bytes 1572872 | tf_op jit(solution)/shard_map/ppermute | solution.py:15
  60.3 11.3 %collective-permute-start.21 = (bf16[256,1024]{1,0:T(8,128)(2,1)S(1)}, bf16[256,1024]{1,0:T(8,128)(2,1)S(1)}, u32[]{:S(2)}, u32[]{:S(2)}) collective-permute-start(bf16[256,1024]{1,0:T(8,128)(2,1)S(1)} %collective-permute-done.19.refs_11_), channel_id=1, source_target_pairs={{0,1},{1,0},{2,3},{3,2},{4,5},{5,4},{6,7},{7,6},{8,9},{9,8},{10,11... | collective-permute-start | bytes 1572872 | tf_op jit(solution)/shard_map/ppermute | solution.py:15
  61.5 1.9 %copy-start.1 = (f32[31,256]{1,0:T(8,128)S(1)}, f32[31,256]{1,0:T(8,128)}, u32[]{:S(2)}) copy-start(f32[31,256]{1,0:T(8,128)} %taps_ref.1) | copy-start | bytes 95236
  63.4 8.2 %copy-start.2 = (f32[2048]{0:T(1024)S(1)}, f32[2048]{0:T(1024)}, u32[]{:S(2)}) copy-start(f32[2048]{0:T(1024)} %param.29) | copy-start | bytes 24580
  64.0 4.3 %collective-permute-start.12 = (bf16[128,384]{1,0:T(8,128)(2,1)S(1)}, bf16[128,384]{1,0:T(8,128)(2,1)S(1)}, u32[]{:S(2)}, u32[]{:S(2)}) collective-permute-start(bf16[128,384]{1,0:T(8,128)(2,1)S(1)} %conv.1.refs_0_), channel_id=1, source_target_pairs={{0,2},{1,3},{2,0},{3,1},{4,6},{5,7},{6,4},{7,5},{8,10},{9,11},{10,... | collective-permute-start | bytes 294920 | tf_op jit(solution)/shard_map/ppermute | solution.py:15
  68.3 1.9 %collective-permute-start.11 = (bf16[128,384]{1,0:T(8,128)(2,1)S(1)}, bf16[128,384]{1,0:T(8,128)(2,1)S(1)}, u32[]{:S(2)}, u32[]{:S(2)}) collective-permute-start(bf16[128,384]{1,0:T(8,128)(2,1)S(1)} %conv.1.refs_0_), channel_id=1, source_target_pairs={{0,1},{1,0},{2,3},{3,2},{4,5},{5,4},{6,7},{7,6},{8,9},{9,8},{10,11... | collective-permute-start | bytes 294920 | tf_op jit(solution)/shard_map/ppermute | solution.py:15
  70.2 1.3 %collective-permute-start.13 = (bf16[128,384]{1,0:T(8,128)(2,1)S(1)}, bf16[128,384]{1,0:T(8,128)(2,1)S(1)}, u32[]{:S(2)}, u32[]{:S(2)}) collective-permute-start(bf16[128,384]{1,0:T(8,128)(2,1)S(1)} %collective-permute-done.12.refs_2_), channel_id=1, source_target_pairs={{0,1},{1,0},{2,3},{3,2},{4,5},{5,4},{6,7},{7,6},{8,9},{9,8},{10,11... | collective-permute-start | bytes 294920 | tf_op jit(solution)/shard_map/ppermute | solution.py:15

commit v9 on v8

--- a/solution.py
+++ b/solution.py
@@ -15,6 +15,12 @@
     return lax.ppermute(value, axis, [(s, s ^ bit) for s in range(count)])
 
 
+def from_cross_behind(value, axis):
+    count = lax.axis_size(axis)
+    pairs = [(source, (source ^ 2) + 1) for source in range(count)]
+    return lax.ppermute(value, axis, [(a, b) for a, b in pairs if b < count])
+
+
 def from_behind(value, axis, steps):
     count = lax.axis_size(axis)
     initial, last = (max(0, -steps), min(count, count - steps))
@@ -51,55 +57,50 @@
     return [pltpu.with_memory_space_constraint(v, pltpu.HBM) for v in values]
 
 
-def pack_qkv_kernel(wq, wk, wv, wc, all_ref, send_ref, wc_ref, sems):
+def pack_qkv_kernel(wq, wk, wv, all_ref, send_ref, sems):
     part, width = send_ref.shape[0], wq.shape[1]
-    group = lax.axis_index("grp")
-    mine = pl.ds(pl.multiple_of(group * part, part), part)
-    columns = wc_ref.shape[1]
+    mine = pl.ds(pl.multiple_of(lax.axis_index("grp") * part, part), part)
     first, rest = [], []
     for n, w in enumerate((wq, wk, wv)):
         at = slice(n * width, (n + 1) * width)
         first.append(pltpu.make_async_copy(w.at[mine, :], send_ref.at[:, at], sems.at[n]))
         rest.append(pltpu.make_async_copy(w, all_ref.at[:, at], sems.at[3 + n]))
-    half = wc.at[:, pl.ds(pl.multiple_of(group * columns, columns), columns)]
-    rest.append(pltpu.make_async_copy(half, wc_ref, sems.at[6]))
     for copy in first + rest:
         copy.start()
     for copy in first + rest:
         copy.wait()
 
 
-def pack_qkv(weights, wc):
+def pack_qkv(weights):
     block, width = weights[0].shape
     return pl.pallas_call(
         pack_qkv_kernel,
-        out_shape=(
-            shape((block, 3 * width)),
-            shape((block // 2, 3 * width)),
-            shape((wc.shape[0], wc.shape[1] // 2)),
-        ),
-        in_specs=[HBM] * 4,
-        out_specs=[VM] * 3,
-        scratch_shapes=[pltpu.SemaphoreType.DMA((7,))],
+        out_shape=(shape((block, 3 * width)), shape((block // 2, 3 * width))),
+        in_specs=[HBM] * 3,
+        out_specs=[VM] * 2,
+        scratch_shapes=[pltpu.SemaphoreType.DMA((6,))],
         cost_estimate=cost(2_000_000, 400_000),
         compiler_params=params(),
         name="pack_qkv",
-    )(*in_hbm(*weights, wc))
-
-
-def norm_kernel(x_hbm, gain_hbm, send_ref, own_ref, pair_ref, x_ref, gain_ref, normed, sems):
+    )(*in_hbm(*weights))
+
+
+def norm_kernel(x_hbm, gain_hbm, wc_hbm, send_ref, own_ref, pair_ref, wc_ref, x_ref, gain_ref, normed, sems):
     side, low = lax.axis_index("sp") // 2, lax.axis_index("sp") % 2
     core = lax.axis_index("tp") % 2
     block = own_ref.shape[1]
     half = 2 * block
     half_rows = send_ref.shape[0]
+    columns = wc_ref.shape[1]
+    mine = pl.ds(pl.multiple_of(lax.axis_index("grp") * columns, columns), columns)
     copies = [
         pltpu.make_async_copy(x_hbm, x_ref, sems.at[0]),
         pltpu.make_async_copy(gain_hbm, gain_ref, sems.at[1]),
+        pltpu.make_async_copy(wc_hbm.at[:, mine], wc_ref, sems.at[2]),
     ]
     for copy in copies:
         copy.start()
-    for copy in copies:
+    for copy in copies[:2]:
         copy.wait()
     x = x_ref[...].astype(F32)
     squares = jnp.mean(x * x, axis=1, keepdims=True)
@@ -109,25 +110,31 @@
     send_ref[...] = normed[pl.ds(first, half_rows), pl.ds(away, half)]
     own_ref[...] = normed[:, pl.ds(pl.multiple_of(side * half + low * block, block), block)]
     pair_ref[...] = normed[:, pl.ds(pl.multiple_of(side * half + (1 - low) * block, block), block)]
-
-
-def norm_parts(tokens, gain, block):
+    copies[2].wait()
+
+
+def norm_parts(tokens, gain, block, wc):
     rows, features = tokens.shape
     return pl.pallas_call(
         norm_kernel,
-        out_shape=(shape((rows // 2, 2 * block)), shape((rows, block)), shape((rows, block))),
-        in_specs=[HBM] * 2,
-        out_specs=[VM] * 3,
+        out_shape=(
+            shape((rows // 2, 2 * block)),
+            shape((rows, block)),
+            shape((rows, block)),
+            shape((wc.shape[0], wc.shape[1] // 2)),
+        ),
+        in_specs=[HBM] * 3,
+        out_specs=[VM] * 4,
         scratch_shapes=[
             pltpu.VMEM((rows, features), BF16),
             pltpu.VMEM((1, features), F32),
             pltpu.VMEM((rows, features), BF16),
-            pltpu.SemaphoreType.DMA((2,)),
+            pltpu.SemaphoreType.DMA((3,)),
         ],
         cost_estimate=cost(2_000_000, 1_000_000),
         compiler_params=params(),
         name="norm_parts",
-    )(*in_hbm(tokens, gain.reshape(1, features)))
+    )(*in_hbm(tokens, gain.reshape(1, features), wc))
 
 
 def pack_kernel(
@@ -282,9 +289,9 @@
     )(keep, got, sent, after)
 
 
-def glu_kernel(x_own, x_pair, gv, gg, gv_same, gv_other, gg_pair, after, keep_ref, send_ref):
+def glu_kernel(x_own, x_pair, gv, gg, gv_same, gv_other, gg_pair, after, keep_ref, send_ref, own_tail, far_tail):
     rows = x_own.shape[0] // 2
-    cw = gv.shape[1]
+    tail, cw = own_tail.shape[0], gv.shape[1]
     for n in range(2):
         own = (gv, gg)[n]
         far = far_dot(x_pair, gv_same, gv_other) if n == 0 else dot_f32(x_pair[...], gg_pair[...])
@@ -292,50 +299,40 @@
         at = slice(n * cw, (n + 1) * cw)
         keep_ref[:, at] = total[:rows]
         send_ref[:, at] = total[rows:].astype(BF16)
-
-
-def project_glu(x_own, x_pair, own, pair, after):
+        own_tail[:, at] = total[rows - tail : rows].astype(BF16)
+        far_tail[:, at] = total[2 * rows - tail :].astype(BF16)
+
+
+def project_glu(x_own, x_pair, own, pair, tail, after):
     rows, width = x_own.shape[0] // 2, 2 * own[0].shape[1]
     return pl.pallas_call(
         glu_kernel,
-        out_shape=(shape((rows, width), F32), shape((rows, width))),
+        out_shape=(
+            shape((rows, width), F32),
+            shape((rows, width)),
+            shape((tail, width)),
+            shape((tail, width)),
+        ),
         in_specs=[VM] * 7 + [ANY],
-        out_specs=[VM] * 2,
+        out_specs=[VM] * 4,
         cost_estimate=cost(270_000_000, 1_000_000),
         compiler_params=params(),
         name="project_glu",
     )(x_own, x_pair, *own, *pair, after)
 
 
-def gate_kernel(keep_ref, got_ref, gated_ref, tail_ref):
-    rows, cw = gated_ref.shape
-    glu = keep_ref[...] + got_ref[...].astype(F32)
-    value = glu[:, :cw].astype(BF16).astype(F32)
-    gate = glu[:, cw:].astype(BF16).astype(F32)
-    gated = (value * jax.nn.sigmoid(gate)).astype(BF16)
-    gated_ref[...] = gated
-    tail_ref[...] = gated[rows - tail_ref.shape[0] :]
-
-
-def gate(keep, got, tail):
-    rows, cw = keep.shape[0], keep.shape[1] // 2
-    return pl.pallas_call(
-        gate_kernel,
-        out_shape=(shape((rows, cw)), shape((tail, cw))),
-        in_specs=[VM] * 2,
-        out_specs=[VM] * 2,
-        cost_estimate=cost(2_000_000, 500_000),
-        compiler_params=params(),
-        name="gate",
-    )(keep, got)
-
-
-def conv_kernel(gated_ref, before_ref, taps_ref, att_ref, act_ref, padded):
+def conv_kernel(keep_ref, got_ref, near_ref, far_ref, taps_ref, att_ref, act_ref, padded):
     rows, aw = att_ref.shape
-    tail = before_ref.shape[0]
+    tail, cw = near_ref.shape[0], taps_ref.shape[1]
     taps = taps_ref.shape[0]
-    padded[:tail, :] = before_ref[...].astype(F32)
-    padded[tail:, :] = gated_ref[...].astype(F32)
+
+    def gated(glu):
+        value = glu[:, :cw].astype(BF16).astype(F32)
+        gate = glu[:, cw:].astype(BF16).astype(F32)
+        return (value * jax.nn.sigmoid(gate)).astype(BF16).astype(F32)
+
+    padded[:tail, :] = gated(near_ref[...].astype(F32) + far_ref[...].astype(F32))
+    padded[tail:, :] = gated(keep_ref[...] + got_ref[...].astype(F32))
     total = None
     for tap in range(taps):
         first = tail - (taps - 1) + tap
@@ -345,18 +342,18 @@
     act_ref[:, aw:] = total.astype(BF16)
 
 
-def conv(gated, before, taps, attended):
-    rows, cw = gated.shape
+def conv(keep, got, near, far, taps, attended):
+    rows, cw = keep.shape[0], taps.shape[1]
     return pl.pallas_call(
         conv_kernel,
         out_shape=shape((rows, attended.shape[1] + cw)),
-        in_specs=[VM] * 4,
+        in_specs=[VM] * 6,
         out_specs=VM,
-        scratch_shapes=[pltpu.VMEM((rows + before.shape[0], cw), F32)],
+        scratch_shapes=[pltpu.VMEM((rows + near.shape[0], cw), F32)],
         cost_estimate=cost(20_000_000, 500_000),
         compiler_params=params(),
         name="conv",
-    )(gated, before, taps, attended)
+    )(keep, got, near, far, taps, attended)
 
 
 def suffix_matrix(keys):
@@ -507,8 +504,33 @@
     )(q, pair, head_gain, *near, after)
 
 
+def heads_part(act, wa, aw, at):
+    w = jnp.concatenate([ref[:aw, at] for ref in wa], axis=0)
+    return dot_f32(jnp.concatenate([ref[:, :aw] for ref in act], axis=1), w)
+
+
+def begin_kernel(act0, act1, wa0, wa1, out_ref):
+    aw = wa0.shape[0] - 16
+    for first in range(0, out_ref.shape[1], CHUNK):
+        at = slice(first, first + CHUNK)
+        out_ref[:, at] = heads_part((act0, act1), (wa0, wa1), aw, at)
+
+
+def begin(act0, act1, wa0, wa1):
+    rows, width = act0.shape[0], wa0.shape[1]
+    return pl.pallas_call(
+        begin_kernel,
+        out_shape=shape((rows, width), F32),
+        in_specs=[VM] * 4,
+        out_specs=VM,
+        cost_estimate=cost(130_000_000, 2_000_000),
+        compiler_params=params(),
+        name="begin_rows",
+    )(act0, act1, wa0, wa1)
+
+
 def final_kernel(*refs):
-    act, wa, wc, gain_ref, out_ref, mix = refs[:4], refs[4:8], refs[8:14], refs[14], refs[15], refs[16]
+    act, wa, wc, begun, gain_ref, out_ref, mix = refs[:4], refs[4:8], refs[8:14], *refs[14:]
     cw = wc[0].shape[0]
     aw = act[0].shape[1] - cw
     convs = [c[:, aw:].astype(F32) for c in act]
@@ -529,7 +551,7 @@
     squares = jnp.zeros((rows, 1), F32)
     for first in range(0, width, CHUNK):
         at = slice(first, first + CHUNK)
-        part = None
+        part = begun[:, at]
         for slot in range(4):
             if slot < 2:
                 w = wc[slot][:, at]
@@ -539,10 +561,8 @@
                 inner = slice(first % half, first % half + CHUNK)
                 w = jnp.where(swap, far[:, inner], near[:, inner])
             one = dot_f32(ys[slot], w)
-            part = one if part is None else part + one
-        for slot in (0, 2):
-            w = jnp.concatenate([wa[slot][:aw, at], wa[slot + 1][:aw, at]], axis=0)
-            part = part + dot_f32(jnp.concatenate([act[slot][:, :aw], act[slot + 1][:, :aw]], axis=1), w)
+            part = part + one
+        part = part + heads_part(act[2:], wa[2:], aw, at)
         mix[:, at] = part
         squares = squares + jnp.sum(part * part, axis=1, keepdims=True)
     out_ref[...] = (mix[...] * lax.rsqrt(squares / width + norm_eps) * gain_ref[...]).astype(BF16)
@@ -551,18 +571,18 @@
 CHUNK = 256
 
 
-def finish(act, wa, wc, out_gain):
+def finish(act, wa, wc, begun, out_gain):
     rows, width = act[0].shape[0], wa[0].shape[1]
     return pl.pallas_call(
         final_kernel,
         out_shape=shape((rows, width)),
-        in_specs=[VM] * 15,
+        in_specs=[VM] * 16,
         out_specs=VM,
         scratch_shapes=[pltpu.VMEM((rows, width), F32)],
         cost_estimate=cost(800_000_000, 7_000_000),
         compiler_params=params(32),
         name="finish_rows",
-    )(*act, *wa, *wc, out_gain.reshape(1, width))
+    )(*act, *wa, *wc, begun, out_gain.reshape(1, width))
 
 
 def paired(
@@ -582,12 +602,12 @@
     w_out_conv,
     out_gain,
 ):
-    own_qkv, half_qkv, wc_half = pack_qkv((w_query, w_key, w_value), w_out_conv)
+    own_qkv, half_qkv = pack_qkv((w_query, w_key, w_value))
     qkv_same = exchange(half_qkv, "sp", 1)
+    x_send, mine_own, mine_pair, wc_half = norm_parts(tokens, norm_gain, w_query.shape[0], w_out_conv)
     wc_x = exchange(wc_half, "tp", 2)
     wc_y = exchange(wc_x, "grp", 1)
     wc_yc = exchange(wc_y, "tp", 1)
-    x_send, mine_own, mine_pair = norm_parts(tokens, norm_gain, w_query.shape[0])
     x_got = exchange(x_send, "sp", 2)
     own_gv, half_gv, own_gg, wa_mine, off, head_rows = pack(
         w_glu_value, w_glu_gate, w_out_attn, key_offset.T, head_gain, channel_gain, channel_bias
@@ -607,23 +627,25 @@
 
     keep, sent = project_qkv(x_own, x_pair, own_qkv, qkv_same, qkv_other, off)
     got = exchange(sent, "sp", 2)
-    glu_keep, glu_sent = project_glu(
-        x_own, x_pair, (own_gv, own_gg), (gv_same, gv_other, gg_pair), sent
+    tail_rows = -(-conv_taps.shape[0] // 16) * 16
+    glu_keep, glu_sent, own_tail, cross_tail = project_glu(
+        x_own, x_pair, (own_gv, own_gg), (gv_same, gv_other, gg_pair), tail_rows, sent
     )
     glu_got = exchange(glu_sent, "sp", 2)
+    tail_near = from_behind(own_tail, "sp", 1)
+    tail_far = from_cross_behind(cross_tail, "sp")
     q, mine_two = sum_qkv(keep, got, sent, glu_sent)
     pair_two = exchange(mine_two, "sp", 1)
     near = near_attention(q, mine_two, head_rows, mine_two)
-    gated, tail = gate(glu_keep, glu_got, -(-conv_taps.shape[0] // 16) * 16)
-    before = from_behind(tail, "sp", 1)
-    attended, log_mass = attention(q, pair_two, head_rows, near, tail)
-    act_mine = conv(gated, before, conv_taps, attended)
+    attended, log_mass = attention(q, pair_two, head_rows, near, mine_two)
+    act_mine = conv(glu_keep, glu_got, tail_near, tail_far, conv_taps, attended)
     act_x = exchange(act_mine, "tp", 2)
     act_core = exchange(act_mine, "tp", 1)
     act = (act_mine, act_core, act_x, exchange(act_x, "tp", 1))
     wa = (wa_mine, wa_core, wa_x, wa_xc)
     wc = (w_out_conv, wc_core, wc_x, wc_y, wc_xc, wc_yc)
-    mixed = finish(act, wa, wc, out_gain)
+    begun = begin(act_mine, act_core, wa_mine, wa_core)
+    mixed = finish(act, wa, wc, begun, out_gain)
     return (mixed, log_mass)
 
 

time: 74.8 us -> 76.1 us (1.017)
  starting transfers between devices: 13.3 us -> 27.1 us
  waiting for transfers between devices: 49.2 us -> 37.4 us
    ppermute x21, waiting for transfers between devices: 45.5 us -> 32.4 us  [exchange(): return lax.ppermute(value, axis, [(s, s ^ bit) for s in range(count)])]
    ppermute x21, starting transfers between devices: 12 us -> 20.6 us  [exchange(): return lax.ppermute(value, axis, [(s, s ^ bit) for s in range(count)])]
    ppermute x0 -> x1, starting transfers between devices: none -> 5.14 us  [from_cross_behind(): return lax.ppermute(value, axis, [(a, b) for a, b in pairs if b < count])]
    ppermute x0 -> x1, waiting for transfers between devices: none -> 1.29 us  [from_cross_behind(): return lax.ppermute(value, axis, [(a, b) for a, b in pairs if b < count])]
  transfers between devices with their start and end apart: 22 -> 23, of which waited for: 8 -> 9; matrix products, arithmetic and copies ran while one was open for 0% -> 0% of each run, Pallas kernels for 9% -> 9%
where the time goes in v9:
time: 76.1 us; the launch traced here: 75.7 us
  waiting for transfers between devices  37.4 us (49%)
  starting transfers between devices  27.1 us (36%)
  Pallas kernels  10.5 us (14%)
  between operations  0.79 us (1%)
    ppermute x21, waiting for transfers between devices, exchange(): return lax.ppermute(value, axis, [(s, s ^ bit) for s in range(count)])  32.4 us
    ppermute x21, starting transfers between devices, exchange(): return lax.ppermute(value, axis, [(s, s ^ bit) for s in range(count)])  20.6 us
    ppermute x1, starting transfers between devices, from_cross_behind(): return lax.ppermute(value, axis, [(a, b) for a, b in pairs if b < count])  5.14 us
    ppermute x1, waiting for transfers between devices, from_behind(): lax.ppermute(value, axis, [(source, source + steps) for source in range(i...  3.65 us
    pallas_call x1, Pallas kernels, finish(): pl.pallas_call(final_kernel, out_shape=shape((rows, width)), in_specs=[VM...  2.09 us
    pallas_call x1, Pallas kernels, attention(): pl.pallas_call(attention_kernel, out_shape=(shape((rows, width)), shape((...  1.86 us
  transfers between devices with their start and end apart: 23, of which 9 were waited for; matrix products, arithmetic and copies ran while one was open for 0% of the time, Pallas kernels for 9%

profile of v9, /device:TPU:25, one launch (start us, length us, event | category | flops | bytes accessed | tf_op | source)
XLA Modules:
  0.0 75.7 jit_solution(15482104086667813161)
XLA Ops:
  0.6 1.3 %norm_parts.1 = (bf16[64,1024]{1,0:T(8,128)(2,1)S(1)}, bf16[128,512]{1,0:T(8,128)(2,1)S(1)}, bf16[128,512]{1,0:T(8,128)(2,1)S(1)}, bf16[256,1024]{1,0:T(8,128)(2,1)S(1)}) custom-call(bf16[128,2048]{1,0:T(8,128)(2,1)} %x_hbm.1, f32[1,2048]{1,0:T(1,128)} %bitcast.6, bf16[256,2048]{1,0:T(8,128)(2,1)} %refs_8_.1), custom_call_target="tpu_custom_call" | custom-call | flops 2000000 | bytes 1000000 | tf_op jit(solution)/shard_map/norm_parts/pallas_call | solution.py:118
  2.0 1.3 %collective-permute-start.19 = (bf16[256,1024]{1,0:T(8,128)(2,1)S(1)}, bf16[256,1024]{1,0:T(8,128)(2,1)S(1)}, u32[]{:S(2)}, u32[]{:S(2)}) collective-permute-start(bf16[256,1024]{1,0:T(8,128)(2,1)S(1)} %get-tuple-element.58), channel_id=1, source_target_pairs={{0,2},{1,3},{2,0},{3,1},{4,6},{5,7},{6,4},{7,5},{8,10},{9,11},{10,... | collective-permute-start | bytes 1572872 | tf_op jit(solution)/shard_map/ppermute | solution.py:15
  3.2 1.2 %pack_qkv.1 = (bf16[512,384]{1,0:T(8,128)(2,1)S(1)}, bf16[256,384]{1,0:T(8,128)(2,1)S(1)}) custom-call(bf16[512,128]{1,0:T(8,128)(2,1)} %wq.1, bf16[512,128]{1,0:T(8,128)(2,1)} %wk.1, bf16[512,128]{1,0:T(8,128)(2,1)} %wv.1), custom_call_target="tpu_custom_call" | custom-call | flops 2000000 | bytes 400000 | tf_op jit(solution)/shard_map/pack_qkv/pallas_call | solution.py:76
  4.7 6.1 %collective-permute-done.got_ref = bf16[64,1024]{1,0:T(8,128)(2,1)S(1)} collective-permute-done((bf16[64,1024]{1,0:T(8,128)(2,1)S(1)}, bf16[64,1024]{1,0:T(8,128)(2,1)S(1)}, u32[]{:S(2)}, u32[]{:S(2)}) %collective-permute-start) | collective-permute-done | bytes 131104 | tf_op jit(solution)/shard_map/ppermute | solution.py:15
  10.8 2.3 %collective-permute-start.1 = (bf16[64,1024]{1,0:T(8,128)(2,1)S(1)}, bf16[64,1024]{1,0:T(8,128)(2,1)S(1)}, u32[]{:S(2)}, u32[]{:S(2)}) collective-permute-start(bf16[64,1024]{1,0:T(8,128)(2,1)S(1)} %collective-permute-done.got_ref), channel_id=1, source_target_pairs={{0,1},{1,0},{2,3},{3,2},{4,5},{5,4},{6,7},{7,6},{8,9},{9,8},{10,11... | collective-permute-start | bytes 393224 | tf_op jit(solution)/shard_map/ppermute | solution.py:15
  13.1 1.4 %pack.1 = (bf16[512,256]{1,0:T(8,128)(2,1)S(1)}, bf16[256,256]{1,0:T(8,128)(2,1)S(1)}, bf16[512,256]{1,0:T(8,128)(2,1)S(1)}, bf16[144,2048]{1,0:T(8,128)(2,1)S(1...) custom-call(bf16[512,256]{1,0:T(8,128)(2,1)} %gv_hbm.1, bf16[512,256]{1,0:T(8,128)(2,1)} %gg_hbm.1, ...), custom_call_target="tpu_custom_call" | custom-call | flops 2000000 | bytes 2000000 | tf_op jit(solution)/shard_map/pack/pallas_call | solution.py:177
  14.5 1.3 %collective-permute-start.6 = (bf16[256,384]{1,0:T(8,128)(2,1)S(1)}, bf16[256,384]{1,0:T(8,128)(2,1)S(1)}, u32[]{:S(2)}, u32[]{:S(2)}) collective-permute-start(bf16[256,384]{1,0:T(8,128)(2,1)S(1)} %collective-permute-done.2.same), channel_id=1, source_target_pairs={{0,16},{16,0},{1,17},{17,1},{2,18},{18,2},{3,19},{19,3},{4,20},{20... | collective-permute-start | bytes 589832 | tf_op jit(solution)/shard_map/ppermute | solution.py:15
  15.8 1.7 %collective-permute-start.5 = (bf16[512,256]{1,0:T(8,128)(2,1)S(1)}, bf16[512,256]{1,0:T(8,128)(2,1)S(1)}, u32[]{:S(2)}, u32[]{:S(2)}) collective-permute-start(bf16[512,256]{1,0:T(8,128)(2,1)S(1)} %get-tuple-element.37.gg), channel_id=1, source_target_pairs={{0,4},{4,0},{8,12},{12,8},{1,5},{5,1},{9,13},{13,9},{2,6},{6,2},{1... | collective-permute-start | bytes 786440 | tf_op jit(solution)/shard_map/ppermute | solution.py:15
  17.8 8.8 %collective-permute-done.3.gv_same = bf16[256,256]{1,0:T(8,128)(2,1)S(1)} collective-permute-done((bf16[256,256]{1,0:T(8,128)(2,1)S(1)}, bf16[256,256]{1,0:T(8,128)(2,1)S(1)}, u32[]{:S(2)}, u32[]{:S(2)}) %collective-permute-start.3) | collective-permute-done | bytes 131104 | tf_op jit(solution)/shard_map/ppermute | solution.py:15
  26.8 1.3 %collective-permute-start.18 = (bf16[256,2048]{1,0:T(8,128)(2,1)S(1)}, bf16[256,2048]{1,0:T(8,128)(2,1)S(1)}, u32[]{:S(2)}, u32[]{:S(2)}) collective-permute-start(bf16[256,2048]{1,0:T(8,128)(2,1)S(1)} %copy-done), channel_id=1, source_target_pairs={{0,1},{1,0},{2,3},{3,2},{4,5},{5,4},{6,7},{7,6},{8,9},{9,8},{10,11... | collective-permute-start | bytes 3145736 | tf_op jit(solution)/shard_map/ppermute | solution.py:15
  28.1 1.2 %collective-permute-start.20 = (bf16[256,1024]{1,0:T(8,128)(2,1)S(1)}, bf16[256,1024]{1,0:T(8,128)(2,1)S(1)}, u32[]{:S(2)}, u32[]{:S(2)}) collective-permute-start(bf16[256,1024]{1,0:T(8,128)(2,1)S(1)} %collective-permute-done.19.refs_10_), channel_id=1, source_target_pairs={{0,16},{16,0},{1,17},{17,1},{2,18},{18,2},{3,19},{19,3},{4,20},{20... | collective-permute-start | bytes 1572872 | tf_op jit(solution)/shard_map/ppermute | solution.py:15
  29.3 0.4 project_qkv.1
  29.8 2.5 %collective-permute-start.10 = (bf16[656,128]{1,0:T(8,128)(2,1)S(1)}, bf16[656,128]{1,0:T(8,128)(2,1)S(1)}, u32[]{:S(2)}, u32[]{:S(2)}) collective-permute-start(bf16[656,128]{1,0:T(8,128)(2,1)S(1)} %get-tuple-element.44.after.sent_ref), channel_id=1, source_target_pairs={{0,8},{4,12},{8,0},{12,4},{1,9},{5,13},{9,1},{13,5},{2,10},{6,14},... | collective-permute-start | bytes 503816 | tf_op jit(solution)/shard_map/ppermute | solution.py:15
  32.3 0.4 project_glu.1
  32.7 1.3 %collective-permute-start.8 = (bf16[32,512]{1,0:T(8,128)(2,1)S(1)}, bf16[32,512]{1,0:T(8,128)(2,1)S(1)}, u32[]{:S(2)}, u32[]{:S(2)}) collective-permute-start(bf16[32,512]{1,0:T(8,128)(2,1)S(1)} %get-tuple-element.47), channel_id=1, source_target_pairs={{0,4},{4,8},{8,12},{1,5},{5,9},{9,13},{2,6},{6,10},{10,14},{3,7},{... | collective-permute-start | bytes 98312 | tf_op jit(solution)/shard_map/ppermute | solution.py:27
  34.0 3.7 %collective-permute-done.8.near_ref = bf16[32,512]{1,0:T(8,128)(2,1)S(1)} collective-permute-done((bf16[32,512]{1,0:T(8,128)(2,1)S(1)}, bf16[32,512]{1,0:T(8,128)(2,1)S(1)}, u32[]{:S(2)}, u32[]{:S(2)}) %collective-permute-start.8) | collective-permute-done | bytes 32800 | tf_op jit(solution)/shard_map/ppermute | solution.py:27
  37.7 5.1 %collective-permute-start.9 = (bf16[32,512]{1,0:T(8,128)(2,1)S(1)}, bf16[32,512]{1,0:T(8,128)(2,1)S(1)}, u32[]{:S(2)}, u32[]{:S(2)}) collective-permute-start(bf16[32,512]{1,0:T(8,128)(2,1)S(1)} %get-tuple-element.48), channel_id=1, source_target_pairs={{0,12},{8,4},{12,8},{1,13},{9,5},{13,9},{2,14},{10,6},{14,10},{3,1... | collective-permute-start | bytes 98312 | tf_op jit(solution)/shard_map/ppermute | solution.py:21
  42.8 1.3 %collective-permute-done.9.far_ref = bf16[32,512]{1,0:T(8,128)(2,1)S(1)} collective-permute-done((bf16[32,512]{1,0:T(8,128)(2,1)S(1)}, bf16[32,512]{1,0:T(8,128)(2,1)S(1)}, u32[]{:S(2)}, u32[]{:S(2)}) %collective-permute-start.9) | collective-permute-done | bytes 32800 | tf_op jit(solution)/shard_map/ppermute | solution.py:21
  44.1 4.5 %collective-permute-start.15 = (bf16[144,2048]{1,0:T(8,128)(2,1)S(1)}, bf16[144,2048]{1,0:T(8,128)(2,1)S(1)}, u32[]{:S(2)}, u32[]{:S(2)}) collective-permute-start(bf16[144,2048]{1,0:T(8,128)(2,1)S(1)} %get-tuple-element.57.wa0.refs_4_), channel_id=1, source_target_pairs={{0,1},{1,0},{2,3},{3,2},{4,5},{5,4},{6,7},{7,6},{8,9},{9,8},{10,11... | collective-permute-start | bytes 1769480 | tf_op jit(solution)/shard_map/ppermute | solution.py:15
  48.7 8.1 %collective-permute-done.7.got_ref = bf16[128,512]{1,0:T(8,128)(2,1)S(1)} collective-permute-done((bf16[128,512]{1,0:T(8,128)(2,1)S(1)}, bf16[128,512]{1,0:T(8,128)(2,1)S(1)}, u32[]{:S(2)}, u32[]{:S(2)}) %collective-permute-start.7) | collective-permute-done | bytes 131104 | tf_op jit(solution)/shard_map/ppermute | solution.py:15
  56.8 0.4 collective-permute-start.17
  57.2 4.3 %collective-permute-done.11.pair_ref = bf16[528,128]{1,0:T(8,128)(2,1)S(1)} collective-permute-done((bf16[528,128]{1,0:T(8,128)(2,1)S(1)}, bf16[528,128]{1,0:T(8,128)(2,1)S(1)}, u32[]{:S(2)}, u32[]{:S(2)}) %collective-permute-start.11) | collective-permute-done | bytes 135200 | tf_op jit(solution)/shard_map/ppermute | solution.py:15
  61.5 1.3 %collective-permute-start.21 = (bf16[256,1024]{1,0:T(8,128)(2,1)S(1)}, bf16[256,1024]{1,0:T(8,128)(2,1)S(1)}, u32[]{:S(2)}, u32[]{:S(2)}) collective-permute-start(bf16[256,1024]{1,0:T(8,128)(2,1)S(1)} %collective-permute-done.19.refs_10_), channel_id=1, source_target_pairs={{0,1},{1,0},{2,3},{3,2},{4,5},{5,4},{6,7},{7,6},{8,9},{9,8},{10,11... | collective-permute-start | bytes 1572872 | tf_op jit(solution)/shard_map/ppermute | solution.py:15
  62.8 0.7 near_attention.1
  63.5 1.9 %stick_attention.1 = (bf16[128,128]{1,0:T(8,128)(2,1)S(1)}, f32[2,128]{1,0:T(2,128)}) custom-call(bf16[128,128]{1,0:T(8,128)(2,1)S(1)} %get-tuple-element.50.q_ref, bf16[528,128]{1,0:T(8,128)(2,1)S(1)} %collective-permute-done.11.pair_ref, f32[2,64]{1,0:T(2,128)S(1)} %get-tuple-element.52.gain_ref, f32[2,128,128]{2,1,0:T(8,128)S(1)} %get-tuple-element.53.mix_ref, ...), custom_call_target="tpu_custom_call" | custom-call | flops 400000000 | bytes 1000000 | tf_op jit(solution)/shard_map/stick_attention/pallas_call | solution.py:491
  65.4 0.6 conv.1.act0.refs_0_
  66.4 3.6 %collective-permute-done.13.refs_2_ = bf16[128,384]{1,0:T(8,128)(2,1)S(1)} collective-permute-done((bf16[128,384]{1,0:T(8,128)(2,1)S(1)}, bf16[128,384]{1,0:T(8,128)(2,1)S(1)}, u32[]{:S(2)}, u32[]{:S(2)}) %collective-permute-start.13) | collective-permute-done | bytes 98336 | tf_op jit(solution)/shard_map/ppermute | solution.py:15
  70.0 1.4 %collective-permute-start.12 = (bf16[128,384]{1,0:T(8,128)(2,1)S(1)}, bf16[128,384]{1,0:T(8,128)(2,1)S(1)}, u32[]{:S(2)}, u32[]{:S(2)}) collective-permute-start(bf16[128,384]{1,0:T(8,128)(2,1)S(1)} %conv.1.act0.refs_0_), channel_id=1, source_target_pairs={{0,1},{1,0},{2,3},{3,2},{4,5},{5,4},{6,7},{7,6},{8,9},{9,8},{10,11... | collective-permute-start | bytes 294920 | tf_op jit(solution)/shard_map/ppermute | solution.py:15
  71.3 0.9 %collective-permute-done.12.act1.refs_1_ = bf16[128,384]{1,0:T(8,128)(2,1)S(1)} collective-permute-done((bf16[128,384]{1,0:T(8,128)(2,1)S(1)}, bf16[128,384]{1,0:T(8,128)(2,1)S(1)}, u32[]{:S(2)}, u32[]{:S(2)}) %collective-permute-start.12) | collective-permute-done | bytes 98336 | tf_op jit(solution)/shard_map/ppermute | solution.py:15
  72.3 0.4 collective-permute-start.14
  73.0 0.6 collective-permute-done.14.refs_3_
  73.6 2.1 %finish_rows.1 = bf16[128,2048]{1,0:T(8,128)(2,1)} custom-call(bf16[128,384]{1,0:T(8,128)(2,1)S(1)} %conv.1.act0.refs_0_, bf16[128,384]{1,0:T(8,128)(2,1)S(1)} %collective-permute-done.12.act1.refs_1_, bf16[128,384]{1,0:T(8,128)(2,1)S(1)} %collective-permute-done.13.refs_2_, bf16[128,384]{1,0:T(8,128)(2,1)S(1)} %collective-permute-done.14.refs_3_, ...), custom_call_target="tpu_custom_call" | custom-call | flops 800000000 | bytes 7000000 | tf_op jit(solution)/shard_map/finish_rows/pallas_call | solution.py:576
  (32 shorter events, 1.6 us)
Async XLA Ops:
  2.0 24.8 %copy-start = (bf16[256,2048]{1,0:T(8,128)(2,1)S(1)}, bf16[256,2048]{1,0:T(8,128)(2,1)}, u32[]{:S(2)}) copy-start(bf16[256,2048]{1,0:T(8,128)(2,1)} %refs_8_.1) | copy-start | bytes 3145732
  2.0 26.1 %collective-permute-start.19 = (bf16[256,1024]{1,0:T(8,128)(2,1)S(1)}, bf16[256,1024]{1,0:T(8,128)(2,1)S(1)}, u32[]{:S(2)}, u32[]{:S(2)}) collective-permute-start(bf16[256,1024]{1,0:T(8,128)(2,1)S(1)} %get-tuple-element.58), channel_id=1, source_target_pairs={{0,2},{1,3},{2,0},{3,1},{4,6},{5,7},{6,4},{7,5},{8,10},{9,11},{10,... | collective-permute-start | bytes 1572872 | tf_op jit(solution)/shard_map/ppermute | solution.py:15
  4.4 10.1 %collective-permute-start.2 = (bf16[256,384]{1,0:T(8,128)(2,1)S(1)}, bf16[256,384]{1,0:T(8,128)(2,1)S(1)}, u32[]{:S(2)}, u32[]{:S(2)}) collective-permute-start(bf16[256,384]{1,0:T(8,128)(2,1)S(1)} %get-tuple-element.38), channel_id=1, source_target_pairs={{0,4},{4,0},{8,12},{12,8},{1,5},{5,1},{9,13},{13,9},{2,6},{6,2},{1... | collective-permute-start | bytes 589832 | tf_op jit(solution)/shard_map/ppermute | solution.py:15
  4.7 6.1 %collective-permute-start = (bf16[64,1024]{1,0:T(8,128)(2,1)S(1)}, bf16[64,1024]{1,0:T(8,128)(2,1)S(1)}, u32[]{:S(2)}, u32[]{:S(2)}) collective-permute-start(bf16[64,1024]{1,0:T(8,128)(2,1)S(1)} %get-tuple-element.33), channel_id=1, source_target_pairs={{0,8},{4,12},{8,0},{12,4},{1,9},{5,13},{9,1},{13,5},{2,10},{6,14},... | collective-permute-start | bytes 393224 | tf_op jit(solution)/shard_map/ppermute | solution.py:15
  10.8 6.7 %collective-permute-start.1 = (bf16[64,1024]{1,0:T(8,128)(2,1)S(1)}, bf16[64,1024]{1,0:T(8,128)(2,1)S(1)}, u32[]{:S(2)}, u32[]{:S(2)}) collective-permute-start(bf16[64,1024]{1,0:T(8,128)(2,1)S(1)} %collective-permute-done.got_ref), channel_id=1, source_target_pairs={{0,1},{1,0},{2,3},{3,2},{4,5},{5,4},{6,7},{7,6},{8,9},{9,8},{10,11... | collective-permute-start | bytes 393224 | tf_op jit(solution)/shard_map/ppermute | solution.py:15
  14.5 12.3 %collective-permute-start.6 = (bf16[256,384]{1,0:T(8,128)(2,1)S(1)}, bf16[256,384]{1,0:T(8,128)(2,1)S(1)}, u32[]{:S(2)}, u32[]{:S(2)}) collective-permute-start(bf16[256,384]{1,0:T(8,128)(2,1)S(1)} %collective-permute-done.2.same), channel_id=1, source_target_pairs={{0,16},{16,0},{1,17},{17,1},{2,18},{18,2},{3,19},{19,3},{4,20},{20... | collective-permute-start | bytes 589832 | tf_op jit(solution)/shard_map/ppermute | solution.py:15
  15.8 14.0 %collective-permute-start.5 = (bf16[512,256]{1,0:T(8,128)(2,1)S(1)}, bf16[512,256]{1,0:T(8,128)(2,1)S(1)}, u32[]{:S(2)}, u32[]{:S(2)}) collective-permute-start(bf16[512,256]{1,0:T(8,128)(2,1)S(1)} %get-tuple-element.37.gg), channel_id=1, source_target_pairs={{0,4},{4,0},{8,12},{12,8},{1,5},{5,1},{9,13},{13,9},{2,6},{6,2},{1... | collective-permute-start | bytes 786440 | tf_op jit(solution)/shard_map/ppermute | solution.py:15
  17.5 9.1 %collective-permute-start.3 = (bf16[256,256]{1,0:T(8,128)(2,1)S(1)}, bf16[256,256]{1,0:T(8,128)(2,1)S(1)}, u32[]{:S(2)}, u32[]{:S(2)}) collective-permute-start(bf16[256,256]{1,0:T(8,128)(2,1)S(1)} %get-tuple-element.40), channel_id=1, source_target_pairs={{0,4},{4,0},{8,12},{12,8},{1,5},{5,1},{9,13},{13,9},{2,6},{6,2},{1... | collective-permute-start | bytes 393224 | tf_op jit(solution)/shard_map/ppermute | solution.py:15
  17.5 39.3 %collective-permute-start.16 = (bf16[144,2048]{1,0:T(8,128)(2,1)S(1)}, bf16[144,2048]{1,0:T(8,128)(2,1)S(1)}, u32[]{:S(2)}, u32[]{:S(2)}) collective-permute-start(bf16[144,2048]{1,0:T(8,128)(2,1)S(1)} %get-tuple-element.57.wa0.refs_4_), channel_id=1, source_target_pairs={{0,2},{1,3},{2,0},{3,1},{4,6},{5,7},{6,4},{7,5},{8,10},{9,11},{10,... | collective-permute-start | bytes 1769480 | tf_op jit(solution)/shard_map/ppermute | solution.py:15
  26.6 5.7 %collective-permute-start.4 = (bf16[256,256]{1,0:T(8,128)(2,1)S(1)}, bf16[256,256]{1,0:T(8,128)(2,1)S(1)}, u32[]{:S(2)}, u32[]{:S(2)}) collective-permute-start(bf16[256,256]{1,0:T(8,128)(2,1)S(1)} %collective-permute-done.3.gv_same), channel_id=1, source_target_pairs={{0,16},{16,0},{1,17},{17,1},{2,18},{18,2},{3,19},{19,3},{4,20},{20... | collective-permute-start | bytes 393224 | tf_op jit(solution)/shard_map/ppermute | solution.py:15
  26.8 46.8 %collective-permute-start.18 = (bf16[256,2048]{1,0:T(8,128)(2,1)S(1)}, bf16[256,2048]{1,0:T(8,128)(2,1)S(1)}, u32[]{:S(2)}, u32[]{:S(2)}) collective-permute-start(bf16[256,2048]{1,0:T(8,128)(2,1)S(1)} %copy-done), channel_id=1, source_target_pairs={{0,1},{1,0},{2,3},{3,2},{4,5},{5,4},{6,7},{7,6},{8,9},{9,8},{10,11... | collective-permute-start | bytes 3145736 | tf_op jit(solution)/shard_map/ppermute | solution.py:15
  28.1 34.7 %collective-permute-start.20 = (bf16[256,1024]{1,0:T(8,128)(2,1)S(1)}, bf16[256,1024]{1,0:T(8,128)(2,1)S(1)}, u32[]{:S(2)}, u32[]{:S(2)}) collective-permute-start(bf16[256,1024]{1,0:T(8,128)(2,1)S(1)} %collective-permute-done.19.refs_10_), channel_id=1, source_target_pairs={{0,16},{16,0},{1,17},{17,1},{2,18},{18,2},{3,19},{19,3},{4,20},{20... | collective-permute-start | bytes 1572872 | tf_op jit(solution)/shard_map/ppermute | solution.py:15
  29.8 18.8 %collective-permute-start.10 = (bf16[656,128]{1,0:T(8,128)(2,1)S(1)}, bf16[656,128]{1,0:T(8,128)(2,1)S(1)}, u32[]{:S(2)}, u32[]{:S(2)}) collective-permute-start(bf16[656,128]{1,0:T(8,128)(2,1)S(1)} %get-tuple-element.44.after.sent_ref), channel_id=1, source_target_pairs={{0,8},{4,12},{8,0},{12,4},{1,9},{5,13},{9,1},{13,5},{2,10},{6,14},... | collective-permute-start | bytes 503816 | tf_op jit(solution)/shard_map/ppermute | solution.py:15
  32.7 5.0 %collective-permute-start.8 = (bf16[32,512]{1,0:T(8,128)(2,1)S(1)}, bf16[32,512]{1,0:T(8,128)(2,1)S(1)}, u32[]{:S(2)}, u32[]{:S(2)}) collective-permute-start(bf16[32,512]{1,0:T(8,128)(2,1)S(1)} %get-tuple-element.47), channel_id=1, source_target_pairs={{0,4},{4,8},{8,12},{1,5},{5,9},{9,13},{2,6},{6,10},{10,14},{3,7},{... | collective-permute-start | bytes 98312 | tf_op jit(solution)/shard_map/ppermute | solution.py:27
  37.7 6.4 %collective-permute-start.9 = (bf16[32,512]{1,0:T(8,128)(2,1)S(1)}, bf16[32,512]{1,0:T(8,128)(2,1)S(1)}, u32[]{:S(2)}, u32[]{:S(2)}) collective-permute-start(bf16[32,512]{1,0:T(8,128)(2,1)S(1)} %get-tuple-element.48), channel_id=1, source_target_pairs={{0,12},{8,4},{12,8},{1,13},{9,5},{13,9},{2,14},{10,6},{14,10},{3,1... | collective-permute-start | bytes 98312 | tf_op jit(solution)/shard_map/ppermute | solution.py:21
  44.1 22.0 %collective-permute-start.15 = (bf16[144,2048]{1,0:T(8,128)(2,1)S(1)}, bf16[144,2048]{1,0:T(8,128)(2,1)S(1)}, u32[]{:S(2)}, u32[]{:S(2)}) collective-permute-start(bf16[144,2048]{1,0:T(8,128)(2,1)S(1)} %get-tuple-element.57.wa0.refs_4_), channel_id=1, source_target_pairs={{0,1},{1,0},{2,3},{3,2},{4,5},{5,4},{6,7},{7,6},{8,9},{9,8},{10,11... | collective-permute-start | bytes 1769480 | tf_op jit(solution)/shard_map/ppermute | solution.py:15
  48.6 8.2 %collective-permute-start.7 = (bf16[128,512]{1,0:T(8,128)(2,1)S(1)}, bf16[128,512]{1,0:T(8,128)(2,1)S(1)}, u32[]{:S(2)}, u32[]{:S(2)}) collective-permute-start(bf16[128,512]{1,0:T(8,128)(2,1)S(1)} %get-tuple-element.46.after), channel_id=1, source_target_pairs={{0,8},{4,12},{8,0},{12,4},{1,9},{5,13},{9,1},{13,5},{2,10},{6,14},... | collective-permute-start | bytes 393224 | tf_op jit(solution)/shard_map/ppermute | solution.py:15
  56.8 4.7 %collective-permute-start.11 = (bf16[528,128]{1,0:T(8,128)(2,1)S(1)}, bf16[528,128]{1,0:T(8,128)(2,1)S(1)}, u32[]{:S(2)}, u32[]{:S(2)}) collective-permute-start(bf16[528,128]{1,0:T(8,128)(2,1)S(1)} %get-tuple-element.51.mine_ref.after), channel_id=1, source_target_pairs={{0,4},{4,0},{8,12},{12,8},{1,5},{5,1},{9,13},{13,9},{2,6},{6,2},{1... | collective-permute-start | bytes 405512 | tf_op jit(solution)/shard_map/ppermute | solution.py:15
  56.8 16.8 %collective-permute-start.17 = (bf16[144,2048]{1,0:T(8,128)(2,1)S(1)}, bf16[144,2048]{1,0:T(8,128)(2,1)S(1)}, u32[]{:S(2)}, u32[]{:S(2)}) collective-permute-start(bf16[144,2048]{1,0:T(8,128)(2,1)S(1)} %collective-permute-done.16.refs_6_), channel_id=1, source_target_pairs={{0,1},{1,0},{2,3},{3,2},{4,5},{5,4},{6,7},{7,6},{8,9},{9,8},{10,11... | collective-permute-start | bytes 1769480 | tf_op jit(solution)/shard_map/ppermute | solution.py:15
  61.5 12.1 %collective-permute-start.21 = (bf16[256,1024]{1,0:T(8,128)(2,1)S(1)}, bf16[256,1024]{1,0:T(8,128)(2,1)S(1)}, u32[]{:S(2)}, u32[]{:S(2)}) collective-permute-start(bf16[256,1024]{1,0:T(8,128)(2,1)S(1)} %collective-permute-done.19.refs_10_), channel_id=1, source_target_pairs={{0,1},{1,0},{2,3},{3,2},{4,5},{5,4},{6,7},{7,6},{8,9},{9,8},{10,11... | collective-permute-start | bytes 1572872 | tf_op jit(solution)/shard_map/ppermute | solution.py:15
  62.8 10.8 %collective-permute-start.22 = (bf16[256,1024]{1,0:T(8,128)(2,1)S(1)}, bf16[256,1024]{1,0:T(8,128)(2,1)S(1)}, u32[]{:S(2)}, u32[]{:S(2)}) collective-permute-start(bf16[256,1024]{1,0:T(8,128)(2,1)S(1)} %collective-permute-done.20.refs_11_), channel_id=1, source_target_pairs={{0,1},{1,0},{2,3},{3,2},{4,5},{5,4},{6,7},{7,6},{8,9},{9,8},{10,11... | collective-permute-start | bytes 1572872 | tf_op jit(solution)/shard_map/ppermute | solution.py:15
  63.5 1.9 %copy-start.1 = (f32[31,256]{1,0:T(8,128)S(1)}, f32[31,256]{1,0:T(8,128)}, u32[]{:S(2)}) copy-start(f32[31,256]{1,0:T(8,128)} %taps_ref.1) | copy-start | bytes 95236
  66.0 7.6 %copy-start.2 = (f32[2048]{0:T(1024)S(1)}, f32[2048]{0:T(1024)}, u32[]{:S(2)}) copy-start(f32[2048]{0:T(1024)} %param.29) | copy-start | bytes 24580
  66.1 3.9 %collective-permute-start.13 = (bf16[128,384]{1,0:T(8,128)(2,1)S(1)}, bf16[128,384]{1,0:T(8,128)(2,1)S(1)}, u32[]{:S(2)}, u32[]{:S(2)}) collective-permute-start(bf16[128,384]{1,0:T(8,128)(2,1)S(1)} %conv.1.act0.refs_0_), channel_id=1, source_target_pairs={{0,2},{1,3},{2,0},{3,1},{4,6},{5,7},{6,4},{7,5},{8,10},{9,11},{10,... | collective-permute-start | bytes 294920 | tf_op jit(solution)/shard_map/ppermute | solution.py:15
  70.0 2.3 %collective-permute-start.12 = (bf16[128,384]{1,0:T(8,128)(2,1)S(1)}, bf16[128,384]{1,0:T(8,128)(2,1)S(1)}, u32[]{:S(2)}, u32[]{:S(2)}) collective-permute-start(bf16[128,384]{1,0:T(8,128)(2,1)S(1)} %conv.1.act0.refs_0_), channel_id=1, source_target_pairs={{0,1},{1,0},{2,3},{3,2},{4,5},{5,4},{6,7},{7,6},{8,9},{9,8},{10,11... | collective-permute-start | bytes 294920 | tf_op jit(solution)/shard_map/ppermute | solution.py:15
  72.3 1.3 %collective-permute-start.14 = (bf16[128,384]{1,0:T(8,128)(2,1)S(1)}, bf16[128,384]{1,0:T(8,128)(2,1)S(1)}, u32[]{:S(2)}, u32[]{:S(2)}) collective-permute-start(bf16[128,384]{1,0:T(8,128)(2,1)S(1)} %collective-permute-done.13.refs_2_), channel_id=1, source_target_pairs={{0,1},{1,0},{2,3},{3,2},{4,5},{5,4},{6,7},{7,6},{8,9},{9,8},{10,11... | collective-permute-start | bytes 294920 | tf_op jit(solution)/shard_map/ppermute | solution.py:15

commit v10 on v9

--- a/solution.py
+++ b/solution.py
@@ -545,26 +545,22 @@
         bias = pieces[3] + pieces[4] + pieces[5]
         y = centered[slot] * inverse * gain + bias
         ys.append((y * jax.nn.sigmoid(y)).astype(BF16))
-    swap = lax.axis_index("grp") == 1
+    group = lax.axis_index("grp")
     rows, width = mix.shape
     half = width // 2
     squares = jnp.zeros((rows, 1), F32)
-    for first in range(0, width, CHUNK):
-        at = slice(first, first + CHUNK)
-        part = begun[:, at]
-        for slot in range(4):
-            if slot < 2:
-                w = wc[slot][:, at]
-            else:
-                pair = wc[2 * slot - 2], wc[2 * slot - 1]
-                near, far = pair if first < half else pair[::-1]
-                inner = slice(first % half, first % half + CHUNK)
-                w = jnp.where(swap, far[:, inner], near[:, inner])
-            one = dot_f32(ys[slot], w)
-            part = part + one
-        part = part + heads_part(act[2:], wa[2:], aw, at)
-        mix[:, at] = part
-        squares = squares + jnp.sum(part * part, axis=1, keepdims=True)
+    for n in range(2):
+        base = (group if n == 0 else 1 - group) * half
+        for first in range(0, half, CHUNK):
+            at = pl.ds(pl.multiple_of(base + first, CHUNK), CHUNK)
+            inner = slice(first, first + CHUNK)
+            part = begun[:, at]
+            for slot in range(4):
+                w = wc[slot][:, at] if slot < 2 else wc[2 * slot - 2 + n][:, inner]
+                part = part + dot_f32(ys[slot], w)
+            part = part + heads_part(act[2:], wa[2:], aw, at)
+            mix[:, at] = part
+            squares = squares + jnp.sum(part * part, axis=1, keepdims=True)
     out_ref[...] = (mix[...] * lax.rsqrt(squares / width + norm_eps) * gain_ref[...]).astype(BF16)
 
 

time: 76.1 us -> 76.1 us (level)
  no operation moved by 1% of the time
where the time goes in v10:
time: 76.1 us; the launch traced here: 75.7 us
  waiting for transfers between devices  37.4 us (49%)
  starting transfers between devices  27.1 us (36%)
  Pallas kernels  10.4 us (14%)
  between operations  0.79 us (1%)
    ppermute x21, waiting for transfers between devices, exchange(): return lax.ppermute(value, axis, [(s, s ^ bit) for s in range(count)])  32.4 us
    ppermute x21, starting transfers between devices, exchange(): return lax.ppermute(value, axis, [(s, s ^ bit) for s in range(count)])  20.6 us
    ppermute x1, starting transfers between devices, from_cross_behind(): return lax.ppermute(value, axis, [(a, b) for a, b in pairs if b < count])  5.14 us
    ppermute x1, waiting for transfers between devices, from_behind(): lax.ppermute(value, axis, [(source, source + steps) for source in range(i...  3.65 us
    pallas_call x1, Pallas kernels, finish(): pl.pallas_call(final_kernel, out_shape=shape((rows, width)), in_specs=[VM...  2.07 us
    pallas_call x1, Pallas kernels, attention(): pl.pallas_call(attention_kernel, out_shape=(shape((rows, width)), shape((...  1.86 us
  transfers between devices with their start and end apart: 23, of which 9 were waited for; matrix products, arithmetic and copies ran while one was open for 0% of the time, Pallas kernels for 9%

profile of v10, /device:TPU:25, one launch (start us, length us, event | category | flops | bytes accessed | tf_op | source)
XLA Modules:
  0.0 75.7 jit_solution(2326075504089097910)
XLA Ops:
  0.6 1.3 %norm_parts.1 = (bf16[64,1024]{1,0:T(8,128)(2,1)S(1)}, bf16[128,512]{1,0:T(8,128)(2,1)S(1)}, bf16[128,512]{1,0:T(8,128)(2,1)S(1)}, bf16[256,1024]{1,0:T(8,128)(2,1)S(1)}) custom-call(bf16[128,2048]{1,0:T(8,128)(2,1)} %x_hbm.1, f32[1,2048]{1,0:T(1,128)} %bitcast.6, bf16[256,2048]{1,0:T(8,128)(2,1)} %refs_8_.1), custom_call_target="tpu_custom_call" | custom-call | flops 2000000 | bytes 1000000 | tf_op jit(solution)/shard_map/norm_parts/pallas_call | solution.py:118
  2.0 1.3 %collective-permute-start.19 = (bf16[256,1024]{1,0:T(8,128)(2,1)S(1)}, bf16[256,1024]{1,0:T(8,128)(2,1)S(1)}, u32[]{:S(2)}, u32[]{:S(2)}) collective-permute-start(bf16[256,1024]{1,0:T(8,128)(2,1)S(1)} %get-tuple-element.58), channel_id=1, source_target_pairs={{0,2},{1,3},{2,0},{3,1},{4,6},{5,7},{6,4},{7,5},{8,10},{9,11},{10,... | collective-permute-start | bytes 1572872 | tf_op jit(solution)/shard_map/ppermute | solution.py:15
  3.2 1.2 %pack_qkv.1 = (bf16[512,384]{1,0:T(8,128)(2,1)S(1)}, bf16[256,384]{1,0:T(8,128)(2,1)S(1)}) custom-call(bf16[512,128]{1,0:T(8,128)(2,1)} %wq.1, bf16[512,128]{1,0:T(8,128)(2,1)} %wk.1, bf16[512,128]{1,0:T(8,128)(2,1)} %wv.1), custom_call_target="tpu_custom_call" | custom-call | flops 2000000 | bytes 400000 | tf_op jit(solution)/shard_map/pack_qkv/pallas_call | solution.py:76
  4.7 6.1 %collective-permute-done.got_ref = bf16[64,1024]{1,0:T(8,128)(2,1)S(1)} collective-permute-done((bf16[64,1024]{1,0:T(8,128)(2,1)S(1)}, bf16[64,1024]{1,0:T(8,128)(2,1)S(1)}, u32[]{:S(2)}, u32[]{:S(2)}) %collective-permute-start) | collective-permute-done | bytes 131104 | tf_op jit(solution)/shard_map/ppermute | solution.py:15
  10.8 2.3 %collective-permute-start.1 = (bf16[64,1024]{1,0:T(8,128)(2,1)S(1)}, bf16[64,1024]{1,0:T(8,128)(2,1)S(1)}, u32[]{:S(2)}, u32[]{:S(2)}) collective-permute-start(bf16[64,1024]{1,0:T(8,128)(2,1)S(1)} %collective-permute-done.got_ref), channel_id=1, source_target_pairs={{0,1},{1,0},{2,3},{3,2},{4,5},{5,4},{6,7},{7,6},{8,9},{9,8},{10,11... | collective-permute-start | bytes 393224 | tf_op jit(solution)/shard_map/ppermute | solution.py:15
  13.1 1.4 %pack.1 = (bf16[512,256]{1,0:T(8,128)(2,1)S(1)}, bf16[256,256]{1,0:T(8,128)(2,1)S(1)}, bf16[512,256]{1,0:T(8,128)(2,1)S(1)}, bf16[144,2048]{1,0:T(8,128)(2,1)S(1...) custom-call(bf16[512,256]{1,0:T(8,128)(2,1)} %gv_hbm.1, bf16[512,256]{1,0:T(8,128)(2,1)} %gg_hbm.1, ...), custom_call_target="tpu_custom_call" | custom-call | flops 2000000 | bytes 2000000 | tf_op jit(solution)/shard_map/pack/pallas_call | solution.py:177
  14.5 1.3 %collective-permute-start.6 = (bf16[256,384]{1,0:T(8,128)(2,1)S(1)}, bf16[256,384]{1,0:T(8,128)(2,1)S(1)}, u32[]{:S(2)}, u32[]{:S(2)}) collective-permute-start(bf16[256,384]{1,0:T(8,128)(2,1)S(1)} %collective-permute-done.2.same), channel_id=1, source_target_pairs={{0,16},{16,0},{1,17},{17,1},{2,18},{18,2},{3,19},{19,3},{4,20},{20... | collective-permute-start | bytes 589832 | tf_op jit(solution)/shard_map/ppermute | solution.py:15
  15.8 1.7 %collective-permute-start.5 = (bf16[512,256]{1,0:T(8,128)(2,1)S(1)}, bf16[512,256]{1,0:T(8,128)(2,1)S(1)}, u32[]{:S(2)}, u32[]{:S(2)}) collective-permute-start(bf16[512,256]{1,0:T(8,128)(2,1)S(1)} %get-tuple-element.37.gg), channel_id=1, source_target_pairs={{0,4},{4,0},{8,12},{12,8},{1,5},{5,1},{9,13},{13,9},{2,6},{6,2},{1... | collective-permute-start | bytes 786440 | tf_op jit(solution)/shard_map/ppermute | solution.py:15
  17.8 8.8 %collective-permute-done.3.gv_same = bf16[256,256]{1,0:T(8,128)(2,1)S(1)} collective-permute-done((bf16[256,256]{1,0:T(8,128)(2,1)S(1)}, bf16[256,256]{1,0:T(8,128)(2,1)S(1)}, u32[]{:S(2)}, u32[]{:S(2)}) %collective-permute-start.3) | collective-permute-done | bytes 131104 | tf_op jit(solution)/shard_map/ppermute | solution.py:15
  26.8 1.3 %collective-permute-start.18 = (bf16[256,2048]{1,0:T(8,128)(2,1)S(1)}, bf16[256,2048]{1,0:T(8,128)(2,1)S(1)}, u32[]{:S(2)}, u32[]{:S(2)}) collective-permute-start(bf16[256,2048]{1,0:T(8,128)(2,1)S(1)} %copy-done), channel_id=1, source_target_pairs={{0,1},{1,0},{2,3},{3,2},{4,5},{5,4},{6,7},{7,6},{8,9},{9,8},{10,11... | collective-permute-start | bytes 3145736 | tf_op jit(solution)/shard_map/ppermute | solution.py:15
  28.1 1.2 %collective-permute-start.20 = (bf16[256,1024]{1,0:T(8,128)(2,1)S(1)}, bf16[256,1024]{1,0:T(8,128)(2,1)S(1)}, u32[]{:S(2)}, u32[]{:S(2)}) collective-permute-start(bf16[256,1024]{1,0:T(8,128)(2,1)S(1)} %collective-permute-done.19.refs_10_), channel_id=1, source_target_pairs={{0,16},{16,0},{1,17},{17,1},{2,18},{18,2},{3,19},{19,3},{4,20},{20... | collective-permute-start | bytes 1572872 | tf_op jit(solution)/shard_map/ppermute | solution.py:15
  29.3 0.4 project_qkv.1
  29.8 2.5 %collective-permute-start.10 = (bf16[656,128]{1,0:T(8,128)(2,1)S(1)}, bf16[656,128]{1,0:T(8,128)(2,1)S(1)}, u32[]{:S(2)}, u32[]{:S(2)}) collective-permute-start(bf16[656,128]{1,0:T(8,128)(2,1)S(1)} %get-tuple-element.44.after.sent_ref), channel_id=1, source_target_pairs={{0,8},{4,12},{8,0},{12,4},{1,9},{5,13},{9,1},{13,5},{2,10},{6,14},... | collective-permute-start | bytes 503816 | tf_op jit(solution)/shard_map/ppermute | solution.py:15
  32.3 0.4 project_glu.1
  32.7 1.3 %collective-permute-start.8 = (bf16[32,512]{1,0:T(8,128)(2,1)S(1)}, bf16[32,512]{1,0:T(8,128)(2,1)S(1)}, u32[]{:S(2)}, u32[]{:S(2)}) collective-permute-start(bf16[32,512]{1,0:T(8,128)(2,1)S(1)} %get-tuple-element.47), channel_id=1, source_target_pairs={{0,4},{4,8},{8,12},{1,5},{5,9},{9,13},{2,6},{6,10},{10,14},{3,7},{... | collective-permute-start | bytes 98312 | tf_op jit(solution)/shard_map/ppermute | solution.py:27
  34.0 3.7 %collective-permute-done.8.near_ref = bf16[32,512]{1,0:T(8,128)(2,1)S(1)} collective-permute-done((bf16[32,512]{1,0:T(8,128)(2,1)S(1)}, bf16[32,512]{1,0:T(8,128)(2,1)S(1)}, u32[]{:S(2)}, u32[]{:S(2)}) %collective-permute-start.8) | collective-permute-done | bytes 32800 | tf_op jit(solution)/shard_map/ppermute | solution.py:27
  37.7 5.1 %collective-permute-start.9 = (bf16[32,512]{1,0:T(8,128)(2,1)S(1)}, bf16[32,512]{1,0:T(8,128)(2,1)S(1)}, u32[]{:S(2)}, u32[]{:S(2)}) collective-permute-start(bf16[32,512]{1,0:T(8,128)(2,1)S(1)} %get-tuple-element.48), channel_id=1, source_target_pairs={{0,12},{8,4},{12,8},{1,13},{9,5},{13,9},{2,14},{10,6},{14,10},{3,1... | collective-permute-start | bytes 98312 | tf_op jit(solution)/shard_map/ppermute | solution.py:21
  42.8 1.3 %collective-permute-done.9.far_ref = bf16[32,512]{1,0:T(8,128)(2,1)S(1)} collective-permute-done((bf16[32,512]{1,0:T(8,128)(2,1)S(1)}, bf16[32,512]{1,0:T(8,128)(2,1)S(1)}, u32[]{:S(2)}, u32[]{:S(2)}) %collective-permute-start.9) | collective-permute-done | bytes 32800 | tf_op jit(solution)/shard_map/ppermute | solution.py:21
  44.1 4.5 %collective-permute-start.15 = (bf16[144,2048]{1,0:T(8,128)(2,1)S(1)}, bf16[144,2048]{1,0:T(8,128)(2,1)S(1)}, u32[]{:S(2)}, u32[]{:S(2)}) collective-permute-start(bf16[144,2048]{1,0:T(8,128)(2,1)S(1)} %get-tuple-element.57.wa0.refs_4_), channel_id=1, source_target_pairs={{0,1},{1,0},{2,3},{3,2},{4,5},{5,4},{6,7},{7,6},{8,9},{9,8},{10,11... | collective-permute-start | bytes 1769480 | tf_op jit(solution)/shard_map/ppermute | solution.py:15
  48.7 8.1 %collective-permute-done.7.got_ref = bf16[128,512]{1,0:T(8,128)(2,1)S(1)} collective-permute-done((bf16[128,512]{1,0:T(8,128)(2,1)S(1)}, bf16[128,512]{1,0:T(8,128)(2,1)S(1)}, u32[]{:S(2)}, u32[]{:S(2)}) %collective-permute-start.7) | collective-permute-done | bytes 131104 | tf_op jit(solution)/shard_map/ppermute | solution.py:15
  56.8 0.4 collective-permute-start.17
  57.2 4.3 %collective-permute-done.11.pair_ref = bf16[528,128]{1,0:T(8,128)(2,1)S(1)} collective-permute-done((bf16[528,128]{1,0:T(8,128)(2,1)S(1)}, bf16[528,128]{1,0:T(8,128)(2,1)S(1)}, u32[]{:S(2)}, u32[]{:S(2)}) %collective-permute-start.11) | collective-permute-done | bytes 135200 | tf_op jit(solution)/shard_map/ppermute | solution.py:15
  61.5 1.3 %collective-permute-start.21 = (bf16[256,1024]{1,0:T(8,128)(2,1)S(1)}, bf16[256,1024]{1,0:T(8,128)(2,1)S(1)}, u32[]{:S(2)}, u32[]{:S(2)}) collective-permute-start(bf16[256,1024]{1,0:T(8,128)(2,1)S(1)} %collective-permute-done.19.refs_10_), channel_id=1, source_target_pairs={{0,1},{1,0},{2,3},{3,2},{4,5},{5,4},{6,7},{7,6},{8,9},{9,8},{10,11... | collective-permute-start | bytes 1572872 | tf_op jit(solution)/shard_map/ppermute | solution.py:15
  62.8 0.7 near_attention.1
  63.5 1.9 %stick_attention.1 = (bf16[128,128]{1,0:T(8,128)(2,1)S(1)}, f32[2,128]{1,0:T(2,128)}) custom-call(bf16[128,128]{1,0:T(8,128)(2,1)S(1)} %get-tuple-element.50.q_ref, bf16[528,128]{1,0:T(8,128)(2,1)S(1)} %collective-permute-done.11.pair_ref, f32[2,64]{1,0:T(2,128)S(1)} %get-tuple-element.52.gain_ref, f32[2,128,128]{2,1,0:T(8,128)S(1)} %get-tuple-element.53.mix_ref, ...), custom_call_target="tpu_custom_call" | custom-call | flops 400000000 | bytes 1000000 | tf_op jit(solution)/shard_map/stick_attention/pallas_call | solution.py:491
  65.4 0.6 conv.1.act0.refs_0_
  66.4 3.6 %collective-permute-done.13.refs_2_ = bf16[128,384]{1,0:T(8,128)(2,1)S(1)} collective-permute-done((bf16[128,384]{1,0:T(8,128)(2,1)S(1)}, bf16[128,384]{1,0:T(8,128)(2,1)S(1)}, u32[]{:S(2)}, u32[]{:S(2)}) %collective-permute-start.13) | collective-permute-done | bytes 98336 | tf_op jit(solution)/shard_map/ppermute | solution.py:15
  70.0 1.4 %collective-permute-start.12 = (bf16[128,384]{1,0:T(8,128)(2,1)S(1)}, bf16[128,384]{1,0:T(8,128)(2,1)S(1)}, u32[]{:S(2)}, u32[]{:S(2)}) collective-permute-start(bf16[128,384]{1,0:T(8,128)(2,1)S(1)} %conv.1.act0.refs_0_), channel_id=1, source_target_pairs={{0,1},{1,0},{2,3},{3,2},{4,5},{5,4},{6,7},{7,6},{8,9},{9,8},{10,11... | collective-permute-start | bytes 294920 | tf_op jit(solution)/shard_map/ppermute | solution.py:15
  71.3 0.9 %collective-permute-done.12.act1.refs_1_ = bf16[128,384]{1,0:T(8,128)(2,1)S(1)} collective-permute-done((bf16[128,384]{1,0:T(8,128)(2,1)S(1)}, bf16[128,384]{1,0:T(8,128)(2,1)S(1)}, u32[]{:S(2)}, u32[]{:S(2)}) %collective-permute-start.12) | collective-permute-done | bytes 98336 | tf_op jit(solution)/shard_map/ppermute | solution.py:15
  72.3 0.4 collective-permute-start.14
  73.0 0.6 collective-permute-done.14.refs_3_
  73.6 2.1 %finish_rows.1 = bf16[128,2048]{1,0:T(8,128)(2,1)} custom-call(bf16[128,384]{1,0:T(8,128)(2,1)S(1)} %conv.1.act0.refs_0_, bf16[128,384]{1,0:T(8,128)(2,1)S(1)} %collective-permute-done.12.act1.refs_1_, bf16[128,384]{1,0:T(8,128)(2,1)S(1)} %collective-permute-done.13.refs_2_, bf16[128,384]{1,0:T(8,128)(2,1)S(1)} %collective-permute-done.14.refs_3_, ...), custom_call_target="tpu_custom_call" | custom-call | flops 800000000 | bytes 7000000 | tf_op jit(solution)/shard_map/finish_rows/pallas_call | solution.py:572
  (32 shorter events, 1.6 us)
Async XLA Ops:
  2.0 24.8 %copy-start = (bf16[256,2048]{1,0:T(8,128)(2,1)S(1)}, bf16[256,2048]{1,0:T(8,128)(2,1)}, u32[]{:S(2)}) copy-start(bf16[256,2048]{1,0:T(8,128)(2,1)} %refs_8_.1) | copy-start | bytes 3145732
  2.0 26.1 %collective-permute-start.19 = (bf16[256,1024]{1,0:T(8,128)(2,1)S(1)}, bf16[256,1024]{1,0:T(8,128)(2,1)S(1)}, u32[]{:S(2)}, u32[]{:S(2)}) collective-permute-start(bf16[256,1024]{1,0:T(8,128)(2,1)S(1)} %get-tuple-element.58), channel_id=1, source_target_pairs={{0,2},{1,3},{2,0},{3,1},{4,6},{5,7},{6,4},{7,5},{8,10},{9,11},{10,... | collective-permute-start | bytes 1572872 | tf_op jit(solution)/shard_map/ppermute | solution.py:15
  4.4 10.1 %collective-permute-start.2 = (bf16[256,384]{1,0:T(8,128)(2,1)S(1)}, bf16[256,384]{1,0:T(8,128)(2,1)S(1)}, u32[]{:S(2)}, u32[]{:S(2)}) collective-permute-start(bf16[256,384]{1,0:T(8,128)(2,1)S(1)} %get-tuple-element.38), channel_id=1, source_target_pairs={{0,4},{4,0},{8,12},{12,8},{1,5},{5,1},{9,13},{13,9},{2,6},{6,2},{1... | collective-permute-start | bytes 589832 | tf_op jit(solution)/shard_map/ppermute | solution.py:15
  4.7 6.1 %collective-permute-start = (bf16[64,1024]{1,0:T(8,128)(2,1)S(1)}, bf16[64,1024]{1,0:T(8,128)(2,1)S(1)}, u32[]{:S(2)}, u32[]{:S(2)}) collective-permute-start(bf16[64,1024]{1,0:T(8,128)(2,1)S(1)} %get-tuple-element.33), channel_id=1, source_target_pairs={{0,8},{4,12},{8,0},{12,4},{1,9},{5,13},{9,1},{13,5},{2,10},{6,14},... | collective-permute-start | bytes 393224 | tf_op jit(solution)/shard_map/ppermute | solution.py:15
  10.8 6.7 %collective-permute-start.1 = (bf16[64,1024]{1,0:T(8,128)(2,1)S(1)}, bf16[64,1024]{1,0:T(8,128)(2,1)S(1)}, u32[]{:S(2)}, u32[]{:S(2)}) collective-permute-start(bf16[64,1024]{1,0:T(8,128)(2,1)S(1)} %collective-permute-done.got_ref), channel_id=1, source_target_pairs={{0,1},{1,0},{2,3},{3,2},{4,5},{5,4},{6,7},{7,6},{8,9},{9,8},{10,11... | collective-permute-start | bytes 393224 | tf_op jit(solution)/shard_map/ppermute | solution.py:15
  14.5 12.3 %collective-permute-start.6 = (bf16[256,384]{1,0:T(8,128)(2,1)S(1)}, bf16[256,384]{1,0:T(8,128)(2,1)S(1)}, u32[]{:S(2)}, u32[]{:S(2)}) collective-permute-start(bf16[256,384]{1,0:T(8,128)(2,1)S(1)} %collective-permute-done.2.same), channel_id=1, source_target_pairs={{0,16},{16,0},{1,17},{17,1},{2,18},{18,2},{3,19},{19,3},{4,20},{20... | collective-permute-start | bytes 589832 | tf_op jit(solution)/shard_map/ppermute | solution.py:15
  15.8 14.0 %collective-permute-start.5 = (bf16[512,256]{1,0:T(8,128)(2,1)S(1)}, bf16[512,256]{1,0:T(8,128)(2,1)S(1)}, u32[]{:S(2)}, u32[]{:S(2)}) collective-permute-start(bf16[512,256]{1,0:T(8,128)(2,1)S(1)} %get-tuple-element.37.gg), channel_id=1, source_target_pairs={{0,4},{4,0},{8,12},{12,8},{1,5},{5,1},{9,13},{13,9},{2,6},{6,2},{1... | collective-permute-start | bytes 786440 | tf_op jit(solution)/shard_map/ppermute | solution.py:15
  17.5 9.1 %collective-permute-start.3 = (bf16[256,256]{1,0:T(8,128)(2,1)S(1)}, bf16[256,256]{1,0:T(8,128)(2,1)S(1)}, u32[]{:S(2)}, u32[]{:S(2)}) collective-permute-start(bf16[256,256]{1,0:T(8,128)(2,1)S(1)} %get-tuple-element.40), channel_id=1, source_target_pairs={{0,4},{4,0},{8,12},{12,8},{1,5},{5,1},{9,13},{13,9},{2,6},{6,2},{1... | collective-permute-start | bytes 393224 | tf_op jit(solution)/shard_map/ppermute | solution.py:15
  17.5 39.3 %collective-permute-start.16 = (bf16[144,2048]{1,0:T(8,128)(2,1)S(1)}, bf16[144,2048]{1,0:T(8,128)(2,1)S(1)}, u32[]{:S(2)}, u32[]{:S(2)}) collective-permute-start(bf16[144,2048]{1,0:T(8,128)(2,1)S(1)} %get-tuple-element.57.wa0.refs_4_), channel_id=1, source_target_pairs={{0,2},{1,3},{2,0},{3,1},{4,6},{5,7},{6,4},{7,5},{8,10},{9,11},{10,... | collective-permute-start | bytes 1769480 | tf_op jit(solution)/shard_map/ppermute | solution.py:15
  26.6 5.7 %collective-permute-start.4 = (bf16[256,256]{1,0:T(8,128)(2,1)S(1)}, bf16[256,256]{1,0:T(8,128)(2,1)S(1)}, u32[]{:S(2)}, u32[]{:S(2)}) collective-permute-start(bf16[256,256]{1,0:T(8,128)(2,1)S(1)} %collective-permute-done.3.gv_same), channel_id=1, source_target_pairs={{0,16},{16,0},{1,17},{17,1},{2,18},{18,2},{3,19},{19,3},{4,20},{20... | collective-permute-start | bytes 393224 | tf_op jit(solution)/shard_map/ppermute | solution.py:15
  26.8 46.8 %collective-permute-start.18 = (bf16[256,2048]{1,0:T(8,128)(2,1)S(1)}, bf16[256,2048]{1,0:T(8,128)(2,1)S(1)}, u32[]{:S(2)}, u32[]{:S(2)}) collective-permute-start(bf16[256,2048]{1,0:T(8,128)(2,1)S(1)} %copy-done), channel_id=1, source_target_pairs={{0,1},{1,0},{2,3},{3,2},{4,5},{5,4},{6,7},{7,6},{8,9},{9,8},{10,11... | collective-permute-start | bytes 3145736 | tf_op jit(solution)/shard_map/ppermute | solution.py:15
  28.1 34.7 %collective-permute-start.20 = (bf16[256,1024]{1,0:T(8,128)(2,1)S(1)}, bf16[256,1024]{1,0:T(8,128)(2,1)S(1)}, u32[]{:S(2)}, u32[]{:S(2)}) collective-permute-start(bf16[256,1024]{1,0:T(8,128)(2,1)S(1)} %collective-permute-done.19.refs_10_), channel_id=1, source_target_pairs={{0,16},{16,0},{1,17},{17,1},{2,18},{18,2},{3,19},{19,3},{4,20},{20... | collective-permute-start | bytes 1572872 | tf_op jit(solution)/shard_map/ppermute | solution.py:15
  29.8 18.8 %collective-permute-start.10 = (bf16[656,128]{1,0:T(8,128)(2,1)S(1)}, bf16[656,128]{1,0:T(8,128)(2,1)S(1)}, u32[]{:S(2)}, u32[]{:S(2)}) collective-permute-start(bf16[656,128]{1,0:T(8,128)(2,1)S(1)} %get-tuple-element.44.after.sent_ref), channel_id=1, source_target_pairs={{0,8},{4,12},{8,0},{12,4},{1,9},{5,13},{9,1},{13,5},{2,10},{6,14},... | collective-permute-start | bytes 503816 | tf_op jit(solution)/shard_map/ppermute | solution.py:15
  32.7 5.0 %collective-permute-start.8 = (bf16[32,512]{1,0:T(8,128)(2,1)S(1)}, bf16[32,512]{1,0:T(8,128)(2,1)S(1)}, u32[]{:S(2)}, u32[]{:S(2)}) collective-permute-start(bf16[32,512]{1,0:T(8,128)(2,1)S(1)} %get-tuple-element.47), channel_id=1, source_target_pairs={{0,4},{4,8},{8,12},{1,5},{5,9},{9,13},{2,6},{6,10},{10,14},{3,7},{... | collective-permute-start | bytes 98312 | tf_op jit(solution)/shard_map/ppermute | solution.py:27
  37.7 6.4 %collective-permute-start.9 = (bf16[32,512]{1,0:T(8,128)(2,1)S(1)}, bf16[32,512]{1,0:T(8,128)(2,1)S(1)}, u32[]{:S(2)}, u32[]{:S(2)}) collective-permute-start(bf16[32,512]{1,0:T(8,128)(2,1)S(1)} %get-tuple-element.48), channel_id=1, source_target_pairs={{0,12},{8,4},{12,8},{1,13},{9,5},{13,9},{2,14},{10,6},{14,10},{3,1... | collective-permute-start | bytes 98312 | tf_op jit(solution)/shard_map/ppermute | solution.py:21
  44.1 22.0 %collective-permute-start.15 = (bf16[144,2048]{1,0:T(8,128)(2,1)S(1)}, bf16[144,2048]{1,0:T(8,128)(2,1)S(1)}, u32[]{:S(2)}, u32[]{:S(2)}) collective-permute-start(bf16[144,2048]{1,0:T(8,128)(2,1)S(1)} %get-tuple-element.57.wa0.refs_4_), channel_id=1, source_target_pairs={{0,1},{1,0},{2,3},{3,2},{4,5},{5,4},{6,7},{7,6},{8,9},{9,8},{10,11... | collective-permute-start | bytes 1769480 | tf_op jit(solution)/shard_map/ppermute | solution.py:15
  48.6 8.2 %collective-permute-start.7 = (bf16[128,512]{1,0:T(8,128)(2,1)S(1)}, bf16[128,512]{1,0:T(8,128)(2,1)S(1)}, u32[]{:S(2)}, u32[]{:S(2)}) collective-permute-start(bf16[128,512]{1,0:T(8,128)(2,1)S(1)} %get-tuple-element.46.after), channel_id=1, source_target_pairs={{0,8},{4,12},{8,0},{12,4},{1,9},{5,13},{9,1},{13,5},{2,10},{6,14},... | collective-permute-start | bytes 393224 | tf_op jit(solution)/shard_map/ppermute | solution.py:15
  56.8 4.7 %collective-permute-start.11 = (bf16[528,128]{1,0:T(8,128)(2,1)S(1)}, bf16[528,128]{1,0:T(8,128)(2,1)S(1)}, u32[]{:S(2)}, u32[]{:S(2)}) collective-permute-start(bf16[528,128]{1,0:T(8,128)(2,1)S(1)} %get-tuple-element.51.mine_ref.after), channel_id=1, source_target_pairs={{0,4},{4,0},{8,12},{12,8},{1,5},{5,1},{9,13},{13,9},{2,6},{6,2},{1... | collective-permute-start | bytes 405512 | tf_op jit(solution)/shard_map/ppermute | solution.py:15
  56.8 16.8 %collective-permute-start.17 = (bf16[144,2048]{1,0:T(8,128)(2,1)S(1)}, bf16[144,2048]{1,0:T(8,128)(2,1)S(1)}, u32[]{:S(2)}, u32[]{:S(2)}) collective-permute-start(bf16[144,2048]{1,0:T(8,128)(2,1)S(1)} %collective-permute-done.16.refs_6_), channel_id=1, source_target_pairs={{0,1},{1,0},{2,3},{3,2},{4,5},{5,4},{6,7},{7,6},{8,9},{9,8},{10,11... | collective-permute-start | bytes 1769480 | tf_op jit(solution)/shard_map/ppermute | solution.py:15
  61.5 12.1 %collective-permute-start.21 = (bf16[256,1024]{1,0:T(8,128)(2,1)S(1)}, bf16[256,1024]{1,0:T(8,128)(2,1)S(1)}, u32[]{:S(2)}, u32[]{:S(2)}) collective-permute-start(bf16[256,1024]{1,0:T(8,128)(2,1)S(1)} %collective-permute-done.19.refs_10_), channel_id=1, source_target_pairs={{0,1},{1,0},{2,3},{3,2},{4,5},{5,4},{6,7},{7,6},{8,9},{9,8},{10,11... | collective-permute-start | bytes 1572872 | tf_op jit(solution)/shard_map/ppermute | solution.py:15
  62.8 10.8 %collective-permute-start.22 = (bf16[256,1024]{1,0:T(8,128)(2,1)S(1)}, bf16[256,1024]{1,0:T(8,128)(2,1)S(1)}, u32[]{:S(2)}, u32[]{:S(2)}) collective-permute-start(bf16[256,1024]{1,0:T(8,128)(2,1)S(1)} %collective-permute-done.20.refs_11_), channel_id=1, source_target_pairs={{0,1},{1,0},{2,3},{3,2},{4,5},{5,4},{6,7},{7,6},{8,9},{9,8},{10,11... | collective-permute-start | bytes 1572872 | tf_op jit(solution)/shard_map/ppermute | solution.py:15
  63.5 1.9 %copy-start.1 = (f32[31,256]{1,0:T(8,128)S(1)}, f32[31,256]{1,0:T(8,128)}, u32[]{:S(2)}) copy-start(f32[31,256]{1,0:T(8,128)} %taps_ref.1) | copy-start | bytes 95236
  66.0 7.6 %copy-start.2 = (f32[2048]{0:T(1024)S(1)}, f32[2048]{0:T(1024)}, u32[]{:S(2)}) copy-start(f32[2048]{0:T(1024)} %param.29) | copy-start | bytes 24580
  66.1 3.9 %collective-permute-start.13 = (bf16[128,384]{1,0:T(8,128)(2,1)S(1)}, bf16[128,384]{1,0:T(8,128)(2,1)S(1)}, u32[]{:S(2)}, u32[]{:S(2)}) collective-permute-start(bf16[128,384]{1,0:T(8,128)(2,1)S(1)} %conv.1.act0.refs_0_), channel_id=1, source_target_pairs={{0,2},{1,3},{2,0},{3,1},{4,6},{5,7},{6,4},{7,5},{8,10},{9,11},{10,... | collective-permute-start | bytes 294920 | tf_op jit(solution)/shard_map/ppermute | solution.py:15
  70.0 2.3 %collective-permute-start.12 = (bf16[128,384]{1,0:T(8,128)(2,1)S(1)}, bf16[128,384]{1,0:T(8,128)(2,1)S(1)}, u32[]{:S(2)}, u32[]{:S(2)}) collective-permute-start(bf16[128,384]{1,0:T(8,128)(2,1)S(1)} %conv.1.act0.refs_0_), channel_id=1, source_target_pairs={{0,1},{1,0},{2,3},{3,2},{4,5},{5,4},{6,7},{7,6},{8,9},{9,8},{10,11... | collective-permute-start | bytes 294920 | tf_op jit(solution)/shard_map/ppermute | solution.py:15
  72.3 1.3 %collective-permute-start.14 = (bf16[128,384]{1,0:T(8,128)(2,1)S(1)}, bf16[128,384]{1,0:T(8,128)(2,1)S(1)}, u32[]{:S(2)}, u32[]{:S(2)}) collective-permute-start(bf16[128,384]{1,0:T(8,128)(2,1)S(1)} %collective-permute-done.13.refs_2_), channel_id=1, source_target_pairs={{0,1},{1,0},{2,3},{3,2},{4,5},{5,4},{6,7},{7,6},{8,9},{9,8},{10,11... | collective-permute-start | bytes 294920 | tf_op jit(solution)/shard_map/ppermute | solution.py:15

commit v11 on v10

--- a/solution.py
+++ b/solution.py
@@ -530,7 +530,7 @@
 
 
 def final_kernel(*refs):
-    act, wa, wc, begun, gain_ref, out_ref, mix = refs[:4], refs[4:8], refs[8:14], *refs[14:]
+    act, wa, wc, begun, gain_ref, out_ref, mix, done, sems = refs[:4], refs[4:8], refs[8:14], *refs[14:]
     cw = wc[0].shape[0]
     aw = act[0].shape[1] - cw
     convs = [c[:, aw:].astype(F32) for c in act]
@@ -561,7 +561,16 @@
             part = part + heads_part(act[2:], wa[2:], aw, at)
             mix[:, at] = part
             squares = squares + jnp.sum(part * part, axis=1, keepdims=True)
-    out_ref[...] = (mix[...] * lax.rsqrt(squares / width + norm_eps) * gain_ref[...]).astype(BF16)
+    inverse = lax.rsqrt(squares / width + norm_eps)
+    step = rows // 4
+    copies = []
+    for n in range(4):
+        at = slice(n * step, (n + 1) * step)
+        done[at, :] = (mix[at, :] * inverse[at] * gain_ref[...]).astype(BF16)
+        copies.append(pltpu.make_async_copy(done.at[at, :], out_ref.at[at, :], sems.at[n]))
+        copies[-1].start()
+    for copy in copies:
+        copy.wait()
 
 
 CHUNK = 256
@@ -573,8 +582,12 @@
         final_kernel,
         out_shape=shape((rows, width)),
         in_specs=[VM] * 16,
-        out_specs=VM,
-        scratch_shapes=[pltpu.VMEM((rows, width), F32)],
+        out_specs=HBM,
+        scratch_shapes=[
+            pltpu.VMEM((rows, width), F32),
+            pltpu.VMEM((rows, width), BF16),
+            pltpu.SemaphoreType.DMA((4,)),
+        ],
         cost_estimate=cost(800_000_000, 7_000_000),
         compiler_params=params(32),
         name="finish_rows",

time: 76.1 us -> 76.1 us (level)
  no operation moved by 1% of the time
where the time goes in v11:
time: 76.1 us; the launch traced here: 75.6 us
  waiting for transfers between devices  37.4 us (49%)
  starting transfers between devices  27.1 us (36%)
  Pallas kernels  10.4 us (14%)
  between operations  0.79 us (1%)
    ppermute x21, waiting for transfers between devices, exchange(): return lax.ppermute(value, axis, [(s, s ^ bit) for s in range(count)])  32.4 us
    ppermute x21, starting transfers between devices, exchange(): return lax.ppermute(value, axis, [(s, s ^ bit) for s in range(count)])  20.6 us
    ppermute x1, starting transfers between devices, from_cross_behind(): return lax.ppermute(value, axis, [(a, b) for a, b in pairs if b < count])  5.14 us
    ppermute x1, waiting for transfers between devices, from_behind(): lax.ppermute(value, axis, [(source, source + steps) for source in range(i...  3.65 us
    pallas_call x1, Pallas kernels, finish(): pl.pallas_call(final_kernel, out_shape=shape((rows, width)), in_specs=[VM...  2.02 us
    pallas_call x1, Pallas kernels, attention(): pl.pallas_call(attention_kernel, out_shape=(shape((rows, width)), shape((...  1.86 us
  transfers between devices with their start and end apart: 23, of which 9 were waited for; matrix products, arithmetic and copies ran while one was open for 0% of the time, Pallas kernels for 9%

profile of v11, /device:TPU:25, one launch (start us, length us, event | category | flops | bytes accessed | tf_op | source)
XLA Modules:
  0.0 75.6 jit_solution(8614377949641281807)
XLA Ops:
  0.6 1.3 %norm_parts.1 = (bf16[64,1024]{1,0:T(8,128)(2,1)S(1)}, bf16[128,512]{1,0:T(8,128)(2,1)S(1)}, bf16[128,512]{1,0:T(8,128)(2,1)S(1)}, bf16[256,1024]{1,0:T(8,128)(2,1)S(1)}) custom-call(bf16[128,2048]{1,0:T(8,128)(2,1)} %x_hbm.1, f32[1,2048]{1,0:T(1,128)} %bitcast.6, bf16[256,2048]{1,0:T(8,128)(2,1)} %refs_8_.1), custom_call_target="tpu_custom_call" | custom-call | flops 2000000 | bytes 1000000 | tf_op jit(solution)/shard_map/norm_parts/pallas_call | solution.py:118
  2.0 1.3 %collective-permute-start.19 = (bf16[256,1024]{1,0:T(8,128)(2,1)S(1)}, bf16[256,1024]{1,0:T(8,128)(2,1)S(1)}, u32[]{:S(2)}, u32[]{:S(2)}) collective-permute-start(bf16[256,1024]{1,0:T(8,128)(2,1)S(1)} %get-tuple-element.58), channel_id=1, source_target_pairs={{0,2},{1,3},{2,0},{3,1},{4,6},{5,7},{6,4},{7,5},{8,10},{9,11},{10,... | collective-permute-start | bytes 1572872 | tf_op jit(solution)/shard_map/ppermute | solution.py:15
  3.2 1.2 %pack_qkv.1 = (bf16[512,384]{1,0:T(8,128)(2,1)S(1)}, bf16[256,384]{1,0:T(8,128)(2,1)S(1)}) custom-call(bf16[512,128]{1,0:T(8,128)(2,1)} %wq.1, bf16[512,128]{1,0:T(8,128)(2,1)} %wk.1, bf16[512,128]{1,0:T(8,128)(2,1)} %wv.1), custom_call_target="tpu_custom_call" | custom-call | flops 2000000 | bytes 400000 | tf_op jit(solution)/shard_map/pack_qkv/pallas_call | solution.py:76
  4.7 6.1 %collective-permute-done.got_ref = bf16[64,1024]{1,0:T(8,128)(2,1)S(1)} collective-permute-done((bf16[64,1024]{1,0:T(8,128)(2,1)S(1)}, bf16[64,1024]{1,0:T(8,128)(2,1)S(1)}, u32[]{:S(2)}, u32[]{:S(2)}) %collective-permute-start) | collective-permute-done | bytes 131104 | tf_op jit(solution)/shard_map/ppermute | solution.py:15
  10.8 2.3 %collective-permute-start.1 = (bf16[64,1024]{1,0:T(8,128)(2,1)S(1)}, bf16[64,1024]{1,0:T(8,128)(2,1)S(1)}, u32[]{:S(2)}, u32[]{:S(2)}) collective-permute-start(bf16[64,1024]{1,0:T(8,128)(2,1)S(1)} %collective-permute-done.got_ref), channel_id=1, source_target_pairs={{0,1},{1,0},{2,3},{3,2},{4,5},{5,4},{6,7},{7,6},{8,9},{9,8},{10,11... | collective-permute-start | bytes 393224 | tf_op jit(solution)/shard_map/ppermute | solution.py:15
  13.1 1.4 %pack.1 = (bf16[512,256]{1,0:T(8,128)(2,1)S(1)}, bf16[256,256]{1,0:T(8,128)(2,1)S(1)}, bf16[512,256]{1,0:T(8,128)(2,1)S(1)}, bf16[144,2048]{1,0:T(8,128)(2,1)S(1...) custom-call(bf16[512,256]{1,0:T(8,128)(2,1)} %gv_hbm.1, bf16[512,256]{1,0:T(8,128)(2,1)} %gg_hbm.1, ...), custom_call_target="tpu_custom_call" | custom-call | flops 2000000 | bytes 2000000 | tf_op jit(solution)/shard_map/pack/pallas_call | solution.py:177
  14.5 1.3 %collective-permute-start.6 = (bf16[256,384]{1,0:T(8,128)(2,1)S(1)}, bf16[256,384]{1,0:T(8,128)(2,1)S(1)}, u32[]{:S(2)}, u32[]{:S(2)}) collective-permute-start(bf16[256,384]{1,0:T(8,128)(2,1)S(1)} %collective-permute-done.2.same), channel_id=1, source_target_pairs={{0,16},{16,0},{1,17},{17,1},{2,18},{18,2},{3,19},{19,3},{4,20},{20... | collective-permute-start | bytes 589832 | tf_op jit(solution)/shard_map/ppermute | solution.py:15
  15.8 1.7 %collective-permute-start.5 = (bf16[512,256]{1,0:T(8,128)(2,1)S(1)}, bf16[512,256]{1,0:T(8,128)(2,1)S(1)}, u32[]{:S(2)}, u32[]{:S(2)}) collective-permute-start(bf16[512,256]{1,0:T(8,128)(2,1)S(1)} %get-tuple-element.37.gg), channel_id=1, source_target_pairs={{0,4},{4,0},{8,12},{12,8},{1,5},{5,1},{9,13},{13,9},{2,6},{6,2},{1... | collective-permute-start | bytes 786440 | tf_op jit(solution)/shard_map/ppermute | solution.py:15
  17.8 8.8 %collective-permute-done.3.gv_same = bf16[256,256]{1,0:T(8,128)(2,1)S(1)} collective-permute-done((bf16[256,256]{1,0:T(8,128)(2,1)S(1)}, bf16[256,256]{1,0:T(8,128)(2,1)S(1)}, u32[]{:S(2)}, u32[]{:S(2)}) %collective-permute-start.3) | collective-permute-done | bytes 131104 | tf_op jit(solution)/shard_map/ppermute | solution.py:15
  26.8 1.3 %collective-permute-start.18 = (bf16[256,2048]{1,0:T(8,128)(2,1)S(1)}, bf16[256,2048]{1,0:T(8,128)(2,1)S(1)}, u32[]{:S(2)}, u32[]{:S(2)}) collective-permute-start(bf16[256,2048]{1,0:T(8,128)(2,1)S(1)} %copy-done), channel_id=1, source_target_pairs={{0,1},{1,0},{2,3},{3,2},{4,5},{5,4},{6,7},{7,6},{8,9},{9,8},{10,11... | collective-permute-start | bytes 3145736 | tf_op jit(solution)/shard_map/ppermute | solution.py:15
  28.1 1.2 %collective-permute-start.20 = (bf16[256,1024]{1,0:T(8,128)(2,1)S(1)}, bf16[256,1024]{1,0:T(8,128)(2,1)S(1)}, u32[]{:S(2)}, u32[]{:S(2)}) collective-permute-start(bf16[256,1024]{1,0:T(8,128)(2,1)S(1)} %collective-permute-done.19.refs_10_), channel_id=1, source_target_pairs={{0,16},{16,0},{1,17},{17,1},{2,18},{18,2},{3,19},{19,3},{4,20},{20... | collective-permute-start | bytes 1572872 | tf_op jit(solution)/shard_map/ppermute | solution.py:15
  29.3 0.4 project_qkv.1
  29.8 2.5 %collective-permute-start.10 = (bf16[656,128]{1,0:T(8,128)(2,1)S(1)}, bf16[656,128]{1,0:T(8,128)(2,1)S(1)}, u32[]{:S(2)}, u32[]{:S(2)}) collective-permute-start(bf16[656,128]{1,0:T(8,128)(2,1)S(1)} %get-tuple-element.44.after.sent_ref), channel_id=1, source_target_pairs={{0,8},{4,12},{8,0},{12,4},{1,9},{5,13},{9,1},{13,5},{2,10},{6,14},... | collective-permute-start | bytes 503816 | tf_op jit(solution)/shard_map/ppermute | solution.py:15
  32.3 0.4 project_glu.1
  32.7 1.3 %collective-permute-start.8 = (bf16[32,512]{1,0:T(8,128)(2,1)S(1)}, bf16[32,512]{1,0:T(8,128)(2,1)S(1)}, u32[]{:S(2)}, u32[]{:S(2)}) collective-permute-start(bf16[32,512]{1,0:T(8,128)(2,1)S(1)} %get-tuple-element.47), channel_id=1, source_target_pairs={{0,4},{4,8},{8,12},{1,5},{5,9},{9,13},{2,6},{6,10},{10,14},{3,7},{... | collective-permute-start | bytes 98312 | tf_op jit(solution)/shard_map/ppermute | solution.py:27
  34.0 3.7 %collective-permute-done.8.near_ref = bf16[32,512]{1,0:T(8,128)(2,1)S(1)} collective-permute-done((bf16[32,512]{1,0:T(8,128)(2,1)S(1)}, bf16[32,512]{1,0:T(8,128)(2,1)S(1)}, u32[]{:S(2)}, u32[]{:S(2)}) %collective-permute-start.8) | collective-permute-done | bytes 32800 | tf_op jit(solution)/shard_map/ppermute | solution.py:27
  37.7 5.1 %collective-permute-start.9 = (bf16[32,512]{1,0:T(8,128)(2,1)S(1)}, bf16[32,512]{1,0:T(8,128)(2,1)S(1)}, u32[]{:S(2)}, u32[]{:S(2)}) collective-permute-start(bf16[32,512]{1,0:T(8,128)(2,1)S(1)} %get-tuple-element.48), channel_id=1, source_target_pairs={{0,12},{8,4},{12,8},{1,13},{9,5},{13,9},{2,14},{10,6},{14,10},{3,1... | collective-permute-start | bytes 98312 | tf_op jit(solution)/shard_map/ppermute | solution.py:21
  42.8 1.3 %collective-permute-done.9.far_ref = bf16[32,512]{1,0:T(8,128)(2,1)S(1)} collective-permute-done((bf16[32,512]{1,0:T(8,128)(2,1)S(1)}, bf16[32,512]{1,0:T(8,128)(2,1)S(1)}, u32[]{:S(2)}, u32[]{:S(2)}) %collective-permute-start.9) | collective-permute-done | bytes 32800 | tf_op jit(solution)/shard_map/ppermute | solution.py:21
  44.1 4.5 %collective-permute-start.15 = (bf16[144,2048]{1,0:T(8,128)(2,1)S(1)}, bf16[144,2048]{1,0:T(8,128)(2,1)S(1)}, u32[]{:S(2)}, u32[]{:S(2)}) collective-permute-start(bf16[144,2048]{1,0:T(8,128)(2,1)S(1)} %get-tuple-element.57.wa0.refs_4_), channel_id=1, source_target_pairs={{0,1},{1,0},{2,3},{3,2},{4,5},{5,4},{6,7},{7,6},{8,9},{9,8},{10,11... | collective-permute-start | bytes 1769480 | tf_op jit(solution)/shard_map/ppermute | solution.py:15
  48.7 8.1 %collective-permute-done.7.got_ref = bf16[128,512]{1,0:T(8,128)(2,1)S(1)} collective-permute-done((bf16[128,512]{1,0:T(8,128)(2,1)S(1)}, bf16[128,512]{1,0:T(8,128)(2,1)S(1)}, u32[]{:S(2)}, u32[]{:S(2)}) %collective-permute-start.7) | collective-permute-done | bytes 131104 | tf_op jit(solution)/shard_map/ppermute | solution.py:15
  56.8 0.4 collective-permute-start.17
  57.2 4.3 %collective-permute-done.11.pair_ref = bf16[528,128]{1,0:T(8,128)(2,1)S(1)} collective-permute-done((bf16[528,128]{1,0:T(8,128)(2,1)S(1)}, bf16[528,128]{1,0:T(8,128)(2,1)S(1)}, u32[]{:S(2)}, u32[]{:S(2)}) %collective-permute-start.11) | collective-permute-done | bytes 135200 | tf_op jit(solution)/shard_map/ppermute | solution.py:15
  61.5 1.3 %collective-permute-start.21 = (bf16[256,1024]{1,0:T(8,128)(2,1)S(1)}, bf16[256,1024]{1,0:T(8,128)(2,1)S(1)}, u32[]{:S(2)}, u32[]{:S(2)}) collective-permute-start(bf16[256,1024]{1,0:T(8,128)(2,1)S(1)} %collective-permute-done.19.refs_10_), channel_id=1, source_target_pairs={{0,1},{1,0},{2,3},{3,2},{4,5},{5,4},{6,7},{7,6},{8,9},{9,8},{10,11... | collective-permute-start | bytes 1572872 | tf_op jit(solution)/shard_map/ppermute | solution.py:15
  62.8 0.7 near_attention.1
  63.5 1.9 %stick_attention.1 = (bf16[128,128]{1,0:T(8,128)(2,1)S(1)}, f32[2,128]{1,0:T(2,128)}) custom-call(bf16[128,128]{1,0:T(8,128)(2,1)S(1)} %get-tuple-element.50.q_ref, bf16[528,128]{1,0:T(8,128)(2,1)S(1)} %collective-permute-done.11.pair_ref, f32[2,64]{1,0:T(2,128)S(1)} %get-tuple-element.52.gain_ref, f32[2,128,128]{2,1,0:T(8,128)S(1)} %get-tuple-element.53.mix_ref, ...), custom_call_target="tpu_custom_call" | custom-call | flops 400000000 | bytes 1000000 | tf_op jit(solution)/shard_map/stick_attention/pallas_call | solution.py:491
  65.4 0.6 conv.1.act0.refs_0_
  66.4 3.6 %collective-permute-done.13.refs_2_ = bf16[128,384]{1,0:T(8,128)(2,1)S(1)} collective-permute-done((bf16[128,384]{1,0:T(8,128)(2,1)S(1)}, bf16[128,384]{1,0:T(8,128)(2,1)S(1)}, u32[]{:S(2)}, u32[]{:S(2)}) %collective-permute-start.13) | collective-permute-done | bytes 98336 | tf_op jit(solution)/shard_map/ppermute | solution.py:15
  70.0 1.4 %collective-permute-start.12 = (bf16[128,384]{1,0:T(8,128)(2,1)S(1)}, bf16[128,384]{1,0:T(8,128)(2,1)S(1)}, u32[]{:S(2)}, u32[]{:S(2)}) collective-permute-start(bf16[128,384]{1,0:T(8,128)(2,1)S(1)} %conv.1.act0.refs_0_), channel_id=1, source_target_pairs={{0,1},{1,0},{2,3},{3,2},{4,5},{5,4},{6,7},{7,6},{8,9},{9,8},{10,11... | collective-permute-start | bytes 294920 | tf_op jit(solution)/shard_map/ppermute | solution.py:15
  71.3 0.9 %collective-permute-done.12.act1.refs_1_ = bf16[128,384]{1,0:T(8,128)(2,1)S(1)} collective-permute-done((bf16[128,384]{1,0:T(8,128)(2,1)S(1)}, bf16[128,384]{1,0:T(8,128)(2,1)S(1)}, u32[]{:S(2)}, u32[]{:S(2)}) %collective-permute-start.12) | collective-permute-done | bytes 98336 | tf_op jit(solution)/shard_map/ppermute | solution.py:15
  72.3 0.4 collective-permute-start.14
  73.0 0.6 collective-permute-done.14.refs_3_
  73.6 2.0 %finish_rows.1 = bf16[128,2048]{1,0:T(8,128)(2,1)} custom-call(bf16[128,384]{1,0:T(8,128)(2,1)S(1)} %conv.1.act0.refs_0_, bf16[128,384]{1,0:T(8,128)(2,1)S(1)} %collective-permute-done.12.act1.refs_1_, bf16[128,384]{1,0:T(8,128)(2,1)S(1)} %collective-permute-done.13.refs_2_, bf16[128,384]{1,0:T(8,128)(2,1)S(1)} %collective-permute-done.14.refs_3_, ...), custom_call_target="tpu_custom_call" | custom-call | flops 800000000 | bytes 7000000 | tf_op jit(solution)/shard_map/finish_rows/pallas_call | solution.py:581
  (32 shorter events, 1.6 us)
Async XLA Ops:
  2.0 24.8 %copy-start = (bf16[256,2048]{1,0:T(8,128)(2,1)S(1)}, bf16[256,2048]{1,0:T(8,128)(2,1)}, u32[]{:S(2)}) copy-start(bf16[256,2048]{1,0:T(8,128)(2,1)} %refs_8_.1) | copy-start | bytes 3145732
  2.0 26.1 %collective-permute-start.19 = (bf16[256,1024]{1,0:T(8,128)(2,1)S(1)}, bf16[256,1024]{1,0:T(8,128)(2,1)S(1)}, u32[]{:S(2)}, u32[]{:S(2)}) collective-permute-start(bf16[256,1024]{1,0:T(8,128)(2,1)S(1)} %get-tuple-element.58), channel_id=1, source_target_pairs={{0,2},{1,3},{2,0},{3,1},{4,6},{5,7},{6,4},{7,5},{8,10},{9,11},{10,... | collective-permute-start | bytes 1572872 | tf_op jit(solution)/shard_map/ppermute | solution.py:15
  4.4 10.1 %collective-permute-start.2 = (bf16[256,384]{1,0:T(8,128)(2,1)S(1)}, bf16[256,384]{1,0:T(8,128)(2,1)S(1)}, u32[]{:S(2)}, u32[]{:S(2)}) collective-permute-start(bf16[256,384]{1,0:T(8,128)(2,1)S(1)} %get-tuple-element.38), channel_id=1, source_target_pairs={{0,4},{4,0},{8,12},{12,8},{1,5},{5,1},{9,13},{13,9},{2,6},{6,2},{1... | collective-permute-start | bytes 589832 | tf_op jit(solution)/shard_map/ppermute | solution.py:15
  4.7 6.1 %collective-permute-start = (bf16[64,1024]{1,0:T(8,128)(2,1)S(1)}, bf16[64,1024]{1,0:T(8,128)(2,1)S(1)}, u32[]{:S(2)}, u32[]{:S(2)}) collective-permute-start(bf16[64,1024]{1,0:T(8,128)(2,1)S(1)} %get-tuple-element.33), channel_id=1, source_target_pairs={{0,8},{4,12},{8,0},{12,4},{1,9},{5,13},{9,1},{13,5},{2,10},{6,14},... | collective-permute-start | bytes 393224 | tf_op jit(solution)/shard_map/ppermute | solution.py:15
  10.8 6.7 %collective-permute-start.1 = (bf16[64,1024]{1,0:T(8,128)(2,1)S(1)}, bf16[64,1024]{1,0:T(8,128)(2,1)S(1)}, u32[]{:S(2)}, u32[]{:S(2)}) collective-permute-start(bf16[64,1024]{1,0:T(8,128)(2,1)S(1)} %collective-permute-done.got_ref), channel_id=1, source_target_pairs={{0,1},{1,0},{2,3},{3,2},{4,5},{5,4},{6,7},{7,6},{8,9},{9,8},{10,11... | collective-permute-start | bytes 393224 | tf_op jit(solution)/shard_map/ppermute | solution.py:15
  14.5 12.3 %collective-permute-start.6 = (bf16[256,384]{1,0:T(8,128)(2,1)S(1)}, bf16[256,384]{1,0:T(8,128)(2,1)S(1)}, u32[]{:S(2)}, u32[]{:S(2)}) collective-permute-start(bf16[256,384]{1,0:T(8,128)(2,1)S(1)} %collective-permute-done.2.same), channel_id=1, source_target_pairs={{0,16},{16,0},{1,17},{17,1},{2,18},{18,2},{3,19},{19,3},{4,20},{20... | collective-permute-start | bytes 589832 | tf_op jit(solution)/shard_map/ppermute | solution.py:15
  15.8 14.0 %collective-permute-start.5 = (bf16[512,256]{1,0:T(8,128)(2,1)S(1)}, bf16[512,256]{1,0:T(8,128)(2,1)S(1)}, u32[]{:S(2)}, u32[]{:S(2)}) collective-permute-start(bf16[512,256]{1,0:T(8,128)(2,1)S(1)} %get-tuple-element.37.gg), channel_id=1, source_target_pairs={{0,4},{4,0},{8,12},{12,8},{1,5},{5,1},{9,13},{13,9},{2,6},{6,2},{1... | collective-permute-start | bytes 786440 | tf_op jit(solution)/shard_map/ppermute | solution.py:15
  17.5 9.1 %collective-permute-start.3 = (bf16[256,256]{1,0:T(8,128)(2,1)S(1)}, bf16[256,256]{1,0:T(8,128)(2,1)S(1)}, u32[]{:S(2)}, u32[]{:S(2)}) collective-permute-start(bf16[256,256]{1,0:T(8,128)(2,1)S(1)} %get-tuple-element.40), channel_id=1, source_target_pairs={{0,4},{4,0},{8,12},{12,8},{1,5},{5,1},{9,13},{13,9},{2,6},{6,2},{1... | collective-permute-start | bytes 393224 | tf_op jit(solution)/shard_map/ppermute | solution.py:15
  17.5 39.3 %collective-permute-start.16 = (bf16[144,2048]{1,0:T(8,128)(2,1)S(1)}, bf16[144,2048]{1,0:T(8,128)(2,1)S(1)}, u32[]{:S(2)}, u32[]{:S(2)}) collective-permute-start(bf16[144,2048]{1,0:T(8,128)(2,1)S(1)} %get-tuple-element.57.wa0.refs_4_), channel_id=1, source_target_pairs={{0,2},{1,3},{2,0},{3,1},{4,6},{5,7},{6,4},{7,5},{8,10},{9,11},{10,... | collective-permute-start | bytes 1769480 | tf_op jit(solution)/shard_map/ppermute | solution.py:15
  26.6 5.7 %collective-permute-start.4 = (bf16[256,256]{1,0:T(8,128)(2,1)S(1)}, bf16[256,256]{1,0:T(8,128)(2,1)S(1)}, u32[]{:S(2)}, u32[]{:S(2)}) collective-permute-start(bf16[256,256]{1,0:T(8,128)(2,1)S(1)} %collective-permute-done.3.gv_same), channel_id=1, source_target_pairs={{0,16},{16,0},{1,17},{17,1},{2,18},{18,2},{3,19},{19,3},{4,20},{20... | collective-permute-start | bytes 393224 | tf_op jit(solution)/shard_map/ppermute | solution.py:15
  26.8 46.8 %collective-permute-start.18 = (bf16[256,2048]{1,0:T(8,128)(2,1)S(1)}, bf16[256,2048]{1,0:T(8,128)(2,1)S(1)}, u32[]{:S(2)}, u32[]{:S(2)}) collective-permute-start(bf16[256,2048]{1,0:T(8,128)(2,1)S(1)} %copy-done), channel_id=1, source_target_pairs={{0,1},{1,0},{2,3},{3,2},{4,5},{5,4},{6,7},{7,6},{8,9},{9,8},{10,11... | collective-permute-start | bytes 3145736 | tf_op jit(solution)/shard_map/ppermute | solution.py:15
  28.1 34.7 %collective-permute-start.20 = (bf16[256,1024]{1,0:T(8,128)(2,1)S(1)}, bf16[256,1024]{1,0:T(8,128)(2,1)S(1)}, u32[]{:S(2)}, u32[]{:S(2)}) collective-permute-start(bf16[256,1024]{1,0:T(8,128)(2,1)S(1)} %collective-permute-done.19.refs_10_), channel_id=1, source_target_pairs={{0,16},{16,0},{1,17},{17,1},{2,18},{18,2},{3,19},{19,3},{4,20},{20... | collective-permute-start | bytes 1572872 | tf_op jit(solution)/shard_map/ppermute | solution.py:15
  29.8 18.8 %collective-permute-start.10 = (bf16[656,128]{1,0:T(8,128)(2,1)S(1)}, bf16[656,128]{1,0:T(8,128)(2,1)S(1)}, u32[]{:S(2)}, u32[]{:S(2)}) collective-permute-start(bf16[656,128]{1,0:T(8,128)(2,1)S(1)} %get-tuple-element.44.after.sent_ref), channel_id=1, source_target_pairs={{0,8},{4,12},{8,0},{12,4},{1,9},{5,13},{9,1},{13,5},{2,10},{6,14},... | collective-permute-start | bytes 503816 | tf_op jit(solution)/shard_map/ppermute | solution.py:15
  32.7 5.0 %collective-permute-start.8 = (bf16[32,512]{1,0:T(8,128)(2,1)S(1)}, bf16[32,512]{1,0:T(8,128)(2,1)S(1)}, u32[]{:S(2)}, u32[]{:S(2)}) collective-permute-start(bf16[32,512]{1,0:T(8,128)(2,1)S(1)} %get-tuple-element.47), channel_id=1, source_target_pairs={{0,4},{4,8},{8,12},{1,5},{5,9},{9,13},{2,6},{6,10},{10,14},{3,7},{... | collective-permute-start | bytes 98312 | tf_op jit(solution)/shard_map/ppermute | solution.py:27
  37.7 6.4 %collective-permute-start.9 = (bf16[32,512]{1,0:T(8,128)(2,1)S(1)}, bf16[32,512]{1,0:T(8,128)(2,1)S(1)}, u32[]{:S(2)}, u32[]{:S(2)}) collective-permute-start(bf16[32,512]{1,0:T(8,128)(2,1)S(1)} %get-tuple-element.48), channel_id=1, source_target_pairs={{0,12},{8,4},{12,8},{1,13},{9,5},{13,9},{2,14},{10,6},{14,10},{3,1... | collective-permute-start | bytes 98312 | tf_op jit(solution)/shard_map/ppermute | solution.py:21
  44.1 22.0 %collective-permute-start.15 = (bf16[144,2048]{1,0:T(8,128)(2,1)S(1)}, bf16[144,2048]{1,0:T(8,128)(2,1)S(1)}, u32[]{:S(2)}, u32[]{:S(2)}) collective-permute-start(bf16[144,2048]{1,0:T(8,128)(2,1)S(1)} %get-tuple-element.57.wa0.refs_4_), channel_id=1, source_target_pairs={{0,1},{1,0},{2,3},{3,2},{4,5},{5,4},{6,7},{7,6},{8,9},{9,8},{10,11... | collective-permute-start | bytes 1769480 | tf_op jit(solution)/shard_map/ppermute | solution.py:15
  48.6 8.2 %collective-permute-start.7 = (bf16[128,512]{1,0:T(8,128)(2,1)S(1)}, bf16[128,512]{1,0:T(8,128)(2,1)S(1)}, u32[]{:S(2)}, u32[]{:S(2)}) collective-permute-start(bf16[128,512]{1,0:T(8,128)(2,1)S(1)} %get-tuple-element.46.after), channel_id=1, source_target_pairs={{0,8},{4,12},{8,0},{12,4},{1,9},{5,13},{9,1},{13,5},{2,10},{6,14},... | collective-permute-start | bytes 393224 | tf_op jit(solution)/shard_map/ppermute | solution.py:15
  56.8 4.7 %collective-permute-start.11 = (bf16[528,128]{1,0:T(8,128)(2,1)S(1)}, bf16[528,128]{1,0:T(8,128)(2,1)S(1)}, u32[]{:S(2)}, u32[]{:S(2)}) collective-permute-start(bf16[528,128]{1,0:T(8,128)(2,1)S(1)} %get-tuple-element.51.mine_ref.after), channel_id=1, source_target_pairs={{0,4},{4,0},{8,12},{12,8},{1,5},{5,1},{9,13},{13,9},{2,6},{6,2},{1... | collective-permute-start | bytes 405512 | tf_op jit(solution)/shard_map/ppermute | solution.py:15
  56.8 16.8 %collective-permute-start.17 = (bf16[144,2048]{1,0:T(8,128)(2,1)S(1)}, bf16[144,2048]{1,0:T(8,128)(2,1)S(1)}, u32[]{:S(2)}, u32[]{:S(2)}) collective-permute-start(bf16[144,2048]{1,0:T(8,128)(2,1)S(1)} %collective-permute-done.16.refs_6_), channel_id=1, source_target_pairs={{0,1},{1,0},{2,3},{3,2},{4,5},{5,4},{6,7},{7,6},{8,9},{9,8},{10,11... | collective-permute-start | bytes 1769480 | tf_op jit(solution)/shard_map/ppermute | solution.py:15
  61.5 12.1 %collective-permute-start.21 = (bf16[256,1024]{1,0:T(8,128)(2,1)S(1)}, bf16[256,1024]{1,0:T(8,128)(2,1)S(1)}, u32[]{:S(2)}, u32[]{:S(2)}) collective-permute-start(bf16[256,1024]{1,0:T(8,128)(2,1)S(1)} %collective-permute-done.19.refs_10_), channel_id=1, source_target_pairs={{0,1},{1,0},{2,3},{3,2},{4,5},{5,4},{6,7},{7,6},{8,9},{9,8},{10,11... | collective-permute-start | bytes 1572872 | tf_op jit(solution)/shard_map/ppermute | solution.py:15
  62.8 10.8 %collective-permute-start.22 = (bf16[256,1024]{1,0:T(8,128)(2,1)S(1)}, bf16[256,1024]{1,0:T(8,128)(2,1)S(1)}, u32[]{:S(2)}, u32[]{:S(2)}) collective-permute-start(bf16[256,1024]{1,0:T(8,128)(2,1)S(1)} %collective-permute-done.20.refs_11_), channel_id=1, source_target_pairs={{0,1},{1,0},{2,3},{3,2},{4,5},{5,4},{6,7},{7,6},{8,9},{9,8},{10,11... | collective-permute-start | bytes 1572872 | tf_op jit(solution)/shard_map/ppermute | solution.py:15
  63.5 1.9 %copy-start.1 = (f32[31,256]{1,0:T(8,128)S(1)}, f32[31,256]{1,0:T(8,128)}, u32[]{:S(2)}) copy-start(f32[31,256]{1,0:T(8,128)} %taps_ref.1) | copy-start | bytes 95236
  66.0 7.6 %copy-start.2 = (f32[2048]{0:T(1024)S(1)}, f32[2048]{0:T(1024)}, u32[]{:S(2)}) copy-start(f32[2048]{0:T(1024)} %param.29) | copy-start | bytes 24580
  66.1 3.9 %collective-permute-start.13 = (bf16[128,384]{1,0:T(8,128)(2,1)S(1)}, bf16[128,384]{1,0:T(8,128)(2,1)S(1)}, u32[]{:S(2)}, u32[]{:S(2)}) collective-permute-start(bf16[128,384]{1,0:T(8,128)(2,1)S(1)} %conv.1.act0.refs_0_), channel_id=1, source_target_pairs={{0,2},{1,3},{2,0},{3,1},{4,6},{5,7},{6,4},{7,5},{8,10},{9,11},{10,... | collective-permute-start | bytes 294920 | tf_op jit(solution)/shard_map/ppermute | solution.py:15
  70.0 2.3 %collective-permute-start.12 = (bf16[128,384]{1,0:T(8,128)(2,1)S(1)}, bf16[128,384]{1,0:T(8,128)(2,1)S(1)}, u32[]{:S(2)}, u32[]{:S(2)}) collective-permute-start(bf16[128,384]{1,0:T(8,128)(2,1)S(1)} %conv.1.act0.refs_0_), channel_id=1, source_target_pairs={{0,1},{1,0},{2,3},{3,2},{4,5},{5,4},{6,7},{7,6},{8,9},{9,8},{10,11... | collective-permute-start | bytes 294920 | tf_op jit(solution)/shard_map/ppermute | solution.py:15
  72.3 1.3 %collective-permute-start.14 = (bf16[128,384]{1,0:T(8,128)(2,1)S(1)}, bf16[128,384]{1,0:T(8,128)(2,1)S(1)}, u32[]{:S(2)}, u32[]{:S(2)}) collective-permute-start(bf16[128,384]{1,0:T(8,128)(2,1)S(1)} %collective-permute-done.13.refs_2_), channel_id=1, source_target_pairs={{0,1},{1,0},{2,3},{3,2},{4,5},{5,4},{6,7},{7,6},{8,9},{9,8},{10,11... | collective-permute-start | bytes 294920 | tf_op jit(solution)/shard_map/ppermute | solution.py:15
